TPU v7x, 512 devices: a whole 4x4x16 slice. The times are simulated.
512 devices in a mesh: sp: 128 (over z, x, core), tp: 4 (over y).
Axes of the slice: x: 4, y: 4, z: 16, core: 2. Of those that a mesh axis runs over, the one named last changes fastest.
Arguments:
- tokens: bfloat16 [65536, 2048], P('sp', 'tp'), may hold values from -72 to 72
- w_query: bfloat16 [2048, 1024], P('sp', 'tp'), may hold values from -0.125 to 0.125
- w_key: bfloat16 [2048, 256], P('sp', 'tp'), may hold values from -0.125 to 0.125
- w_value: bfloat16 [2048, 256], P('sp', 'tp'), may hold values from -0.125 to 0.125
- w_pool_in: bfloat16 [2048, 1024], P('sp', 'tp'), may hold values from -0.125 to 0.125
- sink: float32 [16], P('tp'), may hold values from 3 to 7
- w_pool: bfloat16 [4, 256, 256], P('tp'), may hold values from -0.375 to 0.375
- pool_scale: float32 [1024], P('tp'), may hold values from 0.1 to 1.9
- w_out_attn: bfloat16 [1024, 2048], P('tp', 'sp'), may hold values from -0.5 to 0.5
- w_out_pool: bfloat16 [1024, 2048], P('tp', 'sp'), may hold values from -0.125 to 0.125
- out_gain: float32 [2048], P('tp'), may hold values from 0.1 to 1.9
Outputs:
- mixed: bfloat16 [65536, 2048], P('sp', 'tp')
All inputs are finite; a program needn't handle non-finite values.
Results may differ from a plain program's by a relative error of at most 0.012.
The roundings to bfloat16 on the way count: a program that leaves them out, or rounds other values in their place, can miss the bound.
Values may be sent and summed in bfloat16 or wider, within the bound.
No kernel may reach another device: no remote copies, remote signals or barrier semaphores. Data moves between devices by JAX's collectives and lax.ppermute only.
A program may use at most 64 MiB of HBM per device.

v0:
```python
import jax
import jax.numpy as jnp
from jax import lax
from jax.sharding import Mesh
from jax.sharding import PartitionSpec as P

HEAD_DIM = 64
POOL_GROUPS = 4
WINDOW = 128
SP = ("sp_0", "sp_1", "sp_2")


epsilon = 1e-05
masked_score = -1e30


def from_everyone(shard, axis):
    count = lax.axis_size(axis)
    return lax.all_to_all(
        jnp.broadcast_to(shard[None], (count, *shard.shape)), axis, 0, 0, tiled=True
    )


def in_order(pieces, dim):
    dims = list(pieces.shape[1:])
    dims[dim] *= pieces.shape[0]
    return jnp.moveaxis(pieces, 0, dim).reshape(dims)


def gather_axes(shard, axes, dim):
    far, near = axes
    first = from_everyone(shard, far)
    pieces = jnp.swapaxes(from_everyone(first, near), 0, 1)
    return in_order(pieces.reshape(-1, *shard.shape), dim)


def gather_directly(shard, axis, dim):
    pieces = from_everyone(shard, axis)
    return in_order(pieces, dim)


def side_by_side(arrays, axis, dim, along):
    both = jnp.concatenate(arrays, axis=along)
    out, at, gathered = (lax.all_gather(both, axis, axis=dim, tiled=True), 0, [])
    for a in arrays:
        gathered.append(lax.slice_in_dim(out, at, at + a.shape[along], axis=along))
        at += a.shape[along]
    return tuple(gathered)


def padded(cells, sides, width):
    for axis, dim in sides:
        count = lax.axis_size(axis)
        ends = count - 1
        head = lax.slice_in_dim(cells, 0, width, axis=dim)
        tail = lax.slice_in_dim(cells, cells.shape[dim] - width, cells.shape[dim], axis=dim)
        cells = jnp.concatenate(
            [
                lax.ppermute(tail, axis, [(i, (i + 1) % count) for i in range(ends)]),
                cells,
                lax.ppermute(head, axis, [((i + 1) % count, i) for i in range(ends)]),
            ],
            axis=dim,
        )
    return cells


def cut_along(shard, dim, count):
    dims = shard.shape
    pieces = shard.reshape(*dims[:dim], count, dims[dim] // count, *dims[dim + 1 :])
    return jnp.moveaxis(pieces, dim, 0)


def sent_and_summed(shard, axis, dim):
    count = lax.axis_size(axis)
    pieces = lax.all_to_all(cut_along(shard, dim, count), axis, 0, 0, tiled=True)
    return jnp.sum(pieces.astype(jnp.float32), axis=0)


def of_everyone(shard, axis):
    everything = from_everyone(shard, axis)
    return jnp.sum(everything, axis=0)


def in_one(arrays, axis):
    ends = [0]
    for a in arrays:
        ends.append(ends[-1] + a.size)
    so_far = of_everyone(jnp.concatenate([a.ravel() for a in arrays]), axis)
    return tuple((so_far[b:e].reshape(a.shape) for a, b, e in zip(arrays, ends, ends[1:])))


def make_projector(gathered, pieces):
    piece_query, piece_key, piece_value, piece_chan = pieces
    joined = jnp.concatenate([piece_key, piece_value], axis=1)
    return (
        jnp.dot(gathered, piece_query, preferred_element_type=jnp.float32),
        jnp.dot(gathered, joined, preferred_element_type=jnp.float32),
        jnp.dot(gathered, piece_chan, preferred_element_type=jnp.float32),
    )


def attend_local(query, keys_ext, sinks, offset, seq_len, key_cols):
    tok_rows, query_cols = query.shape
    kv_local = key_cols // HEAD_DIM
    group = query_cols // key_cols
    block_count = tok_rows // WINDOW
    stacked = keys_ext.reshape(block_count + 2, WINDOW, 2 * key_cols)
    banded = jnp.concatenate([stacked[:-2], stacked[1:-1], stacked[2:]], axis=1)
    key_band = banded[:, :, :key_cols].reshape(block_count, 3 * WINDOW, kv_local, HEAD_DIM)
    value_band = banded[:, :, key_cols:].reshape(block_count, 3 * WINDOW, kv_local, HEAD_DIM)
    query_blocks = query.reshape(block_count, WINDOW, kv_local, group, HEAD_DIM)
    scores = jnp.einsum(
        "nqkgd,nskd->nkgqs", query_blocks, key_band, preferred_element_type=jnp.float32
    ) * HEAD_DIM ** (-0.5)
    starts = offset + jnp.arange(block_count, dtype=jnp.int32) * WINDOW
    query_pos = starts[:, None] + jnp.arange(WINDOW, dtype=jnp.int32)[None, :]
    key_pos = starts[:, None] + jnp.arange(3 * WINDOW, dtype=jnp.int32)[None, :] - WINDOW
    distance = key_pos[:, None, :] - query_pos[:, :, None]
    inside = (key_pos >= 0) & (key_pos < seq_len)
    keep = (jnp.abs(distance) <= WINDOW) & inside[:, None, :]
    scores = jnp.where(keep[:, None, None], scores, masked_score)
    sink_logit = sinks.reshape(kv_local, group)[None, :, :, None, None]
    top = jnp.maximum(jnp.max(scores, axis=-1, keepdims=True), sink_logit)
    raised = jnp.exp(scores - top)
    total = jnp.sum(raised, axis=-1, keepdims=True) + jnp.exp(sink_logit - top)
    probs = (raised / total).astype(jnp.bfloat16)
    attended = jnp.einsum(
        "nkgqs,nskd->nqkgd", probs, value_band, preferred_element_type=jnp.float32
    )
    return attended.astype(jnp.bfloat16).reshape(tok_rows, query_cols)


def local(
    tokens,
    w_query,
    w_key,
    w_value,
    w_pool_in,
    sink,
    w_pool,
    pool_scale,
    w_out_attn,
    w_out_pool,
    out_gain,
):
    tok_rows = tokens.shape[0]
    seq_len = tok_rows * lax.axis_size(SP)
    offset = lax.axis_index(SP) * tok_rows
    out_both = jnp.concatenate([w_out_attn, w_out_pool], axis=0)
    out_whole = gather_axes(out_both, (("sp_0", "sp_1"), "sp_2"), 1)
    gathered = gather_directly(tokens, "tp", 1)
    key_cols = w_key.shape[1]
    chan_cols = w_pool_in.shape[1]
    query_sum, joined_sum, chan_sum = make_projector(
        gathered, side_by_side((w_query, w_key, w_value, w_pool_in), SP, 0, 1)
    )
    query = query_sum.astype(jnp.bfloat16)
    key_value = joined_sum.astype(jnp.bfloat16)
    chan = chan_sum.astype(jnp.bfloat16)
    keys_ext = padded(key_value, ((SP, 0),), WINDOW)
    attended = attend_local(query, keys_ext, sink, offset, seq_len, key_cols)
    rim_rows = 2 ** (POOL_GROUPS - 1)
    chan_ext = padded(chan, ((SP, 0),), rim_rows)
    running = jnp.concatenate(
        [jnp.zeros((1, chan_cols), jnp.float32), jnp.cumsum(chan_ext.astype(jnp.float32), axis=0)],
        axis=0,
    )
    chan_float = chan.astype(jnp.float32)
    positions = offset + jnp.arange(tok_rows, dtype=jnp.int32)
    group_count = w_pool.shape[0]
    level = lax.axis_index("tp") * group_count + 0
    half = jnp.left_shift(jnp.int32(1), level)
    upper = lax.dynamic_slice_in_dim(running, rim_rows + half, tok_rows, 0)
    lower = lax.dynamic_slice_in_dim(running, rim_rows - half, tok_rows, 0)
    count = (
        jnp.clip(positions + half, 0, seq_len) - jnp.clip(positions - half, 0, seq_len)
    ).astype(jnp.float32)
    spread = ((upper - lower) / count[:, None] - chan_float).astype(jnp.bfloat16)
    outputs = jnp.dot(spread, w_pool[0], preferred_element_type=jnp.float32)
    pooled = (outputs * pool_scale).astype(jnp.bfloat16)
    hidden = jnp.concatenate([attended, pooled], axis=1)
    terms = jnp.dot(hidden, out_whole, preferred_element_type=jnp.float32)
    share_width = out_gain.shape[0]
    model_width = share_width * lax.axis_size("tp")
    share = sent_and_summed(terms.astype(jnp.bfloat16), "tp", 1)
    row_total, row_square = in_one((jnp.sum(share, axis=1), jnp.sum(share * share, axis=1)), "tp")
    row_mean = row_total / model_width
    variance = row_square / model_width - row_mean * row_mean
    normed = (share - row_mean[:, None]) * lax.rsqrt(variance + epsilon)[:, None] * out_gain
    return normed.astype(jnp.bfloat16)


def solution(mesh):
    finer = Mesh(mesh.devices.reshape(16, 4, 2, mesh.shape["tp"]), ("sp_0", "sp_1", "sp_2", "tp"))
    return jax.shard_map(
        local,
        mesh=finer,
        in_specs=(
            P(SP, "tp"),
            P(SP, "tp"),
            P(SP, "tp"),
            P(SP, "tp"),
            P(SP, "tp"),
            P("tp"),
            P("tp", None, None),
            P("tp"),
            P("tp", SP),
            P("tp", SP),
            P("tp"),
        ),
        out_specs=P(SP, "tp"),
        check_vma=False,
    )
```

profile of v0, /device:TPU:32, one launch (start us, length us, event | category | flops | bytes accessed | tf_op | source)
XLA Modules:
  0.0 244.4 jit_solution(12594577696997631340)
XLA Ops:
  6.6 0.8 pad_maximum_fusion.3
  7.4 1.1 broadcast_in_dim.19
  8.5 18.2 %all-to-all-start.1 = ((bf16[64,512,16]{1,2,0:T(8,128)(2,1)}), bf16[64,512,16]{1,2,0:T(8,128)(2,1)S(1)}, u32[]{:S(2)}, u32[]{:S(2)}) async-start(bf16[64,512,16]{1,2,0:T(8,128)(2,1)} %broadcast_in_dim.19), calls=%async_computation.1 | async-start | bytes 2097152 | tf_op jit(solution)/shard_map/all_to_all | solution.py:19
  26.8 0.7 pad_maximum_fusion.2
  27.7 53.9 %all-to-all-done.1 = bf16[64,512,16]{1,2,0:T(8,128)(2,1)S(1)} async-done(((bf16[64,512,16]{1,2,0:T(8,128)(2,1)}), bf16[64,512,16]{1,2,0:T(8,128)(2,1)S(1)}, u32[]{:S(2)}, u32[]{:S(2)}) %all-to-all-start.1) | async-done | bytes 1048608 | tf_op jit(solution)/shard_map/all_to_all | solution.py:19
  81.7 0.3 broadcast_in_dim.20
  82.0 6.4 %all_to_all.26 = bf16[2,64,512,16]{2,3,1,0:T(8,128)(2,1)} all-to-all(bf16[2,64,512,16]{2,3,1,0:T(8,128)(2,1)S(1)} %broadcast_in_dim.20), channel_id=1, replica_groups=mesh['sp_0'=16,'sp_1'=4,'sp_2'=2,'tp'=4] {'sp_2'}, dimensions={0} | all-to-all | bytes 4194304 | tf_op jit(solution)/shard_map/all_to_all | solution.py:19
  88.3 1.6 broadcast_in_dim.16
  89.9 4.5 %all-to-all-start = ((bf16[4,512,512]{1,2,0:T(8,128)(2,1)}), bf16[4,512,512]{1,2,0:T(8,128)(2,1)S(1)}, u32[]{:S(2)}, u32[]{:S(2)}) async-start(bf16[4,512,512]{1,2,0:T(8,128)(2,1)} %broadcast_in_dim.16), calls=%async_computation | async-start | bytes 4194304 | tf_op jit(solution)/shard_map/all_to_all | solution.py:19
  94.6 0.6 fusion.17
  95.2 3.2 %copy.68 = bf16[2,64,512,16]{2,3,0,1:T(8,128)(2,1)} copy(bf16[2,64,512,16]{2,3,1,0:T(8,128)(2,1)} %all_to_all.26) | data formatting | bytes 4194304 | tf_op jit(solution)/shard_map/all_to_all | solution.py:19
  98.3 22.7 %all-to-all-done = bf16[4,512,512]{1,2,0:T(8,128)(2,1)S(1)} async-done(((bf16[4,512,512]{1,2,0:T(8,128)(2,1)}), bf16[4,512,512]{1,2,0:T(8,128)(2,1)S(1)}, u32[]{:S(2)}, u32[]{:S(2)}) %all-to-all-start) | async-done | bytes 2097184 | tf_op jit(solution)/shard_map/all_to_all | solution.py:19
  121.0 52.2 %all-gather.2.cloned.1.call-done = bf16[2048,640]{1,0:T(8,128)(2,1)} async-done(((bf16[16,640]{1,0:T(8,128)(2,1)}), bf16[2048,640]{1,0:T(8,128)(2,1)}) %all-gather.2.cloned.1.call-update) | async-done | bytes 2621456 | tf_op jit(solution)/shard_map/all_gather | solution.py:44
  173.2 1.7 convolution_convert_fusion.3
  174.8 2.1 collective-permute-start
  177.0 5.5 %collective-permute-start.1 = (bf16[128,128]{0,1:T(8,128)(2,1)S(1)}, bf16[128,128]{0,1:T(8,128)(2,1)S(1)}, u32[]{:S(2)}, u32[]{:S(2)}) collective-permute-start(bf16[128,128]{0,1:T(8,128)(2,1)S(1)} %get-tuple-element.11), channel_id=1, source_target_pairs={{4,0},{8,4},{12,8},{16,12},{20,16},{24,20},{28,24},{32,28},{36,32}... | collective-permute-start | bytes 98312 | tf_op jit(solution)/shard_map/ppermute | solution.py:61
  182.5 0.7 fusion.9
  183.4 1.9 collective-permute-start.2
  185.3 5.8 %collective-permute-start.3 = (bf16[8,256]{0,1:T(8,128)(2,1)S(1)}, bf16[8,256]{0,1:T(8,128)(2,1)S(1)}, u32[]{:S(2)}, u32[]{:S(2)}) collective-permute-start(bf16[8,256]{0,1:T(8,128)(2,1)S(1)} %get-tuple-element.8), channel_id=1, source_target_pairs={{4,0},{8,4},{12,8},{16,12},{20,16},{24,20},{28,24},{32,28},{36,32}... | collective-permute-start | bytes 12296 | tf_op jit(solution)/shard_map/ppermute | solution.py:61
  191.1 0.7 fusion.8
  191.9 1.1 collective-permute-done.3
  193.4 0.7 fusion.15
  194.8 0.6 fusion.4
  195.6 0.6 fusion.1
  196.3 0.7 fusion
  197.1 0.9 fusion.10
  198.3 0.4 copy-done.1
  198.7 1.3 convolution_convert_fusion
  200.2 28.0 %all_to_all.27 = bf16[4,512,512]{2,1,0:T(8,128)(2,1)S(1)} all-to-all(bf16[4,512,512]{2,1,0:T(8,128)(2,1)S(1)} %bitcast.103), channel_id=1, replica_groups=mesh['sp_0'=16,'sp_1'=4,'sp_2'=2,'tp'=4] {'tp'}, dimensions={0} | all-to-all | bytes 4194304 | tf_op jit(solution)/shard_map/all_to_all | solution.py:76
  228.2 0.5 convert_reduce_fusion
  228.8 7.7 %all_to_all.28 = f32[4,1,1024]{2,1,0:T(1,128)S(1)} all-to-all(f32[4,1,1024]{2,1,0:T(1,128)S(1)} %broadcast_in_dim.21), channel_id=1, replica_groups=mesh['sp_0'=16,'sp_1'=4,'sp_2'=2,'tp'=4] {'tp'}, dimensions={0} | all-to-all | bytes 32768 | tf_op jit(solution)/shard_map/all_to_all | solution.py:19
  236.6 1.0 multiply_convert_fusion
  (57 shorter events, 2.7 us)
Async XLA Ops:
  6.5 188.1 %copy-start = (bf16[1,256,256]{2,1,0:T(8,128)(2,1)S(1)}, bf16[1,256,256]{2,1,0:T(8,128)(2,1)}, u32[]{:S(2)}) copy-start(bf16[1,256,256]{2,1,0:T(8,128)(2,1)} %param.17) | copy-start | bytes 393220
  6.5 20.2 %copy-start.5 = (bf16[16,256]{1,0:T(8,128)(2,1)S(1)}, bf16[16,256]{1,0:T(8,128)(2,1)}, u32[]{:S(2)}) copy-start(bf16[16,256]{1,0:T(8,128)(2,1)} %param.12) | copy-start | bytes 24580
  6.5 20.2 %copy-start.7 = (bf16[16,64]{1,0:T(8,128)(2,1)S(1)}, bf16[16,64]{1,0:T(8,128)(2,1)}, u32[]{:S(2)}) copy-start(bf16[16,64]{1,0:T(8,128)(2,1)} %param.13) | copy-start | bytes 6148
  6.5 20.2 %copy-start.6 = (bf16[16,64]{1,0:T(8,128)(2,1)S(1)}, bf16[16,64]{1,0:T(8,128)(2,1)}, u32[]{:S(2)}) copy-start(bf16[16,64]{1,0:T(8,128)(2,1)} %param.14) | copy-start | bytes 6148
  6.5 20.2 %copy-start.4 = (bf16[16,256]{1,0:T(8,128)(2,1)S(1)}, bf16[16,256]{1,0:T(8,128)(2,1)}, u32[]{:S(2)}) copy-start(bf16[16,256]{1,0:T(8,128)(2,1)} %param.15) | copy-start | bytes 24580
  6.5 21.0 %copy-start.2 = (bf16[512,512]{1,0:T(8,128)(2,1)S(1)}, bf16[512,512]{1,0:T(8,128)(2,1)}, u32[]{:S(2)}) copy-start(bf16[512,512]{1,0:T(8,128)(2,1)} %param.11) | copy-start | bytes 1572868
  8.5 73.2 %all-to-all-start.1 = ((bf16[64,512,16]{1,2,0:T(8,128)(2,1)}), bf16[64,512,16]{1,2,0:T(8,128)(2,1)S(1)}, u32[]{:S(2)}, u32[]{:S(2)}) async-start(bf16[64,512,16]{1,2,0:T(8,128)(2,1)} %broadcast_in_dim.19), calls=%async_computation.1 | async-start | bytes 2097152 | tf_op jit(solution)/shard_map/all_to_all | solution.py:19
  26.7 146.5 %all-gather.2.cloned.1.call-start = ((), (), s32[]{:S(2)}) async-start(), calls=%async_computation.5 | async-start | bytes 2641920 | tf_op jit(solution)/shard_map/all_gather | solution.py:44
  89.9 31.1 %all-to-all-start = ((bf16[4,512,512]{1,2,0:T(8,128)(2,1)}), bf16[4,512,512]{1,2,0:T(8,128)(2,1)S(1)}, u32[]{:S(2)}, u32[]{:S(2)}) async-start(bf16[4,512,512]{1,2,0:T(8,128)(2,1)} %broadcast_in_dim.16), calls=%async_computation | async-start | bytes 4194304 | tf_op jit(solution)/shard_map/all_to_all | solution.py:19
  173.2 9.4 %copy-start.3 = (bf16[2048,640]{1,0:T(8,128)(2,1)S(1)}, bf16[2048,640]{1,0:T(8,128)(2,1)}, u32[]{:S(2)}) copy-start(bf16[2048,640]{1,0:T(8,128)(2,1)} %all-gather.2.cloned.1.call-done) | copy-start | bytes 7864324
  174.8 20.6 %collective-permute-start = (bf16[128,128]{0,1:T(8,128)(2,1)S(1)}, bf16[128,128]{0,1:T(8,128)(2,1)S(1)}, u32[]{:S(2)}, u32[]{:S(2)}) collective-permute-start(bf16[128,128]{0,1:T(8,128)(2,1)S(1)} %get-tuple-element.12), channel_id=1, source_target_pairs={{0,4},{4,8},{8,12},{12,16},{16,20},{20,24},{24,28},{28,32},{32,36}... | collective-permute-start | bytes 98312 | tf_op jit(solution)/shard_map/ppermute | solution.py:59
  177.0 18.4 %collective-permute-start.1 = (bf16[128,128]{0,1:T(8,128)(2,1)S(1)}, bf16[128,128]{0,1:T(8,128)(2,1)S(1)}, u32[]{:S(2)}, u32[]{:S(2)}) collective-permute-start(bf16[128,128]{0,1:T(8,128)(2,1)S(1)} %get-tuple-element.11), channel_id=1, source_target_pairs={{4,0},{8,4},{12,8},{16,12},{20,16},{24,20},{28,24},{32,28},{36,32}... | collective-permute-start | bytes 98312 | tf_op jit(solution)/shard_map/ppermute | solution.py:61
  183.4 8.5 %collective-permute-start.2 = (bf16[8,256]{0,1:T(8,128)(2,1)S(1)}, bf16[8,256]{0,1:T(8,128)(2,1)S(1)}, u32[]{:S(2)}, u32[]{:S(2)}) collective-permute-start(bf16[8,256]{0,1:T(8,128)(2,1)S(1)} %get-tuple-element.7), channel_id=1, source_target_pairs={{0,4},{4,8},{8,12},{12,16},{16,20},{20,24},{24,28},{28,32},{32,36}... | collective-permute-start | bytes 12296 | tf_op jit(solution)/shard_map/ppermute | solution.py:59
  185.3 7.6 %collective-permute-start.3 = (bf16[8,256]{0,1:T(8,128)(2,1)S(1)}, bf16[8,256]{0,1:T(8,128)(2,1)S(1)}, u32[]{:S(2)}, u32[]{:S(2)}) collective-permute-start(bf16[8,256]{0,1:T(8,128)(2,1)S(1)} %get-tuple-element.8), channel_id=1, source_target_pairs={{4,0},{8,4},{12,8},{16,12},{20,16},{24,20},{28,24},{32,28},{36,32}... | collective-permute-start | bytes 12296 | tf_op jit(solution)/shard_map/ppermute | solution.py:61
  194.1 0.7 copy-start.10
  195.4 0.9 copy-start.9
  197.1 1.6 copy-start.1
  228.2 8.4 %copy-start.8 = (f32[512]{0:T(512)S(1)}, f32[512]{0:T(512)}, u32[]{:S(2)}) copy-start(f32[512]{0:T(512)} %param.21) | copy-start | bytes 6148
Sparse Core Ops, SparseCore 0:
  30.6 142.5 all-gather.1
where the time goes:
time: 245 us; the launch traced here: 244 us
  waiting for transfers between devices  130 us (53%)
  blocking collectives  42.1 us (17%)
  starting transfers between devices  38.1 us (16%)
  between operations  13.8 us (6%)
  local copies, waits for them, and re-layouts  8.25 us (3%)
  matrix products  6.58 us (3%)
  other arithmetic  5.83 us (2%)
    all_to_all x2, waiting for transfers between devices, from_everyone(): lax.all_to_all(jnp.broadcast_to(shard[None], (count, *shard.shape)), axis...  76.6 us
    all_gather x1, waiting for transfers between devices, side_by_side(): lax.all_gather(both, axis, axis=dim, tiled=True)  52.2 us
    all_to_all x1, blocking collectives, sent_and_summed(): lax.all_to_all(cut_along(shard, dim, count), axis, 0, 0, tiled=True)  28 us
    all_to_all x2, starting transfers between devices, from_everyone(): lax.all_to_all(jnp.broadcast_to(shard[None], (count, *shard.shape)), axis...  22.7 us
    all_to_all x2, blocking collectives, from_everyone(): lax.all_to_all(jnp.broadcast_to(shard[None], (count, *shard.shape)), axis...  14.1 us
    ppermute x2, starting transfers between devices, padded(): lax.ppermute(head, axis, [((i + 1) % count, i) for i in range(ends)])  11.3 us
  transfers between devices with their start and end apart: 7, of which 4 were waited for; matrix products, arithmetic and copies ran while one was open for 4% of the time, Pallas kernels for 0%

commit v1 on v0

--- a/solution.py
+++ b/solution.py
@@ -4,10 +4,12 @@
 from jax.sharding import Mesh
 from jax.sharding import PartitionSpec as P
 
+
 HEAD_DIM = 64
 POOL_GROUPS = 4
 WINDOW = 128
 SP = ("sp_0", "sp_1", "sp_2")
+Z, X, CORE = SP
 
 
 epsilon = 1e-05
@@ -27,42 +29,31 @@
     return jnp.moveaxis(pieces, 0, dim).reshape(dims)
 
 
-def gather_axes(shard, axes, dim):
-    far, near = axes
-    first = from_everyone(shard, far)
-    pieces = jnp.swapaxes(from_everyone(first, near), 0, 1)
-    return in_order(pieces.reshape(-1, *shard.shape), dim)
-
-
 def gather_directly(shard, axis, dim):
     pieces = from_everyone(shard, axis)
     return in_order(pieces, dim)
 
 
-def side_by_side(arrays, axis, dim, along):
-    both = jnp.concatenate(arrays, axis=along)
-    out, at, gathered = (lax.all_gather(both, axis, axis=dim, tiled=True), 0, [])
-    for a in arrays:
-        gathered.append(lax.slice_in_dim(out, at, at + a.shape[along], axis=along))
-        at += a.shape[along]
-    return tuple(gathered)
-
-
-def padded(cells, sides, width):
-    for axis, dim in sides:
-        count = lax.axis_size(axis)
-        ends = count - 1
-        head = lax.slice_in_dim(cells, 0, width, axis=dim)
-        tail = lax.slice_in_dim(cells, cells.shape[dim] - width, cells.shape[dim], axis=dim)
-        cells = jnp.concatenate(
-            [
-                lax.ppermute(tail, axis, [(i, (i + 1) % count) for i in range(ends)]),
-                cells,
-                lax.ppermute(head, axis, [((i + 1) % count, i) for i in range(ends)]),
-            ],
-            axis=dim,
-        )
-    return cells
+def gather_weights(pieces):
+    packed = jnp.concatenate(pieces, axis=1)
+    over_z = lax.all_gather(packed, Z, axis=0)
+    return over_z
+
+
+def over_x_and_cores(over_z):
+    own = from_everyone(over_z, X).reshape(lax.axis_size(X), *over_z.shape)
+    other = lax.ppermute(own, CORE, [(0, 1), (1, 0)])
+    first = lax.axis_index(CORE) == 0
+    both = jnp.stack([jnp.where(first, own, other), jnp.where(first, other, own)])
+    core, x, z, rows, cols = both.shape
+    return both.transpose(2, 1, 0, 3, 4).reshape(z * x * core * rows, cols)
+
+
+def neighbours(head, tail, axis):
+    count = lax.axis_size(axis)
+    before = lax.ppermute(tail, axis, [(i, i + 1) for i in range(count - 1)])
+    after = lax.ppermute(head, axis, [(i + 1, i) for i in range(count - 1)])
+    return before, after
 
 
 def cut_along(shard, dim, count):
@@ -88,16 +79,6 @@
         ends.append(ends[-1] + a.size)
     so_far = of_everyone(jnp.concatenate([a.ravel() for a in arrays]), axis)
     return tuple((so_far[b:e].reshape(a.shape) for a, b, e in zip(arrays, ends, ends[1:])))
-
-
-def make_projector(gathered, pieces):
-    piece_query, piece_key, piece_value, piece_chan = pieces
-    joined = jnp.concatenate([piece_key, piece_value], axis=1)
-    return (
-        jnp.dot(gathered, piece_query, preferred_element_type=jnp.float32),
-        jnp.dot(gathered, joined, preferred_element_type=jnp.float32),
-        jnp.dot(gathered, piece_chan, preferred_element_type=jnp.float32),
-    )
 
 
 def attend_local(query, keys_ext, sinks, offset, seq_len, key_cols):
@@ -131,7 +112,7 @@
     return attended.astype(jnp.bfloat16).reshape(tok_rows, query_cols)
 
 
-def local(
+def layer(
     tokens,
     w_query,
     w_key,
@@ -147,21 +128,39 @@
     tok_rows = tokens.shape[0]
     seq_len = tok_rows * lax.axis_size(SP)
     offset = lax.axis_index(SP) * tok_rows
-    out_both = jnp.concatenate([w_out_attn, w_out_pool], axis=0)
-    out_whole = gather_axes(out_both, (("sp_0", "sp_1"), "sp_2"), 1)
-    gathered = gather_directly(tokens, "tp", 1)
     key_cols = w_key.shape[1]
     chan_cols = w_pool_in.shape[1]
-    query_sum, joined_sum, chan_sum = make_projector(
-        gathered, side_by_side((w_query, w_key, w_value, w_pool_in), SP, 0, 1)
-    )
-    query = query_sum.astype(jnp.bfloat16)
-    key_value = joined_sum.astype(jnp.bfloat16)
-    chan = chan_sum.astype(jnp.bfloat16)
-    keys_ext = padded(key_value, ((SP, 0),), WINDOW)
+    gathered = gather_directly(tokens, "tp", 1)
+    pieces = (w_query, w_key, w_value, w_pool_in, w_out_attn.T, w_out_pool.T)
+    in_cols = w_query.shape[1] + 2 * key_cols + chan_cols
+    over_z = gather_weights(pieces)
+    in_whole = over_x_and_cores(over_z[:, :, :in_cols])
+    out_whole = over_x_and_cores(over_z[:, :, in_cols:])
+    projected = jnp.dot(gathered, in_whole, preferred_element_type=jnp.float32)
+    projected = projected.astype(jnp.bfloat16)
+    query = projected[:, : w_query.shape[1]]
+    key_value = projected[:, w_query.shape[1] : in_cols - chan_cols]
+    chan = projected[:, in_cols - chan_cols :]
+    rim_rows = 2 ** (POOL_GROUPS - 1)
+
+    def rim(start_kv, start_chan):
+        return jnp.concatenate(
+            [
+                key_value[start_kv : start_kv + WINDOW],
+                chan[start_chan : start_chan + rim_rows].reshape(-1, 2 * key_cols),
+            ]
+        )
+
+    before, after = neighbours(rim(0, 0), rim(tok_rows - WINDOW, tok_rows - rim_rows), SP)
+    keys_ext = jnp.concatenate([before[:WINDOW], key_value, after[:WINDOW]])
+    chan_ext = jnp.concatenate(
+        [
+            before[WINDOW:].reshape(rim_rows, chan_cols),
+            chan,
+            after[WINDOW:].reshape(rim_rows, chan_cols),
+        ]
+    )
     attended = attend_local(query, keys_ext, sink, offset, seq_len, key_cols)
-    rim_rows = 2 ** (POOL_GROUPS - 1)
-    chan_ext = padded(chan, ((SP, 0),), rim_rows)
     running = jnp.concatenate(
         [jnp.zeros((1, chan_cols), jnp.float32), jnp.cumsum(chan_ext.astype(jnp.float32), axis=0)],
         axis=0,
@@ -180,7 +179,9 @@
     outputs = jnp.dot(spread, w_pool[0], preferred_element_type=jnp.float32)
     pooled = (outputs * pool_scale).astype(jnp.bfloat16)
     hidden = jnp.concatenate([attended, pooled], axis=1)
-    terms = jnp.dot(hidden, out_whole, preferred_element_type=jnp.float32)
+    terms = lax.dot_general(
+        hidden, out_whole, (((1,), (1,)), ((), ())), preferred_element_type=jnp.float32
+    )
     share_width = out_gain.shape[0]
     model_width = share_width * lax.axis_size("tp")
     share = sent_and_summed(terms.astype(jnp.bfloat16), "tp", 1)
@@ -194,7 +195,7 @@
 def solution(mesh):
     finer = Mesh(mesh.devices.reshape(16, 4, 2, mesh.shape["tp"]), ("sp_0", "sp_1", "sp_2", "tp"))
     return jax.shard_map(
-        local,
+        layer,
         mesh=finer,
         in_specs=(
             P(SP, "tp"),

time: 245 us -> 156 us (0.64)
  the two profiles are of different devices: /device:TPU:32 before, /device:TPU:6 now
where the time goes in v1:
time: 156 us; the launch traced here: 155 us
  blocking collectives  76.6 us (49%)
  waiting for transfers between devices  28 us (18%)
  starting transfers between devices  24.4 us (16%)
  local copies, waits for them, and re-layouts  9.58 us (6%)
  other arithmetic  9.55 us (6%)
  matrix products  6.79 us (4%)
    all_gather x1, blocking collectives, gather_weights(): over_z = lax.all_gather(packed, Z, axis=0)  38.9 us
    all_to_all x1, blocking collectives, sent_and_summed(): lax.all_to_all(cut_along(shard, dim, count), axis, 0, 0, tiled=True)  30 us
    all_to_all x3, waiting for transfers between devices, from_everyone(): lax.all_to_all(jnp.broadcast_to(shard[None], (count, *shard.shape)), axis...  26.9 us
    all_to_all x3, starting transfers between devices, from_everyone(): lax.all_to_all(jnp.broadcast_to(shard[None], (count, *shard.shape)), axis...  14.9 us
    all_to_all x1, blocking collectives, from_everyone(): lax.all_to_all(jnp.broadcast_to(shard[None], (count, *shard.shape)), axis...  7.71 us
    another operation x4, other arithmetic, over_x_and_cores(): jnp.stack([jnp.where(first, own, other), jnp.where(first, other, own)])  4.7 us
    ppermute x2, starting transfers between devices, over_x_and_cores(): other = lax.ppermute(own, CORE, [(0, 1), (1, 0)])  3.82 us
    broadcast_in_dim x4, local copies, waits for them, and re-layouts, from_everyone(): jnp.broadcast_to(shard[None], (count, *shard.shape))  3.75 us
  transfers between devices with their start and end apart: 7, of which 4 were waited for; matrix products, arithmetic and copies ran while one was open for 7% of the time, Pallas kernels for 0%

profile of v1, /device:TPU:6, one launch (start us, length us, event | category | flops | bytes accessed | tf_op | source)
XLA Modules:
  0.0 155.4 jit_solution(12818065805638688181)
XLA Ops:
  0.0 0.9 concatenate.31
  0.9 38.9 %all-gather = bf16[256,1152]{1,0:T(8,128)(2,1)S(1)} all-gather(bf16[16,1152]{1,0:T(8,128)(2,1)S(1)} %concatenate.31), channel_id=2, replica_groups=mesh['sp_0'=16,'sp_1'=4,'sp_2'=2,'tp'=4] {'sp_0'}, dimensions={0}, use_global_device_ids=true | all-gather | bytes 626688 | tf_op jit(solution)/shard_map/all_gather | solution.py:39
  39.8 1.1 broadcast_in_dim.20
  40.9 4.8 %all-to-all-start.2 = ((bf16[4,16,16,512]{3,2,1,0:T(8,128)(2,1)}), bf16[4,16,16,512]{3,2,1,0:T(8,128)(2,1)S(1)}, u32[]{:S(2)}, u32[]{:S(2)}) async-start(bf16[4,16,16,512]{3,2,1,0:T(8,128)(2,1)} %broadcast_in_dim.20), calls=%async_computation.2 | async-start | bytes 2097152 | tf_op jit(solution)/shard_map/all_to_all | solution.py:21
  45.7 8.9 %all-to-all-done.2 = bf16[4,16,16,512]{3,2,1,0:T(8,128)(2,1)S(1)} async-done(((bf16[4,16,16,512]{3,2,1,0:T(8,128)(2,1)}), bf16[4,16,16,512]{3,2,1,0:T(8,128)(2,1)S(1)}, u32[]{:S(2)}, u32[]{:S(2)}) %all-to-all-start.2) | async-done | bytes 1048608 | tf_op jit(solution)/shard_map/all_to_all | solution.py:21
  54.6 1.2 broadcast_in_dim.16
  55.8 5.6 %all-to-all-start = ((bf16[4,16,16,640]{3,2,1,0:T(8,128)(2,1)}), bf16[4,16,16,640]{3,2,1,0:T(8,128)(2,1)S(1)}, u32[]{:S(2)}, u32[]{:S(2)}) async-start(bf16[4,16,16,640]{3,2,1,0:T(8,128)(2,1)} %broadcast_in_dim.16), calls=%async_computation | async-start | bytes 2621440 | tf_op jit(solution)/shard_map/all_to_all | solution.py:21
  61.4 1.1 copy.84
  62.5 1.9 %collective-permute-start.3 = (bf16[4,16,16,512]{3,2,0,1:T(8,128)(2,1)}, bf16[4,16,16,512]{3,2,0,1:T(8,128)(2,1)}, u32[]{:S(2)}, u32[]{:S(2)}) collective-permute-start(bf16[4,16,16,512]{3,2,0,1:T(8,128)(2,1)} %copy.84), channel_id=1, source_target_pairs={{0,4},{4,0},{1,5},{5,1},{2,6},{6,2},{3,7},{7,3},{8,12},{12,8},{9,1... | collective-permute-start | bytes 3145736 | tf_op jit(solution)/shard_map/ppermute | solution.py:45
  64.6 7.0 %all-to-all-done = bf16[4,16,16,640]{3,2,1,0:T(8,128)(2,1)S(1)} async-done(((bf16[4,16,16,640]{3,2,1,0:T(8,128)(2,1)}), bf16[4,16,16,640]{3,2,1,0:T(8,128)(2,1)S(1)}, u32[]{:S(2)}, u32[]{:S(2)}) %all-to-all-start) | async-done | bytes 1310752 | tf_op jit(solution)/shard_map/all_to_all | solution.py:21
  71.6 1.5 broadcast_in_dim.17
  73.1 4.5 %all-to-all-start.1 = ((bf16[4,512,512]{1,2,0:T(8,128)(2,1)}), bf16[4,512,512]{1,2,0:T(8,128)(2,1)}, u32[]{:S(2)}, u32[]{:S(2)}) async-start(bf16[4,512,512]{1,2,0:T(8,128)(2,1)} %broadcast_in_dim.17), calls=%async_computation.1 | async-start | bytes 4194304 | tf_op jit(solution)/shard_map/all_to_all | solution.py:21
  77.6 1.3 copy.70
  78.8 1.9 %collective-permute-start = (bf16[4,16,16,640]{3,2,0,1:T(8,128)(2,1)}, bf16[4,16,16,640]{3,2,0,1:T(8,128)(2,1)}, u32[]{:S(2)}, u32[]{:S(2)}) collective-permute-start(bf16[4,16,16,640]{3,2,0,1:T(8,128)(2,1)} %copy.70), channel_id=1, source_target_pairs={{0,4},{4,0},{1,5},{5,1},{2,6},{6,2},{3,7},{7,3},{8,12},{12,8},{9,1... | collective-permute-start | bytes 3932168 | tf_op jit(solution)/shard_map/ppermute | solution.py:45
  81.0 1.2 fusion.14
  82.2 1.4 select_bitcast_fusion.3
  83.5 1.5 pad_maximum_fusion.1
  85.1 1.6 %select_bitcast_fusion.1 = (bf16[1,4,16,16,640]{4,3,0,1,2:T(8,128)(2,1)S(1)}, bf16[1,4,16,16,640]{4,3,0,1,2:T(8,128)(2,1)S(1)}) fusion(bf16[4,16,16,640]{3,2,0,1:T(8,128)(2,1)} %collective-permute-done, pred[]{:T(512)S(6)} %eq.4, bf16[4,16,16,640]{3,2,1,0:T(8,128)(2,1)S(1)} %all-to-all-done), kind=kLoop, calls=%fused_computation.15 | loop fusion | flops 1310720 | bytes 5242881 | tf_op jit(solution)/shard_map/stack | solution.py:47
  86.9 11.0 %all-to-all-done.1 = bf16[4,512,512]{1,2,0:T(8,128)(2,1)} async-done(((bf16[4,512,512]{1,2,0:T(8,128)(2,1)}), bf16[4,512,512]{1,2,0:T(8,128)(2,1)}, u32[]{:S(2)}, u32[]{:S(2)}) %all-to-all-start.1) | async-done | bytes 2097184 | tf_op jit(solution)/shard_map/all_to_all | solution.py:21
  97.9 3.4 %fusion.4 = bf16[512,640]{1,0:T(8,128)(2,1)S(1)} fusion(bf16[2048,640]{1,0:T(8,128)(2,1)S(1)} %bitcast.100, bf16[512,2048]{0,1:T(8,128)(2,1)} %bitcast.9), kind=kOutput, calls=%fused_computation.16 | convolution fusion | flops 1342504960 | bytes 5373952 | tf_op jit(solution)/shard_map/dot_general | solution.py:139
  101.4 2.1 %collective-permute-start.1 = (bf16[144,128]{1,0:T(8,128)(2,1)S(1)}, bf16[144,128]{1,0:T(8,128)(2,1)S(1)}, u32[]{:S(2)}, u32[]{:S(2)}) collective-permute-start(bf16[144,128]{1,0:T(8,128)(2,1)S(1)} %pad_maximum_fusion.5), channel_id=1, source_target_pairs={{0,4},{4,8},{8,12},{12,16},{16,20},{20,24},{24,28},{28,32},{32,36}... | collective-permute-start | bytes 110600 | tf_op jit(solution)/shard_map/ppermute | solution.py:54
  103.5 3.6 %collective-permute-start.2 = (bf16[144,128]{1,0:T(8,128)(2,1)S(1)}, bf16[144,128]{1,0:T(8,128)(2,1)S(1)}, u32[]{:S(2)}, u32[]{:S(2)}) collective-permute-start(bf16[144,128]{1,0:T(8,128)(2,1)S(1)} %pad_maximum_fusion.6), channel_id=1, source_target_pairs={{4,0},{8,4},{12,8},{16,12},{20,16},{24,20},{28,24},{32,28},{36,32}... | collective-permute-start | bytes 110600 | tf_op jit(solution)/shard_map/ppermute | solution.py:55
  107.6 1.1 collective-permute-done.2
  109.1 0.7 fusion.1
  109.9 0.7 fusion
  110.7 1.0 fusion.9
  112.1 0.7 fusion.12
  113.8 0.6 copy-done.1
  114.5 1.3 convolution_convert_fusion
  115.9 30.0 %all_to_all.26 = bf16[4,512,512]{2,1,0:T(8,128)(2,1)S(1)} all-to-all(bf16[4,512,512]{2,1,0:T(8,128)(2,1)S(1)} %bitcast.99), channel_id=1, replica_groups=mesh['sp_0'=16,'sp_1'=4,'sp_2'=2,'tp'=4] {'tp'}, dimensions={0} | all-to-all | bytes 4194304 | tf_op jit(solution)/shard_map/all_to_all | solution.py:67
  146.6 7.7 %all_to_all.27 = f32[4,1,1024]{2,1,0:T(1,128)S(1)} all-to-all(f32[4,1,1024]{2,1,0:T(1,128)S(1)} %broadcast_in_dim.21), channel_id=1, replica_groups=mesh['sp_0'=16,'sp_1'=4,'sp_2'=2,'tp'=4] {'tp'}, dimensions={0} | all-to-all | bytes 32768 | tf_op jit(solution)/shard_map/all_to_all | solution.py:21
  154.4 1.0 multiply_convert_fusion
  (65 shorter events, 4.0 us)
Async XLA Ops:
  0.0 113.1 %copy-start = (bf16[1,256,256]{2,1,0:T(8,128)(2,1)S(1)}, bf16[1,256,256]{2,1,0:T(8,128)(2,1)}, u32[]{:S(2)}) copy-start(bf16[1,256,256]{2,1,0:T(8,128)(2,1)} %param.17) | copy-start | bytes 393220
  40.9 13.7 %all-to-all-start.2 = ((bf16[4,16,16,512]{3,2,1,0:T(8,128)(2,1)}), bf16[4,16,16,512]{3,2,1,0:T(8,128)(2,1)S(1)}, u32[]{:S(2)}, u32[]{:S(2)}) async-start(bf16[4,16,16,512]{3,2,1,0:T(8,128)(2,1)} %broadcast_in_dim.20), calls=%async_computation.2 | async-start | bytes 2097152 | tf_op jit(solution)/shard_map/all_to_all | solution.py:21
  55.7 8.7 %copy-start.3 = (bf16[512,512]{1,0:T(8,128)(2,1)S(1)}, bf16[512,512]{1,0:T(8,128)(2,1)}, u32[]{:S(2)}) copy-start(bf16[512,512]{1,0:T(8,128)(2,1)} %param.11) | copy-start | bytes 1572868
  55.8 15.9 %all-to-all-start = ((bf16[4,16,16,640]{3,2,1,0:T(8,128)(2,1)}), bf16[4,16,16,640]{3,2,1,0:T(8,128)(2,1)S(1)}, u32[]{:S(2)}, u32[]{:S(2)}) async-start(bf16[4,16,16,640]{3,2,1,0:T(8,128)(2,1)} %broadcast_in_dim.16), calls=%async_computation | async-start | bytes 2621440 | tf_op jit(solution)/shard_map/all_to_all | solution.py:21
  62.5 19.7 %collective-permute-start.3 = (bf16[4,16,16,512]{3,2,0,1:T(8,128)(2,1)}, bf16[4,16,16,512]{3,2,0,1:T(8,128)(2,1)}, u32[]{:S(2)}, u32[]{:S(2)}) collective-permute-start(bf16[4,16,16,512]{3,2,0,1:T(8,128)(2,1)} %copy.84), channel_id=1, source_target_pairs={{0,4},{4,0},{1,5},{5,1},{2,6},{6,2},{3,7},{7,3},{8,12},{12,8},{9,1... | collective-permute-start | bytes 3145736 | tf_op jit(solution)/shard_map/ppermute | solution.py:45
  73.1 24.8 %all-to-all-start.1 = ((bf16[4,512,512]{1,2,0:T(8,128)(2,1)}), bf16[4,512,512]{1,2,0:T(8,128)(2,1)}, u32[]{:S(2)}, u32[]{:S(2)}) async-start(bf16[4,512,512]{1,2,0:T(8,128)(2,1)} %broadcast_in_dim.17), calls=%async_computation.1 | async-start | bytes 4194304 | tf_op jit(solution)/shard_map/all_to_all | solution.py:21
  78.8 6.2 %collective-permute-start = (bf16[4,16,16,640]{3,2,0,1:T(8,128)(2,1)}, bf16[4,16,16,640]{3,2,0,1:T(8,128)(2,1)}, u32[]{:S(2)}, u32[]{:S(2)}) collective-permute-start(bf16[4,16,16,640]{3,2,0,1:T(8,128)(2,1)} %copy.70), channel_id=1, source_target_pairs={{0,4},{4,0},{1,5},{5,1},{2,6},{6,2},{3,7},{7,3},{8,12},{12,8},{9,1... | collective-permute-start | bytes 3932168 | tf_op jit(solution)/shard_map/ppermute | solution.py:45
  101.3 7.8 %copy-start.2 = (pred[4,128,384]{1,2,0:T(8,128)(4,1)S(1)}, pred[4,128,384]{1,2,0:T(8,128)(4,1)}, u32[]{:S(2)}) copy-start(pred[4,128,384]{1,2,0:T(8,128)(4,1)} %fusion.14) | copy-start | bytes 589828
  101.4 6.2 %collective-permute-start.1 = (bf16[144,128]{1,0:T(8,128)(2,1)S(1)}, bf16[144,128]{1,0:T(8,128)(2,1)S(1)}, u32[]{:S(2)}, u32[]{:S(2)}) collective-permute-start(bf16[144,128]{1,0:T(8,128)(2,1)S(1)} %pad_maximum_fusion.5), channel_id=1, source_target_pairs={{0,4},{4,8},{8,12},{12,16},{16,20},{20,24},{24,28},{28,32},{32,36}... | collective-permute-start | bytes 110600 | tf_op jit(solution)/shard_map/ppermute | solution.py:54
  103.5 5.3 %collective-permute-start.2 = (bf16[144,128]{1,0:T(8,128)(2,1)S(1)}, bf16[144,128]{1,0:T(8,128)(2,1)S(1)}, u32[]{:S(2)}, u32[]{:S(2)}) collective-permute-start(bf16[144,128]{1,0:T(8,128)(2,1)S(1)} %pad_maximum_fusion.6), channel_id=1, source_target_pairs={{4,0},{8,4},{12,8},{16,12},{20,16},{24,20},{28,24},{32,28},{36,32}... | collective-permute-start | bytes 110600 | tf_op jit(solution)/shard_map/ppermute | solution.py:55
  108.9 0.9 copy-start.5
  112.7 0.7 copy-start.6
  112.9 1.6 %copy-start.1 = (bf16[2,4,16,16,512]{4,3,0,1,2:T(8,128)(2,1)S(1)}, bf16[2,4,16,16,512]{4,3,0,1,2:T(8,128)(2,1)}, u32[]{:S(2)}) copy-start(bf16[2,4,16,16,512]{4,3,0,1,2:T(8,128)(2,1)} %pad_maximum_fusion.1) | copy-start | bytes 6291460
  146.0 8.4 %copy-start.4 = (f32[512]{0:T(512)S(1)}, f32[512]{0:T(512)}, u32[]{:S(2)}) copy-start(f32[512]{0:T(512)} %param.21) | copy-start | bytes 6148

commit v2 on v1

v2 whole, which is shorter than its diff:
```python
import functools

import jax
import jax.numpy as jnp
from jax import lax
from jax.experimental import pallas as pl
from jax.experimental.pallas import tpu as pltpu
from jax.sharding import Mesh
from jax.sharding import PartitionSpec as P


HEAD_DIM = 64
PAIR = 2 * HEAD_DIM
POOL_GROUPS = 4
RIM = 2 ** (POOL_GROUPS - 1)
WINDOW = 128
SP = ("sp_0", "sp_1", "sp_2")
Z, X, CORE = SP
TP = "tp"
BF16, F32 = jnp.bfloat16, jnp.float32

epsilon = 1e-05
masked_score = -1e30
nt = (((1,), (1,)), ((), ()))


def from_everyone(shard, axis):
    count = lax.axis_size(axis)
    return lax.all_to_all(
        jnp.broadcast_to(shard[None], (count, *shard.shape)), axis, 0, 0, tiled=True
    )


def of_everyone(shard, axis):
    return jnp.sum(from_everyone(shard, axis), axis=0)


def swapped(shard, axis, mask):
    return lax.ppermute(shard, axis, [(i, i ^ mask) for i in range(lax.axis_size(axis))])


def neighbours(head, tail, axis):
    count = lax.axis_size(axis)
    before = lax.ppermute(tail, axis, [(i, i + 1) for i in range(count - 1)])
    after = lax.ppermute(head, axis, [(i + 1, i) for i in range(count - 1)])
    return before, after


def in_stored_order(place, own_ref, other_ref, first, count):
    core = lax.axis_index(CORE)
    xs, rows = own_ref.shape[0], own_ref.shape[2]
    for z in range(count):
        for x in range(xs):
            base = ((first + z) * xs + x) * 2 * rows
            place(pl.multiple_of(base + core * rows, rows), own_ref[x, first + z])
            place(pl.multiple_of(base + (1 - core) * rows, rows), other_ref[x, first + z])


def project_kernel(
    widths, tokens_ref, own_ref, other_ref, query_ref, kv_ref, chan_ref, head_ref, tail_ref, w_ref
):
    pieces, rows, depth = tokens_ref.shape

    def place(at, block):
        w_ref[pl.ds(at, block.shape[0]), :] = block

    in_stored_order(place, own_ref, other_ref, 0, own_ref.shape[1])
    at = 0
    for ref, width in zip((query_ref, kv_ref, chan_ref), widths):
        total = jnp.dot(tokens_ref[0], w_ref[:depth, at : at + width], preferred_element_type=F32)
        for p in range(1, pieces):
            total += jnp.dot(
                tokens_ref[p],
                w_ref[p * depth : (p + 1) * depth, at : at + width],
                preferred_element_type=F32,
            )
        ref[...] = total.astype(BF16)
        at += width
    for ref, kv_at, chan_at in ((head_ref, 0, 0), (tail_ref, rows - WINDOW, rows - RIM)):
        ref[:WINDOW] = kv_ref[kv_at : kv_at + WINDOW]
        edge = chan_ref[chan_at : chan_at + RIM].astype(F32)
        ref[WINDOW:] = jnp.concatenate([edge[:, :PAIR], edge[:, PAIR:]]).astype(BF16)


def mix_kernel(
    half,
    seq_len,
    query_ref,
    kv_ref,
    chan_ref,
    rim_ref,
    sink_ref,
    w_pool_ref,
    scale_ref,
    own_ref,
    other_ref,
    sent_ref,
    kept_ref,
    band_ref,
    hidden_ref,
    w_ref,
):
    rows = query_ref.shape[0] // 2
    row0 = half * rows
    y = lax.axis_index(TP)
    offset = lax.axis_index(SP) * query_ref.shape[0] + row0
    blocks = rows // WINDOW
    query_cols = query_ref.shape[1]

    rim_kv = rim_ref[:WINDOW]
    rim_chan = rim_ref[WINDOW:].astype(F32)
    rim_chan = jnp.concatenate([rim_chan[:RIM], rim_chan[RIM:]], axis=1)
    if half == 0:
        kv = jnp.concatenate([rim_kv, kv_ref[: rows + WINDOW]])
        chan = jnp.concatenate([rim_chan, chan_ref[: rows + 2 * RIM].astype(F32)[: rows + RIM]])
    else:
        kv = jnp.concatenate([kv_ref[row0 - WINDOW :], rim_kv])
        chan = jnp.concatenate([chan_ref[row0 - 2 * RIM :].astype(F32)[RIM:], rim_chan])

    kv = kv.astype(F32)
    turned = pltpu.roll(kv, HEAD_DIM, 1)
    low = lax.broadcasted_iota(jnp.int32, kv.shape, 1) < HEAD_DIM
    band_ref[0] = jnp.where(low, kv, 0.0).astype(BF16)
    band_ref[1] = jnp.where(low, 0.0, turned).astype(BF16)
    band_ref[2] = jnp.where(low, turned, 0.0).astype(BF16)
    band_ref[3] = jnp.where(low, 0.0, kv).astype(BF16)

    row = lax.broadcasted_iota(jnp.int32, (WINDOW, 3 * WINDOW), 0)
    col = lax.broadcasted_iota(jnp.int32, (WINDOW, 3 * WINDOW), 1)
    near = (col >= row) & (col <= row + 2 * WINDOW)
    for b in range(blocks):
        key_pos = col + (offset + (b - 1) * WINDOW)
        keep = near & (key_pos >= 0) & (key_pos < seq_len)
        band = pl.ds(b * WINDOW, 3 * WINDOW)
        for pair in range(query_cols // PAIR):
            queries = query_ref[
                row0 + b * WINDOW : row0 + (b + 1) * WINDOW, pair * PAIR : (pair + 1) * PAIR
            ]
            attended = jnp.zeros((WINDOW, PAIR), F32)
            for side in range(2):
                scores = lax.dot_general(
                    queries, band_ref[side, band], nt, preferred_element_type=F32
                ) * HEAD_DIM ** (-0.5)
                scores = jnp.where(keep, scores, masked_score)
                sink = sink_ref[2 * pair + side]
                top = jnp.maximum(jnp.max(scores, axis=1, keepdims=True), sink)
                raised = jnp.exp(scores - top)
                total = jnp.sum(raised, axis=1, keepdims=True) + jnp.exp(sink - top)
                probs = (raised * (1.0 / total)).astype(BF16)
                attended += jnp.dot(probs, band_ref[2 + side, band], preferred_element_type=F32)
            hidden_ref[b * WINDOW : (b + 1) * WINDOW, pair * PAIR : (pair + 1) * PAIR] = (
                attended.astype(BF16)
            )

    length = chan.shape[0]
    sums = chan + pltpu.roll(chan, 1, 0)
    window_sum = sums
    for level in range(1, POOL_GROUPS):
        step = 2 ** (level - 1)
        sums = pltpu.roll(sums, step, 0) + pltpu.roll(sums, length - step, 0)
        window_sum = jnp.where(y >= level, sums, window_sum)
    half_width = jnp.left_shift(jnp.int32(1), y)
    pos = offset + lax.broadcasted_iota(jnp.int32, (rows, 1), 0)
    count = jnp.minimum(pos + half_width, seq_len) - jnp.maximum(pos - half_width, 0)
    spread = window_sum[RIM : RIM + rows] / count.astype(F32) - chan[RIM : RIM + rows]
    pooled = jnp.dot(spread.astype(BF16), w_pool_ref[0], preferred_element_type=F32)
    hidden_ref[:, query_cols:] = (pooled * scale_ref[...]).astype(BF16)

    def place(at, block):
        w_ref[pl.ds(at, block.shape[0]), :] = block

    in_stored_order(place, own_ref, other_ref, 0, own_ref.shape[1])
    share = sent_ref.shape[2]
    near_mask, far_mask = (1, 3) if half == 0 else (3, 1)
    hidden = hidden_ref[...]
    for ref, slot, mask in (
        (sent_ref, 0, near_mask),
        (sent_ref, 1, 2),
        (kept_ref, 0, 0),
        (kept_ref, 1, far_mask),
    ):
        columns = w_ref[pl.ds(pl.multiple_of((y ^ mask) * share, share), share)]
        ref[slot] = lax.dot_general(hidden, columns, nt, preferred_element_type=F32).astype(BF16)


VMEM = pl.BlockSpec(memory_space=pltpu.VMEM)
SMEM = pl.BlockSpec(memory_space=pltpu.SMEM)
LIMIT = pltpu.CompilerParams(vmem_limit_bytes=48 * 1024 * 1024)


def layer(
    tokens,
    w_query,
    w_key,
    w_value,
    w_pool_in,
    sink,
    w_pool,
    pool_scale,
    w_out_attn,
    w_out_pool,
    out_gain,
):
    rows = tokens.shape[0]
    seq_len = rows * lax.axis_size(SP)
    query_cols, key_cols, chan_cols = w_query.shape[1], w_key.shape[1], w_pool_in.shape[1]
    widths = (query_cols, 2 * key_cols, chan_cols)
    in_cols = sum(widths)
    hidden_cols = query_cols + chan_cols
    share = out_gain.shape[0]
    model_width = share * lax.axis_size(TP)

    gathered = from_everyone(tokens, TP)
    packed = jnp.concatenate(
        (w_query, w_key, w_value, w_pool_in, w_out_attn.T, w_out_pool.T), axis=1
    )
    over_z = lax.all_gather(packed, Z, axis=0)

    def over_x_and_cores(part):
        own = from_everyone(part, X)
        return own, swapped(own, CORE, 1)

    in_own, in_other = over_x_and_cores(over_z[:, :, :in_cols])
    out_own, out_other = over_x_and_cores(over_z[:, :, in_cols:])

    rim_shape = jax.ShapeDtypeStruct((WINDOW + 2 * RIM, PAIR), BF16)
    query, kv, chan, head, tail = pl.pallas_call(
        functools.partial(project_kernel, widths),
        out_shape=[jax.ShapeDtypeStruct((rows, w), BF16) for w in widths] + [rim_shape] * 2,
        in_specs=[VMEM] * 3,
        out_specs=[VMEM] * 5,
        scratch_shapes=[pltpu.VMEM((model_width, in_cols), BF16)],
        compiler_params=LIMIT,
        cost_estimate=pl.CostEstimate(
            flops=2 * rows * model_width * in_cols, bytes_accessed=6 << 20, transcendentals=0
        ),
        name="project",
    )(gathered, in_own, in_other)
    rims = neighbours(head, tail, SP)

    def mixed_half(half):
        block = jax.ShapeDtypeStruct((2, rows // 2, share), BF16)
        return pl.pallas_call(
            functools.partial(mix_kernel, half, seq_len),
            out_shape=[block, block],
            in_specs=[VMEM] * 4 + [SMEM] + [VMEM] * 4,
            out_specs=[VMEM] * 2,
            scratch_shapes=[
                pltpu.VMEM((4, rows // 2 + 2 * WINDOW, PAIR), BF16),
                pltpu.VMEM((rows // 2, hidden_cols), BF16),
                pltpu.VMEM((model_width, hidden_cols), BF16),
            ],
            compiler_params=LIMIT,
            cost_estimate=pl.CostEstimate(
                flops=rows * model_width * hidden_cols,
                bytes_accessed=6 << 20,
                transcendentals=0,
            ),
        )(query, kv, chan, rims[half], sink, w_pool, pool_scale.reshape(1, -1), out_own, out_other)

    def summed(half):
        near_mask, far_mask = (1, 3) if half == 0 else (3, 1)
        sent, kept = mixed_half(half)
        came = swapped(sent, TP, near_mask)
        both = kept.astype(F32) + came.astype(F32)
        rest = swapped(both[1].astype(BF16), TP, far_mask)
        return both[0] + rest.astype(F32)

    mix = jnp.concatenate([summed(0), summed(1)])
    stats = jnp.stack([jnp.sum(mix, axis=1), jnp.sum(mix * mix, axis=1)])
    stats = of_everyone(stats, TP)
    row_mean = stats[0] / model_width
    variance = stats[1] / model_width - row_mean * row_mean
    normed = (mix - row_mean[:, None]) * lax.rsqrt(variance + epsilon)[:, None] * out_gain
    return normed.astype(BF16)


def solution(mesh):
    finer = Mesh(mesh.devices.reshape(16, 4, 2, mesh.shape["tp"]), ("sp_0", "sp_1", "sp_2", "tp"))
    return jax.shard_map(
        layer,
        mesh=finer,
        in_specs=(
            P(SP, "tp"),
            P(SP, "tp"),
            P(SP, "tp"),
            P(SP, "tp"),
            P(SP, "tp"),
            P("tp"),
            P("tp", None, None),
            P("tp"),
            P("tp", SP),
            P("tp", SP),
            P("tp"),
        ),
        out_specs=P(SP, "tp"),
        check_vma=False,
    )
```

time: 156 us -> 154 us (0.987)
  the two profiles are of different devices: /device:TPU:6 before, /device:TPU:2 now
where the time goes in v2:
time: 154 us
  blocking collectives  62.3 us (40%)
  waiting for transfers between devices  46.5 us (30%)
  starting transfers between devices  28.5 us (19%)
  Pallas kernels  10.7 us (7%)
  local copies, waits for them, and re-layouts  3.7 us (2%)
  other arithmetic  1.77 us (1%)
    all_gather x1, blocking collectives, layer(): over_z = lax.all_gather(packed, Z, axis=0)  38.9 us
    all_to_all x2, waiting for transfers between devices, from_everyone(): lax.all_to_all(jnp.broadcast_to(shard[None], (count, *shard.shape)), axis...  23.7 us
    all_to_all x2, blocking collectives, from_everyone(): lax.all_to_all(jnp.broadcast_to(shard[None], (count, *shard.shape)), axis...  23.4 us
    ppermute x6, waiting for transfers between devices, swapped(): lax.ppermute(shard, axis, [(i, i ^ mask) for i in range(lax.axis_size(axi...  17.9 us
    ppermute x6, starting transfers between devices, swapped(): lax.ppermute(shard, axis, [(i, i ^ mask) for i in range(lax.axis_size(axi...  15.3 us
    all_to_all x2, starting transfers between devices, from_everyone(): lax.all_to_all(jnp.broadcast_to(shard[None], (count, *shard.shape)), axis...  9.29 us
    pallas_call x2, Pallas kernels, mixed_half(): pl.pallas_call(functools.partial(mix_kernel, half, seq_len), out_shape=[b...  6.68 us
    pallas_call x1, Pallas kernels, layer(): pl.pallas_call(functools.partial(project_kernel, widths), out_shape=[jax....  4 us
  transfers between devices with their start and end apart: 10, of which 7 were waited for; matrix products, arithmetic and copies ran while one was open for 0% of the time, Pallas kernels for 5%

profile of v2, /device:TPU:2, one launch (start us, length us, event | category | flops | bytes accessed | tf_op | source)
XLA Modules:
  0.0 153.7 jit_solution(405194729471350620)
XLA Ops:
  0.0 0.9 concatenate.6
  0.9 38.9 %all-gather = bf16[256,1152]{1,0:T(8,128)(2,1)S(1)} all-gather(bf16[16,1152]{1,0:T(8,128)(2,1)S(1)} %concatenate.6), channel_id=2, replica_groups=mesh['sp_0'=16,'sp_1'=4,'sp_2'=2,'tp'=4] {'sp_0'}, dimensions={0}, use_global_device_ids=true | all-gather | bytes 626688 | tf_op jit(solution)/shard_map/all_gather | solution.py:217
  39.7 1.1 broadcast_in_dim.10
  40.9 4.8 %all-to-all-start.2 = ((bf16[4,16,16,512]{3,2,1,0:T(8,128)(2,1)}), bf16[4,16,16,512]{3,2,1,0:T(8,128)(2,1)S(1)}, u32[]{:S(2)}, u32[]{:S(2)}) async-start(bf16[4,16,16,512]{3,2,1,0:T(8,128)(2,1)} %broadcast_in_dim.10), calls=%async_computation.2 | async-start | bytes 2097152 | tf_op jit(solution)/shard_map/all_to_all | solution.py:29
  45.7 11.6 %all-to-all-done.2.own_ref = bf16[4,16,16,512]{3,2,1,0:T(8,128)(2,1)S(1)} async-done(((bf16[4,16,16,512]{3,2,1,0:T(8,128)(2,1)}), bf16[4,16,16,512]{3,2,1,0:T(8,128)(2,1)S(1)}, u32[]{:S(2)}, u32[]{:S(2)}) %all-to-all-start.2) | async-done | bytes 1048608 | tf_op jit(solution)/shard_map/all_to_all | solution.py:29
  57.3 0.1 broadcast_in_dim.9
  57.4 14.9 %all_to_all.20.own_ref = bf16[4,16,16,640]{3,2,1,0:T(8,128)(2,1)S(1)} all-to-all(bf16[4,16,16,640]{3,2,1,0:T(8,128)(2,1)S(1)} %broadcast_in_dim.9), channel_id=1, replica_groups=mesh['sp_0'=16,'sp_1'=4,'sp_2'=2,'tp'=4] {'sp_1'}, dimensions={0} | all-to-all | bytes 2621440 | tf_op jit(solution)/shard_map/all_to_all | solution.py:29
  72.3 1.5 broadcast_in_dim.8
  73.7 4.5 %all-to-all-start = ((bf16[4,512,512]{2,1,0:T(8,128)(2,1)}), bf16[4,512,512]{2,1,0:T(8,128)(2,1)}, u32[]{:S(2)}, u32[]{:S(2)}) async-start(bf16[4,512,512]{2,1,0:T(8,128)(2,1)} %broadcast_in_dim.8), calls=%async_computation | async-start | bytes 4194304 | tf_op jit(solution)/shard_map/all_to_all | solution.py:29
  78.2 2.1 %collective-permute-start = (bf16[4,16,16,640]{3,2,1,0:T(8,128)(2,1)S(1)}, bf16[4,16,16,640]{3,2,1,0:T(8,128)(2,1)}, u32[]{:S(2)}, u32[]{:S(2)}) collective-permute-start(bf16[4,16,16,640]{3,2,1,0:T(8,128)(2,1)S(1)} %all_to_all.20.own_ref), channel_id=1, source_target_pairs={{0,4},{4,0},{1,5},{5,1},{2,6},{6,2},{3,7},{7,3},{8,12},{12,8},{9,1... | collective-permute-start | bytes 3932168 | tf_op jit(solution)/shard_map/ppermute | solution.py:39
  80.3 2.4 %collective-permute-start.2 = (bf16[4,16,16,512]{3,2,1,0:T(8,128)(2,1)S(1)}, bf16[4,16,16,512]{3,2,1,0:T(8,128)(2,1)S(1)}, u32[]{:S(2)}, u32[]{:S(2)}) collective-permute-start(bf16[4,16,16,512]{3,2,1,0:T(8,128)(2,1)S(1)} %all-to-all-done.2.own_ref), channel_id=1, source_target_pairs={{0,4},{4,0},{1,5},{5,1},{2,6},{6,2},{3,7},{7,3},{8,12},{12,8},{9,1... | collective-permute-start | bytes 3145736 | tf_op jit(solution)/shard_map/ppermute | solution.py:39
  82.7 12.1 %all-to-all-done.tokens_ref = bf16[4,512,512]{2,1,0:T(8,128)(2,1)} async-done(((bf16[4,512,512]{2,1,0:T(8,128)(2,1)}), bf16[4,512,512]{2,1,0:T(8,128)(2,1)}, u32[]{:S(2)}, u32[]{:S(2)}) %all-to-all-start) | async-done | bytes 2097184 | tf_op jit(solution)/shard_map/all_to_all | solution.py:29
  94.8 4.0 %project.1 = (bf16[512,256]{1,0:T(8,128)(2,1)S(1)}, bf16[512,128]{1,0:T(8,128)(2,1)S(1)}, bf16[512,256]{1,0:T(8,128)(2,1)S(1)}, bf16[144,128]{1,0:T(8,128)(2,1)S(1)}, bf16[144,128]{1,0:T(8,128)(2,1)S(1)}) custom-call(bf16[4,512,512]{2,1,0:T(8,128)(2,1)} %all-to-all-done.tokens_ref, bf16[4,16,16,640]{3,2,1,0:T(8,128)(2,1)S(1)} %all_to_all.20.own_ref, ...), custom_call_target="tpu_custom_call" | custom-call | flops 1342177280 | bytes 6291456 | tf_op jit(solution)/shard_map/project/pallas_call | solution.py:227
  98.8 1.9 %collective-permute-start.5 = (bf16[144,128]{1,0:T(8,128)(2,1)S(1)}, bf16[144,128]{1,0:T(8,128)(2,1)S(1)}, u32[]{:S(2)}, u32[]{:S(2)}) collective-permute-start(bf16[144,128]{1,0:T(8,128)(2,1)S(1)} %get-tuple-element.20), channel_id=1, source_target_pairs={{4,0},{8,4},{12,8},{16,12},{20,16},{24,20},{28,24},{32,28},{36,32}... | collective-permute-start | bytes 110600 | tf_op jit(solution)/shard_map/ppermute | solution.py:45
  100.8 1.6 %collective-permute-done.5.rim_ref = bf16[144,128]{1,0:T(8,128)(2,1)S(1)} collective-permute-done((bf16[144,128]{1,0:T(8,128)(2,1)S(1)}, bf16[144,128]{1,0:T(8,128)(2,1)S(1)}, u32[]{:S(2)}, u32[]{:S(2)}) %collective-permute-start.5) | collective-permute-done | bytes 36896 | tf_op jit(solution)/shard_map/ppermute | solution.py:45
  102.4 3.3 %shard_map.110 = (bf16[2,256,512]{2,1,0:T(8,128)(2,1)S(1)}, bf16[2,256,512]{2,1,0:T(8,128)(2,1)S(1)}) custom-call(bf16[512,256]{1,0:T(8,128)(2,1)S(1)} %get-tuple-element.14.query_ref, bf16[512,128]{1,0:T(8,128)(2,1)S(1)} %get-tuple-element.15.kv_ref, bf16[512,256]{1,0:T(8,128)(2,1)S(1)} %get-tuple-element.16.chan_ref, ...), custom_call_target="tpu_custom_call" | custom-call | flops 536870912 | bytes 6291456 | tf_op jit(solution)/shard_map/pallas_call | solution.py:243
  105.7 3.1 %collective-permute-start.6 = (bf16[2,256,512]{2,1,0:T(8,128)(2,1)S(1)}, bf16[2,256,512]{2,1,0:T(8,128)(2,1)S(1)}, u32[]{:S(2)}, u32[]{:S(2)}) collective-permute-start(bf16[2,256,512]{2,1,0:T(8,128)(2,1)S(1)} %get-tuple-element.22), channel_id=1, source_target_pairs={{0,3},{1,2},{2,1},{3,0},{4,7},{5,6},{6,5},{7,4},{8,11},{9,10},{10,... | collective-permute-start | bytes 1572872 | tf_op jit(solution)/shard_map/ppermute | solution.py:39
  108.8 2.0 %collective-permute-start.1 = (bf16[144,128]{1,0:T(8,128)(2,1)S(1)}, bf16[144,128]{1,0:T(8,128)(2,1)S(1)}, u32[]{:S(2)}, u32[]{:S(2)}) collective-permute-start(bf16[144,128]{1,0:T(8,128)(2,1)S(1)} %get-tuple-element.17), channel_id=1, source_target_pairs={{0,4},{4,8},{8,12},{12,16},{16,20},{20,24},{24,28},{28,32},{32,36}... | collective-permute-start | bytes 110600 | tf_op jit(solution)/shard_map/ppermute | solution.py:44
  110.8 3.3 %collective-permute-done.1.rim_ref = bf16[144,128]{1,0:T(8,128)(2,1)S(1)} collective-permute-done((bf16[144,128]{1,0:T(8,128)(2,1)S(1)}, bf16[144,128]{1,0:T(8,128)(2,1)S(1)}, u32[]{:S(2)}, u32[]{:S(2)}) %collective-permute-start.1) | collective-permute-done | bytes 36896 | tf_op jit(solution)/shard_map/ppermute | solution.py:44
  114.1 3.4 %shard_map.109 = (bf16[2,256,512]{2,1,0:T(8,128)(2,1)S(1)}, bf16[2,256,512]{2,1,0:T(8,128)(2,1)S(1)}) custom-call(bf16[512,256]{1,0:T(8,128)(2,1)S(1)} %get-tuple-element.14.query_ref, bf16[512,128]{1,0:T(8,128)(2,1)S(1)} %get-tuple-element.15.kv_ref, bf16[512,256]{1,0:T(8,128)(2,1)S(1)} %get-tuple-element.16.chan_ref, ...), custom_call_target="tpu_custom_call" | custom-call | flops 536870912 | bytes 6291456 | tf_op jit(solution)/shard_map/pallas_call | solution.py:243
  117.4 1.9 %collective-permute-start.3 = (bf16[2,256,512]{2,1,0:T(8,128)(2,1)S(1)}, bf16[2,256,512]{2,1,0:T(8,128)(2,1)S(1)}, u32[]{:S(2)}, u32[]{:S(2)}) collective-permute-start(bf16[2,256,512]{2,1,0:T(8,128)(2,1)S(1)} %get-tuple-element.19), channel_id=1, source_target_pairs={{0,1},{1,0},{2,3},{3,2},{4,5},{5,4},{6,7},{7,6},{8,9},{9,8},{10,11... | collective-permute-start | bytes 1572872 | tf_op jit(solution)/shard_map/ppermute | solution.py:39
  119.3 3.6 %collective-permute-done.6 = bf16[2,256,512]{2,1,0:T(8,128)(2,1)S(1)} collective-permute-done((bf16[2,256,512]{2,1,0:T(8,128)(2,1)S(1)}, bf16[2,256,512]{2,1,0:T(8,128)(2,1)S(1)}, u32[]{:S(2)}, u32[]{:S(2)}) %collective-permute-start.6) | collective-permute-done | bytes 524320 | tf_op jit(solution)/shard_map/ppermute | solution.py:39
  123.0 0.2 convert_add_fusion
  123.2 1.9 %collective-permute-start.7 = (bf16[256,512]{1,0:T(8,128)(2,1)S(1)}, bf16[256,512]{1,0:T(8,128)(2,1)S(1)}, u32[]{:S(2)}, u32[]{:S(2)}) collective-permute-start(bf16[256,512]{1,0:T(8,128)(2,1)S(1)} %fusion.4), channel_id=1, source_target_pairs={{0,1},{1,0},{2,3},{3,2},{4,5},{5,4},{6,7},{7,6},{8,9},{9,8},{10,11... | collective-permute-start | bytes 786440 | tf_op jit(solution)/shard_map/ppermute | solution.py:39
  125.1 8.9 %collective-permute-done.3 = bf16[2,256,512]{2,1,0:T(8,128)(2,1)S(1)} collective-permute-done((bf16[2,256,512]{2,1,0:T(8,128)(2,1)S(1)}, bf16[2,256,512]{2,1,0:T(8,128)(2,1)S(1)}, u32[]{:S(2)}, u32[]{:S(2)}) %collective-permute-start.3) | collective-permute-done | bytes 524320 | tf_op jit(solution)/shard_map/ppermute | solution.py:39
  134.0 0.1 convert_add_fusion.1
  134.2 4.0 %collective-permute-start.4 = (bf16[256,512]{1,0:T(8,128)(2,1)S(1)}, bf16[256,512]{1,0:T(8,128)(2,1)S(1)}, u32[]{:S(2)}, u32[]{:S(2)}) collective-permute-start(bf16[256,512]{1,0:T(8,128)(2,1)S(1)} %fusion.3), channel_id=1, source_target_pairs={{0,3},{1,2},{2,1},{3,0},{4,7},{5,6},{6,5},{7,4},{8,11},{9,10},{10,... | collective-permute-start | bytes 786440 | tf_op jit(solution)/shard_map/ppermute | solution.py:39
  138.1 0.1 fusion.1
  138.2 5.4 %collective-permute-done.4 = bf16[256,512]{1,0:T(8,128)(2,1)S(1)} collective-permute-done((bf16[256,512]{1,0:T(8,128)(2,1)S(1)}, bf16[256,512]{1,0:T(8,128)(2,1)S(1)}, u32[]{:S(2)}, u32[]{:S(2)}) %collective-permute-start.4) | collective-permute-done | bytes 262176 | tf_op jit(solution)/shard_map/ppermute | solution.py:39
  143.7 0.3 fusion
  144.0 8.6 %all_to_all.21 = f32[4,2,512]{2,1,0:T(2,128)S(1)} all-to-all(f32[4,2,512]{2,1,0:T(2,128)S(1)} %broadcast_in_dim.11), channel_id=1, replica_groups=mesh['sp_0'=16,'sp_1'=4,'sp_2'=2,'tp'=4] {'tp'}, dimensions={0} | all-to-all | bytes 32768 | tf_op jit(solution)/shard_map/all_to_all | solution.py:29
  152.6 1.0 multiply_convert_fusion
  (23 shorter events, 0.3 us)
Async XLA Ops:
  40.9 16.4 %all-to-all-start.2 = ((bf16[4,16,16,512]{3,2,1,0:T(8,128)(2,1)}), bf16[4,16,16,512]{3,2,1,0:T(8,128)(2,1)S(1)}, u32[]{:S(2)}, u32[]{:S(2)}) async-start(bf16[4,16,16,512]{3,2,1,0:T(8,128)(2,1)} %broadcast_in_dim.10), calls=%async_computation.2 | async-start | bytes 2097152 | tf_op jit(solution)/shard_map/all_to_all | solution.py:29
  57.4 14.9 %copy-start.3 = (bf16[512,512]{1,0:T(8,128)(2,1)S(1)}, bf16[512,512]{1,0:T(8,128)(2,1)}, u32[]{:S(2)}) copy-start(bf16[512,512]{1,0:T(8,128)(2,1)} %param.11) | copy-start | bytes 1572868
  73.7 21.1 %all-to-all-start = ((bf16[4,512,512]{2,1,0:T(8,128)(2,1)}), bf16[4,512,512]{2,1,0:T(8,128)(2,1)}, u32[]{:S(2)}, u32[]{:S(2)}) async-start(bf16[4,512,512]{2,1,0:T(8,128)(2,1)} %broadcast_in_dim.8), calls=%async_computation | async-start | bytes 4194304 | tf_op jit(solution)/shard_map/all_to_all | solution.py:29
  78.2 24.2 %copy-start = (bf16[1,256,256]{2,1,0:T(8,128)(2,1)S(1)}, bf16[1,256,256]{2,1,0:T(8,128)(2,1)}, u32[]{:S(2)}) copy-start(bf16[1,256,256]{2,1,0:T(8,128)(2,1)} %w_pool_ref.3) | copy-start | bytes 393220
  78.2 24.2 %copy-start.1 = (f32[256]{0:T(256)S(1)}, f32[256]{0:T(256)}, u32[]{:S(2)}) copy-start(f32[256]{0:T(256)} %param.18) | copy-start | bytes 3076
  78.2 24.2 %copy-start.2 = (f32[4]{0:T(128)S(1)}, f32[4]{0:T(128)}, u32[]{:S(2)}) copy-start(f32[4]{0:T(128)} %sink_ref.3) | copy-start | bytes 52
  78.2 16.6 %collective-permute-start = (bf16[4,16,16,640]{3,2,1,0:T(8,128)(2,1)S(1)}, bf16[4,16,16,640]{3,2,1,0:T(8,128)(2,1)}, u32[]{:S(2)}, u32[]{:S(2)}) collective-permute-start(bf16[4,16,16,640]{3,2,1,0:T(8,128)(2,1)S(1)} %all_to_all.20.own_ref), channel_id=1, source_target_pairs={{0,4},{4,0},{1,5},{5,1},{2,6},{6,2},{3,7},{7,3},{8,12},{12,8},{9,1... | collective-permute-start | bytes 3932168 | tf_op jit(solution)/shard_map/ppermute | solution.py:39
  80.3 20.5 %collective-permute-start.2 = (bf16[4,16,16,512]{3,2,1,0:T(8,128)(2,1)S(1)}, bf16[4,16,16,512]{3,2,1,0:T(8,128)(2,1)S(1)}, u32[]{:S(2)}, u32[]{:S(2)}) collective-permute-start(bf16[4,16,16,512]{3,2,1,0:T(8,128)(2,1)S(1)} %all-to-all-done.2.own_ref), channel_id=1, source_target_pairs={{0,4},{4,0},{1,5},{5,1},{2,6},{6,2},{3,7},{7,3},{8,12},{12,8},{9,1... | collective-permute-start | bytes 3145736 | tf_op jit(solution)/shard_map/ppermute | solution.py:39
  98.8 3.5 %collective-permute-start.5 = (bf16[144,128]{1,0:T(8,128)(2,1)S(1)}, bf16[144,128]{1,0:T(8,128)(2,1)S(1)}, u32[]{:S(2)}, u32[]{:S(2)}) collective-permute-start(bf16[144,128]{1,0:T(8,128)(2,1)S(1)} %get-tuple-element.20), channel_id=1, source_target_pairs={{4,0},{8,4},{12,8},{16,12},{20,16},{24,20},{28,24},{32,28},{36,32}... | collective-permute-start | bytes 110600 | tf_op jit(solution)/shard_map/ppermute | solution.py:45
  105.7 17.3 %collective-permute-start.6 = (bf16[2,256,512]{2,1,0:T(8,128)(2,1)S(1)}, bf16[2,256,512]{2,1,0:T(8,128)(2,1)S(1)}, u32[]{:S(2)}, u32[]{:S(2)}) collective-permute-start(bf16[2,256,512]{2,1,0:T(8,128)(2,1)S(1)} %get-tuple-element.22), channel_id=1, source_target_pairs={{0,3},{1,2},{2,1},{3,0},{4,7},{5,6},{6,5},{7,4},{8,11},{9,10},{10,... | collective-permute-start | bytes 1572872 | tf_op jit(solution)/shard_map/ppermute | solution.py:39
  108.8 5.3 %collective-permute-start.1 = (bf16[144,128]{1,0:T(8,128)(2,1)S(1)}, bf16[144,128]{1,0:T(8,128)(2,1)S(1)}, u32[]{:S(2)}, u32[]{:S(2)}) collective-permute-start(bf16[144,128]{1,0:T(8,128)(2,1)S(1)} %get-tuple-element.17), channel_id=1, source_target_pairs={{0,4},{4,8},{8,12},{12,16},{16,20},{20,24},{24,28},{28,32},{32,36}... | collective-permute-start | bytes 110600 | tf_op jit(solution)/shard_map/ppermute | solution.py:44
  117.4 16.5 %collective-permute-start.3 = (bf16[2,256,512]{2,1,0:T(8,128)(2,1)S(1)}, bf16[2,256,512]{2,1,0:T(8,128)(2,1)S(1)}, u32[]{:S(2)}, u32[]{:S(2)}) collective-permute-start(bf16[2,256,512]{2,1,0:T(8,128)(2,1)S(1)} %get-tuple-element.19), channel_id=1, source_target_pairs={{0,1},{1,0},{2,3},{3,2},{4,5},{5,4},{6,7},{7,6},{8,9},{9,8},{10,11... | collective-permute-start | bytes 1572872 | tf_op jit(solution)/shard_map/ppermute | solution.py:39
  123.2 15.0 %collective-permute-start.7 = (bf16[256,512]{1,0:T(8,128)(2,1)S(1)}, bf16[256,512]{1,0:T(8,128)(2,1)S(1)}, u32[]{:S(2)}, u32[]{:S(2)}) collective-permute-start(bf16[256,512]{1,0:T(8,128)(2,1)S(1)} %fusion.4), channel_id=1, source_target_pairs={{0,1},{1,0},{2,3},{3,2},{4,5},{5,4},{6,7},{7,6},{8,9},{9,8},{10,11... | collective-permute-start | bytes 786440 | tf_op jit(solution)/shard_map/ppermute | solution.py:39
  134.2 9.5 %collective-permute-start.4 = (bf16[256,512]{1,0:T(8,128)(2,1)S(1)}, bf16[256,512]{1,0:T(8,128)(2,1)S(1)}, u32[]{:S(2)}, u32[]{:S(2)}) collective-permute-start(bf16[256,512]{1,0:T(8,128)(2,1)S(1)} %fusion.3), channel_id=1, source_target_pairs={{0,3},{1,2},{2,1},{3,0},{4,7},{5,6},{6,5},{7,4},{8,11},{9,10},{10,... | collective-permute-start | bytes 786440 | tf_op jit(solution)/shard_map/ppermute | solution.py:39
  138.2 14.4 %copy-start.4 = (f32[512]{0:T(512)S(1)}, f32[512]{0:T(512)}, u32[]{:S(2)}) copy-start(f32[512]{0:T(512)} %param.21) | copy-start | bytes 6148

commit v3 on v2

v3 whole, which is shorter than its diff:
```python
import functools

import jax
import jax.numpy as jnp
from jax import lax
from jax.experimental import pallas as pl
from jax.experimental.pallas import tpu as pltpu
from jax.sharding import Mesh
from jax.sharding import PartitionSpec as P


HEAD_DIM = 64
PAIR = 2 * HEAD_DIM
POOL_GROUPS = 4
RIM = 2 ** (POOL_GROUPS - 1)
WINDOW = 128
SP = ("sp_0", "sp_1", "sp_2")
Z, X, CORE = SP
TP = "tp"
BF16, F32 = jnp.bfloat16, jnp.float32

epsilon = 1e-05
masked_score = -1e30
nt = (((1,), (1,)), ((), ()))


def from_everyone(shard, axis):
    count = lax.axis_size(axis)
    return lax.all_to_all(
        jnp.broadcast_to(shard[None], (count, *shard.shape)), axis, 0, 0, tiled=True
    )


def of_everyone(shard, axis):
    return jnp.sum(from_everyone(shard, axis), axis=0)


def swapped(shard, axis, mask):
    return lax.ppermute(shard, axis, [(i, i ^ mask) for i in range(lax.axis_size(axis))])


def neighbours(head, tail, axis):
    count = lax.axis_size(axis)
    before = lax.ppermute(tail, axis, [(i, i + 1) for i in range(count - 1)])
    after = lax.ppermute(head, axis, [(i + 1, i) for i in range(count - 1)])
    return before, after


def in_stored_order(place, own_ref, other_ref, count):
    core = lax.axis_index(CORE)
    xs, rows = own_ref.shape[0], own_ref.shape[2]
    for z in range(count):
        for x in range(xs):
            base = (z * xs + x) * 2 * rows
            place(pl.multiple_of(base + core * rows, rows), own_ref[x, z])
            place(pl.multiple_of(base + (1 - core) * rows, rows), other_ref[x, z])


def whole_weights(own_ref, other_ref, w_ref, at):
    def place(row, block):
        w_ref[pl.ds(row, block.shape[0]), :] = block[:, at : at + w_ref.shape[1]]

    in_stored_order(place, own_ref, other_ref, own_ref.shape[1])


def side_by_side(tokens_ref, rows_ref):
    depth = tokens_ref.shape[2]
    for p in range(tokens_ref.shape[0]):
        rows_ref[:, p * depth : (p + 1) * depth] = tokens_ref[p]


def project_kernel(
    tokens_ref, own_ref, other_ref, kv_ref, chan_ref, head_ref, tail_ref, rows_ref, w_ref
):
    rows = tokens_ref.shape[1]
    whole_weights(own_ref, other_ref, w_ref, 0)
    side_by_side(tokens_ref, rows_ref)
    at = 0
    for ref in (kv_ref, chan_ref):
        width = ref.shape[1]
        ref[...] = jnp.dot(
            rows_ref[...], w_ref[:, at : at + width], preferred_element_type=F32
        ).astype(BF16)
        at += width
    for ref, kv_at, chan_at in ((head_ref, 0, 0), (tail_ref, rows - WINDOW, rows - RIM)):
        ref[:WINDOW] = kv_ref[kv_at : kv_at + WINDOW]
        edge = chan_ref[chan_at : chan_at + RIM].astype(F32)
        ref[WINDOW:] = jnp.concatenate([edge[:, :PAIR], edge[:, PAIR:]]).astype(BF16)


def pool_kernel(seq_len, chan_ref, before_ref, after_ref, w_pool_ref, scale_ref, pooled_ref):
    rows = chan_ref.shape[0]
    y = lax.axis_index(TP)
    offset = lax.axis_index(SP) * rows

    def rim(ref):
        packed = ref[WINDOW:].astype(F32)
        return jnp.concatenate([packed[:RIM], packed[RIM:]], axis=1)

    own = chan_ref[...].astype(F32)
    chan = jnp.concatenate([rim(before_ref), own, rim(after_ref)])
    length = chan.shape[0]
    sums = chan + pltpu.roll(chan, 1, 0)
    window_sum = sums
    for level in range(1, POOL_GROUPS):
        step = 2 ** (level - 1)
        sums = pltpu.roll(sums, step, 0) + pltpu.roll(sums, length - step, 0)
        window_sum = jnp.where(y >= level, sums, window_sum)
    half_width = jnp.left_shift(jnp.int32(1), y)
    pos = offset + lax.broadcasted_iota(jnp.int32, (rows, 1), 0)
    count = jnp.minimum(pos + half_width, seq_len) - jnp.maximum(pos - half_width, 0)
    spread = window_sum[RIM : RIM + rows] / count.astype(F32) - own
    pooled = jnp.dot(spread.astype(BF16), w_pool_ref[0], preferred_element_type=F32)
    pooled_ref[...] = (pooled * scale_ref[...]).astype(BF16)


def mix_kernel(
    seq_len,
    tokens_ref,
    kv_ref,
    before_ref,
    after_ref,
    pooled_ref,
    sink_ref,
    own_ref,
    other_ref,
    sent0_ref,
    sent1_ref,
    kept0_ref,
    kept1_ref,
    rows_ref,
    query_ref,
    band_ref,
    hidden_ref,
    w_query_ref,
    w_out_ref,
):
    rows, query_cols = query_ref.shape
    y = lax.axis_index(TP)
    offset = lax.axis_index(SP) * rows

    whole_weights(own_ref, other_ref, w_query_ref, 0)
    side_by_side(tokens_ref, rows_ref)
    query_ref[...] = jnp.dot(
        rows_ref[...], w_query_ref[...], preferred_element_type=F32
    ).astype(BF16)
    whole_weights(own_ref, other_ref, w_out_ref, query_cols)

    kv = jnp.concatenate([before_ref[:WINDOW], kv_ref[...], after_ref[:WINDOW]]).astype(F32)
    turned = pltpu.roll(kv, HEAD_DIM, 1)
    low = lax.broadcasted_iota(jnp.int32, kv.shape, 1) < HEAD_DIM
    band_ref[0] = jnp.where(low, kv, 0.0).astype(BF16)
    band_ref[1] = jnp.where(low, 0.0, turned).astype(BF16)
    band_ref[2] = jnp.where(low, turned, 0.0).astype(BF16)
    band_ref[3] = jnp.where(low, 0.0, kv).astype(BF16)

    row = lax.broadcasted_iota(jnp.int32, (WINDOW, 3 * WINDOW), 0)
    col = lax.broadcasted_iota(jnp.int32, (WINDOW, 3 * WINDOW), 1)
    near = (col >= row) & (col <= row + 2 * WINDOW)
    for b in range(rows // WINDOW):
        key_pos = col + (offset + (b - 1) * WINDOW)
        keep = near & (key_pos >= 0) & (key_pos < seq_len)
        here = pl.ds(b * WINDOW, WINDOW)
        band = pl.ds(b * WINDOW, 3 * WINDOW)
        for pair in range(query_cols // PAIR):
            lanes = slice(pair * PAIR, (pair + 1) * PAIR)
            queries = query_ref[here, lanes]
            attended = jnp.zeros((WINDOW, PAIR), F32)
            for side in range(2):
                scores = lax.dot_general(
                    queries, band_ref[side, band], nt, preferred_element_type=F32
                ) * HEAD_DIM ** (-0.5)
                scores = jnp.where(keep, scores, masked_score)
                sink = sink_ref[2 * pair + side]
                top = jnp.maximum(jnp.max(scores, axis=1, keepdims=True), sink)
                raised = jnp.exp(scores - top)
                total = jnp.sum(raised, axis=1, keepdims=True) + jnp.exp(sink - top)
                probs = (raised * (1.0 / total)).astype(BF16)
                attended += jnp.dot(probs, band_ref[2 + side, band], preferred_element_type=F32)
            hidden_ref[here, lanes] = attended.astype(BF16)
    hidden_ref[:, query_cols:] = pooled_ref[...]

    half, share = sent0_ref.shape[1:]
    for at, sent_ref, kept_ref, near_mask, far_mask in (
        (0, sent0_ref, kept0_ref, 1, 3),
        (half, sent1_ref, kept1_ref, 3, 1),
    ):
        hidden = hidden_ref[at : at + half]
        for ref, slot, mask in (
            (sent_ref, 0, near_mask),
            (sent_ref, 1, 2),
            (kept_ref, 0, 0),
            (kept_ref, 1, far_mask),
        ):
            columns = w_out_ref[pl.ds(pl.multiple_of((y ^ mask) * share, share), share)]
            ref[slot] = lax.dot_general(
                hidden, columns, nt, preferred_element_type=F32
            ).astype(BF16)


VMEM = pl.BlockSpec(memory_space=pltpu.VMEM)
SMEM = pl.BlockSpec(memory_space=pltpu.SMEM)
LIMIT = pltpu.CompilerParams(vmem_limit_bytes=20 * 1024 * 1024)


def layer(
    tokens,
    w_query,
    w_key,
    w_value,
    w_pool_in,
    sink,
    w_pool,
    pool_scale,
    w_out_attn,
    w_out_pool,
    out_gain,
):
    rows = tokens.shape[0]
    seq_len = rows * lax.axis_size(SP)
    query_cols, key_cols, chan_cols = w_query.shape[1], w_key.shape[1], w_pool_in.shape[1]
    first_cols = 2 * key_cols + chan_cols
    hidden_cols = query_cols + chan_cols
    share = out_gain.shape[0]
    model_width = share * lax.axis_size(TP)

    gathered = from_everyone(tokens, TP)
    packed = jnp.concatenate(
        (w_key, w_value, w_pool_in, w_query, w_out_attn.T, w_out_pool.T), axis=1
    )
    over_z = lax.all_gather(packed, Z, axis=0)

    def over_x_and_cores(part):
        own = from_everyone(part, X)
        return own, swapped(own, CORE, 1)

    own1, other1 = over_x_and_cores(over_z[:, :, :first_cols])
    own2, other2 = over_x_and_cores(over_z[:, :, first_cols:])

    def rows_of(width):
        return jax.ShapeDtypeStruct((rows, width), BF16)

    def cost(flops, size):
        return pl.CostEstimate(flops=flops, bytes_accessed=size, transcendentals=0)

    rim_shape = jax.ShapeDtypeStruct((WINDOW + 2 * RIM, PAIR), BF16)
    kv, chan, head, tail = pl.pallas_call(
        project_kernel,
        out_shape=[rows_of(2 * key_cols), rows_of(chan_cols), rim_shape, rim_shape],
        in_specs=[VMEM] * 3,
        out_specs=[VMEM] * 4,
        scratch_shapes=[
            pltpu.VMEM((rows, model_width), BF16),
            pltpu.VMEM((model_width, first_cols), BF16),
        ],
        compiler_params=LIMIT,
        cost_estimate=cost(2 * rows * model_width * first_cols, 4 << 20),
        name="project",
    )(gathered, own1, other1)
    before, after = neighbours(head, tail, SP)
    pooled = pl.pallas_call(
        functools.partial(pool_kernel, seq_len),
        out_shape=rows_of(chan_cols),
        in_specs=[VMEM] * 5,
        out_specs=VMEM,
        compiler_params=LIMIT,
        cost_estimate=cost(2 * rows * chan_cols * chan_cols, 1 << 20),
        name="pool",
    )(chan, before, after, w_pool, pool_scale.reshape(1, -1))
    block = jax.ShapeDtypeStruct((2, rows // 2, share), BF16)
    sent0, sent1, kept0, kept1 = pl.pallas_call(
        functools.partial(mix_kernel, seq_len),
        out_shape=[block] * 4,
        in_specs=[VMEM] * 5 + [SMEM] + [VMEM] * 2,
        out_specs=[VMEM] * 4,
        scratch_shapes=[
            pltpu.VMEM((rows, model_width), BF16),
            pltpu.VMEM((rows, query_cols), BF16),
            pltpu.VMEM((4, rows + 2 * WINDOW, PAIR), BF16),
            pltpu.VMEM((rows, hidden_cols), BF16),
            pltpu.VMEM((model_width, query_cols), BF16),
            pltpu.VMEM((model_width, hidden_cols), BF16),
        ],
        compiler_params=LIMIT,
        cost_estimate=cost(2 * rows * model_width * (hidden_cols + query_cols), 8 << 20),
        name="mix",
    )(gathered, kv, before, after, pooled, sink, own2, other2)

    def exchanged(sent, kept, near_mask, far_mask):
        came = swapped(sent, TP, near_mask)
        both = kept.astype(F32) + came.astype(F32)
        passed = both[1].astype(BF16)
        rest = swapped(passed, TP, far_mask)
        return both[0] + rest.astype(F32)

    mix = (exchanged(sent0, kept0, 1, 3), exchanged(sent1, kept1, 3, 1))
    mix = jnp.concatenate(mix)
    stats = jnp.stack([jnp.sum(mix, axis=1), jnp.sum(mix * mix, axis=1)])
    stats = of_everyone(stats, TP)
    row_mean = stats[0] / model_width
    variance = stats[1] / model_width - row_mean * row_mean
    normed = (mix - row_mean[:, None]) * lax.rsqrt(variance + epsilon)[:, None] * out_gain
    return normed.astype(BF16)


def solution(mesh):
    finer = Mesh(mesh.devices.reshape(16, 4, 2, mesh.shape["tp"]), ("sp_0", "sp_1", "sp_2", "tp"))
    return jax.shard_map(
        layer,
        mesh=finer,
        in_specs=(
            P(SP, "tp"),
            P(SP, "tp"),
            P(SP, "tp"),
            P(SP, "tp"),
            P(SP, "tp"),
            P("tp"),
            P("tp", None, None),
            P("tp"),
            P("tp", SP),
            P("tp", SP),
            P("tp"),
        ),
        out_specs=P(SP, "tp"),
        check_vma=False,
    )
```

time: 154 us -> 153 us (level)
  the two profiles are of different devices: /device:TPU:2 before, /device:TPU:4 now
where the time goes in v3:
time: 153 us; the launch traced here: 152 us
  blocking collectives  64.6 us (42%)
  waiting for transfers between devices  40.2 us (26%)
  starting transfers between devices  29.5 us (19%)
  Pallas kernels  10.2 us (7%)
  local copies, waits for them, and re-layouts  5.68 us (4%)
  other arithmetic  1.77 us (1%)
    all_gather x1, blocking collectives, layer(): over_z = lax.all_gather(packed, Z, axis=0)  38.9 us
    all_to_all x2, blocking collectives, from_everyone(): lax.all_to_all(jnp.broadcast_to(shard[None], (count, *shard.shape)), axis...  25.8 us
    ppermute x6, waiting for transfers between devices, swapped(): lax.ppermute(shard, axis, [(i, i ^ mask) for i in range(lax.axis_size(axi...  22.1 us
    all_to_all x2, waiting for transfers between devices, from_everyone(): lax.all_to_all(jnp.broadcast_to(shard[None], (count, *shard.shape)), axis...  16.6 us
    ppermute x6, starting transfers between devices, swapped(): lax.ppermute(shard, axis, [(i, i ^ mask) for i in range(lax.axis_size(axi...  14.6 us
    all_to_all x2, starting transfers between devices, from_everyone(): lax.all_to_all(jnp.broadcast_to(shard[None], (count, *shard.shape)), axis...  9.39 us
    pallas_call x1, Pallas kernels, layer(): pl.pallas_call(functools.partial(mix_kernel, seq_len), out_shape=[block]...  8.06 us
    ppermute x1, starting transfers between devices, neighbours(): after = lax.ppermute(head, axis, [(i + 1, i) for i in range(count - 1)])  3.64 us
  transfers between devices with their start and end apart: 10, of which 8 were waited for; matrix products, arithmetic and copies ran while one was open for 0% of the time, Pallas kernels for 1%

profile of v3, /device:TPU:4, one launch (start us, length us, event | category | flops | bytes accessed | tf_op | source)
XLA Modules:
  0.0 152.2 jit_solution(10945054687434481542)
XLA Ops:
  0.0 0.9 concatenate.6
  0.9 38.9 %all-gather = bf16[256,1152]{1,0:T(8,128)(2,1)S(1)} all-gather(bf16[16,1152]{1,0:T(8,128)(2,1)S(1)} %concatenate.6), channel_id=2, replica_groups=mesh['sp_0'=16,'sp_1'=4,'sp_2'=2,'tp'=4] {'sp_0'}, dimensions={0}, use_global_device_ids=true | all-gather | bytes 626688 | tf_op jit(solution)/shard_map/all_gather | solution.py:231
  39.7 1.0 broadcast_in_dim.9
  40.7 4.8 %all-to-all-start.1 = ((bf16[4,16,16,384]{3,2,1,0:T(8,128)(2,1)}), bf16[4,16,16,384]{3,2,1,0:T(8,128)(2,1)S(1)}, u32[]{:S(2)}, u32[]{:S(2)}) async-start(bf16[4,16,16,384]{3,2,1,0:T(8,128)(2,1)} %broadcast_in_dim.9), calls=%async_computation.1 | async-start | bytes 1572864 | tf_op jit(solution)/shard_map/all_to_all | solution.py:29
  45.5 7.6 %all-to-all-done.1.own_ref = bf16[4,16,16,384]{3,2,1,0:T(8,128)(2,1)S(1)} async-done(((bf16[4,16,16,384]{3,2,1,0:T(8,128)(2,1)}), bf16[4,16,16,384]{3,2,1,0:T(8,128)(2,1)S(1)}, u32[]{:S(2)}, u32[]{:S(2)}) %all-to-all-start.1) | async-done | bytes 786464 | tf_op jit(solution)/shard_map/all_to_all | solution.py:29
  53.3 17.6 %all_to_all.20.own_ref = bf16[4,16,16,768]{3,2,1,0:T(8,128)(2,1)} all-to-all(bf16[4,16,16,768]{3,2,1,0:T(8,128)(2,1)S(1)} %broadcast_in_dim.10), channel_id=1, replica_groups=mesh['sp_0'=16,'sp_1'=4,'sp_2'=2,'tp'=4] {'sp_1'}, dimensions={0} | all-to-all | bytes 3145728 | tf_op jit(solution)/shard_map/all_to_all | solution.py:29
  71.0 1.5 broadcast_in_dim.8
  72.5 4.6 %all-to-all-start = ((bf16[4,512,512]{2,1,0:T(8,128)(2,1)}), bf16[4,512,512]{2,1,0:T(8,128)(2,1)S(1)}, u32[]{:S(2)}, u32[]{:S(2)}) async-start(bf16[4,512,512]{2,1,0:T(8,128)(2,1)} %broadcast_in_dim.8), calls=%async_computation | async-start | bytes 4194304 | tf_op jit(solution)/shard_map/all_to_all | solution.py:29
  77.1 1.9 %collective-permute-start.3 = (bf16[4,16,16,768]{3,2,1,0:T(8,128)(2,1)}, bf16[4,16,16,768]{3,2,1,0:T(8,128)(2,1)}, u32[]{:S(2)}, u32[]{:S(2)}) collective-permute-start(bf16[4,16,16,768]{3,2,1,0:T(8,128)(2,1)} %all_to_all.20.own_ref), channel_id=1, source_target_pairs={{0,4},{4,0},{1,5},{5,1},{2,6},{6,2},{3,7},{7,3},{8,12},{12,8},{9,1... | collective-permute-start | bytes 4718600 | tf_op jit(solution)/shard_map/ppermute | solution.py:39
  79.0 2.4 %collective-permute-start = (bf16[4,16,16,384]{3,2,1,0:T(8,128)(2,1)S(1)}, bf16[4,16,16,384]{3,2,1,0:T(8,128)(2,1)S(1)}, u32[]{:S(2)}, u32[]{:S(2)}) collective-permute-start(bf16[4,16,16,384]{3,2,1,0:T(8,128)(2,1)S(1)} %all-to-all-done.1.own_ref), channel_id=1, source_target_pairs={{0,4},{4,0},{1,5},{5,1},{2,6},{6,2},{3,7},{7,3},{8,12},{12,8},{9,1... | collective-permute-start | bytes 2359304 | tf_op jit(solution)/shard_map/ppermute | solution.py:39
  81.4 2.3 %collective-permute-done.other_ref = bf16[4,16,16,384]{3,2,1,0:T(8,128)(2,1)S(1)} collective-permute-done((bf16[4,16,16,384]{3,2,1,0:T(8,128)(2,1)S(1)}, bf16[4,16,16,384]{3,2,1,0:T(8,128)(2,1)S(1)}, u32[]{:S(2)}, u32[]{:S(2)}) %collective-permute-start) | collective-permute-done | bytes 786464 | tf_op jit(solution)/shard_map/ppermute | solution.py:39
  83.7 0.9 copy-done.1
  84.6 8.9 %all-to-all-done.tokens_ref = bf16[4,512,512]{2,1,0:T(8,128)(2,1)S(1)} async-done(((bf16[4,512,512]{2,1,0:T(8,128)(2,1)}), bf16[4,512,512]{2,1,0:T(8,128)(2,1)S(1)}, u32[]{:S(2)}, u32[]{:S(2)}) %all-to-all-start) | async-done | bytes 2097184 | tf_op jit(solution)/shard_map/all_to_all | solution.py:29
  93.6 1.1 copy-done.2
  94.7 1.5 project.1
  96.2 1.9 %collective-permute-start.1 = (bf16[144,128]{1,0:T(8,128)(2,1)S(1)}, bf16[144,128]{1,0:T(8,128)(2,1)S(1)}, u32[]{:S(2)}, u32[]{:S(2)}) collective-permute-start(bf16[144,128]{1,0:T(8,128)(2,1)S(1)} %get-tuple-element.14), channel_id=1, source_target_pairs={{0,4},{4,8},{8,12},{12,16},{16,20},{20,24},{24,28},{28,32},{32,36}... | collective-permute-start | bytes 110600 | tf_op jit(solution)/shard_map/ppermute | solution.py:44
  98.1 3.6 %collective-permute-start.2 = (bf16[144,128]{1,0:T(8,128)(2,1)S(1)}, bf16[144,128]{1,0:T(8,128)(2,1)S(1)}, u32[]{:S(2)}, u32[]{:S(2)}) collective-permute-start(bf16[144,128]{1,0:T(8,128)(2,1)S(1)} %get-tuple-element.15), channel_id=1, source_target_pairs={{4,0},{8,4},{12,8},{16,12},{20,16},{24,20},{28,24},{32,28},{36,32}... | collective-permute-start | bytes 110600 | tf_op jit(solution)/shard_map/ppermute | solution.py:45
  101.8 1.6 %collective-permute-done.2.after_ref = bf16[144,128]{1,0:T(8,128)(2,1)S(1)} collective-permute-done((bf16[144,128]{1,0:T(8,128)(2,1)S(1)}, bf16[144,128]{1,0:T(8,128)(2,1)S(1)}, u32[]{:S(2)}, u32[]{:S(2)}) %collective-permute-start.2) | collective-permute-done | bytes 36896 | tf_op jit(solution)/shard_map/ppermute | solution.py:45
  103.4 0.7 pool.1.pooled_ref
  104.1 8.1 %mix.1 = (bf16[2,256,512]{2,1,0:T(8,128)(2,1)S(1)}, bf16[2,256,512]{2,1,0:T(8,128)(2,1)S(1)}, bf16[2,256,512]{2,1,0:T(8,128)(2,1)S(1)}, bf16[2,256,512]{2,1,0:T(8,128)(2,1)S(1)}) custom-call(bf16[4,512,512]{2,1,0:T(8,128)(2,1)S(1)} %all-to-all-done.tokens_ref, bf16[512,128]{1,0:T(8,128)(2,1)S(1)} %get-tuple-element.13.kv_ref, ...), custom_call_target="tpu_custom_call" | custom-call | flops 1610612736 | bytes 8388608 | tf_op jit(solution)/shard_map/mix/pallas_call | solution.py:271
  112.1 2.5 %collective-permute-start.4 = (bf16[2,256,512]{2,1,0:T(8,128)(2,1)S(1)}, bf16[2,256,512]{2,1,0:T(8,128)(2,1)S(1)}, u32[]{:S(2)}, u32[]{:S(2)}) collective-permute-start(bf16[2,256,512]{2,1,0:T(8,128)(2,1)S(1)} %get-tuple-element.18), channel_id=1, source_target_pairs={{0,1},{1,0},{2,3},{3,2},{4,5},{5,4},{6,7},{7,6},{8,9},{9,8},{10,11... | collective-permute-start | bytes 1572872 | tf_op jit(solution)/shard_map/ppermute | solution.py:39
  114.6 2.5 %collective-permute-start.6 = (bf16[2,256,512]{2,1,0:T(8,128)(2,1)S(1)}, bf16[2,256,512]{2,1,0:T(8,128)(2,1)S(1)}, u32[]{:S(2)}, u32[]{:S(2)}) collective-permute-start(bf16[2,256,512]{2,1,0:T(8,128)(2,1)S(1)} %get-tuple-element.20), channel_id=1, source_target_pairs={{0,3},{1,2},{2,1},{3,0},{4,7},{5,6},{6,5},{7,4},{8,11},{9,10},{10,... | collective-permute-start | bytes 1572872 | tf_op jit(solution)/shard_map/ppermute | solution.py:39
  117.2 10.7 %collective-permute-done.4 = bf16[2,256,512]{2,1,0:T(8,128)(2,1)S(1)} collective-permute-done((bf16[2,256,512]{2,1,0:T(8,128)(2,1)S(1)}, bf16[2,256,512]{2,1,0:T(8,128)(2,1)S(1)}, u32[]{:S(2)}, u32[]{:S(2)}) %collective-permute-start.4) | collective-permute-done | bytes 524320 | tf_op jit(solution)/shard_map/ppermute | solution.py:39
  128.1 3.1 %collective-permute-start.5 = (bf16[256,512]{1,0:T(8,128)(2,1)S(1)}, bf16[256,512]{1,0:T(8,128)(2,1)S(1)}, u32[]{:S(2)}, u32[]{:S(2)}) collective-permute-start(bf16[256,512]{1,0:T(8,128)(2,1)S(1)} %fusion.3), channel_id=1, source_target_pairs={{0,3},{1,2},{2,1},{3,0},{4,7},{5,6},{6,5},{7,4},{8,11},{9,10},{10,... | collective-permute-start | bytes 786440 | tf_op jit(solution)/shard_map/ppermute | solution.py:39
  131.2 0.7 collective-permute-done.6
  131.8 0.2 convert_add_fusion
  132.1 2.2 %collective-permute-start.7 = (bf16[256,512]{1,0:T(8,128)(2,1)S(1)}, bf16[256,512]{1,0:T(8,128)(2,1)S(1)}, u32[]{:S(2)}, u32[]{:S(2)}) collective-permute-start(bf16[256,512]{1,0:T(8,128)(2,1)S(1)} %fusion.4), channel_id=1, source_target_pairs={{0,1},{1,0},{2,3},{3,2},{4,5},{5,4},{6,7},{7,6},{8,9},{9,8},{10,11... | collective-permute-start | bytes 786440 | tf_op jit(solution)/shard_map/ppermute | solution.py:39
  134.2 6.0 %collective-permute-done.5 = bf16[256,512]{1,0:T(8,128)(2,1)S(1)} collective-permute-done((bf16[256,512]{1,0:T(8,128)(2,1)S(1)}, bf16[256,512]{1,0:T(8,128)(2,1)S(1)}, u32[]{:S(2)}, u32[]{:S(2)}) %collective-permute-start.5) | collective-permute-done | bytes 262176 | tf_op jit(solution)/shard_map/ppermute | solution.py:39
  140.3 2.3 %collective-permute-done.7 = bf16[256,512]{1,0:T(8,128)(2,1)S(1)} collective-permute-done((bf16[256,512]{1,0:T(8,128)(2,1)S(1)}, bf16[256,512]{1,0:T(8,128)(2,1)S(1)}, u32[]{:S(2)}, u32[]{:S(2)}) %collective-permute-start.7) | collective-permute-done | bytes 262176 | tf_op jit(solution)/shard_map/ppermute | solution.py:39
  142.7 0.3 fusion
  143.0 8.1 %all_to_all.21 = f32[4,2,512]{2,1,0:T(2,128)S(1)} all-to-all(f32[4,2,512]{2,1,0:T(2,128)S(1)} %broadcast_in_dim.11), channel_id=1, replica_groups=mesh['sp_0'=16,'sp_1'=4,'sp_2'=2,'tp'=4] {'tp'}, dimensions={0} | all-to-all | bytes 32768 | tf_op jit(solution)/shard_map/all_to_all | solution.py:29
  151.2 1.0 multiply_convert_fusion
  (29 shorter events, 0.6 us)
Async XLA Ops:
  40.7 12.4 %all-to-all-start.1 = ((bf16[4,16,16,384]{3,2,1,0:T(8,128)(2,1)}), bf16[4,16,16,384]{3,2,1,0:T(8,128)(2,1)S(1)}, u32[]{:S(2)}, u32[]{:S(2)}) async-start(bf16[4,16,16,384]{3,2,1,0:T(8,128)(2,1)} %broadcast_in_dim.9), calls=%async_computation.1 | async-start | bytes 1572864 | tf_op jit(solution)/shard_map/all_to_all | solution.py:29
  53.3 17.7 %copy-start.6 = (bf16[512,512]{1,0:T(8,128)(2,1)S(1)}, bf16[512,512]{1,0:T(8,128)(2,1)}, u32[]{:S(2)}) copy-start(bf16[512,512]{1,0:T(8,128)(2,1)} %param.11) | copy-start | bytes 1572868
  72.5 30.9 %copy-start.3 = (bf16[1,256,256]{2,1,0:T(8,128)(2,1)S(1)}, bf16[1,256,256]{2,1,0:T(8,128)(2,1)}, u32[]{:S(2)}) copy-start(bf16[1,256,256]{2,1,0:T(8,128)(2,1)} %w_pool_ref.1) | copy-start | bytes 393220
  72.5 30.9 %copy-start.4 = (f32[256]{0:T(256)S(1)}, f32[256]{0:T(256)}, u32[]{:S(2)}) copy-start(f32[256]{0:T(256)} %param.18) | copy-start | bytes 3076
  72.5 31.6 %copy-start.5 = (f32[4]{0:T(128)S(1)}, f32[4]{0:T(128)}, u32[]{:S(2)}) copy-start(f32[4]{0:T(128)} %sink_ref.1) | copy-start | bytes 52
  72.5 21.1 %all-to-all-start = ((bf16[4,512,512]{2,1,0:T(8,128)(2,1)}), bf16[4,512,512]{2,1,0:T(8,128)(2,1)S(1)}, u32[]{:S(2)}, u32[]{:S(2)}) async-start(bf16[4,512,512]{2,1,0:T(8,128)(2,1)} %broadcast_in_dim.8), calls=%async_computation | async-start | bytes 4194304 | tf_op jit(solution)/shard_map/all_to_all | solution.py:29
  77.1 27.0 %collective-permute-start.3 = (bf16[4,16,16,768]{3,2,1,0:T(8,128)(2,1)}, bf16[4,16,16,768]{3,2,1,0:T(8,128)(2,1)}, u32[]{:S(2)}, u32[]{:S(2)}) collective-permute-start(bf16[4,16,16,768]{3,2,1,0:T(8,128)(2,1)} %all_to_all.20.own_ref), channel_id=1, source_target_pairs={{0,4},{4,0},{1,5},{5,1},{2,6},{6,2},{3,7},{7,3},{8,12},{12,8},{9,1... | collective-permute-start | bytes 4718600 | tf_op jit(solution)/shard_map/ppermute | solution.py:39
  79.0 4.7 %collective-permute-start = (bf16[4,16,16,384]{3,2,1,0:T(8,128)(2,1)S(1)}, bf16[4,16,16,384]{3,2,1,0:T(8,128)(2,1)S(1)}, u32[]{:S(2)}, u32[]{:S(2)}) collective-permute-start(bf16[4,16,16,384]{3,2,1,0:T(8,128)(2,1)S(1)} %all-to-all-done.1.own_ref), channel_id=1, source_target_pairs={{0,4},{4,0},{1,5},{5,1},{2,6},{6,2},{3,7},{7,3},{8,12},{12,8},{9,1... | collective-permute-start | bytes 2359304 | tf_op jit(solution)/shard_map/ppermute | solution.py:39
  83.7 0.9 copy-start.1
  93.6 1.1 copy-start.2
  94.7 9.4 %copy-start = (bf16[4,16,16,768]{3,2,1,0:T(8,128)(2,1)S(1)}, bf16[4,16,16,768]{3,2,1,0:T(8,128)(2,1)}, u32[]{:S(2)}) copy-start(bf16[4,16,16,768]{3,2,1,0:T(8,128)(2,1)} %all_to_all.20.own_ref) | copy-start | bytes 4718596
  96.2 5.6 %collective-permute-start.1 = (bf16[144,128]{1,0:T(8,128)(2,1)S(1)}, bf16[144,128]{1,0:T(8,128)(2,1)S(1)}, u32[]{:S(2)}, u32[]{:S(2)}) collective-permute-start(bf16[144,128]{1,0:T(8,128)(2,1)S(1)} %get-tuple-element.14), channel_id=1, source_target_pairs={{0,4},{4,8},{8,12},{12,16},{16,20},{20,24},{24,28},{28,32},{32,36}... | collective-permute-start | bytes 110600 | tf_op jit(solution)/shard_map/ppermute | solution.py:44
  98.1 5.3 %collective-permute-start.2 = (bf16[144,128]{1,0:T(8,128)(2,1)S(1)}, bf16[144,128]{1,0:T(8,128)(2,1)S(1)}, u32[]{:S(2)}, u32[]{:S(2)}) collective-permute-start(bf16[144,128]{1,0:T(8,128)(2,1)S(1)} %get-tuple-element.15), channel_id=1, source_target_pairs={{4,0},{8,4},{12,8},{16,12},{20,16},{24,20},{28,24},{32,28},{36,32}... | collective-permute-start | bytes 110600 | tf_op jit(solution)/shard_map/ppermute | solution.py:45
  112.1 15.7 %collective-permute-start.4 = (bf16[2,256,512]{2,1,0:T(8,128)(2,1)S(1)}, bf16[2,256,512]{2,1,0:T(8,128)(2,1)S(1)}, u32[]{:S(2)}, u32[]{:S(2)}) collective-permute-start(bf16[2,256,512]{2,1,0:T(8,128)(2,1)S(1)} %get-tuple-element.18), channel_id=1, source_target_pairs={{0,1},{1,0},{2,3},{3,2},{4,5},{5,4},{6,7},{7,6},{8,9},{9,8},{10,11... | collective-permute-start | bytes 1572872 | tf_op jit(solution)/shard_map/ppermute | solution.py:39
  114.6 17.2 %collective-permute-start.6 = (bf16[2,256,512]{2,1,0:T(8,128)(2,1)S(1)}, bf16[2,256,512]{2,1,0:T(8,128)(2,1)S(1)}, u32[]{:S(2)}, u32[]{:S(2)}) collective-permute-start(bf16[2,256,512]{2,1,0:T(8,128)(2,1)S(1)} %get-tuple-element.20), channel_id=1, source_target_pairs={{0,3},{1,2},{2,1},{3,0},{4,7},{5,6},{6,5},{7,4},{8,11},{9,10},{10,... | collective-permute-start | bytes 1572872 | tf_op jit(solution)/shard_map/ppermute | solution.py:39
  128.1 12.2 %collective-permute-start.5 = (bf16[256,512]{1,0:T(8,128)(2,1)S(1)}, bf16[256,512]{1,0:T(8,128)(2,1)S(1)}, u32[]{:S(2)}, u32[]{:S(2)}) collective-permute-start(bf16[256,512]{1,0:T(8,128)(2,1)S(1)} %fusion.3), channel_id=1, source_target_pairs={{0,3},{1,2},{2,1},{3,0},{4,7},{5,6},{6,5},{7,4},{8,11},{9,10},{10,... | collective-permute-start | bytes 786440 | tf_op jit(solution)/shard_map/ppermute | solution.py:39
  132.0 19.2 %copy-start.7 = (f32[512]{0:T(512)S(1)}, f32[512]{0:T(512)}, u32[]{:S(2)}) copy-start(f32[512]{0:T(512)} %param.21) | copy-start | bytes 6148
  132.1 10.6 %collective-permute-start.7 = (bf16[256,512]{1,0:T(8,128)(2,1)S(1)}, bf16[256,512]{1,0:T(8,128)(2,1)S(1)}, u32[]{:S(2)}, u32[]{:S(2)}) collective-permute-start(bf16[256,512]{1,0:T(8,128)(2,1)S(1)} %fusion.4), channel_id=1, source_target_pairs={{0,1},{1,0},{2,3},{3,2},{4,5},{5,4},{6,7},{7,6},{8,9},{9,8},{10,11... | collective-permute-start | bytes 786440 | tf_op jit(solution)/shard_map/ppermute | solution.py:39

commit v4 on v3

v4 whole, which is shorter than its diff:
```python
import functools

import jax
import jax.numpy as jnp
from jax import lax
from jax.experimental import pallas as pl
from jax.experimental.pallas import tpu as pltpu
from jax.sharding import Mesh
from jax.sharding import PartitionSpec as P


HEAD_DIM = 64
PAIR = 2 * HEAD_DIM
POOL_GROUPS = 4
RIM = 2 ** (POOL_GROUPS - 1)
WINDOW = 128
SP = ("sp_0", "sp_1", "sp_2")
Z, X, CORE = SP
TP = "tp"
BF16, F32 = jnp.bfloat16, jnp.float32

epsilon = 1e-05
masked_score = -1e30
nt = (((1,), (1,)), ((), ()))


def from_everyone(shard, axis):
    count = lax.axis_size(axis)
    return lax.all_to_all(
        jnp.broadcast_to(shard[None], (count, *shard.shape)), axis, 0, 0, tiled=True
    )


def of_everyone(shard, axis):
    return jnp.sum(from_everyone(shard, axis), axis=0)


def swapped(shard, axis, mask):
    return lax.ppermute(shard, axis, [(i, i ^ mask) for i in range(lax.axis_size(axis))])


def neighbours(head, tail, axis):
    count = lax.axis_size(axis)
    before = lax.ppermute(tail, axis, [(i, i + 1) for i in range(count - 1)])
    after = lax.ppermute(head, axis, [(i + 1, i) for i in range(count - 1)])
    return before, after


def whole_weights(own_ref, other_ref, w_ref, at):
    core = lax.axis_index(CORE)
    xs, zs, rows = own_ref.shape[:3]
    lanes = slice(at, at + w_ref.shape[1])
    for z in range(zs):
        for x in range(xs):
            base = (z * xs + x) * 2 * rows
            w_ref[pl.ds(pl.multiple_of(base + core * rows, rows), rows), :] = own_ref[
                x, z, :, lanes
            ]
            w_ref[pl.ds(pl.multiple_of(base + (1 - core) * rows, rows), rows), :] = other_ref[
                x, z, :, lanes
            ]


def projected(tokens_ref, w_ref, at, width):
    depth = tokens_ref.shape[2]
    total = None
    for p in range(tokens_ref.shape[0]):
        part = jnp.dot(
            tokens_ref[p],
            w_ref[p * depth : (p + 1) * depth, at : at + width],
            preferred_element_type=F32,
        )
        total = part if total is None else total + part
    return total.astype(BF16)


def project_kernel(tokens_ref, own_ref, other_ref, kv_ref, chan_ref, head_ref, tail_ref, w_ref):
    rows = tokens_ref.shape[1]
    whole_weights(own_ref, other_ref, w_ref, 0)
    kv_cols = kv_ref.shape[1]
    kv_ref[...] = projected(tokens_ref, w_ref, 0, kv_cols)
    chan_ref[...] = projected(tokens_ref, w_ref, kv_cols, chan_ref.shape[1])
    for ref, kv_at, chan_at in ((head_ref, 0, 0), (tail_ref, rows - WINDOW, rows - RIM)):
        ref[:WINDOW] = kv_ref[kv_at : kv_at + WINDOW]
        edge = chan_ref[chan_at : chan_at + RIM].astype(F32)
        ref[WINDOW:] = jnp.concatenate([edge[:, :PAIR], edge[:, PAIR:]]).astype(BF16)


def split_band(kv, band_ref):
    kv = kv.astype(F32)
    turned = pltpu.roll(kv, HEAD_DIM, 1)
    low = lax.broadcasted_iota(jnp.int32, kv.shape, 1) < HEAD_DIM
    band_ref[0] = jnp.where(low, kv, 0.0).astype(BF16)
    band_ref[1] = jnp.where(low, 0.0, turned).astype(BF16)
    band_ref[2] = jnp.where(low, turned, 0.0).astype(BF16)
    band_ref[3] = jnp.where(low, 0.0, kv).astype(BF16)


def attend_block(queries, first_key, edge, seq_len, band_ref, at, sink_ref, attended_ref, to):
    row = lax.broadcasted_iota(jnp.int32, (WINDOW, 3 * WINDOW), 0)
    col = lax.broadcasted_iota(jnp.int32, (WINDOW, 3 * WINDOW), 1)
    keep = (col >= row) & (col <= row + 2 * WINDOW)
    if edge:
        key_pos = col + first_key
        keep = keep & (key_pos >= 0) & (key_pos < seq_len)
    band = pl.ds(at, 3 * WINDOW)
    for pair in range(queries.shape[1] // PAIR):
        lanes = slice(pair * PAIR, (pair + 1) * PAIR)
        attended = jnp.zeros((WINDOW, PAIR), F32)
        for side in range(2):
            scores = lax.dot_general(
                queries[:, lanes], band_ref[side, band], nt, preferred_element_type=F32
            ) * HEAD_DIM ** (-0.5)
            scores = jnp.where(keep, scores, masked_score)
            sink = sink_ref[2 * pair + side]
            top = jnp.maximum(jnp.max(scores, axis=1, keepdims=True), sink)
            raised = jnp.exp(scores - top)
            total = jnp.sum(raised, axis=1, keepdims=True) + jnp.exp(sink - top)
            probs = (raised * (1.0 / total)).astype(BF16)
            attended += jnp.dot(probs, band_ref[2 + side, band], preferred_element_type=F32)
        attended_ref[to : to + WINDOW, lanes] = attended.astype(BF16)


def inner_kernel(
    seq_len,
    tokens_ref,
    own_ref,
    other_ref,
    kv_ref,
    sink_ref,
    query_ref,
    attended_ref,
    w_ref,
    band_ref,
):
    rows, query_cols = query_ref.shape
    whole_weights(own_ref, other_ref, w_ref, own_ref.shape[3] - query_cols)
    query_ref[...] = projected(tokens_ref, w_ref, 0, query_cols)
    split_band(kv_ref[...], band_ref)
    for b in range(1, rows // WINDOW - 1):
        attend_block(
            query_ref[b * WINDOW : (b + 1) * WINDOW],
            0,
            False,
            seq_len,
            band_ref,
            (b - 1) * WINDOW,
            sink_ref,
            attended_ref,
            (b - 1) * WINDOW,
        )


def outer_kernel(
    seq_len,
    query_ref,
    kv_ref,
    chan_ref,
    before_ref,
    after_ref,
    sink_ref,
    w_pool_ref,
    scale_ref,
    attended_ref,
    pooled_ref,
    band_ref,
):
    rows = chan_ref.shape[0]
    y = lax.axis_index(TP)
    offset = lax.axis_index(SP) * rows

    split_band(
        jnp.concatenate(
            [
                before_ref[:WINDOW],
                kv_ref[: 2 * WINDOW],
                kv_ref[rows - 2 * WINDOW :],
                after_ref[:WINDOW],
            ]
        ),
        band_ref,
    )
    for edge, start in enumerate((0, rows - WINDOW)):
        attend_block(
            query_ref[start : start + WINDOW],
            offset + start - WINDOW,
            True,
            seq_len,
            band_ref,
            edge * 3 * WINDOW,
            sink_ref,
            attended_ref,
            edge * WINDOW,
        )

    def rim(ref):
        packed = ref[WINDOW:].astype(F32)
        return jnp.concatenate([packed[:RIM], packed[RIM:]], axis=1)

    own = chan_ref[...].astype(F32)
    chan = jnp.concatenate([rim(before_ref), own, rim(after_ref)])
    length = chan.shape[0]
    sums = chan + pltpu.roll(chan, 1, 0)
    window_sum = sums
    for level in range(1, POOL_GROUPS):
        step = 2 ** (level - 1)
        sums = pltpu.roll(sums, step, 0) + pltpu.roll(sums, length - step, 0)
        window_sum = jnp.where(y >= level, sums, window_sum)
    half_width = jnp.left_shift(jnp.int32(1), y)
    pos = offset + lax.broadcasted_iota(jnp.int32, (rows, 1), 0)
    count = jnp.minimum(pos + half_width, seq_len) - jnp.maximum(pos - half_width, 0)
    spread = window_sum[RIM : RIM + rows] / count.astype(F32) - own
    pooled = jnp.dot(spread.astype(BF16), w_pool_ref[0], preferred_element_type=F32)
    pooled_ref[...] = (pooled * scale_ref[...]).astype(BF16)


def out_kernel(blocks, attended_refs, pooled_ref, own_ref, other_ref, out_refs, hidden_ref, w_ref):
    y = lax.axis_index(TP)
    whole_weights(own_ref, other_ref, w_ref, 0)
    _, query_cols = attended_refs[0].shape
    share = out_refs[0].shape[2]
    for half, attended_ref in zip(sorted({half for half, _ in sum(blocks, ())}), attended_refs):
        hidden_ref[:, :query_cols] = attended_ref[...]
        if half == 0:
            hidden_ref[:, query_cols:] = pooled_ref[WINDOW:-WINDOW]
        else:
            hidden_ref[:WINDOW, query_cols:] = pooled_ref[:WINDOW]
            hidden_ref[WINDOW:, query_cols:] = pooled_ref[pooled_ref.shape[0] - WINDOW :]
        for ref, slots in zip(out_refs, blocks):
            for slot, (of_half, mask) in enumerate(slots):
                if of_half == half:
                    columns = w_ref[pl.ds(pl.multiple_of((y ^ mask) * share, share), share)]
                    ref[slot] = lax.dot_general(
                        hidden_ref[...], columns, nt, preferred_element_type=F32
                    ).astype(BF16)


VMEM = pl.BlockSpec(memory_space=pltpu.VMEM)
SMEM = pl.BlockSpec(memory_space=pltpu.SMEM)
LIMIT = pltpu.CompilerParams(vmem_limit_bytes=20 * 1024 * 1024)


def layer(
    tokens,
    w_query,
    w_key,
    w_value,
    w_pool_in,
    sink,
    w_pool,
    pool_scale,
    w_out_attn,
    w_out_pool,
    out_gain,
):
    rows = tokens.shape[0]
    seq_len = rows * lax.axis_size(SP)
    query_cols, key_cols, chan_cols = w_query.shape[1], w_key.shape[1], w_pool_in.shape[1]
    in_cols = 2 * key_cols + chan_cols + query_cols
    hidden_cols = query_cols + chan_cols
    share = out_gain.shape[0]
    model_width = share * lax.axis_size(TP)

    gathered = from_everyone(tokens, TP)
    packed = jnp.concatenate(
        (w_key, w_value, w_pool_in, w_query, w_out_attn.T, w_out_pool.T), axis=1
    )
    over_z = lax.all_gather(packed, Z, axis=0)
    for_x = [
        jnp.broadcast_to(part[None], (lax.axis_size(X), *part.shape))
        for part in (over_z[:, :, :in_cols], over_z[:, :, in_cols:])
    ]
    for_x = lax.optimization_barrier(for_x)
    own1 = lax.all_to_all(for_x[0], X, 0, 0, tiled=True)
    own2 = lax.all_to_all(for_x[1], X, 0, 0, tiled=True)
    other1 = swapped(own1, CORE, 1)
    other2 = swapped(own2, CORE, 1)

    def rows_of(width, count=rows):
        return jax.ShapeDtypeStruct((count, width), BF16)

    def cost(flops, size):
        return pl.CostEstimate(flops=flops, bytes_accessed=size, transcendentals=0)

    rim_shape = rows_of(PAIR, WINDOW + 2 * RIM)
    kv, chan, head, tail = pl.pallas_call(
        project_kernel,
        out_shape=[rows_of(2 * key_cols), rows_of(chan_cols), rim_shape, rim_shape],
        in_specs=[VMEM] * 3,
        out_specs=[VMEM] * 4,
        scratch_shapes=[pltpu.VMEM((model_width, 2 * key_cols + chan_cols), BF16)],
        compiler_params=LIMIT,
        cost_estimate=cost(2 * rows * model_width * (in_cols - query_cols), 4 << 20),
        name="project",
    )(gathered, own1, other1)
    before, after = neighbours(head, tail, SP)
    band = pltpu.VMEM((4, rows, PAIR), BF16)
    query, attended0 = pl.pallas_call(
        functools.partial(inner_kernel, seq_len),
        out_shape=[rows_of(query_cols), rows_of(query_cols, rows - 2 * WINDOW)],
        in_specs=[VMEM] * 4 + [SMEM],
        out_specs=[VMEM] * 2,
        scratch_shapes=[pltpu.VMEM((model_width, query_cols), BF16), band],
        compiler_params=LIMIT,
        cost_estimate=cost(2 * rows * model_width * query_cols, 4 << 20),
        name="inner",
    )(gathered, own1, other1, kv, sink)
    attended1, pooled = pl.pallas_call(
        functools.partial(outer_kernel, seq_len),
        out_shape=[rows_of(query_cols, 2 * WINDOW), rows_of(chan_cols)],
        in_specs=[VMEM] * 5 + [SMEM] + [VMEM] * 2,
        out_specs=[VMEM] * 2,
        scratch_shapes=[pltpu.VMEM((4, 6 * WINDOW, PAIR), BF16)],
        compiler_params=LIMIT,
        cost_estimate=cost(2 * rows * model_width * query_cols, 2 << 20),
        name="outer",
    )(query, kv, chan, before, after, sink, w_pool, pool_scale.reshape(1, -1))

    def multiplied(blocks, *attended):
        count = len(attended)
        outs = len(blocks)

        def kernel(*refs):
            out_kernel(
                blocks,
                refs[:count],
                *refs[count : count + 3],
                refs[count + 3 : count + 3 + outs],
                *refs[count + 3 + outs :],
            )

        return pl.pallas_call(
            kernel,
            out_shape=[jax.ShapeDtypeStruct((2, rows // 2, share), BF16)] * outs,
            in_specs=[VMEM] * (count + 3),
            out_specs=[VMEM] * outs,
            scratch_shapes=[
                pltpu.VMEM((rows // 2, hidden_cols), BF16),
                pltpu.VMEM((model_width, hidden_cols), BF16),
            ],
            compiler_params=LIMIT,
            cost_estimate=cost(outs * rows // 2 * model_width * hidden_cols, 4 << 20),
        )(*attended, pooled, own2, other2)

    (sent0,) = multiplied((((0, 1), (0, 2)),), attended0)
    sent1, kept0, kept1 = multiplied(
        (((1, 3), (1, 2)), ((0, 0), (0, 3)), ((1, 0), (1, 1))), attended0, attended1
    )

    def exchanged(sent, kept, near_mask, far_mask):
        came = swapped(sent, TP, near_mask)
        both = kept.astype(F32) + came.astype(F32)
        passed = both[1].astype(BF16)
        rest = swapped(passed, TP, far_mask)
        return both[0] + rest.astype(F32)

    middle = exchanged(sent0, kept0, 1, 3)
    edges = exchanged(sent1, kept1, 3, 1)
    mix = jnp.concatenate([edges[:WINDOW], middle, edges[WINDOW:]])
    stats = jnp.stack([jnp.sum(mix, axis=1), jnp.sum(mix * mix, axis=1)])
    stats = of_everyone(stats, TP)
    row_mean = stats[0] / model_width
    variance = stats[1] / model_width - row_mean * row_mean
    normed = (mix - row_mean[:, None]) * lax.rsqrt(variance + epsilon)[:, None] * out_gain
    return normed.astype(BF16)


def solution(mesh):
    finer = Mesh(mesh.devices.reshape(16, 4, 2, mesh.shape["tp"]), ("sp_0", "sp_1", "sp_2", "tp"))
    return jax.shard_map(
        layer,
        mesh=finer,
        in_specs=(
            P(SP, "tp"),
            P(SP, "tp"),
            P(SP, "tp"),
            P(SP, "tp"),
            P(SP, "tp"),
            P("tp"),
            P("tp", None, None),
            P("tp"),
            P("tp", SP),
            P("tp", SP),
            P("tp"),
        ),
        out_specs=P(SP, "tp"),
        check_vma=False,
    )
```

time: 153 us -> 154 us (level)
  the two profiles are of different devices: /device:TPU:4 before, /device:TPU:2 now
where the time goes in v4:
time: 154 us; the launch traced here: 153 us
  blocking collectives  79.5 us (52%)
  waiting for transfers between devices  27.5 us (18%)
  starting transfers between devices  26.3 us (17%)
  Pallas kernels  15 us (10%)
  local copies, waits for them, and re-layouts  2.78 us (2%)
  other arithmetic  1.78 us (1%)
    all_gather x1, blocking collectives, layer(): over_z = lax.all_gather(packed, Z, axis=0)  38.9 us
    all_to_all x1, blocking collectives, layer(): own2 = lax.all_to_all(for_x[1], X, 0, 0, tiled=True)  16.4 us
    ppermute x6, starting transfers between devices, swapped(): lax.ppermute(shard, axis, [(i, i ^ mask) for i in range(lax.axis_size(axi...  16.2 us
    ppermute x6, waiting for transfers between devices, swapped(): lax.ppermute(shard, axis, [(i, i ^ mask) for i in range(lax.axis_size(axi...  15.5 us
    all_to_all x1, blocking collectives, layer(): own1 = lax.all_to_all(for_x[0], X, 0, 0, tiled=True)  14.8 us
    all_to_all x1, waiting for transfers between devices, from_everyone(): lax.all_to_all(jnp.broadcast_to(shard[None], (count, *shard.shape)), axis...  12 us
    all_to_all x1, blocking collectives, from_everyone(): lax.all_to_all(jnp.broadcast_to(shard[None], (count, *shard.shape)), axis...  9.39 us
    pallas_call x1, Pallas kernels, layer(): pl.pallas_call(functools.partial(inner_kernel, seq_len), out_shape=[rows_...  4.94 us
  transfers between devices with their start and end apart: 9, of which 4 were waited for; matrix products, arithmetic and copies ran while one was open for 0% of the time, Pallas kernels for 8%

profile of v4, /device:TPU:2, one launch (start us, length us, event | category | flops | bytes accessed | tf_op | source)
XLA Modules:
  0.0 153.1 jit_solution(12065670592201924382)
XLA Ops:
  0.0 0.9 concatenate.6
  0.9 38.9 %all-gather = bf16[256,1152]{1,0:T(8,128)(2,1)S(1)} all-gather(bf16[16,1152]{1,0:T(8,128)(2,1)S(1)} %concatenate.6), channel_id=2, replica_groups=mesh['sp_0'=16,'sp_1'=4,'sp_2'=2,'tp'=4] {'sp_0'}, dimensions={0}, use_global_device_ids=true | all-gather | bytes 626688 | tf_op jit(solution)/shard_map/all_gather | solution.py:268
  39.8 0.1 broadcast_in_dim.9
  39.9 0.1 broadcast_in_dim.10
  40.0 16.4 %all_to_all.20.refs_3_.refs_2_ = bf16[4,16,16,512]{3,2,1,0:T(8,128)(2,1)} all-to-all(bf16[4,16,16,512]{3,2,1,0:T(8,128)(2,1)S(1)} %broadcast_in_dim.10), channel_id=1, replica_groups=mesh['sp_0'=16,'sp_1'=4,'sp_2'=2,'tp'=4] {'sp_1'}, dimensions={0} | all-to-all | bytes 2097152 | tf_op jit(solution)/shard_map/all_to_all | solution.py:275
  56.4 14.8 %all_to_all.21.own_ref = bf16[4,16,16,640]{3,2,1,0:T(8,128)(2,1)S(1)} all-to-all(bf16[4,16,16,640]{3,2,1,0:T(8,128)(2,1)S(1)} %broadcast_in_dim.9), channel_id=1, replica_groups=mesh['sp_0'=16,'sp_1'=4,'sp_2'=2,'tp'=4] {'sp_1'}, dimensions={0} | all-to-all | bytes 2621440 | tf_op jit(solution)/shard_map/all_to_all | solution.py:274
  71.2 1.5 broadcast_in_dim.8
  72.7 4.5 %all-to-all-start = ((bf16[4,512,512]{2,1,0:T(8,128)(2,1)}), bf16[4,512,512]{2,1,0:T(8,128)(2,1)S(1)}, u32[]{:S(2)}, u32[]{:S(2)}) async-start(bf16[4,512,512]{2,1,0:T(8,128)(2,1)} %broadcast_in_dim.8), calls=%async_computation | async-start | bytes 4194304 | tf_op jit(solution)/shard_map/all_to_all | solution.py:29
  77.2 2.0 %collective-permute-start = (bf16[4,16,16,640]{3,2,1,0:T(8,128)(2,1)S(1)}, bf16[4,16,16,640]{3,2,1,0:T(8,128)(2,1)}, u32[]{:S(2)}, u32[]{:S(2)}) collective-permute-start(bf16[4,16,16,640]{3,2,1,0:T(8,128)(2,1)S(1)} %all_to_all.21.own_ref), channel_id=1, source_target_pairs={{0,4},{4,0},{1,5},{5,1},{2,6},{6,2},{3,7},{7,3},{8,12},{12,8},{9,1... | collective-permute-start | bytes 3932168 | tf_op jit(solution)/shard_map/ppermute | solution.py:39
  79.3 2.4 %collective-permute-start.3 = (bf16[4,16,16,512]{3,2,1,0:T(8,128)(2,1)}, bf16[4,16,16,512]{3,2,1,0:T(8,128)(2,1)}, u32[]{:S(2)}, u32[]{:S(2)}) collective-permute-start(bf16[4,16,16,512]{3,2,1,0:T(8,128)(2,1)} %all_to_all.20.refs_3_.refs_2_), channel_id=1, source_target_pairs={{0,4},{4,0},{1,5},{5,1},{2,6},{6,2},{3,7},{7,3},{8,12},{12,8},{9,1... | collective-permute-start | bytes 3145736 | tf_op jit(solution)/shard_map/ppermute | solution.py:39
  81.7 12.0 %all-to-all-done.tokens_ref = bf16[4,512,512]{2,1,0:T(8,128)(2,1)S(1)} async-done(((bf16[4,512,512]{2,1,0:T(8,128)(2,1)}), bf16[4,512,512]{2,1,0:T(8,128)(2,1)S(1)}, u32[]{:S(2)}, u32[]{:S(2)}) %all-to-all-start) | async-done | bytes 2097184 | tf_op jit(solution)/shard_map/all_to_all | solution.py:29
  93.7 2.8 %project.1 = (bf16[512,128]{1,0:T(8,128)(2,1)S(1)}, bf16[512,256]{1,0:T(8,128)(2,1)S(1)}, bf16[144,128]{1,0:T(8,128)(2,1)S(1)}, bf16[144,128]{1,0:T(8,128)(2,1)S(1)}) custom-call(bf16[4,512,512]{2,1,0:T(8,128)(2,1)S(1)} %all-to-all-done.tokens_ref, bf16[4,16,16,640]{3,2,1,0:T(8,128)(2,1)S(1)} %all_to_all.21.own_ref, ...), custom_call_target="tpu_custom_call" | custom-call | flops 805306368 | bytes 4194304 | tf_op jit(solution)/shard_map/project/pallas_call | solution.py:286
  96.5 1.9 %collective-permute-start.1 = (bf16[144,128]{1,0:T(8,128)(2,1)S(1)}, bf16[144,128]{1,0:T(8,128)(2,1)S(1)}, u32[]{:S(2)}, u32[]{:S(2)}) collective-permute-start(bf16[144,128]{1,0:T(8,128)(2,1)S(1)} %get-tuple-element.23), channel_id=1, source_target_pairs={{0,4},{4,8},{8,12},{12,16},{16,20},{20,24},{24,28},{28,32},{32,36}... | collective-permute-start | bytes 110600 | tf_op jit(solution)/shard_map/ppermute | solution.py:44
  98.4 3.6 %collective-permute-start.2 = (bf16[144,128]{1,0:T(8,128)(2,1)S(1)}, bf16[144,128]{1,0:T(8,128)(2,1)S(1)}, u32[]{:S(2)}, u32[]{:S(2)}) collective-permute-start(bf16[144,128]{1,0:T(8,128)(2,1)S(1)} %get-tuple-element.24), channel_id=1, source_target_pairs={{4,0},{8,4},{12,8},{16,12},{20,16},{24,20},{28,24},{32,28},{36,32}... | collective-permute-start | bytes 110600 | tf_op jit(solution)/shard_map/ppermute | solution.py:45
  102.1 4.9 %inner.1 = (bf16[512,256]{1,0:T(8,128)(2,1)S(1)}, bf16[256,256]{1,0:T(8,128)(2,1)S(1)}) custom-call(bf16[4,512,512]{2,1,0:T(8,128)(2,1)S(1)} %all-to-all-done.tokens_ref, bf16[4,16,16,640]{3,2,1,0:T(8,128)(2,1)S(1)} %all_to_all.21.own_ref, bf16[4,16,16,640]{3,2,1,0:T(8,128)(2,1)} %collective-permute-done.other_ref, ...), custom_call_target="tpu_custom_call" | custom-call | flops 536870912 | bytes 4194304 | tf_op jit(solution)/shard_map/inner/pallas_call | solution.py:298
  107.1 3.1 %outer.1 = (bf16[256,256]{1,0:T(8,128)(2,1)S(1)}, bf16[512,256]{1,0:T(8,128)(2,1)S(1)}) custom-call(bf16[512,256]{1,0:T(8,128)(2,1)S(1)} %get-tuple-element.21.query_ref, bf16[512,128]{1,0:T(8,128)(2,1)S(1)} %get-tuple-element.19.kv_ref, bf16[512,256]{1,0:T(8,128)(2,1)S(1)} %get-tuple-element.22.chan_ref, ...), custom_call_target="tpu_custom_call" | custom-call | flops 536870912 | bytes 2097152 | tf_op jit(solution)/shard_map/outer/pallas_call | solution.py:308
  110.2 2.4 %shard_map.109 = (bf16[2,256,512]{2,1,0:T(8,128)(2,1)S(1)}, bf16[2,256,512]{2,1,0:T(8,128)(2,1)S(1)}, bf16[2,256,512]{2,1,0:T(8,128)(2,1)S(1)}) custom-call(bf16[256,256]{1,0:T(8,128)(2,1)S(1)} %get-tuple-element.20.refs_0_, bf16[256,256]{1,0:T(8,128)(2,1)S(1)} %get-tuple-element.25.refs_1_, bf16[512,256]{1,0:T(8,128)(2,1)S(1)} %get-tuple-element.26.refs_2_.refs_1_, ...), custom_call_target="tpu_custom_call" | custom-call | flops 805306368 | bytes 4194304 | tf_op jit(solution)/shard_map/pallas_call | solution.py:332
  112.6 3.1 %collective-permute-start.4 = (bf16[2,256,512]{2,1,0:T(8,128)(2,1)S(1)}, bf16[2,256,512]{2,1,0:T(8,128)(2,1)S(1)}, u32[]{:S(2)}, u32[]{:S(2)}) collective-permute-start(bf16[2,256,512]{2,1,0:T(8,128)(2,1)S(1)} %get-tuple-element.29), channel_id=1, source_target_pairs={{0,3},{1,2},{2,1},{3,0},{4,7},{5,6},{6,5},{7,4},{8,11},{9,10},{10,... | collective-permute-start | bytes 1572872 | tf_op jit(solution)/shard_map/ppermute | solution.py:39
  115.7 1.8 %shard_map.110 = bf16[2,256,512]{2,1,0:T(8,128)(2,1)S(1)} custom-call(bf16[256,256]{1,0:T(8,128)(2,1)S(1)} %get-tuple-element.20.refs_0_, bf16[512,256]{1,0:T(8,128)(2,1)S(1)} %get-tuple-element.26.refs_2_.refs_1_, bf16[4,16,16,512]{3,2,1,0:T(8,128)(2,1)S(1)} %copy-done, bf16[4,16,16,512]{3,2,1,0:T(8,128)(2,1)} %collective-permute-done.3.refs_4_.refs_3_), custom_call_target="tpu_custom_call" | custom-call | flops 268435456 | bytes 4194304 | tf_op jit(solution)/shard_map/pallas_call | solution.py:332
  117.5 1.9 %collective-permute-start.6 = (bf16[2,256,512]{2,1,0:T(8,128)(2,1)S(1)}, bf16[2,256,512]{2,1,0:T(8,128)(2,1)S(1)}, u32[]{:S(2)}, u32[]{:S(2)}) collective-permute-start(bf16[2,256,512]{2,1,0:T(8,128)(2,1)S(1)} %shard_map.110), channel_id=1, source_target_pairs={{0,1},{1,0},{2,3},{3,2},{4,5},{5,4},{6,7},{7,6},{8,9},{9,8},{10,11... | collective-permute-start | bytes 1572872 | tf_op jit(solution)/shard_map/ppermute | solution.py:39
  119.4 8.8 %collective-permute-done.4 = bf16[2,256,512]{2,1,0:T(8,128)(2,1)S(1)} collective-permute-done((bf16[2,256,512]{2,1,0:T(8,128)(2,1)S(1)}, bf16[2,256,512]{2,1,0:T(8,128)(2,1)S(1)}, u32[]{:S(2)}, u32[]{:S(2)}) %collective-permute-start.4) | collective-permute-done | bytes 524320 | tf_op jit(solution)/shard_map/ppermute | solution.py:39
  128.3 0.2 convert_add_fusion.1
  128.5 1.9 %collective-permute-start.5 = (bf16[256,512]{1,0:T(8,128)(2,1)S(1)}, bf16[256,512]{1,0:T(8,128)(2,1)S(1)}, u32[]{:S(2)}, u32[]{:S(2)}) collective-permute-start(bf16[256,512]{1,0:T(8,128)(2,1)S(1)} %fusion.3), channel_id=1, source_target_pairs={{0,1},{1,0},{2,3},{3,2},{4,5},{5,4},{6,7},{7,6},{8,9},{9,8},{10,11... | collective-permute-start | bytes 786440 | tf_op jit(solution)/shard_map/ppermute | solution.py:39
  130.4 2.2 %collective-permute-done.6 = bf16[2,256,512]{2,1,0:T(8,128)(2,1)S(1)} collective-permute-done((bf16[2,256,512]{2,1,0:T(8,128)(2,1)S(1)}, bf16[2,256,512]{2,1,0:T(8,128)(2,1)S(1)}, u32[]{:S(2)}, u32[]{:S(2)}) %collective-permute-start.6) | collective-permute-done | bytes 524320 | tf_op jit(solution)/shard_map/ppermute | solution.py:39
  132.6 0.2 convert_add_fusion
  132.8 4.9 %collective-permute-start.7 = (bf16[256,512]{1,0:T(8,128)(2,1)S(1)}, bf16[256,512]{1,0:T(8,128)(2,1)S(1)}, u32[]{:S(2)}, u32[]{:S(2)}) collective-permute-start(bf16[256,512]{1,0:T(8,128)(2,1)S(1)} %fusion.4), channel_id=1, source_target_pairs={{0,3},{1,2},{2,1},{3,0},{4,7},{5,6},{6,5},{7,4},{8,11},{9,10},{10,... | collective-permute-start | bytes 786440 | tf_op jit(solution)/shard_map/ppermute | solution.py:39
  137.7 0.1 fusion.1
  137.8 4.5 %collective-permute-done.7 = bf16[256,512]{1,0:T(8,128)(2,1)S(1)} collective-permute-done((bf16[256,512]{1,0:T(8,128)(2,1)S(1)}, bf16[256,512]{1,0:T(8,128)(2,1)S(1)}, u32[]{:S(2)}, u32[]{:S(2)}) %collective-permute-start.7) | collective-permute-done | bytes 262176 | tf_op jit(solution)/shard_map/ppermute | solution.py:39
  142.3 0.1 fusion
  142.3 0.3 fusion.2
  142.6 9.4 %all_to_all.22 = f32[4,2,512]{2,1,0:T(2,128)S(1)} all-to-all(f32[4,2,512]{2,1,0:T(2,128)S(1)} %broadcast_in_dim.11), channel_id=1, replica_groups=mesh['sp_0'=16,'sp_1'=4,'sp_2'=2,'tp'=4] {'tp'}, dimensions={0} | all-to-all | bytes 32768 | tf_op jit(solution)/shard_map/all_to_all | solution.py:29
  152.1 1.0 multiply_convert_fusion
  (27 shorter events, 0.2 us)
Async XLA Ops:
  56.4 14.8 %copy-start.4 = (bf16[512,512]{1,0:T(8,128)(2,1)S(1)}, bf16[512,512]{1,0:T(8,128)(2,1)}, u32[]{:S(2)}) copy-start(bf16[512,512]{1,0:T(8,128)(2,1)} %param.11) | copy-start | bytes 1572868
  72.7 21.0 %all-to-all-start = ((bf16[4,512,512]{2,1,0:T(8,128)(2,1)}), bf16[4,512,512]{2,1,0:T(8,128)(2,1)S(1)}, u32[]{:S(2)}, u32[]{:S(2)}) async-start(bf16[4,512,512]{2,1,0:T(8,128)(2,1)} %broadcast_in_dim.8), calls=%async_computation | async-start | bytes 4194304 | tf_op jit(solution)/shard_map/all_to_all | solution.py:29
  77.2 24.9 %copy-start.1 = (f32[4]{0:T(128)S(1)}, f32[4]{0:T(128)}, u32[]{:S(2)}) copy-start(f32[4]{0:T(128)} %sink_ref.3) | copy-start | bytes 52
  77.2 16.5 %collective-permute-start = (bf16[4,16,16,640]{3,2,1,0:T(8,128)(2,1)S(1)}, bf16[4,16,16,640]{3,2,1,0:T(8,128)(2,1)}, u32[]{:S(2)}, u32[]{:S(2)}) collective-permute-start(bf16[4,16,16,640]{3,2,1,0:T(8,128)(2,1)S(1)} %all_to_all.21.own_ref), channel_id=1, source_target_pairs={{0,4},{4,0},{1,5},{5,1},{2,6},{6,2},{3,7},{7,3},{8,12},{12,8},{9,1... | collective-permute-start | bytes 3932168 | tf_op jit(solution)/shard_map/ppermute | solution.py:39
  79.3 30.9 %collective-permute-start.3 = (bf16[4,16,16,512]{3,2,1,0:T(8,128)(2,1)}, bf16[4,16,16,512]{3,2,1,0:T(8,128)(2,1)}, u32[]{:S(2)}, u32[]{:S(2)}) collective-permute-start(bf16[4,16,16,512]{3,2,1,0:T(8,128)(2,1)} %all_to_all.20.refs_3_.refs_2_), channel_id=1, source_target_pairs={{0,4},{4,0},{1,5},{5,1},{2,6},{6,2},{3,7},{7,3},{8,12},{12,8},{9,1... | collective-permute-start | bytes 3145736 | tf_op jit(solution)/shard_map/ppermute | solution.py:39
  96.5 10.6 %collective-permute-start.1 = (bf16[144,128]{1,0:T(8,128)(2,1)S(1)}, bf16[144,128]{1,0:T(8,128)(2,1)S(1)}, u32[]{:S(2)}, u32[]{:S(2)}) collective-permute-start(bf16[144,128]{1,0:T(8,128)(2,1)S(1)} %get-tuple-element.23), channel_id=1, source_target_pairs={{0,4},{4,8},{8,12},{12,16},{16,20},{20,24},{24,28},{28,32},{32,36}... | collective-permute-start | bytes 110600 | tf_op jit(solution)/shard_map/ppermute | solution.py:44
  98.4 8.7 %collective-permute-start.2 = (bf16[144,128]{1,0:T(8,128)(2,1)S(1)}, bf16[144,128]{1,0:T(8,128)(2,1)S(1)}, u32[]{:S(2)}, u32[]{:S(2)}) collective-permute-start(bf16[144,128]{1,0:T(8,128)(2,1)S(1)} %get-tuple-element.24), channel_id=1, source_target_pairs={{4,0},{8,4},{12,8},{16,12},{20,16},{24,20},{28,24},{32,28},{36,32}... | collective-permute-start | bytes 110600 | tf_op jit(solution)/shard_map/ppermute | solution.py:45
  102.1 5.0 %copy-start.2 = (bf16[1,256,256]{2,1,0:T(8,128)(2,1)S(1)}, bf16[1,256,256]{2,1,0:T(8,128)(2,1)}, u32[]{:S(2)}) copy-start(bf16[1,256,256]{2,1,0:T(8,128)(2,1)} %w_pool_ref.1) | copy-start | bytes 393220
  102.1 5.0 %copy-start.3 = (f32[256]{0:T(256)S(1)}, f32[256]{0:T(256)}, u32[]{:S(2)}) copy-start(f32[256]{0:T(256)} %param.18) | copy-start | bytes 3076
  107.1 3.1 %copy-start = (bf16[4,16,16,512]{3,2,1,0:T(8,128)(2,1)S(1)}, bf16[4,16,16,512]{3,2,1,0:T(8,128)(2,1)}, u32[]{:S(2)}) copy-start(bf16[4,16,16,512]{3,2,1,0:T(8,128)(2,1)} %all_to_all.20.refs_3_.refs_2_) | copy-start | bytes 3145732
  112.6 15.7 %collective-permute-start.4 = (bf16[2,256,512]{2,1,0:T(8,128)(2,1)S(1)}, bf16[2,256,512]{2,1,0:T(8,128)(2,1)S(1)}, u32[]{:S(2)}, u32[]{:S(2)}) collective-permute-start(bf16[2,256,512]{2,1,0:T(8,128)(2,1)S(1)} %get-tuple-element.29), channel_id=1, source_target_pairs={{0,3},{1,2},{2,1},{3,0},{4,7},{5,6},{6,5},{7,4},{8,11},{9,10},{10,... | collective-permute-start | bytes 1572872 | tf_op jit(solution)/shard_map/ppermute | solution.py:39
  117.5 15.1 %collective-permute-start.6 = (bf16[2,256,512]{2,1,0:T(8,128)(2,1)S(1)}, bf16[2,256,512]{2,1,0:T(8,128)(2,1)S(1)}, u32[]{:S(2)}, u32[]{:S(2)}) collective-permute-start(bf16[2,256,512]{2,1,0:T(8,128)(2,1)S(1)} %shard_map.110), channel_id=1, source_target_pairs={{0,1},{1,0},{2,3},{3,2},{4,5},{5,4},{6,7},{7,6},{8,9},{9,8},{10,11... | collective-permute-start | bytes 1572872 | tf_op jit(solution)/shard_map/ppermute | solution.py:39
  128.5 9.2 %collective-permute-start.5 = (bf16[256,512]{1,0:T(8,128)(2,1)S(1)}, bf16[256,512]{1,0:T(8,128)(2,1)S(1)}, u32[]{:S(2)}, u32[]{:S(2)}) collective-permute-start(bf16[256,512]{1,0:T(8,128)(2,1)S(1)} %fusion.3), channel_id=1, source_target_pairs={{0,1},{1,0},{2,3},{3,2},{4,5},{5,4},{6,7},{7,6},{8,9},{9,8},{10,11... | collective-permute-start | bytes 786440 | tf_op jit(solution)/shard_map/ppermute | solution.py:39
  132.8 9.5 %collective-permute-start.7 = (bf16[256,512]{1,0:T(8,128)(2,1)S(1)}, bf16[256,512]{1,0:T(8,128)(2,1)S(1)}, u32[]{:S(2)}, u32[]{:S(2)}) collective-permute-start(bf16[256,512]{1,0:T(8,128)(2,1)S(1)} %fusion.4), channel_id=1, source_target_pairs={{0,3},{1,2},{2,1},{3,0},{4,7},{5,6},{6,5},{7,4},{8,11},{9,10},{10,... | collective-permute-start | bytes 786440 | tf_op jit(solution)/shard_map/ppermute | solution.py:39
  137.8 14.3 %copy-start.5 = (f32[512]{0:T(512)S(1)}, f32[512]{0:T(512)}, u32[]{:S(2)}) copy-start(f32[512]{0:T(512)} %param.21) | copy-start | bytes 6148

commit v5 on v4

--- a/solution.py
+++ b/solution.py
@@ -35,8 +35,8 @@
     return jnp.sum(from_everyone(shard, axis), axis=0)
 
 
-def swapped(shard, axis, mask):
-    return lax.ppermute(shard, axis, [(i, i ^ mask) for i in range(lax.axis_size(axis))])
+def swapped(shard):
+    return lax.ppermute(shard, CORE, [(0, 1), (1, 0)])
 
 
 def neighbours(head, tail, axis):
@@ -214,25 +214,23 @@
     pooled_ref[...] = (pooled * scale_ref[...]).astype(BF16)
 
 
-def out_kernel(blocks, attended_refs, pooled_ref, own_ref, other_ref, out_refs, hidden_ref, w_ref):
-    y = lax.axis_index(TP)
-    whole_weights(own_ref, other_ref, w_ref, 0)
-    _, query_cols = attended_refs[0].shape
-    share = out_refs[0].shape[2]
-    for half, attended_ref in zip(sorted({half for half, _ in sum(blocks, ())}), attended_refs):
-        hidden_ref[:, :query_cols] = attended_ref[...]
-        if half == 0:
-            hidden_ref[:, query_cols:] = pooled_ref[WINDOW:-WINDOW]
-        else:
-            hidden_ref[:WINDOW, query_cols:] = pooled_ref[:WINDOW]
-            hidden_ref[WINDOW:, query_cols:] = pooled_ref[pooled_ref.shape[0] - WINDOW :]
-        for ref, slots in zip(out_refs, blocks):
-            for slot, (of_half, mask) in enumerate(slots):
-                if of_half == half:
-                    columns = w_ref[pl.ds(pl.multiple_of((y ^ mask) * share, share), share)]
-                    ref[slot] = lax.dot_general(
-                        hidden_ref[...], columns, nt, preferred_element_type=F32
-                    ).astype(BF16)
+def out_kernel(
+    ahead, first_ref, middle_ref, pooled_ref, own_ref, other_ref, out_ref, hidden_ref, w_ref
+):
+    edge = WINDOW
+    rows, query_cols = pooled_ref.shape[0], first_ref.shape[1]
+    to = lax.rem(lax.axis_index(TP) + ahead, lax.axis_size(TP))
+    zs = own_ref.shape[1] // lax.axis_size(TP)
+    at = own_ref.shape[3] - hidden_ref.shape[1]
+    mine = pl.ds(to * zs, zs)
+    whole_weights(own_ref.at[:, mine], other_ref.at[:, mine], w_ref, at)
+    hidden_ref[:edge, :query_cols] = first_ref[:edge]
+    hidden_ref[edge : rows - edge, :query_cols] = middle_ref[...]
+    hidden_ref[rows - edge :, :query_cols] = first_ref[edge:]
+    hidden_ref[:, query_cols:] = pooled_ref[...]
+    out_ref[...] = lax.dot_general(
+        hidden_ref[...], w_ref[...], nt, preferred_element_type=F32
+    ).astype(BF16)
 
 
 VMEM = pl.BlockSpec(memory_space=pltpu.VMEM)
@@ -266,15 +264,10 @@
         (w_key, w_value, w_pool_in, w_query, w_out_attn.T, w_out_pool.T), axis=1
     )
     over_z = lax.all_gather(packed, Z, axis=0)
-    for_x = [
-        jnp.broadcast_to(part[None], (lax.axis_size(X), *part.shape))
-        for part in (over_z[:, :, :in_cols], over_z[:, :, in_cols:])
-    ]
-    for_x = lax.optimization_barrier(for_x)
-    own1 = lax.all_to_all(for_x[0], X, 0, 0, tiled=True)
-    own2 = lax.all_to_all(for_x[1], X, 0, 0, tiled=True)
-    other1 = swapped(own1, CORE, 1)
-    other2 = swapped(own2, CORE, 1)
+    over_x = from_everyone(over_z, X)
+    own1, own2 = over_x[..., :in_cols], over_x[..., in_cols:]
+    other1 = swapped(own1)
+    other2 = swapped(own2)
 
     def rows_of(width, count=rows):
         return jax.ShapeDtypeStruct((count, width), BF16)
@@ -316,47 +309,29 @@
         name="outer",
     )(query, kv, chan, before, after, sink, w_pool, pool_scale.reshape(1, -1))
 
-    def multiplied(blocks, *attended):
-        count = len(attended)
-        outs = len(blocks)
-
-        def kernel(*refs):
-            out_kernel(
-                blocks,
-                refs[:count],
-                *refs[count : count + 3],
-                refs[count + 3 : count + 3 + outs],
-                *refs[count + 3 + outs :],
-            )
-
+    def multiplied(ahead):
         return pl.pallas_call(
-            kernel,
-            out_shape=[jax.ShapeDtypeStruct((2, rows // 2, share), BF16)] * outs,
-            in_specs=[VMEM] * (count + 3),
-            out_specs=[VMEM] * outs,
+            functools.partial(out_kernel, ahead),
+            out_shape=rows_of(share),
+            in_specs=[VMEM] * 5,
+            out_specs=VMEM,
             scratch_shapes=[
-                pltpu.VMEM((rows // 2, hidden_cols), BF16),
-                pltpu.VMEM((model_width, hidden_cols), BF16),
+                pltpu.VMEM((rows, hidden_cols), BF16),
+                pltpu.VMEM((share, hidden_cols), BF16),
             ],
             compiler_params=LIMIT,
-            cost_estimate=cost(outs * rows // 2 * model_width * hidden_cols, 4 << 20),
-        )(*attended, pooled, own2, other2)
-
-    (sent0,) = multiplied((((0, 1), (0, 2)),), attended0)
-    sent1, kept0, kept1 = multiplied(
-        (((1, 3), (1, 2)), ((0, 0), (0, 3)), ((1, 0), (1, 1))), attended0, attended1
-    )
-
-    def exchanged(sent, kept, near_mask, far_mask):
-        came = swapped(sent, TP, near_mask)
-        both = kept.astype(F32) + came.astype(F32)
-        passed = both[1].astype(BF16)
-        rest = swapped(passed, TP, far_mask)
-        return both[0] + rest.astype(F32)
-
-    middle = exchanged(sent0, kept0, 1, 3)
-    edges = exchanged(sent1, kept1, 3, 1)
-    mix = jnp.concatenate([edges[:WINDOW], middle, edges[WINDOW:]])
+            cost_estimate=cost(2 * rows * share * hidden_cols, 1 << 20),
+        )(attended1, attended0, pooled, own2, other2)
+
+    count = lax.axis_size(TP)
+    partials = []
+    for ahead in (2, 1, 3):
+        block = multiplied(ahead)
+        perm = [(i, (i + ahead) % count) for i in range(count)]
+        partials.append(lax.ppermute(block, TP, perm))
+    mix = multiplied(0).astype(F32)
+    for partial in partials[1:] + partials[:1]:
+        mix = mix + partial.astype(F32)
     stats = jnp.stack([jnp.sum(mix, axis=1), jnp.sum(mix * mix, axis=1)])
     stats = of_everyone(stats, TP)
     row_mean = stats[0] / model_width

time: 154 us -> 146 us (0.948)
  the two profiles are of different devices: /device:TPU:2 before, /device:TPU:6 now
where the time goes in v5:
time: 146 us; the launch traced here: 145 us
  blocking collectives  70.9 us (49%)
  waiting for transfers between devices  24.4 us (17%)
  starting transfers between devices  23.3 us (16%)
  Pallas kernels  18.5 us (13%)
  local copies, waits for them, and re-layouts  6.36 us (4%)
  other arithmetic  1.64 us (1%)
    all_gather x1, blocking collectives, layer(): over_z = lax.all_gather(packed, Z, axis=0)  38.9 us
    all_to_all x2, blocking collectives, from_everyone(): lax.all_to_all(jnp.broadcast_to(shard[None], (count, *shard.shape)), axis...  32 us
    ppermute x3, waiting for transfers between devices, layer(): partials.append(lax.ppermute(block, TP, perm))  15.2 us
    all_to_all x1, waiting for transfers between devices, from_everyone(): lax.all_to_all(jnp.broadcast_to(shard[None], (count, *shard.shape)), axis...  9.17 us
    ppermute x3, starting transfers between devices, layer(): partials.append(lax.ppermute(block, TP, perm))  8.98 us
    pallas_call x4, Pallas kernels, multiplied(): pl.pallas_call(functools.partial(out_kernel, ahead), out_shape=rows_of(sh...  6.95 us
    pallas_call x1, Pallas kernels, layer(): pl.pallas_call(functools.partial(inner_kernel, seq_len), out_shape=[rows_...  5.34 us
    all_to_all x1, starting transfers between devices, from_everyone(): lax.all_to_all(jnp.broadcast_to(shard[None], (count, *shard.shape)), axis...  4.46 us
  transfers between devices with their start and end apart: 8, of which 4 were waited for; matrix products, arithmetic and copies ran while one was open for 3% of the time, Pallas kernels for 12%

profile of v5, /device:TPU:6, one launch (start us, length us, event | category | flops | bytes accessed | tf_op | source)
XLA Modules:
  0.0 145.3 jit_solution(10603299214837739641)
XLA Ops:
  0.0 0.9 concatenate.3
  0.9 38.9 %all-gather = bf16[256,1152]{1,0:T(8,128)(2,1)S(1)} all-gather(bf16[16,1152]{1,0:T(8,128)(2,1)S(1)} %concatenate.3), channel_id=2, replica_groups=mesh['sp_0'=16,'sp_1'=4,'sp_2'=2,'tp'=4] {'sp_0'}, dimensions={0}, use_global_device_ids=true | all-gather | bytes 626688 | tf_op jit(solution)/shard_map/all_gather | solution.py:266
  39.7 0.2 broadcast_in_dim.7
  39.9 24.3 %all_to_all.15 = bf16[4,16,16,1152]{3,2,1,0:T(8,128)(2,1)} all-to-all(bf16[4,16,16,1152]{3,2,1,0:T(8,128)(2,1)S(1)} %broadcast_in_dim.7), channel_id=1, replica_groups=mesh['sp_0'=16,'sp_1'=4,'sp_2'=2,'tp'=4] {'sp_1'}, dimensions={0} | all-to-all | bytes 4718592 | tf_op jit(solution)/shard_map/all_to_all | solution.py:29
  64.2 1.5 %broadcast_in_dim.6 = bf16[4,512,512]{2,1,0:T(8,128)(2,1)} broadcast(bf16[512,512]{1,0:T(8,128)(2,1)S(1)} %copy-done.3), dimensions={1,2} | broadcast | bytes 2621440 | tf_op jit(solution)/shard_map/broadcast_in_dim | solution.py:30
  65.7 4.5 %all-to-all-start = ((bf16[4,512,512]{2,1,0:T(8,128)(2,1)}), bf16[4,512,512]{2,1,0:T(8,128)(2,1)S(1)}, u32[]{:S(2)}, u32[]{:S(2)}) async-start(bf16[4,512,512]{2,1,0:T(8,128)(2,1)} %broadcast_in_dim.6), calls=%async_computation | async-start | bytes 4194304 | tf_op jit(solution)/shard_map/all_to_all | solution.py:29
  70.2 2.5 %slice.16.own_ref = bf16[4,16,16,640]{3,2,1,0:T(8,128)(2,1)} slice(bf16[4,16,16,1152]{3,2,1,0:T(8,128)(2,1)} %all_to_all.15), slice={[0:4], [0:16], [0:16], [0:640]} | slice | bytes 2621440 | tf_op jit(solution)/shard_map/slice | solution.py:268
  72.7 1.9 %collective-permute-start = (bf16[4,16,16,640]{3,2,1,0:T(8,128)(2,1)}, bf16[4,16,16,640]{3,2,1,0:T(8,128)(2,1)}, u32[]{:S(2)}, u32[]{:S(2)}) collective-permute-start(bf16[4,16,16,640]{3,2,1,0:T(8,128)(2,1)} %slice.16.own_ref), channel_id=1, source_target_pairs={{0,4},{4,0},{1,5},{5,1},{2,6},{6,2},{3,7},{7,3},{8,12},{12,8},{9,1... | collective-permute-start | bytes 3932168 | tf_op jit(solution)/shard_map/ppermute | solution.py:39
  74.6 1.3 slice.17.own_ref
  75.9 0.0 copy-start
  75.9 2.4 %collective-permute-start.3 = (bf16[4,16,16,512]{3,2,1,0:T(8,128)(2,1)S(1)}, bf16[4,16,16,512]{3,2,1,0:T(8,128)(2,1)}, u32[]{:S(2)}, u32[]{:S(2)}) collective-permute-start(bf16[4,16,16,512]{3,2,1,0:T(8,128)(2,1)S(1)} %slice.17.own_ref), channel_id=1, source_target_pairs={{0,4},{4,0},{1,5},{5,1},{2,6},{6,2},{3,7},{7,3},{8,12},{12,8},{9,1... | collective-permute-start | bytes 3145736 | tf_op jit(solution)/shard_map/ppermute | solution.py:39
  78.3 9.2 %all-to-all-done.tokens_ref = bf16[4,512,512]{2,1,0:T(8,128)(2,1)S(1)} async-done(((bf16[4,512,512]{2,1,0:T(8,128)(2,1)}), bf16[4,512,512]{2,1,0:T(8,128)(2,1)S(1)}, u32[]{:S(2)}, u32[]{:S(2)}) %all-to-all-start) | async-done | bytes 2097184 | tf_op jit(solution)/shard_map/all_to_all | solution.py:29
  87.5 3.2 %project.1 = (bf16[512,128]{1,0:T(8,128)(2,1)S(1)}, bf16[512,256]{1,0:T(8,128)(2,1)S(1)}, bf16[144,128]{1,0:T(8,128)(2,1)S(1)}, bf16[144,128]{1,0:T(8,128)(2,1)S(1)}) custom-call(bf16[4,512,512]{2,1,0:T(8,128)(2,1)S(1)} %all-to-all-done.tokens_ref, bf16[4,16,16,640]{3,2,1,0:T(8,128)(2,1)} %slice.16.own_ref, ...), custom_call_target="tpu_custom_call" | custom-call | flops 805306368 | bytes 4194304 | tf_op jit(solution)/shard_map/project/pallas_call | solution.py:279
  90.7 1.9 %collective-permute-start.1 = (bf16[144,128]{1,0:T(8,128)(2,1)S(1)}, bf16[144,128]{1,0:T(8,128)(2,1)S(1)}, u32[]{:S(2)}, u32[]{:S(2)}) collective-permute-start(bf16[144,128]{1,0:T(8,128)(2,1)S(1)} %get-tuple-element.16), channel_id=1, source_target_pairs={{0,4},{4,8},{8,12},{12,16},{16,20},{20,24},{24,28},{28,32},{32,36}... | collective-permute-start | bytes 110600 | tf_op jit(solution)/shard_map/ppermute | solution.py:44
  92.6 3.6 %collective-permute-start.2 = (bf16[144,128]{1,0:T(8,128)(2,1)S(1)}, bf16[144,128]{1,0:T(8,128)(2,1)S(1)}, u32[]{:S(2)}, u32[]{:S(2)}) collective-permute-start(bf16[144,128]{1,0:T(8,128)(2,1)S(1)} %get-tuple-element.17), channel_id=1, source_target_pairs={{4,0},{8,4},{12,8},{16,12},{20,16},{24,20},{28,24},{32,28},{36,32}... | collective-permute-start | bytes 110600 | tf_op jit(solution)/shard_map/ppermute | solution.py:45
  96.3 0.0 copy-start.1
  96.3 0.0 copy-start.2
  96.3 5.3 %inner.1 = (bf16[512,256]{1,0:T(8,128)(2,1)S(1)}, bf16[256,256]{1,0:T(8,128)(2,1)S(1)}) custom-call(bf16[4,512,512]{2,1,0:T(8,128)(2,1)S(1)} %all-to-all-done.tokens_ref, bf16[4,16,16,640]{3,2,1,0:T(8,128)(2,1)} %slice.16.own_ref, bf16[4,16,16,640]{3,2,1,0:T(8,128)(2,1)} %collective-permute-done.other_ref, bf16[512,128]{1,0:T(8,128)(2,1)S(1)} %get-tuple-element.13.kv_ref, ...), custom_call_target="tpu_custom_call" | custom-call | flops 536870912 | bytes 4194304 | tf_op jit(solution)/shard_map/inner/pallas_call | solution.py:291
  101.7 3.1 %outer.1 = (bf16[256,256]{1,0:T(8,128)(2,1)S(1)}, bf16[512,256]{1,0:T(8,128)(2,1)S(1)}) custom-call(bf16[512,256]{1,0:T(8,128)(2,1)S(1)} %get-tuple-element.14.query_ref, bf16[512,128]{1,0:T(8,128)(2,1)S(1)} %get-tuple-element.13.kv_ref, bf16[512,256]{1,0:T(8,128)(2,1)S(1)} %get-tuple-element.15.chan_ref, ...), custom_call_target="tpu_custom_call" | custom-call | flops 536870912 | bytes 2097152 | tf_op jit(solution)/shard_map/outer/pallas_call | solution.py:301
  104.8 1.7 %shard_map.112 = bf16[512,512]{1,0:T(8,128)(2,1)S(1)} custom-call(bf16[256,256]{1,0:T(8,128)(2,1)S(1)} %get-tuple-element.18.first_ref, bf16[256,256]{1,0:T(8,128)(2,1)S(1)} %get-tuple-element.19.middle_ref, bf16[512,256]{1,0:T(8,128)(2,1)S(1)} %get-tuple-element.20.pooled_ref, bf16[4,16,16,512]{3,2,1,0:T(8,128)(2,1)S(1)} %slice.17.own_ref, ...), custom_call_target="tpu_custom_call" | custom-call | flops 268435456 | bytes 1048576 | tf_op jit(solution)/shard_map/pallas_call | solution.py:313
  106.5 2.5 %collective-permute-start.6 = (bf16[512,512]{1,0:T(8,128)(2,1)S(1)}, bf16[512,512]{1,0:T(8,128)(2,1)S(1)}, u32[]{:S(2)}, u32[]{:S(2)}) collective-permute-start(bf16[512,512]{1,0:T(8,128)(2,1)S(1)} %shard_map.112), channel_id=1, source_target_pairs={{0,2},{1,3},{2,0},{3,1},{4,6},{5,7},{6,4},{7,5},{8,10},{9,11},{10,... | collective-permute-start | bytes 1572872 | tf_op jit(solution)/shard_map/ppermute | solution.py:331
  109.0 1.7 %shard_map.111 = bf16[512,512]{1,0:T(8,128)(2,1)S(1)} custom-call(bf16[256,256]{1,0:T(8,128)(2,1)S(1)} %get-tuple-element.18.first_ref, bf16[256,256]{1,0:T(8,128)(2,1)S(1)} %get-tuple-element.19.middle_ref, bf16[512,256]{1,0:T(8,128)(2,1)S(1)} %get-tuple-element.20.pooled_ref, bf16[4,16,16,512]{3,2,1,0:T(8,128)(2,1)S(1)} %slice.17.own_ref, ...), custom_call_target="tpu_custom_call" | custom-call | flops 268435456 | bytes 1048576 | tf_op jit(solution)/shard_map/pallas_call | solution.py:313
  110.8 4.5 %collective-permute-start.5 = (bf16[512,512]{1,0:T(8,128)(2,1)S(1)}, bf16[512,512]{1,0:T(8,128)(2,1)S(1)}, u32[]{:S(2)}, u32[]{:S(2)}) collective-permute-start(bf16[512,512]{1,0:T(8,128)(2,1)S(1)} %shard_map.111), channel_id=1, source_target_pairs={{0,3},{1,0},{2,1},{3,2},{4,7},{5,4},{6,5},{7,6},{8,11},{9,8},{10,9... | collective-permute-start | bytes 1572872 | tf_op jit(solution)/shard_map/ppermute | solution.py:331
  115.3 1.7 %shard_map.110 = bf16[512,512]{1,0:T(8,128)(2,1)S(1)} custom-call(bf16[256,256]{1,0:T(8,128)(2,1)S(1)} %get-tuple-element.18.first_ref, bf16[256,256]{1,0:T(8,128)(2,1)S(1)} %get-tuple-element.19.middle_ref, bf16[512,256]{1,0:T(8,128)(2,1)S(1)} %get-tuple-element.20.pooled_ref, bf16[4,16,16,512]{3,2,1,0:T(8,128)(2,1)S(1)} %slice.17.own_ref, ...), custom_call_target="tpu_custom_call" | custom-call | flops 268435456 | bytes 1048576 | tf_op jit(solution)/shard_map/pallas_call | solution.py:313
  117.1 1.9 %collective-permute-start.4 = (bf16[512,512]{1,0:T(8,128)(2,1)S(1)}, bf16[512,512]{1,0:T(8,128)(2,1)S(1)}, u32[]{:S(2)}, u32[]{:S(2)}) collective-permute-start(bf16[512,512]{1,0:T(8,128)(2,1)S(1)} %shard_map.110), channel_id=1, source_target_pairs={{0,1},{1,2},{2,3},{3,0},{4,5},{5,6},{6,7},{7,4},{8,9},{9,10},{10,1... | collective-permute-start | bytes 1572872 | tf_op jit(solution)/shard_map/ppermute | solution.py:331
  119.0 1.7 %shard_map.109 = bf16[512,512]{1,0:T(8,128)(2,1)S(1)} custom-call(bf16[256,256]{1,0:T(8,128)(2,1)S(1)} %get-tuple-element.18.first_ref, bf16[256,256]{1,0:T(8,128)(2,1)S(1)} %get-tuple-element.19.middle_ref, bf16[512,256]{1,0:T(8,128)(2,1)S(1)} %get-tuple-element.20.pooled_ref, bf16[4,16,16,512]{3,2,1,0:T(8,128)(2,1)S(1)} %slice.17.own_ref, ...), custom_call_target="tpu_custom_call" | custom-call | flops 268435456 | bytes 1048576 | tf_op jit(solution)/shard_map/pallas_call | solution.py:313
  120.7 3.9 %collective-permute-done.6 = bf16[512,512]{1,0:T(8,128)(2,1)S(1)} collective-permute-done((bf16[512,512]{1,0:T(8,128)(2,1)S(1)}, bf16[512,512]{1,0:T(8,128)(2,1)S(1)}, u32[]{:S(2)}, u32[]{:S(2)}) %collective-permute-start.6) | collective-permute-done | bytes 524320 | tf_op jit(solution)/shard_map/ppermute | solution.py:331
  124.6 9.7 %collective-permute-done.5 = bf16[512,512]{1,0:T(8,128)(2,1)S(1)} collective-permute-done((bf16[512,512]{1,0:T(8,128)(2,1)S(1)}, bf16[512,512]{1,0:T(8,128)(2,1)S(1)}, u32[]{:S(2)}, u32[]{:S(2)}) %collective-permute-start.5) | collective-permute-done | bytes 524320 | tf_op jit(solution)/shard_map/ppermute | solution.py:331
  134.3 1.7 %collective-permute-done.4 = bf16[512,512]{1,0:T(8,128)(2,1)S(1)} collective-permute-done((bf16[512,512]{1,0:T(8,128)(2,1)S(1)}, bf16[512,512]{1,0:T(8,128)(2,1)S(1)}, u32[]{:S(2)}, u32[]{:S(2)}) %collective-permute-start.4) | collective-permute-done | bytes 524320 | tf_op jit(solution)/shard_map/ppermute | solution.py:331
  135.9 0.4 fusion
  136.4 7.7 %all_to_all.16 = f32[4,2,512]{2,1,0:T(2,128)S(1)} all-to-all(f32[4,2,512]{2,1,0:T(2,128)S(1)} %broadcast_in_dim.8), channel_id=1, replica_groups=mesh['sp_0'=16,'sp_1'=4,'sp_2'=2,'tp'=4] {'tp'}, dimensions={0} | all-to-all | bytes 32768 | tf_op jit(solution)/shard_map/all_to_all | solution.py:29
  144.2 1.2 multiply_convert_fusion
  (16 shorter events, 0.1 us)
Async XLA Ops:
  39.9 24.3 %copy-start.3 = (bf16[512,512]{1,0:T(8,128)(2,1)S(1)}, bf16[512,512]{1,0:T(8,128)(2,1)}, u32[]{:S(2)}) copy-start(bf16[512,512]{1,0:T(8,128)(2,1)} %param.11) | copy-start | bytes 1572868
  65.7 21.8 %all-to-all-start = ((bf16[4,512,512]{2,1,0:T(8,128)(2,1)}), bf16[4,512,512]{2,1,0:T(8,128)(2,1)S(1)}, u32[]{:S(2)}, u32[]{:S(2)}) async-start(bf16[4,512,512]{2,1,0:T(8,128)(2,1)} %broadcast_in_dim.6), calls=%async_computation | async-start | bytes 4194304 | tf_op jit(solution)/shard_map/all_to_all | solution.py:29
  72.7 14.8 %collective-permute-start = (bf16[4,16,16,640]{3,2,1,0:T(8,128)(2,1)}, bf16[4,16,16,640]{3,2,1,0:T(8,128)(2,1)}, u32[]{:S(2)}, u32[]{:S(2)}) collective-permute-start(bf16[4,16,16,640]{3,2,1,0:T(8,128)(2,1)} %slice.16.own_ref), channel_id=1, source_target_pairs={{0,4},{4,0},{1,5},{5,1},{2,6},{6,2},{3,7},{7,3},{8,12},{12,8},{9,1... | collective-permute-start | bytes 3932168 | tf_op jit(solution)/shard_map/ppermute | solution.py:39
  75.9 20.4 %copy-start = (f32[4]{0:T(128)S(1)}, f32[4]{0:T(128)}, u32[]{:S(2)}) copy-start(f32[4]{0:T(128)} %sink_ref.3) | copy-start | bytes 52
  75.9 28.8 %collective-permute-start.3 = (bf16[4,16,16,512]{3,2,1,0:T(8,128)(2,1)S(1)}, bf16[4,16,16,512]{3,2,1,0:T(8,128)(2,1)}, u32[]{:S(2)}, u32[]{:S(2)}) collective-permute-start(bf16[4,16,16,512]{3,2,1,0:T(8,128)(2,1)S(1)} %slice.17.own_ref), channel_id=1, source_target_pairs={{0,4},{4,0},{1,5},{5,1},{2,6},{6,2},{3,7},{7,3},{8,12},{12,8},{9,1... | collective-permute-start | bytes 3145736 | tf_op jit(solution)/shard_map/ppermute | solution.py:39
  90.7 11.0 %collective-permute-start.1 = (bf16[144,128]{1,0:T(8,128)(2,1)S(1)}, bf16[144,128]{1,0:T(8,128)(2,1)S(1)}, u32[]{:S(2)}, u32[]{:S(2)}) collective-permute-start(bf16[144,128]{1,0:T(8,128)(2,1)S(1)} %get-tuple-element.16), channel_id=1, source_target_pairs={{0,4},{4,8},{8,12},{12,16},{16,20},{20,24},{24,28},{28,32},{32,36}... | collective-permute-start | bytes 110600 | tf_op jit(solution)/shard_map/ppermute | solution.py:44
  92.6 9.0 %collective-permute-start.2 = (bf16[144,128]{1,0:T(8,128)(2,1)S(1)}, bf16[144,128]{1,0:T(8,128)(2,1)S(1)}, u32[]{:S(2)}, u32[]{:S(2)}) collective-permute-start(bf16[144,128]{1,0:T(8,128)(2,1)S(1)} %get-tuple-element.17), channel_id=1, source_target_pairs={{4,0},{8,4},{12,8},{16,12},{20,16},{24,20},{28,24},{32,28},{36,32}... | collective-permute-start | bytes 110600 | tf_op jit(solution)/shard_map/ppermute | solution.py:45
  96.3 5.4 %copy-start.1 = (bf16[1,256,256]{2,1,0:T(8,128)(2,1)S(1)}, bf16[1,256,256]{2,1,0:T(8,128)(2,1)}, u32[]{:S(2)}) copy-start(bf16[1,256,256]{2,1,0:T(8,128)(2,1)} %w_pool_ref.1) | copy-start | bytes 393220
  96.3 5.4 %copy-start.2 = (f32[256]{0:T(256)S(1)}, f32[256]{0:T(256)}, u32[]{:S(2)}) copy-start(f32[256]{0:T(256)} %param.18) | copy-start | bytes 3076
  106.5 18.1 %collective-permute-start.6 = (bf16[512,512]{1,0:T(8,128)(2,1)S(1)}, bf16[512,512]{1,0:T(8,128)(2,1)S(1)}, u32[]{:S(2)}, u32[]{:S(2)}) collective-permute-start(bf16[512,512]{1,0:T(8,128)(2,1)S(1)} %shard_map.112), channel_id=1, source_target_pairs={{0,2},{1,3},{2,0},{3,1},{4,6},{5,7},{6,4},{7,5},{8,10},{9,11},{10,... | collective-permute-start | bytes 1572872 | tf_op jit(solution)/shard_map/ppermute | solution.py:331
  110.8 23.5 %collective-permute-start.5 = (bf16[512,512]{1,0:T(8,128)(2,1)S(1)}, bf16[512,512]{1,0:T(8,128)(2,1)S(1)}, u32[]{:S(2)}, u32[]{:S(2)}) collective-permute-start(bf16[512,512]{1,0:T(8,128)(2,1)S(1)} %shard_map.111), channel_id=1, source_target_pairs={{0,3},{1,0},{2,1},{3,2},{4,7},{5,4},{6,5},{7,6},{8,11},{9,8},{10,9... | collective-permute-start | bytes 1572872 | tf_op jit(solution)/shard_map/ppermute | solution.py:331
  117.0 27.1 %copy-start.4 = (f32[512]{0:T(512)S(1)}, f32[512]{0:T(512)}, u32[]{:S(2)}) copy-start(f32[512]{0:T(512)} %param.21) | copy-start | bytes 6148
  117.1 18.9 %collective-permute-start.4 = (bf16[512,512]{1,0:T(8,128)(2,1)S(1)}, bf16[512,512]{1,0:T(8,128)(2,1)S(1)}, u32[]{:S(2)}, u32[]{:S(2)}) collective-permute-start(bf16[512,512]{1,0:T(8,128)(2,1)S(1)} %shard_map.110), channel_id=1, source_target_pairs={{0,1},{1,2},{2,3},{3,0},{4,5},{5,6},{6,7},{7,4},{8,9},{9,10},{10,1... | collective-permute-start | bytes 1572872 | tf_op jit(solution)/shard_map/ppermute | solution.py:331

commit v6 on v5

--- a/solution.py
+++ b/solution.py
@@ -21,6 +21,7 @@
 
 epsilon = 1e-05
 masked_score = -1e30
+BACK = (0, 2, 1, 3)
 nt = (((1,), (1,)), ((), ()))
 
 
@@ -35,6 +36,11 @@
     return jnp.sum(from_everyone(shard, axis), axis=0)
 
 
+def ahead_by(shard, axis, places):
+    count = lax.axis_size(axis)
+    return lax.ppermute(shard, axis, [(i, (i + places) % count) for i in range(count)])
+
+
 def swapped(shard):
     return lax.ppermute(shard, CORE, [(0, 1), (1, 0)])
 
@@ -47,17 +53,18 @@
 
 
 def whole_weights(own_ref, other_ref, w_ref, at):
-    core = lax.axis_index(CORE)
+    core, x = lax.axis_index(CORE), lax.axis_index(X)
     xs, zs, rows = own_ref.shape[:3]
     lanes = slice(at, at + w_ref.shape[1])
-    for z in range(zs):
-        for x in range(xs):
-            base = (z * xs + x) * 2 * rows
+    for slot, back in enumerate(BACK):
+        source = lax.rem(x + xs - back, xs)
+        for z in range(zs):
+            base = (z * xs + source) * 2 * rows
             w_ref[pl.ds(pl.multiple_of(base + core * rows, rows), rows), :] = own_ref[
-                x, z, :, lanes
+                slot, z, :, lanes
             ]
             w_ref[pl.ds(pl.multiple_of(base + (1 - core) * rows, rows), rows), :] = other_ref[
-                x, z, :, lanes
+                slot, z, :, lanes
             ]
 
 
@@ -264,8 +271,15 @@
         (w_key, w_value, w_pool_in, w_query, w_out_attn.T, w_out_pool.T), axis=1
     )
     over_z = lax.all_gather(packed, Z, axis=0)
-    over_x = from_everyone(over_z, X)
-    own1, own2 = over_x[..., :in_cols], over_x[..., in_cols:]
+
+    def gathered_over_x(part):
+        pieces = [part]
+        for back in BACK[1:]:
+            pieces.append(ahead_by(part, X, back))
+        return jnp.stack(pieces)
+
+    own1 = gathered_over_x(over_z[..., :in_cols])
+    own2 = gathered_over_x(over_z[..., in_cols:])
     other1 = swapped(own1)
     other2 = swapped(own2)
 
@@ -323,12 +337,10 @@
             cost_estimate=cost(2 * rows * share * hidden_cols, 1 << 20),
         )(attended1, attended0, pooled, own2, other2)
 
-    count = lax.axis_size(TP)
     partials = []
-    for ahead in (2, 1, 3):
+    for ahead in BACK[1:]:
         block = multiplied(ahead)
-        perm = [(i, (i + ahead) % count) for i in range(count)]
-        partials.append(lax.ppermute(block, TP, perm))
+        partials.append(ahead_by(block, TP, ahead))
     mix = multiplied(0).astype(F32)
     for partial in partials[1:] + partials[:1]:
         mix = mix + partial.astype(F32)

time: 146 us -> 147 us (level)
  the two profiles are of different devices: /device:TPU:6 before, /device:TPU:1 now
where the time goes in v6:
time: 147 us; the launch traced here: 146 us
  starting transfers between devices  51.7 us (35%)
  blocking collectives  39.9 us (27%)
  waiting for transfers between devices  26.1 us (18%)
  Pallas kernels  18.5 us (13%)
  other arithmetic  5.48 us (4%)
  local copies, waits for them, and re-layouts  3.8 us (3%)
    all_gather x1, blocking collectives, layer(): over_z = lax.all_gather(packed, Z, axis=0)  32.1 us
    ppermute x9, starting transfers between devices, ahead_by(): lax.ppermute(shard, axis, [(i, (i + places) % count) for i in range(count)])  28.6 us
    ppermute x9, waiting for transfers between devices, ahead_by(): lax.ppermute(shard, axis, [(i, (i + places) % count) for i in range(count)])  26.1 us
    ppermute x2, starting transfers between devices, swapped(): return lax.ppermute(shard, CORE, [(0, 1), (1, 0)])  14.6 us
    all_to_all x1, blocking collectives, from_everyone(): lax.all_to_all(jnp.broadcast_to(shard[None], (count, *shard.shape)), axis...  7.78 us
    pallas_call x4, Pallas kernels, multiplied(): pl.pallas_call(functools.partial(out_kernel, ahead), out_shape=rows_of(sh...  6.95 us
    pallas_call x1, Pallas kernels, layer(): pl.pallas_call(functools.partial(inner_kernel, seq_len), out_shape=[rows_...  5.36 us
    all_to_all x1, starting transfers between devices, from_everyone(): lax.all_to_all(jnp.broadcast_to(shard[None], (count, *shard.shape)), axis...  4.18 us
  transfers between devices with their start and end apart: 14, of which 5 were waited for; matrix products, arithmetic and copies ran while one was open for 3% of the time, Pallas kernels for 12%

profile of v6, /device:TPU:1, one launch (start us, length us, event | category | flops | bytes accessed | tf_op | source)
XLA Modules:
  0.0 145.9 jit_solution(1122200711965400667)
XLA Ops:
  0.0 0.9 concatenate.3
  0.9 32.1 %all-gather = bf16[256,1152]{1,0:T(8,128)(2,1)S(1)} all-gather(bf16[16,1152]{1,0:T(8,128)(2,1)S(1)} %concatenate.3), channel_id=2, replica_groups=mesh['sp_0'=16,'sp_1'=4,'sp_2'=2,'tp'=4] {'sp_0'}, dimensions={0}, use_global_device_ids=true | all-gather | bytes 626688 | tf_op jit(solution)/shard_map/all_gather | solution.py:273
  33.8 4.4 %collective-permute-start.2 = (bf16[16,16,640]{2,1,0:T(8,128)(2,1)}, bf16[16,16,640]{2,1,0:T(8,128)(2,1)S(1)}, u32[]{:S(2)}, u32[]{:S(2)}) collective-permute-start(bf16[16,16,640]{2,1,0:T(8,128)(2,1)} %get-tuple-element.26), channel_id=1, source_target_pairs={{0,24},{8,0},{16,8},{24,16},{1,25},{9,1},{17,9},{25,17},{2,26},{10... | collective-permute-start | bytes 983048 | tf_op jit(solution)/shard_map/ppermute | solution.py:41
  38.2 1.9 %collective-permute-start.1 = (bf16[16,16,640]{2,1,0:T(8,128)(2,1)}, bf16[16,16,640]{2,1,0:T(8,128)(2,1)}, u32[]{:S(2)}, u32[]{:S(2)}) collective-permute-start(bf16[16,16,640]{2,1,0:T(8,128)(2,1)} %get-tuple-element.26), channel_id=1, source_target_pairs={{0,8},{8,16},{16,24},{24,0},{1,9},{9,17},{17,25},{25,1},{2,10},{10... | collective-permute-start | bytes 983048 | tf_op jit(solution)/shard_map/ppermute | solution.py:41
  40.1 3.6 %collective-permute-start = (bf16[16,16,640]{2,1,0:T(8,128)(2,1)}, bf16[16,16,640]{2,1,0:T(8,128)(2,1)}, u32[]{:S(2)}, u32[]{:S(2)}) collective-permute-start(bf16[16,16,640]{2,1,0:T(8,128)(2,1)} %get-tuple-element.26), channel_id=1, source_target_pairs={{0,16},{8,24},{16,0},{24,8},{1,17},{9,25},{17,1},{25,9},{2,18},{10... | collective-permute-start | bytes 983048 | tf_op jit(solution)/shard_map/ppermute | solution.py:41
  43.8 1.5 %broadcast_in_dim.4 = bf16[4,512,512]{2,1,0:T(8,128)(2,1)} broadcast(bf16[512,512]{1,0:T(8,128)(2,1)S(1)} %copy-done.6), dimensions={1,2} | broadcast | bytes 2621440 | tf_op jit(solution)/shard_map/broadcast_in_dim | solution.py:31
  45.3 4.2 %all-to-all-start = ((bf16[4,512,512]{2,1,0:T(8,128)(2,1)}), bf16[4,512,512]{2,1,0:T(8,128)(2,1)S(1)}, u32[]{:S(2)}, u32[]{:S(2)}) async-start(bf16[4,512,512]{2,1,0:T(8,128)(2,1)} %broadcast_in_dim.4), calls=%async_computation | async-start | bytes 4194304 | tf_op jit(solution)/shard_map/all_to_all | solution.py:30
  49.5 1.6 %collective-permute-done.1 = bf16[16,16,640]{2,1,0:T(8,128)(2,1)} collective-permute-done((bf16[16,16,640]{2,1,0:T(8,128)(2,1)}, bf16[16,16,640]{2,1,0:T(8,128)(2,1)}, u32[]{:S(2)}, u32[]{:S(2)}) %collective-permute-start.1) | collective-permute-done | bytes 327712 | tf_op jit(solution)/shard_map/ppermute | solution.py:41
  51.1 2.3 %pad_maximum_fusion.own_ref = bf16[4,16,16,640]{3,2,1,0:T(8,128)(2,1)} fusion(bf16[1,16,16,640]{3,2,1,0:T(8,128)(2,1)S(1)} %bitcast.21, bf16[1,16,16,640]{3,2,1,0:T(8,128)(2,1)} %bitcast.5, bf16[1,16,16,640]{3,2,1,0:T(8,128)(2,1)} %bitcast.4, bf16[1,16,16,640]{3,2,1,0:T(8,128)(2,1)S(1)} %get-tuple-element.25), kind=kLoop, calls=%fused_computation | loop fusion | flops 1966080 | bytes 2621440 | tf_op jit(solution)/shard_map/stack | solution.py:279
  53.4 11.6 %collective-permute-start.3 = (bf16[4,16,16,640]{3,2,1,0:T(8,128)(2,1)}, bf16[4,16,16,640]{3,2,1,0:T(8,128)(2,1)}, u32[]{:S(2)}, u32[]{:S(2)}) collective-permute-start(bf16[4,16,16,640]{3,2,1,0:T(8,128)(2,1)} %pad_maximum_fusion.own_ref), channel_id=1, source_target_pairs={{0,4},{4,0},{1,5},{5,1},{2,6},{6,2},{3,7},{7,3},{8,12},{12,8},{9,1... | collective-permute-start | bytes 3932168 | tf_op jit(solution)/shard_map/ppermute | solution.py:45
  65.0 3.6 %collective-permute-start.8 = (bf16[16,16,512]{2,1,0:T(8,128)(2,1)S(1)}, bf16[16,16,512]{2,1,0:T(8,128)(2,1)S(1)}, u32[]{:S(2)}, u32[]{:S(2)}) collective-permute-start(bf16[16,16,512]{2,1,0:T(8,128)(2,1)S(1)} %get-tuple-element.24), channel_id=1, source_target_pairs={{0,24},{8,0},{16,8},{24,16},{1,25},{9,1},{17,9},{25,17},{2,26},{10... | collective-permute-start | bytes 786440 | tf_op jit(solution)/shard_map/ppermute | solution.py:41
  68.6 1.9 %collective-permute-start.7 = (bf16[16,16,512]{2,1,0:T(8,128)(2,1)S(1)}, bf16[16,16,512]{2,1,0:T(8,128)(2,1)S(1)}, u32[]{:S(2)}, u32[]{:S(2)}) collective-permute-start(bf16[16,16,512]{2,1,0:T(8,128)(2,1)S(1)} %get-tuple-element.24), channel_id=1, source_target_pairs={{0,8},{8,16},{16,24},{24,0},{1,9},{9,17},{17,25},{25,1},{2,10},{10... | collective-permute-start | bytes 786440 | tf_op jit(solution)/shard_map/ppermute | solution.py:41
  70.5 3.1 %collective-permute-start.6 = (bf16[16,16,512]{2,1,0:T(8,128)(2,1)S(1)}, bf16[16,16,512]{2,1,0:T(8,128)(2,1)S(1)}, u32[]{:S(2)}, u32[]{:S(2)}) collective-permute-start(bf16[16,16,512]{2,1,0:T(8,128)(2,1)S(1)} %get-tuple-element.24), channel_id=1, source_target_pairs={{0,16},{8,24},{16,0},{24,8},{1,17},{9,25},{17,1},{25,9},{2,18},{10... | collective-permute-start | bytes 786440 | tf_op jit(solution)/shard_map/ppermute | solution.py:41
  73.6 1.1 collective-permute-done.8
  74.8 10.1 %collective-permute-done.7 = bf16[16,16,512]{2,1,0:T(8,128)(2,1)S(1)} collective-permute-done((bf16[16,16,512]{2,1,0:T(8,128)(2,1)S(1)}, bf16[16,16,512]{2,1,0:T(8,128)(2,1)S(1)}, u32[]{:S(2)}, u32[]{:S(2)}) %collective-permute-start.7) | collective-permute-done | bytes 262176 | tf_op jit(solution)/shard_map/ppermute | solution.py:41
  85.0 3.1 %collective-permute-start.9 = (bf16[4,16,16,512]{3,2,1,0:T(8,128)(2,1)S(1)}, bf16[4,16,16,512]{3,2,1,0:T(8,128)(2,1)}, u32[]{:S(2)}, u32[]{:S(2)}) collective-permute-start(bf16[4,16,16,512]{3,2,1,0:T(8,128)(2,1)S(1)} %pad_maximum_fusion.1.own_ref), channel_id=1, source_target_pairs={{0,4},{4,0},{1,5},{5,1},{2,6},{6,2},{3,7},{7,3},{8,12},{12,8},{9,1... | collective-permute-start | bytes 3145736 | tf_op jit(solution)/shard_map/ppermute | solution.py:45
  88.1 3.2 %project.1 = (bf16[512,128]{1,0:T(8,128)(2,1)S(1)}, bf16[512,256]{1,0:T(8,128)(2,1)S(1)}, bf16[144,128]{1,0:T(8,128)(2,1)S(1)}, bf16[144,128]{1,0:T(8,128)(2,1)S(1)}) custom-call(bf16[4,512,512]{2,1,0:T(8,128)(2,1)S(1)} %all-to-all-done.tokens_ref, bf16[4,16,16,640]{3,2,1,0:T(8,128)(2,1)} %pad_maximum_fusion.own_ref, ...), custom_call_target="tpu_custom_call" | custom-call | flops 805306368 | bytes 4194304 | tf_op jit(solution)/shard_map/project/pallas_call | solution.py:293
  91.3 1.9 %collective-permute-start.4 = (bf16[144,128]{1,0:T(8,128)(2,1)S(1)}, bf16[144,128]{1,0:T(8,128)(2,1)S(1)}, u32[]{:S(2)}, u32[]{:S(2)}) collective-permute-start(bf16[144,128]{1,0:T(8,128)(2,1)S(1)} %get-tuple-element.16), channel_id=1, source_target_pairs={{0,4},{4,8},{8,12},{12,16},{16,20},{20,24},{24,28},{28,32},{32,36}... | collective-permute-start | bytes 110600 | tf_op jit(solution)/shard_map/ppermute | solution.py:50
  93.2 2.4 %collective-permute-start.5 = (bf16[144,128]{1,0:T(8,128)(2,1)S(1)}, bf16[144,128]{1,0:T(8,128)(2,1)S(1)}, u32[]{:S(2)}, u32[]{:S(2)}) collective-permute-start(bf16[144,128]{1,0:T(8,128)(2,1)S(1)} %get-tuple-element.17), channel_id=1, source_target_pairs={{4,0},{8,4},{12,8},{16,12},{20,16},{24,20},{28,24},{32,28},{36,32}... | collective-permute-start | bytes 110600 | tf_op jit(solution)/shard_map/ppermute | solution.py:51
  95.7 5.4 %inner.1 = (bf16[512,256]{1,0:T(8,128)(2,1)S(1)}, bf16[256,256]{1,0:T(8,128)(2,1)S(1)}) custom-call(bf16[4,512,512]{2,1,0:T(8,128)(2,1)S(1)} %all-to-all-done.tokens_ref, bf16[4,16,16,640]{3,2,1,0:T(8,128)(2,1)} %pad_maximum_fusion.own_ref, bf16[4,16,16,640]{3,2,1,0:T(8,128)(2,1)} %collective-permute-done.3.other_ref, ...), custom_call_target="tpu_custom_call" | custom-call | flops 536870912 | bytes 4194304 | tf_op jit(solution)/shard_map/inner/pallas_call | solution.py:305
  101.1 3.1 %outer.1 = (bf16[256,256]{1,0:T(8,128)(2,1)S(1)}, bf16[512,256]{1,0:T(8,128)(2,1)S(1)}) custom-call(bf16[512,256]{1,0:T(8,128)(2,1)S(1)} %get-tuple-element.14.query_ref, bf16[512,128]{1,0:T(8,128)(2,1)S(1)} %get-tuple-element.13.kv_ref, bf16[512,256]{1,0:T(8,128)(2,1)S(1)} %get-tuple-element.15.chan_ref, ...), custom_call_target="tpu_custom_call" | custom-call | flops 536870912 | bytes 2097152 | tf_op jit(solution)/shard_map/outer/pallas_call | solution.py:315
  104.1 1.7 %shard_map.112 = bf16[512,512]{1,0:T(8,128)(2,1)S(1)} custom-call(bf16[256,256]{1,0:T(8,128)(2,1)S(1)} %get-tuple-element.18.first_ref, bf16[256,256]{1,0:T(8,128)(2,1)S(1)} %get-tuple-element.19.middle_ref, bf16[512,256]{1,0:T(8,128)(2,1)S(1)} %get-tuple-element.20.pooled_ref, bf16[4,16,16,512]{3,2,1,0:T(8,128)(2,1)S(1)} %pad_maximum_fusion.1.own_ref, ...), custom_call_target="tpu_custom_call" | custom-call | flops 268435456 | bytes 1048576 | tf_op jit(solution)/shard_map/pallas_call | solution.py:327
  105.9 4.8 %collective-permute-start.12 = (bf16[512,512]{1,0:T(8,128)(2,1)S(1)}, bf16[512,512]{1,0:T(8,128)(2,1)S(1)}, u32[]{:S(2)}, u32[]{:S(2)}) collective-permute-start(bf16[512,512]{1,0:T(8,128)(2,1)S(1)} %shard_map.112), channel_id=1, source_target_pairs={{0,2},{1,3},{2,0},{3,1},{4,6},{5,7},{6,4},{7,5},{8,10},{9,11},{10,... | collective-permute-start | bytes 1572872 | tf_op jit(solution)/shard_map/ppermute | solution.py:41
  110.7 1.7 %shard_map.111 = bf16[512,512]{1,0:T(8,128)(2,1)S(1)} custom-call(bf16[256,256]{1,0:T(8,128)(2,1)S(1)} %get-tuple-element.18.first_ref, bf16[256,256]{1,0:T(8,128)(2,1)S(1)} %get-tuple-element.19.middle_ref, bf16[512,256]{1,0:T(8,128)(2,1)S(1)} %get-tuple-element.20.pooled_ref, bf16[4,16,16,512]{3,2,1,0:T(8,128)(2,1)S(1)} %pad_maximum_fusion.1.own_ref, ...), custom_call_target="tpu_custom_call" | custom-call | flops 268435456 | bytes 1048576 | tf_op jit(solution)/shard_map/pallas_call | solution.py:327
  112.5 2.7 %collective-permute-start.11 = (bf16[512,512]{1,0:T(8,128)(2,1)S(1)}, bf16[512,512]{1,0:T(8,128)(2,1)S(1)}, u32[]{:S(2)}, u32[]{:S(2)}) collective-permute-start(bf16[512,512]{1,0:T(8,128)(2,1)S(1)} %shard_map.111), channel_id=1, source_target_pairs={{0,3},{1,0},{2,1},{3,2},{4,7},{5,4},{6,5},{7,6},{8,11},{9,8},{10,9... | collective-permute-start | bytes 1572872 | tf_op jit(solution)/shard_map/ppermute | solution.py:41
  115.2 1.7 %shard_map.110 = bf16[512,512]{1,0:T(8,128)(2,1)S(1)} custom-call(bf16[256,256]{1,0:T(8,128)(2,1)S(1)} %get-tuple-element.18.first_ref, bf16[256,256]{1,0:T(8,128)(2,1)S(1)} %get-tuple-element.19.middle_ref, bf16[512,256]{1,0:T(8,128)(2,1)S(1)} %get-tuple-element.20.pooled_ref, bf16[4,16,16,512]{3,2,1,0:T(8,128)(2,1)S(1)} %pad_maximum_fusion.1.own_ref, ...), custom_call_target="tpu_custom_call" | custom-call | flops 268435456 | bytes 1048576 | tf_op jit(solution)/shard_map/pallas_call | solution.py:327
  116.9 2.6 %collective-permute-start.10 = (bf16[512,512]{1,0:T(8,128)(2,1)S(1)}, bf16[512,512]{1,0:T(8,128)(2,1)S(1)}, u32[]{:S(2)}, u32[]{:S(2)}) collective-permute-start(bf16[512,512]{1,0:T(8,128)(2,1)S(1)} %shard_map.110), channel_id=1, source_target_pairs={{0,1},{1,2},{2,3},{3,0},{4,5},{5,6},{6,7},{7,4},{8,9},{9,10},{10,1... | collective-permute-start | bytes 1572872 | tf_op jit(solution)/shard_map/ppermute | solution.py:41
  119.5 1.7 %shard_map.109 = bf16[512,512]{1,0:T(8,128)(2,1)S(1)} custom-call(bf16[256,256]{1,0:T(8,128)(2,1)S(1)} %get-tuple-element.18.first_ref, bf16[256,256]{1,0:T(8,128)(2,1)S(1)} %get-tuple-element.19.middle_ref, bf16[512,256]{1,0:T(8,128)(2,1)S(1)} %get-tuple-element.20.pooled_ref, bf16[4,16,16,512]{3,2,1,0:T(8,128)(2,1)S(1)} %pad_maximum_fusion.1.own_ref, ...), custom_call_target="tpu_custom_call" | custom-call | flops 268435456 | bytes 1048576 | tf_op jit(solution)/shard_map/pallas_call | solution.py:327
  121.3 1.7 %collective-permute-done.12 = bf16[512,512]{1,0:T(8,128)(2,1)S(1)} collective-permute-done((bf16[512,512]{1,0:T(8,128)(2,1)S(1)}, bf16[512,512]{1,0:T(8,128)(2,1)S(1)}, u32[]{:S(2)}, u32[]{:S(2)}) %collective-permute-start.12) | collective-permute-done | bytes 524320 | tf_op jit(solution)/shard_map/ppermute | solution.py:41
  122.9 11.6 %collective-permute-done.11 = bf16[512,512]{1,0:T(8,128)(2,1)S(1)} collective-permute-done((bf16[512,512]{1,0:T(8,128)(2,1)S(1)}, bf16[512,512]{1,0:T(8,128)(2,1)S(1)}, u32[]{:S(2)}, u32[]{:S(2)}) %collective-permute-start.11) | collective-permute-done | bytes 524320 | tf_op jit(solution)/shard_map/ppermute | solution.py:41
  135.5 7.8 %all_to_all.10 = f32[4,2,512]{2,1,0:T(2,128)S(1)} all-to-all(f32[4,2,512]{2,1,0:T(2,128)S(1)} %broadcast_in_dim.5), channel_id=1, replica_groups=mesh['sp_0'=16,'sp_1'=4,'sp_2'=2,'tp'=4] {'tp'}, dimensions={0} | all-to-all | bytes 32768 | tf_op jit(solution)/shard_map/all_to_all | solution.py:30
  143.4 2.5 %multiply_convert_fusion = bf16[512,512]{1,0:T(8,128)(2,1)} fusion(f32[512]{0:T(512)S(1)} %copy-done.7, f32[512]{0:T(512)S(1)} %add_rsqrt_fusion, f32[512]{0:T(512)S(1)} %bitcast.26, bf16[512,512]{1,0:T(8,128)(2,1)} %copy-done.3, bf16[512,512]{1,0:T(8,128)(2,1)} %copy-done.4, bf16[512,512]{1,0:T(8,128)(2,1)} %copy-done.5, bf16[512,512]{1,0:T(8,128)(2,1)S(1)} %shard_map.109), kind=kLoop, calls=%fused_computation.2 | loop fusion | flops 2883584 | bytes 2627584 | tf_op jit(solution)/shard_map/convert_element_type | solution.py:352
  (34 shorter events, 2.0 us)
Async XLA Ops:
  0.0 43.8 %copy-start.6 = (bf16[512,512]{1,0:T(8,128)(2,1)S(1)}, bf16[512,512]{1,0:T(8,128)(2,1)}, u32[]{:S(2)}) copy-start(bf16[512,512]{1,0:T(8,128)(2,1)} %param.11) | copy-start | bytes 1572868
  33.8 15.6 %collective-permute-start.2 = (bf16[16,16,640]{2,1,0:T(8,128)(2,1)}, bf16[16,16,640]{2,1,0:T(8,128)(2,1)S(1)}, u32[]{:S(2)}, u32[]{:S(2)}) collective-permute-start(bf16[16,16,640]{2,1,0:T(8,128)(2,1)} %get-tuple-element.26), channel_id=1, source_target_pairs={{0,24},{8,0},{16,8},{24,16},{1,25},{9,1},{17,9},{25,17},{2,26},{10... | collective-permute-start | bytes 983048 | tf_op jit(solution)/shard_map/ppermute | solution.py:41
  38.2 12.9 %collective-permute-start.1 = (bf16[16,16,640]{2,1,0:T(8,128)(2,1)}, bf16[16,16,640]{2,1,0:T(8,128)(2,1)}, u32[]{:S(2)}, u32[]{:S(2)}) collective-permute-start(bf16[16,16,640]{2,1,0:T(8,128)(2,1)} %get-tuple-element.26), channel_id=1, source_target_pairs={{0,8},{8,16},{16,24},{24,0},{1,9},{9,17},{17,25},{25,1},{2,10},{10... | collective-permute-start | bytes 983048 | tf_op jit(solution)/shard_map/ppermute | solution.py:41
  40.1 10.9 %collective-permute-start = (bf16[16,16,640]{2,1,0:T(8,128)(2,1)}, bf16[16,16,640]{2,1,0:T(8,128)(2,1)}, u32[]{:S(2)}, u32[]{:S(2)}) collective-permute-start(bf16[16,16,640]{2,1,0:T(8,128)(2,1)} %get-tuple-element.26), channel_id=1, source_target_pairs={{0,16},{8,24},{16,0},{24,8},{1,17},{9,25},{17,1},{25,9},{2,18},{10... | collective-permute-start | bytes 983048 | tf_op jit(solution)/shard_map/ppermute | solution.py:41
  45.3 42.8 %all-to-all-start = ((bf16[4,512,512]{2,1,0:T(8,128)(2,1)}), bf16[4,512,512]{2,1,0:T(8,128)(2,1)S(1)}, u32[]{:S(2)}, u32[]{:S(2)}) async-start(bf16[4,512,512]{2,1,0:T(8,128)(2,1)} %broadcast_in_dim.4), calls=%async_computation | async-start | bytes 4194304 | tf_op jit(solution)/shard_map/all_to_all | solution.py:30
  53.4 34.7 %collective-permute-start.3 = (bf16[4,16,16,640]{3,2,1,0:T(8,128)(2,1)}, bf16[4,16,16,640]{3,2,1,0:T(8,128)(2,1)}, u32[]{:S(2)}, u32[]{:S(2)}) collective-permute-start(bf16[4,16,16,640]{3,2,1,0:T(8,128)(2,1)} %pad_maximum_fusion.own_ref), channel_id=1, source_target_pairs={{0,4},{4,0},{1,5},{5,1},{2,6},{6,2},{3,7},{7,3},{8,12},{12,8},{9,1... | collective-permute-start | bytes 3932168 | tf_op jit(solution)/shard_map/ppermute | solution.py:45
  65.0 9.7 %collective-permute-start.8 = (bf16[16,16,512]{2,1,0:T(8,128)(2,1)S(1)}, bf16[16,16,512]{2,1,0:T(8,128)(2,1)S(1)}, u32[]{:S(2)}, u32[]{:S(2)}) collective-permute-start(bf16[16,16,512]{2,1,0:T(8,128)(2,1)S(1)} %get-tuple-element.24), channel_id=1, source_target_pairs={{0,24},{8,0},{16,8},{24,16},{1,25},{9,1},{17,9},{25,17},{2,26},{10... | collective-permute-start | bytes 786440 | tf_op jit(solution)/shard_map/ppermute | solution.py:41
  68.6 16.3 %collective-permute-start.7 = (bf16[16,16,512]{2,1,0:T(8,128)(2,1)S(1)}, bf16[16,16,512]{2,1,0:T(8,128)(2,1)S(1)}, u32[]{:S(2)}, u32[]{:S(2)}) collective-permute-start(bf16[16,16,512]{2,1,0:T(8,128)(2,1)S(1)} %get-tuple-element.24), channel_id=1, source_target_pairs={{0,8},{8,16},{16,24},{24,0},{1,9},{9,17},{17,25},{25,1},{2,10},{10... | collective-permute-start | bytes 786440 | tf_op jit(solution)/shard_map/ppermute | solution.py:41
  70.5 14.4 %collective-permute-start.6 = (bf16[16,16,512]{2,1,0:T(8,128)(2,1)S(1)}, bf16[16,16,512]{2,1,0:T(8,128)(2,1)S(1)}, u32[]{:S(2)}, u32[]{:S(2)}) collective-permute-start(bf16[16,16,512]{2,1,0:T(8,128)(2,1)S(1)} %get-tuple-element.24), channel_id=1, source_target_pairs={{0,16},{8,24},{16,0},{24,8},{1,17},{9,25},{17,1},{25,9},{2,18},{10... | collective-permute-start | bytes 786440 | tf_op jit(solution)/shard_map/ppermute | solution.py:41
  85.0 10.6 %copy-start = (f32[4]{0:T(128)S(1)}, f32[4]{0:T(128)}, u32[]{:S(2)}) copy-start(f32[4]{0:T(128)} %sink_ref.3) | copy-start | bytes 52
  85.0 19.1 %collective-permute-start.9 = (bf16[4,16,16,512]{3,2,1,0:T(8,128)(2,1)S(1)}, bf16[4,16,16,512]{3,2,1,0:T(8,128)(2,1)}, u32[]{:S(2)}, u32[]{:S(2)}) collective-permute-start(bf16[4,16,16,512]{3,2,1,0:T(8,128)(2,1)S(1)} %pad_maximum_fusion.1.own_ref), channel_id=1, source_target_pairs={{0,4},{4,0},{1,5},{5,1},{2,6},{6,2},{3,7},{7,3},{8,12},{12,8},{9,1... | collective-permute-start | bytes 3145736 | tf_op jit(solution)/shard_map/ppermute | solution.py:45
  91.3 9.7 %collective-permute-start.4 = (bf16[144,128]{1,0:T(8,128)(2,1)S(1)}, bf16[144,128]{1,0:T(8,128)(2,1)S(1)}, u32[]{:S(2)}, u32[]{:S(2)}) collective-permute-start(bf16[144,128]{1,0:T(8,128)(2,1)S(1)} %get-tuple-element.16), channel_id=1, source_target_pairs={{0,4},{4,8},{8,12},{12,16},{16,20},{20,24},{24,28},{28,32},{32,36}... | collective-permute-start | bytes 110600 | tf_op jit(solution)/shard_map/ppermute | solution.py:50
  93.2 7.8 %collective-permute-start.5 = (bf16[144,128]{1,0:T(8,128)(2,1)S(1)}, bf16[144,128]{1,0:T(8,128)(2,1)S(1)}, u32[]{:S(2)}, u32[]{:S(2)}) collective-permute-start(bf16[144,128]{1,0:T(8,128)(2,1)S(1)} %get-tuple-element.17), channel_id=1, source_target_pairs={{4,0},{8,4},{12,8},{16,12},{20,16},{24,20},{28,24},{32,28},{36,32}... | collective-permute-start | bytes 110600 | tf_op jit(solution)/shard_map/ppermute | solution.py:51
  95.6 5.4 %copy-start.1 = (bf16[1,256,256]{2,1,0:T(8,128)(2,1)S(1)}, bf16[1,256,256]{2,1,0:T(8,128)(2,1)}, u32[]{:S(2)}) copy-start(bf16[1,256,256]{2,1,0:T(8,128)(2,1)} %w_pool_ref.1) | copy-start | bytes 393220
  95.6 5.4 %copy-start.2 = (f32[256]{0:T(256)S(1)}, f32[256]{0:T(256)}, u32[]{:S(2)}) copy-start(f32[256]{0:T(256)} %param.18) | copy-start | bytes 3076
  105.9 17.0 %collective-permute-start.12 = (bf16[512,512]{1,0:T(8,128)(2,1)S(1)}, bf16[512,512]{1,0:T(8,128)(2,1)S(1)}, u32[]{:S(2)}, u32[]{:S(2)}) collective-permute-start(bf16[512,512]{1,0:T(8,128)(2,1)S(1)} %shard_map.112), channel_id=1, source_target_pairs={{0,2},{1,3},{2,0},{3,1},{4,6},{5,7},{6,4},{7,5},{8,10},{9,11},{10,... | collective-permute-start | bytes 1572872 | tf_op jit(solution)/shard_map/ppermute | solution.py:41
  112.5 22.1 %collective-permute-start.11 = (bf16[512,512]{1,0:T(8,128)(2,1)S(1)}, bf16[512,512]{1,0:T(8,128)(2,1)S(1)}, u32[]{:S(2)}, u32[]{:S(2)}) collective-permute-start(bf16[512,512]{1,0:T(8,128)(2,1)S(1)} %shard_map.111), channel_id=1, source_target_pairs={{0,3},{1,0},{2,1},{3,2},{4,7},{5,4},{6,5},{7,6},{8,11},{9,8},{10,9... | collective-permute-start | bytes 1572872 | tf_op jit(solution)/shard_map/ppermute | solution.py:41
  116.9 17.6 %collective-permute-start.10 = (bf16[512,512]{1,0:T(8,128)(2,1)S(1)}, bf16[512,512]{1,0:T(8,128)(2,1)S(1)}, u32[]{:S(2)}, u32[]{:S(2)}) collective-permute-start(bf16[512,512]{1,0:T(8,128)(2,1)S(1)} %shard_map.110), channel_id=1, source_target_pairs={{0,1},{1,2},{2,3},{3,0},{4,5},{5,6},{6,7},{7,4},{8,9},{9,10},{10,1... | collective-permute-start | bytes 1572872 | tf_op jit(solution)/shard_map/ppermute | solution.py:41
  121.3 22.1 %copy-start.7 = (f32[512]{0:T(512)S(1)}, f32[512]{0:T(512)}, u32[]{:S(2)}) copy-start(f32[512]{0:T(512)} %param.21) | copy-start | bytes 6148
  122.9 11.6 %copy-start.3 = (bf16[512,512]{1,0:T(8,128)(2,1)}, bf16[512,512]{1,0:T(8,128)(2,1)S(1)}, u32[]{:S(2)}) copy-start(bf16[512,512]{1,0:T(8,128)(2,1)S(1)} %collective-permute-done.12) | copy-start | bytes 1572868
  134.5 0.8 copy-start.4
  134.5 1.0 copy-start.5

commit v7 on v5

--- a/solution.py
+++ b/solution.py
@@ -121,15 +121,38 @@
         attended_ref[to : to + WINDOW, lanes] = attended.astype(BF16)
 
 
+def pooled_rows(chan, centre, first_pos, seq_len, w_pool_ref, scale_ref):
+    y = lax.axis_index(TP)
+    length = chan.shape[0]
+    sums = chan + pltpu.roll(chan, 1, 0)
+    window_sum = sums
+    for level in range(1, POOL_GROUPS):
+        step = 2 ** (level - 1)
+        sums = pltpu.roll(sums, step, 0) + pltpu.roll(sums, length - step, 0)
+        window_sum = jnp.where(y >= level, sums, window_sum)
+    half_width = jnp.left_shift(jnp.int32(1), y)
+    rows = 2 * WINDOW
+    row = lax.broadcasted_iota(jnp.int32, (rows, 1), 0)
+    pos = row + jnp.where(row < WINDOW, first_pos[0], first_pos[1])
+    count = jnp.minimum(pos + half_width, seq_len) - jnp.maximum(pos - half_width, 0)
+    spread = centre(window_sum) / count.astype(F32) - centre(chan)
+    pooled = jnp.dot(spread.astype(BF16), w_pool_ref[0], preferred_element_type=F32)
+    return (pooled * scale_ref[...]).astype(BF16)
+
+
 def inner_kernel(
     seq_len,
     tokens_ref,
     own_ref,
     other_ref,
     kv_ref,
+    chan_ref,
     sink_ref,
+    w_pool_ref,
+    scale_ref,
     query_ref,
     attended_ref,
+    pooled_ref,
     w_ref,
     band_ref,
 ):
@@ -149,6 +172,12 @@
             attended_ref,
             (b - 1) * WINDOW,
         )
+    near = 2 * RIM
+    chan = chan_ref[WINDOW - near : rows - WINDOW + near].astype(F32)
+    offset = lax.axis_index(SP) * rows + WINDOW
+    pooled_ref[...] = pooled_rows(
+        chan, lambda a: a[near:-near], (offset, offset), seq_len, w_pool_ref, scale_ref
+    )
 
 
 def outer_kernel(
@@ -166,7 +195,6 @@
     band_ref,
 ):
     rows = chan_ref.shape[0]
-    y = lax.axis_index(TP)
     offset = lax.axis_index(SP) * rows
 
     split_band(
@@ -197,37 +225,32 @@
         packed = ref[WINDOW:].astype(F32)
         return jnp.concatenate([packed[:RIM], packed[RIM:]], axis=1)
 
-    own = chan_ref[...].astype(F32)
-    chan = jnp.concatenate([rim(before_ref), own, rim(after_ref)])
-    length = chan.shape[0]
-    sums = chan + pltpu.roll(chan, 1, 0)
-    window_sum = sums
-    for level in range(1, POOL_GROUPS):
-        step = 2 ** (level - 1)
-        sums = pltpu.roll(sums, step, 0) + pltpu.roll(sums, length - step, 0)
-        window_sum = jnp.where(y >= level, sums, window_sum)
-    half_width = jnp.left_shift(jnp.int32(1), y)
-    pos = offset + lax.broadcasted_iota(jnp.int32, (rows, 1), 0)
-    count = jnp.minimum(pos + half_width, seq_len) - jnp.maximum(pos - half_width, 0)
-    spread = window_sum[RIM : RIM + rows] / count.astype(F32) - own
-    pooled = jnp.dot(spread.astype(BF16), w_pool_ref[0], preferred_element_type=F32)
-    pooled_ref[...] = (pooled * scale_ref[...]).astype(BF16)
-
-
-def out_kernel(
-    ahead, first_ref, middle_ref, pooled_ref, own_ref, other_ref, out_ref, hidden_ref, w_ref
-):
-    edge = WINDOW
-    rows, query_cols = pooled_ref.shape[0], first_ref.shape[1]
+    near = 2 * RIM
+    first = chan_ref[: WINDOW + near].astype(F32)
+    last = chan_ref[rows - WINDOW - near :].astype(F32)
+    chan = jnp.concatenate([rim(before_ref), first, last, rim(after_ref)])
+
+    def centre(a):
+        return jnp.concatenate([a[RIM : RIM + WINDOW], a[-RIM - WINDOW : -RIM]])
+
+    pooled_ref[...] = pooled_rows(
+        chan, centre, (offset, offset + rows - 2 * WINDOW), seq_len, w_pool_ref, scale_ref
+    )
+
+
+def out_kernel(ahead, count, *refs):
+    mixed_refs, (own_ref, other_ref, out_ref, hidden_ref, w_ref) = refs[: 2 * count], refs[2 * count :]
     to = lax.rem(lax.axis_index(TP) + ahead, lax.axis_size(TP))
     zs = own_ref.shape[1] // lax.axis_size(TP)
     at = own_ref.shape[3] - hidden_ref.shape[1]
     mine = pl.ds(to * zs, zs)
     whole_weights(own_ref.at[:, mine], other_ref.at[:, mine], w_ref, at)
-    hidden_ref[:edge, :query_cols] = first_ref[:edge]
-    hidden_ref[edge : rows - edge, :query_cols] = middle_ref[...]
-    hidden_ref[rows - edge :, :query_cols] = first_ref[edge:]
-    hidden_ref[:, query_cols:] = pooled_ref[...]
+    for part in range(count):
+        attended_ref, pooled_ref = mixed_refs[2 * part : 2 * part + 2]
+        rows, query_cols = attended_ref.shape
+        here = slice(part * rows, (part + 1) * rows)
+        hidden_ref[here, :query_cols] = attended_ref[...]
+        hidden_ref[here, query_cols:] = pooled_ref[...]
     out_ref[...] = lax.dot_general(
         hidden_ref[...], w_ref[...], nt, preferred_element_type=F32
     ).astype(BF16)
@@ -287,57 +310,64 @@
         name="project",
     )(gathered, own1, other1)
     before, after = neighbours(head, tail, SP)
-    band = pltpu.VMEM((4, rows, PAIR), BF16)
-    query, attended0 = pl.pallas_call(
+    half = rows // 2
+    scale = pool_scale.reshape(1, -1)
+    query, *inner = pl.pallas_call(
         functools.partial(inner_kernel, seq_len),
-        out_shape=[rows_of(query_cols), rows_of(query_cols, rows - 2 * WINDOW)],
-        in_specs=[VMEM] * 4 + [SMEM],
-        out_specs=[VMEM] * 2,
-        scratch_shapes=[pltpu.VMEM((model_width, query_cols), BF16), band],
+        out_shape=[rows_of(query_cols), rows_of(query_cols, half), rows_of(chan_cols, half)],
+        in_specs=[VMEM] * 5 + [SMEM] + [VMEM] * 2,
+        out_specs=[VMEM] * 3,
+        scratch_shapes=[
+            pltpu.VMEM((model_width, query_cols), BF16),
+            pltpu.VMEM((4, rows, PAIR), BF16),
+        ],
         compiler_params=LIMIT,
         cost_estimate=cost(2 * rows * model_width * query_cols, 4 << 20),
         name="inner",
-    )(gathered, own1, other1, kv, sink)
-    attended1, pooled = pl.pallas_call(
+    )(gathered, own1, other1, kv, chan, sink, w_pool, scale)
+    outer = pl.pallas_call(
         functools.partial(outer_kernel, seq_len),
-        out_shape=[rows_of(query_cols, 2 * WINDOW), rows_of(chan_cols)],
+        out_shape=[rows_of(query_cols, half), rows_of(chan_cols, half)],
         in_specs=[VMEM] * 5 + [SMEM] + [VMEM] * 2,
         out_specs=[VMEM] * 2,
         scratch_shapes=[pltpu.VMEM((4, 6 * WINDOW, PAIR), BF16)],
         compiler_params=LIMIT,
         cost_estimate=cost(2 * rows * model_width * query_cols, 2 << 20),
         name="outer",
-    )(query, kv, chan, before, after, sink, w_pool, pool_scale.reshape(1, -1))
-
-    def multiplied(ahead):
+    )(query, kv, chan, before, after, sink, w_pool, scale)
+
+    def multiplied(ahead, *mixed):
+        count = len(mixed)
         return pl.pallas_call(
-            functools.partial(out_kernel, ahead),
-            out_shape=rows_of(share),
-            in_specs=[VMEM] * 5,
+            functools.partial(out_kernel, ahead, count),
+            out_shape=rows_of(share, count * half),
+            in_specs=[VMEM] * (2 * count + 2),
             out_specs=VMEM,
             scratch_shapes=[
-                pltpu.VMEM((rows, hidden_cols), BF16),
+                pltpu.VMEM((count * half, hidden_cols), BF16),
                 pltpu.VMEM((share, hidden_cols), BF16),
             ],
             compiler_params=LIMIT,
-            cost_estimate=cost(2 * rows * share * hidden_cols, 1 << 20),
-        )(attended1, attended0, pooled, own2, other2)
-
-    count = lax.axis_size(TP)
-    partials = []
-    for ahead in (2, 1, 3):
-        block = multiplied(ahead)
-        perm = [(i, (i + ahead) % count) for i in range(count)]
-        partials.append(lax.ppermute(block, TP, perm))
-    mix = multiplied(0).astype(F32)
-    for partial in partials[1:] + partials[:1]:
+            cost_estimate=cost(2 * count * half * share * hidden_cols, 1 << 20),
+        )(*(a for pair in mixed for a in pair), own2, other2)
+
+    def sent(ahead, *mixed):
+        block = multiplied(ahead, *mixed)
+        count = lax.axis_size(TP)
+        return lax.ppermute(block, TP, [(i, (i + ahead) % count) for i in range(count)])
+
+    far = jnp.concatenate([sent(2, inner), sent(2, outer)])
+    partials = [sent(1, inner, outer), sent(3, inner, outer), far]
+    mix = multiplied(0, inner, outer).astype(F32)
+    for partial in partials:
         mix = mix + partial.astype(F32)
     stats = jnp.stack([jnp.sum(mix, axis=1), jnp.sum(mix * mix, axis=1)])
     stats = of_everyone(stats, TP)
     row_mean = stats[0] / model_width
     variance = stats[1] / model_width - row_mean * row_mean
     normed = (mix - row_mean[:, None]) * lax.rsqrt(variance + epsilon)[:, None] * out_gain
-    return normed.astype(BF16)
+    normed = normed.astype(BF16)
+    return jnp.concatenate([normed[half : half + WINDOW], normed[:half], normed[half + WINDOW :]])
 
 
 def solution(mesh):

time: 146 us -> 151 us (1.034)
  starting transfers between devices: 23.3 us -> 27.7 us
  Pallas kernels: 18.5 us -> 14.4 us
  waiting for transfers between devices: 24.4 us -> 28 us
    pallas_call x4 -> x5, Pallas kernels: 6.95 us -> 2.34 us  [multiplied(): pl.pallas_call(functools.partial(out_kernel, ahead, count), out_shape=row...]
    ppermute x3 -> x4, starting transfers between devices: 8.98 us -> 13.2 us  [sent(): lax.ppermute(block, TP, [(i, (i + ahead) % count) for i in range(count)])]
    ppermute x3 -> x4, waiting for transfers between devices: 15.2 us -> 17.5 us  [sent(): lax.ppermute(block, TP, [(i, (i + ahead) % count) for i in range(count)])]
  transfers between devices with their start and end apart: 8 -> 9, of which waited for: 4 -> 4; matrix products, arithmetic and copies ran while one was open for 3% -> 2% of each run, Pallas kernels for 12% -> 9%
where the time goes in v7:
time: 151 us; the launch traced here: 150 us
  blocking collectives  70.9 us (47%)
  waiting for transfers between devices  28 us (19%)
  starting transfers between devices  27.7 us (18%)
  Pallas kernels  14.4 us (10%)
  local copies, waits for them, and re-layouts  6.16 us (4%)
  other arithmetic  2.8 us (2%)
    all_gather x1, blocking collectives, layer(): over_z = lax.all_gather(packed, Z, axis=0)  38.9 us
    all_to_all x2, blocking collectives, from_everyone(): lax.all_to_all(jnp.broadcast_to(shard[None], (count, *shard.shape)), axis...  32 us
    ppermute x4, waiting for transfers between devices, sent(): lax.ppermute(block, TP, [(i, (i + ahead) % count) for i in range(count)])  17.5 us
    ppermute x4, starting transfers between devices, sent(): lax.ppermute(block, TP, [(i, (i + ahead) % count) for i in range(count)])  13.2 us
    all_to_all x1, waiting for transfers between devices, from_everyone(): lax.all_to_all(jnp.broadcast_to(shard[None], (count, *shard.shape)), axis...  10.4 us
    pallas_call x1, Pallas kernels, layer(): pl.pallas_call(functools.partial(inner_kernel, seq_len), out_shape=[rows_...  5.82 us
    all_to_all x1, starting transfers between devices, from_everyone(): lax.all_to_all(jnp.broadcast_to(shard[None], (count, *shard.shape)), axis...  4.46 us
    ppermute x2, starting transfers between devices, swapped(): return lax.ppermute(shard, CORE, [(0, 1), (1, 0)])  4.46 us
  transfers between devices with their start and end apart: 9, of which 4 were waited for; matrix products, arithmetic and copies ran while one was open for 2% of the time, Pallas kernels for 9%

profile of v7, /device:TPU:6, one launch (start us, length us, event | category | flops | bytes accessed | tf_op | source)
XLA Modules:
  0.0 150.1 jit_solution(8679055490830086552)
XLA Ops:
  0.0 0.9 concatenate.9
  0.9 38.9 %all-gather = bf16[256,1152]{1,0:T(8,128)(2,1)S(1)} all-gather(bf16[16,1152]{1,0:T(8,128)(2,1)S(1)} %concatenate.9), channel_id=2, replica_groups=mesh['sp_0'=16,'sp_1'=4,'sp_2'=2,'tp'=4] {'sp_0'}, dimensions={0}, use_global_device_ids=true | all-gather | bytes 626688 | tf_op jit(solution)/shard_map/all_gather | solution.py:289
  39.9 24.3 %all_to_all.15 = bf16[4,16,16,1152]{3,2,1,0:T(8,128)(2,1)} all-to-all(bf16[4,16,16,1152]{3,2,1,0:T(8,128)(2,1)S(1)} %broadcast_in_dim.7), channel_id=1, replica_groups=mesh['sp_0'=16,'sp_1'=4,'sp_2'=2,'tp'=4] {'sp_1'}, dimensions={0} | all-to-all | bytes 4718592 | tf_op jit(solution)/shard_map/all_to_all | solution.py:29
  64.2 1.5 %broadcast_in_dim.6 = bf16[4,512,512]{2,1,0:T(8,128)(2,1)} broadcast(bf16[512,512]{1,0:T(8,128)(2,1)S(1)} %copy-done.5), dimensions={1,2} | broadcast | bytes 2621440 | tf_op jit(solution)/shard_map/broadcast_in_dim | solution.py:30
  65.8 4.5 %all-to-all-start = ((bf16[4,512,512]{2,1,0:T(8,128)(2,1)}), bf16[4,512,512]{2,1,0:T(8,128)(2,1)}, u32[]{:S(2)}, u32[]{:S(2)}) async-start(bf16[4,512,512]{2,1,0:T(8,128)(2,1)} %broadcast_in_dim.6), calls=%async_computation | async-start | bytes 4194304 | tf_op jit(solution)/shard_map/all_to_all | solution.py:29
  70.2 1.4 slice.28.own_ref
  71.7 1.9 %collective-permute-start = (bf16[4,16,16,640]{3,2,1,0:T(8,128)(2,1)S(1)}, bf16[4,16,16,640]{3,2,1,0:T(8,128)(2,1)}, u32[]{:S(2)}, u32[]{:S(2)}) collective-permute-start(bf16[4,16,16,640]{3,2,1,0:T(8,128)(2,1)S(1)} %slice.28.own_ref), channel_id=1, source_target_pairs={{0,4},{4,0},{1,5},{5,1},{2,6},{6,2},{3,7},{7,3},{8,12},{12,8},{9,1... | collective-permute-start | bytes 3932168 | tf_op jit(solution)/shard_map/ppermute | solution.py:39
  73.6 1.3 slice.29.refs_4_.refs_2_
  74.9 2.5 %collective-permute-start.3 = (bf16[4,16,16,512]{3,2,1,0:T(8,128)(2,1)S(1)}, bf16[4,16,16,512]{3,2,1,0:T(8,128)(2,1)S(1)}, u32[]{:S(2)}, u32[]{:S(2)}) collective-permute-start(bf16[4,16,16,512]{3,2,1,0:T(8,128)(2,1)S(1)} %slice.29.refs_4_.refs_2_), channel_id=1, source_target_pairs={{0,4},{4,0},{1,5},{5,1},{2,6},{6,2},{3,7},{7,3},{8,12},{12,8},{9,1... | collective-permute-start | bytes 3145736 | tf_op jit(solution)/shard_map/ppermute | solution.py:39
  77.5 10.4 %all-to-all-done.tokens_ref = bf16[4,512,512]{2,1,0:T(8,128)(2,1)} async-done(((bf16[4,512,512]{2,1,0:T(8,128)(2,1)}), bf16[4,512,512]{2,1,0:T(8,128)(2,1)}, u32[]{:S(2)}, u32[]{:S(2)}) %all-to-all-start) | async-done | bytes 2097184 | tf_op jit(solution)/shard_map/all_to_all | solution.py:29
  87.9 3.4 %project.1 = (bf16[512,128]{1,0:T(8,128)(2,1)S(1)}, bf16[512,256]{1,0:T(8,128)(2,1)S(1)}, bf16[144,128]{1,0:T(8,128)(2,1)S(1)}, bf16[144,128]{1,0:T(8,128)(2,1)S(1)}) custom-call(bf16[4,512,512]{2,1,0:T(8,128)(2,1)} %all-to-all-done.tokens_ref, bf16[4,16,16,640]{3,2,1,0:T(8,128)(2,1)S(1)} %slice.28.own_ref, ...), custom_call_target="tpu_custom_call" | custom-call | flops 805306368 | bytes 4194304 | tf_op jit(solution)/shard_map/project/pallas_call | solution.py:302
  91.3 1.9 %collective-permute-start.1 = (bf16[144,128]{1,0:T(8,128)(2,1)S(1)}, bf16[144,128]{1,0:T(8,128)(2,1)S(1)}, u32[]{:S(2)}, u32[]{:S(2)}) collective-permute-start(bf16[144,128]{1,0:T(8,128)(2,1)S(1)} %get-tuple-element.19), channel_id=1, source_target_pairs={{0,4},{4,8},{8,12},{12,16},{16,20},{20,24},{24,28},{28,32},{32,36}... | collective-permute-start | bytes 110600 | tf_op jit(solution)/shard_map/ppermute | solution.py:44
  93.2 3.6 %collective-permute-start.2 = (bf16[144,128]{1,0:T(8,128)(2,1)S(1)}, bf16[144,128]{1,0:T(8,128)(2,1)S(1)}, u32[]{:S(2)}, u32[]{:S(2)}) collective-permute-start(bf16[144,128]{1,0:T(8,128)(2,1)S(1)} %get-tuple-element.20), channel_id=1, source_target_pairs={{4,0},{8,4},{12,8},{16,12},{20,16},{24,20},{28,24},{32,28},{36,32}... | collective-permute-start | bytes 110600 | tf_op jit(solution)/shard_map/ppermute | solution.py:45
  96.9 5.8 %inner.1 = (bf16[512,256]{1,0:T(8,128)(2,1)S(1)}, bf16[256,256]{1,0:T(8,128)(2,1)S(1)}, bf16[256,256]{1,0:T(8,128)(2,1)S(1)}) custom-call(bf16[4,512,512]{2,1,0:T(8,128)(2,1)} %all-to-all-done.tokens_ref, bf16[4,16,16,640]{3,2,1,0:T(8,128)(2,1)S(1)} %slice.28.own_ref, bf16[4,16,16,640]{3,2,1,0:T(8,128)(2,1)} %collective-permute-done.other_ref, ...), custom_call_target="tpu_custom_call" | custom-call | flops 536870912 | bytes 4194304 | tf_op jit(solution)/shard_map/inner/pallas_call | solution.py:315
  102.8 2.8 %outer.1 = (bf16[256,256]{1,0:T(8,128)(2,1)S(1)}, bf16[256,256]{1,0:T(8,128)(2,1)S(1)}) custom-call(bf16[512,256]{1,0:T(8,128)(2,1)S(1)} %get-tuple-element.18.query_ref, bf16[512,128]{1,0:T(8,128)(2,1)S(1)} %get-tuple-element.14.kv_ref, bf16[512,256]{1,0:T(8,128)(2,1)S(1)} %get-tuple-element.15.chan_ref, ...), custom_call_target="tpu_custom_call" | custom-call | flops 536870912 | bytes 2097152 | tf_op jit(solution)/shard_map/outer/pallas_call | solution.py:328
  105.6 0.5 shard_map.111
  106.1 3.1 %collective-permute-start.5 = (bf16[512,512]{1,0:T(8,128)(2,1)S(1)}, bf16[512,512]{1,0:T(8,128)(2,1)S(1)}, u32[]{:S(2)}, u32[]{:S(2)}) collective-permute-start(bf16[512,512]{1,0:T(8,128)(2,1)S(1)} %shard_map.111), channel_id=1, source_target_pairs={{0,3},{1,0},{2,1},{3,2},{4,7},{5,4},{6,5},{7,6},{8,11},{9,8},{10,9... | collective-permute-start | bytes 1572872 | tf_op jit(solution)/shard_map/ppermute | solution.py:357
  109.2 0.5 shard_map.110
  109.7 2.8 %collective-permute-start.4 = (bf16[512,512]{1,0:T(8,128)(2,1)S(1)}, bf16[512,512]{1,0:T(8,128)(2,1)S(1)}, u32[]{:S(2)}, u32[]{:S(2)}) collective-permute-start(bf16[512,512]{1,0:T(8,128)(2,1)S(1)} %shard_map.110), channel_id=1, source_target_pairs={{0,1},{1,2},{2,3},{3,0},{4,5},{5,6},{6,7},{7,4},{8,9},{9,10},{10,1... | collective-permute-start | bytes 1572872 | tf_op jit(solution)/shard_map/ppermute | solution.py:357
  112.5 0.4 shard_map.112
  112.9 2.6 %collective-permute-start.6 = (bf16[256,512]{1,0:T(8,128)(2,1)S(1)}, bf16[256,512]{1,0:T(8,128)(2,1)S(1)}, u32[]{:S(2)}, u32[]{:S(2)}) collective-permute-start(bf16[256,512]{1,0:T(8,128)(2,1)S(1)} %shard_map.112), channel_id=1, source_target_pairs={{0,2},{1,3},{2,0},{3,1},{4,6},{5,7},{6,4},{7,5},{8,10},{9,11},{10,... | collective-permute-start | bytes 786440 | tf_op jit(solution)/shard_map/ppermute | solution.py:357
  115.5 0.4 shard_map.113
  115.9 4.8 %collective-permute-start.7 = (bf16[256,512]{1,0:T(8,128)(2,1)S(1)}, bf16[256,512]{1,0:T(8,128)(2,1)S(1)}, u32[]{:S(2)}, u32[]{:S(2)}) collective-permute-start(bf16[256,512]{1,0:T(8,128)(2,1)S(1)} %shard_map.113), channel_id=1, source_target_pairs={{0,2},{1,3},{2,0},{3,1},{4,6},{5,7},{6,4},{7,5},{8,10},{9,11},{10,... | collective-permute-start | bytes 786440 | tf_op jit(solution)/shard_map/ppermute | solution.py:357
  120.7 0.5 shard_map.109
  121.2 10.3 %collective-permute-done.6 = bf16[256,512]{1,0:T(8,128)(2,1)S(1)} collective-permute-done((bf16[256,512]{1,0:T(8,128)(2,1)S(1)}, bf16[256,512]{1,0:T(8,128)(2,1)S(1)}, u32[]{:S(2)}, u32[]{:S(2)}) %collective-permute-start.6) | collective-permute-done | bytes 262176 | tf_op jit(solution)/shard_map/ppermute | solution.py:357
  131.5 5.6 %collective-permute-done.7 = bf16[256,512]{1,0:T(8,128)(2,1)S(1)} collective-permute-done((bf16[256,512]{1,0:T(8,128)(2,1)S(1)}, bf16[256,512]{1,0:T(8,128)(2,1)S(1)}, u32[]{:S(2)}, u32[]{:S(2)}) %collective-permute-start.7) | collective-permute-done | bytes 262176 | tf_op jit(solution)/shard_map/ppermute | solution.py:357
  137.1 1.6 %collective-permute-done.4 = bf16[512,512]{1,0:T(8,128)(2,1)S(1)} collective-permute-done((bf16[512,512]{1,0:T(8,128)(2,1)S(1)}, bf16[512,512]{1,0:T(8,128)(2,1)S(1)}, u32[]{:S(2)}, u32[]{:S(2)}) %collective-permute-start.4) | collective-permute-done | bytes 524320 | tf_op jit(solution)/shard_map/ppermute | solution.py:357
  138.7 0.8 copy-done.3
  139.5 0.4 fusion
  140.0 7.7 %all_to_all.16 = f32[4,2,512]{2,1,0:T(2,128)S(1)} all-to-all(f32[4,2,512]{2,1,0:T(2,128)S(1)} %broadcast_in_dim.8), channel_id=1, replica_groups=mesh['sp_0'=16,'sp_1'=4,'sp_2'=2,'tp'=4] {'tp'}, dimensions={0} | all-to-all | bytes 32768 | tf_op jit(solution)/shard_map/all_to_all | solution.py:29
  147.7 1.5 multiply_convert_fusion
  149.3 0.8 pad_maximum_fusion
  (26 shorter events, 0.3 us)
Async XLA Ops:
  39.9 24.3 %copy-start.5 = (bf16[512,512]{1,0:T(8,128)(2,1)S(1)}, bf16[512,512]{1,0:T(8,128)(2,1)}, u32[]{:S(2)}) copy-start(bf16[512,512]{1,0:T(8,128)(2,1)} %param.11) | copy-start | bytes 1572868
  65.8 22.2 %all-to-all-start = ((bf16[4,512,512]{2,1,0:T(8,128)(2,1)}), bf16[4,512,512]{2,1,0:T(8,128)(2,1)}, u32[]{:S(2)}, u32[]{:S(2)}) async-start(bf16[4,512,512]{2,1,0:T(8,128)(2,1)} %broadcast_in_dim.6), calls=%async_computation | async-start | bytes 4194304 | tf_op jit(solution)/shard_map/all_to_all | solution.py:29
  71.7 16.2 %collective-permute-start = (bf16[4,16,16,640]{3,2,1,0:T(8,128)(2,1)S(1)}, bf16[4,16,16,640]{3,2,1,0:T(8,128)(2,1)}, u32[]{:S(2)}, u32[]{:S(2)}) collective-permute-start(bf16[4,16,16,640]{3,2,1,0:T(8,128)(2,1)S(1)} %slice.28.own_ref), channel_id=1, source_target_pairs={{0,4},{4,0},{1,5},{5,1},{2,6},{6,2},{3,7},{7,3},{8,12},{12,8},{9,1... | collective-permute-start | bytes 3932168 | tf_op jit(solution)/shard_map/ppermute | solution.py:39
  74.9 22.0 %copy-start = (bf16[1,256,256]{2,1,0:T(8,128)(2,1)S(1)}, bf16[1,256,256]{2,1,0:T(8,128)(2,1)}, u32[]{:S(2)}) copy-start(bf16[1,256,256]{2,1,0:T(8,128)(2,1)} %w_pool_ref.3) | copy-start | bytes 393220
  74.9 22.0 %copy-start.1 = (f32[256]{0:T(256)S(1)}, f32[256]{0:T(256)}, u32[]{:S(2)}) copy-start(f32[256]{0:T(256)} %param.18) | copy-start | bytes 3076
  74.9 22.0 %copy-start.2 = (f32[4]{0:T(128)S(1)}, f32[4]{0:T(128)}, u32[]{:S(2)}) copy-start(f32[4]{0:T(128)} %sink_ref.3) | copy-start | bytes 52
  74.9 30.7 %collective-permute-start.3 = (bf16[4,16,16,512]{3,2,1,0:T(8,128)(2,1)S(1)}, bf16[4,16,16,512]{3,2,1,0:T(8,128)(2,1)S(1)}, u32[]{:S(2)}, u32[]{:S(2)}) collective-permute-start(bf16[4,16,16,512]{3,2,1,0:T(8,128)(2,1)S(1)} %slice.29.refs_4_.refs_2_), channel_id=1, source_target_pairs={{0,4},{4,0},{1,5},{5,1},{2,6},{6,2},{3,7},{7,3},{8,12},{12,8},{9,1... | collective-permute-start | bytes 3145736 | tf_op jit(solution)/shard_map/ppermute | solution.py:39
  91.3 11.4 %collective-permute-start.1 = (bf16[144,128]{1,0:T(8,128)(2,1)S(1)}, bf16[144,128]{1,0:T(8,128)(2,1)S(1)}, u32[]{:S(2)}, u32[]{:S(2)}) collective-permute-start(bf16[144,128]{1,0:T(8,128)(2,1)S(1)} %get-tuple-element.19), channel_id=1, source_target_pairs={{0,4},{4,8},{8,12},{12,16},{16,20},{20,24},{24,28},{28,32},{32,36}... | collective-permute-start | bytes 110600 | tf_op jit(solution)/shard_map/ppermute | solution.py:44
  93.2 9.5 %collective-permute-start.2 = (bf16[144,128]{1,0:T(8,128)(2,1)S(1)}, bf16[144,128]{1,0:T(8,128)(2,1)S(1)}, u32[]{:S(2)}, u32[]{:S(2)}) collective-permute-start(bf16[144,128]{1,0:T(8,128)(2,1)S(1)} %get-tuple-element.20), channel_id=1, source_target_pairs={{4,0},{8,4},{12,8},{16,12},{20,16},{24,20},{28,24},{32,28},{36,32}... | collective-permute-start | bytes 110600 | tf_op jit(solution)/shard_map/ppermute | solution.py:45
  106.1 31.0 %collective-permute-start.5 = (bf16[512,512]{1,0:T(8,128)(2,1)S(1)}, bf16[512,512]{1,0:T(8,128)(2,1)S(1)}, u32[]{:S(2)}, u32[]{:S(2)}) collective-permute-start(bf16[512,512]{1,0:T(8,128)(2,1)S(1)} %shard_map.111), channel_id=1, source_target_pairs={{0,3},{1,0},{2,1},{3,2},{4,7},{5,4},{6,5},{7,6},{8,11},{9,8},{10,9... | collective-permute-start | bytes 1572872 | tf_op jit(solution)/shard_map/ppermute | solution.py:357
  109.7 29.0 %collective-permute-start.4 = (bf16[512,512]{1,0:T(8,128)(2,1)S(1)}, bf16[512,512]{1,0:T(8,128)(2,1)S(1)}, u32[]{:S(2)}, u32[]{:S(2)}) collective-permute-start(bf16[512,512]{1,0:T(8,128)(2,1)S(1)} %shard_map.110), channel_id=1, source_target_pairs={{0,1},{1,2},{2,3},{3,0},{4,5},{5,6},{6,7},{7,4},{8,9},{9,10},{10,1... | collective-permute-start | bytes 1572872 | tf_op jit(solution)/shard_map/ppermute | solution.py:357
  112.9 18.6 %collective-permute-start.6 = (bf16[256,512]{1,0:T(8,128)(2,1)S(1)}, bf16[256,512]{1,0:T(8,128)(2,1)S(1)}, u32[]{:S(2)}, u32[]{:S(2)}) collective-permute-start(bf16[256,512]{1,0:T(8,128)(2,1)S(1)} %shard_map.112), channel_id=1, source_target_pairs={{0,2},{1,3},{2,0},{3,1},{4,6},{5,7},{6,4},{7,5},{8,10},{9,11},{10,... | collective-permute-start | bytes 786440 | tf_op jit(solution)/shard_map/ppermute | solution.py:357
  115.9 31.9 %copy-start.6 = (f32[512]{0:T(512)S(1)}, f32[512]{0:T(512)}, u32[]{:S(2)}) copy-start(f32[512]{0:T(512)} %param.21) | copy-start | bytes 6148
  115.9 21.2 %collective-permute-start.7 = (bf16[256,512]{1,0:T(8,128)(2,1)S(1)}, bf16[256,512]{1,0:T(8,128)(2,1)S(1)}, u32[]{:S(2)}, u32[]{:S(2)}) collective-permute-start(bf16[256,512]{1,0:T(8,128)(2,1)S(1)} %shard_map.113), channel_id=1, source_target_pairs={{0,2},{1,3},{2,0},{3,1},{4,6},{5,7},{6,4},{7,5},{8,10},{9,11},{10,... | collective-permute-start | bytes 786440 | tf_op jit(solution)/shard_map/ppermute | solution.py:357
  137.1 2.8 %copy-start.4 = (bf16[256,512]{1,0:T(8,128)(2,1)}, bf16[256,512]{1,0:T(8,128)(2,1)S(1)}, u32[]{:S(2)}) copy-start(bf16[256,512]{1,0:T(8,128)(2,1)S(1)} %collective-permute-done.7) | copy-start | bytes 786436
  138.7 0.8 copy-start.3

commit v8 on v7

--- a/solution.py
+++ b/solution.py
@@ -39,11 +39,10 @@
     return lax.ppermute(shard, CORE, [(0, 1), (1, 0)])
 
 
-def neighbours(head, tail, axis):
-    count = lax.axis_size(axis)
-    before = lax.ppermute(tail, axis, [(i, i + 1) for i in range(count - 1)])
-    after = lax.ppermute(head, axis, [(i + 1, i) for i in range(count - 1)])
-    return before, after
+def neighbours(inside, outside):
+    count = lax.axis_size(SP)
+    pairs = [(i, i + 1) for i in range(1, count - 1, 2)]
+    return swapped(inside), lax.ppermute(outside, SP, pairs + [(b, a) for a, b in pairs])
 
 
 def whole_weights(own_ref, other_ref, w_ref, at):
@@ -74,16 +73,24 @@
     return total.astype(BF16)
 
 
-def project_kernel(tokens_ref, own_ref, other_ref, kv_ref, chan_ref, head_ref, tail_ref, w_ref):
+def project_kernel(
+    tokens_ref, own_ref, other_ref, kv_ref, chan_ref, inside_ref, outside_ref, w_ref
+):
     rows = tokens_ref.shape[1]
     whole_weights(own_ref, other_ref, w_ref, 0)
     kv_cols = kv_ref.shape[1]
     kv_ref[...] = projected(tokens_ref, w_ref, 0, kv_cols)
     chan_ref[...] = projected(tokens_ref, w_ref, kv_cols, chan_ref.shape[1])
-    for ref, kv_at, chan_at in ((head_ref, 0, 0), (tail_ref, rows - WINDOW, rows - RIM)):
-        ref[:WINDOW] = kv_ref[kv_at : kv_at + WINDOW]
+
+    def rim(kv_at, chan_at):
         edge = chan_ref[chan_at : chan_at + RIM].astype(F32)
-        ref[WINDOW:] = jnp.concatenate([edge[:, :PAIR], edge[:, PAIR:]]).astype(BF16)
+        kv = kv_ref[kv_at : kv_at + WINDOW].astype(F32)
+        return jnp.concatenate([kv, edge[:, :PAIR], edge[:, PAIR:]])
+
+    first, last = rim(0, 0), rim(rows - WINDOW, rows - RIM)
+    ahead = lax.axis_index(CORE) == 0
+    inside_ref[...] = jnp.where(ahead, last, first).astype(BF16)
+    outside_ref[...] = jnp.where(ahead, first, last).astype(BF16)
 
 
 def split_band(kv, band_ref):
@@ -185,8 +192,8 @@
     query_ref,
     kv_ref,
     chan_ref,
-    before_ref,
-    after_ref,
+    inside_ref,
+    outside_ref,
     sink_ref,
     w_pool_ref,
     scale_ref,
@@ -196,14 +203,17 @@
 ):
     rows = chan_ref.shape[0]
     offset = lax.axis_index(SP) * rows
+    ahead = lax.axis_index(CORE) == 0
+    inside, outside = inside_ref[...].astype(F32), outside_ref[...].astype(F32)
+    before, after = jnp.where(ahead, outside, inside), jnp.where(ahead, inside, outside)
 
     split_band(
         jnp.concatenate(
             [
-                before_ref[:WINDOW],
-                kv_ref[: 2 * WINDOW],
-                kv_ref[rows - 2 * WINDOW :],
-                after_ref[:WINDOW],
+                before[:WINDOW],
+                kv_ref[: 2 * WINDOW].astype(F32),
+                kv_ref[rows - 2 * WINDOW :].astype(F32),
+                after[:WINDOW],
             ]
         ),
         band_ref,
@@ -221,14 +231,13 @@
             edge * WINDOW,
         )
 
-    def rim(ref):
-        packed = ref[WINDOW:].astype(F32)
-        return jnp.concatenate([packed[:RIM], packed[RIM:]], axis=1)
+    def rim(packed):
+        return jnp.concatenate([packed[WINDOW : WINDOW + RIM], packed[WINDOW + RIM :]], axis=1)
 
     near = 2 * RIM
     first = chan_ref[: WINDOW + near].astype(F32)
     last = chan_ref[rows - WINDOW - near :].astype(F32)
-    chan = jnp.concatenate([rim(before_ref), first, last, rim(after_ref)])
+    chan = jnp.concatenate([rim(before), first, last, rim(after)])
 
     def centre(a):
         return jnp.concatenate([a[RIM : RIM + WINDOW], a[-RIM - WINDOW : -RIM]])
@@ -238,9 +247,9 @@
     )
 
 
-def out_kernel(ahead, count, *refs):
+def out_kernel(mask, count, *refs):
     mixed_refs, (own_ref, other_ref, out_ref, hidden_ref, w_ref) = refs[: 2 * count], refs[2 * count :]
-    to = lax.rem(lax.axis_index(TP) + ahead, lax.axis_size(TP))
+    to = lax.axis_index(TP) ^ mask
     zs = own_ref.shape[1] // lax.axis_size(TP)
     at = own_ref.shape[3] - hidden_ref.shape[1]
     mine = pl.ds(to * zs, zs)
@@ -299,7 +308,7 @@
         return pl.CostEstimate(flops=flops, bytes_accessed=size, transcendentals=0)
 
     rim_shape = rows_of(PAIR, WINDOW + 2 * RIM)
-    kv, chan, head, tail = pl.pallas_call(
+    kv, chan, inside, outside = pl.pallas_call(
         project_kernel,
         out_shape=[rows_of(2 * key_cols), rows_of(chan_cols), rim_shape, rim_shape],
         in_specs=[VMEM] * 3,
@@ -309,7 +318,7 @@
         cost_estimate=cost(2 * rows * model_width * (in_cols - query_cols), 4 << 20),
         name="project",
     )(gathered, own1, other1)
-    before, after = neighbours(head, tail, SP)
+    inside, outside = neighbours(inside, outside)
     half = rows // 2
     scale = pool_scale.reshape(1, -1)
     query, *inner = pl.pallas_call(
@@ -334,12 +343,12 @@
         compiler_params=LIMIT,
         cost_estimate=cost(2 * rows * model_width * query_cols, 2 << 20),
         name="outer",
-    )(query, kv, chan, before, after, sink, w_pool, scale)
-
-    def multiplied(ahead, *mixed):
+    )(query, kv, chan, inside, outside, sink, w_pool, scale)
+
+    def multiplied(mask, *mixed):
         count = len(mixed)
         return pl.pallas_call(
-            functools.partial(out_kernel, ahead, count),
+            functools.partial(out_kernel, mask, count),
             out_shape=rows_of(share, count * half),
             in_specs=[VMEM] * (2 * count + 2),
             out_specs=VMEM,
@@ -351,10 +360,10 @@
             cost_estimate=cost(2 * count * half * share * hidden_cols, 1 << 20),
         )(*(a for pair in mixed for a in pair), own2, other2)
 
-    def sent(ahead, *mixed):
-        block = multiplied(ahead, *mixed)
+    def sent(mask, *mixed):
+        block = multiplied(mask, *mixed)
         count = lax.axis_size(TP)
-        return lax.ppermute(block, TP, [(i, (i + ahead) % count) for i in range(count)])
+        return lax.ppermute(block, TP, [(i, i ^ mask) for i in range(count)])
 
     far = jnp.concatenate([sent(2, inner), sent(2, outer)])
     partials = [sent(1, inner, outer), sent(3, inner, outer), far]

time: 151 us -> 150 us (level)
  the two profiles are of different devices: /device:TPU:6 before, /device:TPU:32 now
where the time goes in v8:
time: 150 us; the launch traced here: 149 us
  blocking collectives  70.9 us (47%)
  waiting for transfers between devices  28 us (19%)
  starting transfers between devices  26.6 us (18%)
  Pallas kernels  14.4 us (10%)
  local copies, waits for them, and re-layouts  6.18 us (4%)
  other arithmetic  2.8 us (2%)
    all_gather x1, blocking collectives, layer(): over_z = lax.all_gather(packed, Z, axis=0)  36.4 us
    all_to_all x2, blocking collectives, from_everyone(): lax.all_to_all(jnp.broadcast_to(shard[None], (count, *shard.shape)), axis...  34.5 us
    ppermute x4, waiting for transfers between devices, sent(): return lax.ppermute(block, TP, [(i, i ^ mask) for i in range(count)])  16.7 us
    ppermute x4, starting transfers between devices, sent(): return lax.ppermute(block, TP, [(i, i ^ mask) for i in range(count)])  12.3 us
    all_to_all x1, waiting for transfers between devices, from_everyone(): lax.all_to_all(jnp.broadcast_to(shard[None], (count, *shard.shape)), axis...  11.3 us
    ppermute x3, starting transfers between devices, swapped(): return lax.ppermute(shard, CORE, [(0, 1), (1, 0)])  6.38 us
    pallas_call x1, Pallas kernels, layer(): pl.pallas_call(functools.partial(inner_kernel, seq_len), out_shape=[rows_...  5.82 us
    all_to_all x1, starting transfers between devices, from_everyone(): lax.all_to_all(jnp.broadcast_to(shard[None], (count, *shard.shape)), axis...  4.46 us
  transfers between devices with their start and end apart: 9, of which 3 were waited for; matrix products, arithmetic and copies ran while one was open for 2% of the time, Pallas kernels for 9%

profile of v8, /device:TPU:32, one launch (start us, length us, event | category | flops | bytes accessed | tf_op | source)
XLA Modules:
  0.0 149.2 jit_solution(12860227852095476218)
XLA Ops:
  0.0 0.9 concatenate.9
  0.9 36.4 %all-gather = bf16[256,1152]{1,0:T(8,128)(2,1)S(1)} all-gather(bf16[16,1152]{1,0:T(8,128)(2,1)S(1)} %concatenate.9), channel_id=2, replica_groups=mesh['sp_0'=16,'sp_1'=4,'sp_2'=2,'tp'=4] {'sp_0'}, dimensions={0}, use_global_device_ids=true | all-gather | bytes 626688 | tf_op jit(solution)/shard_map/all_gather | solution.py:298
  37.3 0.2 broadcast_in_dim.7
  37.5 26.8 %all_to_all.15 = bf16[4,16,16,1152]{3,2,1,0:T(8,128)(2,1)} all-to-all(bf16[4,16,16,1152]{3,2,1,0:T(8,128)(2,1)S(1)} %broadcast_in_dim.7), channel_id=1, replica_groups=mesh['sp_0'=16,'sp_1'=4,'sp_2'=2,'tp'=4] {'sp_1'}, dimensions={0} | all-to-all | bytes 4718592 | tf_op jit(solution)/shard_map/all_to_all | solution.py:29
  64.3 1.5 %broadcast_in_dim.6 = bf16[4,512,512]{2,1,0:T(8,128)(2,1)} broadcast(bf16[512,512]{1,0:T(8,128)(2,1)S(1)} %copy-done.5), dimensions={1,2} | broadcast | bytes 2621440 | tf_op jit(solution)/shard_map/broadcast_in_dim | solution.py:30
  65.8 4.5 %all-to-all-start = ((bf16[4,512,512]{2,1,0:T(8,128)(2,1)}), bf16[4,512,512]{2,1,0:T(8,128)(2,1)}, u32[]{:S(2)}, u32[]{:S(2)}) async-start(bf16[4,512,512]{2,1,0:T(8,128)(2,1)} %broadcast_in_dim.6), calls=%async_computation | async-start | bytes 4194304 | tf_op jit(solution)/shard_map/all_to_all | solution.py:29
  70.2 1.4 slice.28.own_ref
  71.7 1.9 %collective-permute-start = (bf16[4,16,16,640]{3,2,1,0:T(8,128)(2,1)S(1)}, bf16[4,16,16,640]{3,2,1,0:T(8,128)(2,1)}, u32[]{:S(2)}, u32[]{:S(2)}) collective-permute-start(bf16[4,16,16,640]{3,2,1,0:T(8,128)(2,1)S(1)} %slice.28.own_ref), channel_id=1, source_target_pairs={{0,4},{4,0},{1,5},{5,1},{2,6},{6,2},{3,7},{7,3},{8,12},{12,8},{9,1... | collective-permute-start | bytes 3932168 | tf_op jit(solution)/shard_map/ppermute | solution.py:39
  73.6 1.3 slice.29.refs_4_.refs_2_
  74.9 2.5 %collective-permute-start.3 = (bf16[4,16,16,512]{3,2,1,0:T(8,128)(2,1)S(1)}, bf16[4,16,16,512]{3,2,1,0:T(8,128)(2,1)S(1)}, u32[]{:S(2)}, u32[]{:S(2)}) collective-permute-start(bf16[4,16,16,512]{3,2,1,0:T(8,128)(2,1)S(1)} %slice.29.refs_4_.refs_2_), channel_id=1, source_target_pairs={{0,4},{4,0},{1,5},{5,1},{2,6},{6,2},{3,7},{7,3},{8,12},{12,8},{9,1... | collective-permute-start | bytes 3145736 | tf_op jit(solution)/shard_map/ppermute | solution.py:39
  77.5 11.3 %all-to-all-done.tokens_ref = bf16[4,512,512]{2,1,0:T(8,128)(2,1)} async-done(((bf16[4,512,512]{2,1,0:T(8,128)(2,1)}), bf16[4,512,512]{2,1,0:T(8,128)(2,1)}, u32[]{:S(2)}, u32[]{:S(2)}) %all-to-all-start) | async-done | bytes 2097184 | tf_op jit(solution)/shard_map/all_to_all | solution.py:29
  88.8 3.4 %project.1 = (bf16[512,128]{1,0:T(8,128)(2,1)S(1)}, bf16[512,256]{1,0:T(8,128)(2,1)S(1)}, bf16[144,128]{1,0:T(8,128)(2,1)S(1)}, bf16[144,128]{1,0:T(8,128)(2,1)S(1)}) custom-call(bf16[4,512,512]{2,1,0:T(8,128)(2,1)} %all-to-all-done.tokens_ref, bf16[4,16,16,640]{3,2,1,0:T(8,128)(2,1)S(1)} %slice.28.own_ref, ...), custom_call_target="tpu_custom_call" | custom-call | flops 805306368 | bytes 4194304 | tf_op jit(solution)/shard_map/project/pallas_call | solution.py:311
  92.2 1.9 %collective-permute-start.1 = (bf16[144,128]{1,0:T(8,128)(2,1)S(1)}, bf16[144,128]{1,0:T(8,128)(2,1)S(1)}, u32[]{:S(2)}, u32[]{:S(2)}) collective-permute-start(bf16[144,128]{1,0:T(8,128)(2,1)S(1)} %get-tuple-element.19), channel_id=1, source_target_pairs={{0,4},{4,0},{1,5},{5,1},{2,6},{6,2},{3,7},{7,3},{8,12},{12,8},{9,1... | collective-permute-start | bytes 110600 | tf_op jit(solution)/shard_map/ppermute | solution.py:39
  94.1 3.4 %collective-permute-start.2 = (bf16[144,128]{1,0:T(8,128)(2,1)S(1)}, bf16[144,128]{1,0:T(8,128)(2,1)S(1)}, u32[]{:S(2)}, u32[]{:S(2)}) collective-permute-start(bf16[144,128]{1,0:T(8,128)(2,1)S(1)} %get-tuple-element.20), channel_id=1, source_target_pairs={{4,8},{12,16},{20,24},{28,32},{36,40},{44,48},{52,56},{60,64},{68,... | collective-permute-start | bytes 110600 | tf_op jit(solution)/shard_map/ppermute | solution.py:45
  97.6 5.8 %inner.1 = (bf16[512,256]{1,0:T(8,128)(2,1)S(1)}, bf16[256,256]{1,0:T(8,128)(2,1)S(1)}, bf16[256,256]{1,0:T(8,128)(2,1)S(1)}) custom-call(bf16[4,512,512]{2,1,0:T(8,128)(2,1)} %all-to-all-done.tokens_ref, bf16[4,16,16,640]{3,2,1,0:T(8,128)(2,1)S(1)} %slice.28.own_ref, bf16[4,16,16,640]{3,2,1,0:T(8,128)(2,1)} %collective-permute-done.other_ref, ...), custom_call_target="tpu_custom_call" | custom-call | flops 536870912 | bytes 4194304 | tf_op jit(solution)/shard_map/inner/pallas_call | solution.py:324
  103.4 2.8 %outer.1 = (bf16[256,256]{1,0:T(8,128)(2,1)S(1)}, bf16[256,256]{1,0:T(8,128)(2,1)S(1)}) custom-call(bf16[512,256]{1,0:T(8,128)(2,1)S(1)} %get-tuple-element.18.query_ref, bf16[512,128]{1,0:T(8,128)(2,1)S(1)} %get-tuple-element.14.kv_ref, bf16[512,256]{1,0:T(8,128)(2,1)S(1)} %get-tuple-element.15.chan_ref, ...), custom_call_target="tpu_custom_call" | custom-call | flops 536870912 | bytes 2097152 | tf_op jit(solution)/shard_map/outer/pallas_call | solution.py:337
  106.2 0.5 shard_map.111
  106.8 3.1 %collective-permute-start.5 = (bf16[512,512]{1,0:T(8,128)(2,1)S(1)}, bf16[512,512]{1,0:T(8,128)(2,1)S(1)}, u32[]{:S(2)}, u32[]{:S(2)}) collective-permute-start(bf16[512,512]{1,0:T(8,128)(2,1)S(1)} %shard_map.111), channel_id=1, source_target_pairs={{0,3},{1,2},{2,1},{3,0},{4,7},{5,6},{6,5},{7,4},{8,11},{9,10},{10,... | collective-permute-start | bytes 1572872 | tf_op jit(solution)/shard_map/ppermute | solution.py:366
  109.8 0.5 shard_map.110
  110.4 1.9 %collective-permute-start.4 = (bf16[512,512]{1,0:T(8,128)(2,1)S(1)}, bf16[512,512]{1,0:T(8,128)(2,1)S(1)}, u32[]{:S(2)}, u32[]{:S(2)}) collective-permute-start(bf16[512,512]{1,0:T(8,128)(2,1)S(1)} %shard_map.110), channel_id=1, source_target_pairs={{0,1},{1,0},{2,3},{3,2},{4,5},{5,4},{6,7},{7,6},{8,9},{9,8},{10,11... | collective-permute-start | bytes 1572872 | tf_op jit(solution)/shard_map/ppermute | solution.py:366
  112.3 0.4 shard_map.112
  112.7 5.4 %collective-permute-start.6 = (bf16[256,512]{1,0:T(8,128)(2,1)S(1)}, bf16[256,512]{1,0:T(8,128)(2,1)S(1)}, u32[]{:S(2)}, u32[]{:S(2)}) collective-permute-start(bf16[256,512]{1,0:T(8,128)(2,1)S(1)} %shard_map.112), channel_id=1, source_target_pairs={{0,2},{1,3},{2,0},{3,1},{4,6},{5,7},{6,4},{7,5},{8,10},{9,11},{10,... | collective-permute-start | bytes 786440 | tf_op jit(solution)/shard_map/ppermute | solution.py:366
  118.1 0.4 shard_map.113
  118.5 1.9 %collective-permute-start.7 = (bf16[256,512]{1,0:T(8,128)(2,1)S(1)}, bf16[256,512]{1,0:T(8,128)(2,1)S(1)}, u32[]{:S(2)}, u32[]{:S(2)}) collective-permute-start(bf16[256,512]{1,0:T(8,128)(2,1)S(1)} %shard_map.113), channel_id=1, source_target_pairs={{0,2},{1,3},{2,0},{3,1},{4,6},{5,7},{6,4},{7,5},{8,10},{9,11},{10,... | collective-permute-start | bytes 786440 | tf_op jit(solution)/shard_map/ppermute | solution.py:366
  120.5 0.5 shard_map.109
  121.0 13.2 %collective-permute-done.6 = bf16[256,512]{1,0:T(8,128)(2,1)S(1)} collective-permute-done((bf16[256,512]{1,0:T(8,128)(2,1)S(1)}, bf16[256,512]{1,0:T(8,128)(2,1)S(1)}, u32[]{:S(2)}, u32[]{:S(2)}) %collective-permute-start.6) | collective-permute-done | bytes 262176 | tf_op jit(solution)/shard_map/ppermute | solution.py:366
  134.2 3.5 %collective-permute-done.7 = bf16[256,512]{1,0:T(8,128)(2,1)S(1)} collective-permute-done((bf16[256,512]{1,0:T(8,128)(2,1)S(1)}, bf16[256,512]{1,0:T(8,128)(2,1)S(1)}, u32[]{:S(2)}, u32[]{:S(2)}) %collective-permute-start.7) | collective-permute-done | bytes 262176 | tf_op jit(solution)/shard_map/ppermute | solution.py:366
  137.7 0.8 copy-done.3
  138.6 0.4 fusion
  139.0 7.7 %all_to_all.16 = f32[4,2,512]{2,1,0:T(2,128)S(1)} all-to-all(f32[4,2,512]{2,1,0:T(2,128)S(1)} %broadcast_in_dim.8), channel_id=1, replica_groups=mesh['sp_0'=16,'sp_1'=4,'sp_2'=2,'tp'=4] {'tp'}, dimensions={0} | all-to-all | bytes 32768 | tf_op jit(solution)/shard_map/all_to_all | solution.py:29
  146.8 1.5 multiply_convert_fusion
  148.3 0.8 pad_maximum_fusion
  (26 shorter events, 0.1 us)
Async XLA Ops:
  37.5 26.8 %copy-start.5 = (bf16[512,512]{1,0:T(8,128)(2,1)S(1)}, bf16[512,512]{1,0:T(8,128)(2,1)}, u32[]{:S(2)}) copy-start(bf16[512,512]{1,0:T(8,128)(2,1)} %param.11) | copy-start | bytes 1572868
  65.8 23.0 %all-to-all-start = ((bf16[4,512,512]{2,1,0:T(8,128)(2,1)}), bf16[4,512,512]{2,1,0:T(8,128)(2,1)}, u32[]{:S(2)}, u32[]{:S(2)}) async-start(bf16[4,512,512]{2,1,0:T(8,128)(2,1)} %broadcast_in_dim.6), calls=%async_computation | async-start | bytes 4194304 | tf_op jit(solution)/shard_map/all_to_all | solution.py:29
  71.7 17.1 %collective-permute-start = (bf16[4,16,16,640]{3,2,1,0:T(8,128)(2,1)S(1)}, bf16[4,16,16,640]{3,2,1,0:T(8,128)(2,1)}, u32[]{:S(2)}, u32[]{:S(2)}) collective-permute-start(bf16[4,16,16,640]{3,2,1,0:T(8,128)(2,1)S(1)} %slice.28.own_ref), channel_id=1, source_target_pairs={{0,4},{4,0},{1,5},{5,1},{2,6},{6,2},{3,7},{7,3},{8,12},{12,8},{9,1... | collective-permute-start | bytes 3932168 | tf_op jit(solution)/shard_map/ppermute | solution.py:39
  74.9 22.6 %copy-start = (bf16[1,256,256]{2,1,0:T(8,128)(2,1)S(1)}, bf16[1,256,256]{2,1,0:T(8,128)(2,1)}, u32[]{:S(2)}) copy-start(bf16[1,256,256]{2,1,0:T(8,128)(2,1)} %w_pool_ref.3) | copy-start | bytes 393220
  74.9 22.6 %copy-start.1 = (f32[256]{0:T(256)S(1)}, f32[256]{0:T(256)}, u32[]{:S(2)}) copy-start(f32[256]{0:T(256)} %param.18) | copy-start | bytes 3076
  74.9 22.6 %copy-start.2 = (f32[4]{0:T(128)S(1)}, f32[4]{0:T(128)}, u32[]{:S(2)}) copy-start(f32[4]{0:T(128)} %sink_ref.3) | copy-start | bytes 52
  74.9 31.3 %collective-permute-start.3 = (bf16[4,16,16,512]{3,2,1,0:T(8,128)(2,1)S(1)}, bf16[4,16,16,512]{3,2,1,0:T(8,128)(2,1)S(1)}, u32[]{:S(2)}, u32[]{:S(2)}) collective-permute-start(bf16[4,16,16,512]{3,2,1,0:T(8,128)(2,1)S(1)} %slice.29.refs_4_.refs_2_), channel_id=1, source_target_pairs={{0,4},{4,0},{1,5},{5,1},{2,6},{6,2},{3,7},{7,3},{8,12},{12,8},{9,1... | collective-permute-start | bytes 3145736 | tf_op jit(solution)/shard_map/ppermute | solution.py:39
  92.2 11.2 %collective-permute-start.1 = (bf16[144,128]{1,0:T(8,128)(2,1)S(1)}, bf16[144,128]{1,0:T(8,128)(2,1)S(1)}, u32[]{:S(2)}, u32[]{:S(2)}) collective-permute-start(bf16[144,128]{1,0:T(8,128)(2,1)S(1)} %get-tuple-element.19), channel_id=1, source_target_pairs={{0,4},{4,0},{1,5},{5,1},{2,6},{6,2},{3,7},{7,3},{8,12},{12,8},{9,1... | collective-permute-start | bytes 110600 | tf_op jit(solution)/shard_map/ppermute | solution.py:39
  94.1 9.3 %collective-permute-start.2 = (bf16[144,128]{1,0:T(8,128)(2,1)S(1)}, bf16[144,128]{1,0:T(8,128)(2,1)S(1)}, u32[]{:S(2)}, u32[]{:S(2)}) collective-permute-start(bf16[144,128]{1,0:T(8,128)(2,1)S(1)} %get-tuple-element.20), channel_id=1, source_target_pairs={{4,8},{12,16},{20,24},{28,32},{36,40},{44,48},{52,56},{60,64},{68,... | collective-permute-start | bytes 110600 | tf_op jit(solution)/shard_map/ppermute | solution.py:45
  106.8 31.0 %collective-permute-start.5 = (bf16[512,512]{1,0:T(8,128)(2,1)S(1)}, bf16[512,512]{1,0:T(8,128)(2,1)S(1)}, u32[]{:S(2)}, u32[]{:S(2)}) collective-permute-start(bf16[512,512]{1,0:T(8,128)(2,1)S(1)} %shard_map.111), channel_id=1, source_target_pairs={{0,3},{1,2},{2,1},{3,0},{4,7},{5,6},{6,5},{7,4},{8,11},{9,10},{10,... | collective-permute-start | bytes 1572872 | tf_op jit(solution)/shard_map/ppermute | solution.py:366
  110.4 27.4 %collective-permute-start.4 = (bf16[512,512]{1,0:T(8,128)(2,1)S(1)}, bf16[512,512]{1,0:T(8,128)(2,1)S(1)}, u32[]{:S(2)}, u32[]{:S(2)}) collective-permute-start(bf16[512,512]{1,0:T(8,128)(2,1)S(1)} %shard_map.110), channel_id=1, source_target_pairs={{0,1},{1,0},{2,3},{3,2},{4,5},{5,4},{6,7},{7,6},{8,9},{9,8},{10,11... | collective-permute-start | bytes 1572872 | tf_op jit(solution)/shard_map/ppermute | solution.py:366
  112.7 21.5 %collective-permute-start.6 = (bf16[256,512]{1,0:T(8,128)(2,1)S(1)}, bf16[256,512]{1,0:T(8,128)(2,1)S(1)}, u32[]{:S(2)}, u32[]{:S(2)}) collective-permute-start(bf16[256,512]{1,0:T(8,128)(2,1)S(1)} %shard_map.112), channel_id=1, source_target_pairs={{0,2},{1,3},{2,0},{3,1},{4,6},{5,7},{6,4},{7,5},{8,10},{9,11},{10,... | collective-permute-start | bytes 786440 | tf_op jit(solution)/shard_map/ppermute | solution.py:366
  118.5 28.3 %copy-start.6 = (f32[512]{0:T(512)S(1)}, f32[512]{0:T(512)}, u32[]{:S(2)}) copy-start(f32[512]{0:T(512)} %param.21) | copy-start | bytes 6148
  118.5 19.2 %collective-permute-start.7 = (bf16[256,512]{1,0:T(8,128)(2,1)S(1)}, bf16[256,512]{1,0:T(8,128)(2,1)S(1)}, u32[]{:S(2)}, u32[]{:S(2)}) collective-permute-start(bf16[256,512]{1,0:T(8,128)(2,1)S(1)} %shard_map.113), channel_id=1, source_target_pairs={{0,2},{1,3},{2,0},{3,1},{4,6},{5,7},{6,4},{7,5},{8,10},{9,11},{10,... | collective-permute-start | bytes 786440 | tf_op jit(solution)/shard_map/ppermute | solution.py:366
  137.7 1.3 copy-start.4
  137.7 0.8 copy-start.3

commit v9 on v8

--- a/solution.py
+++ b/solution.py
@@ -21,6 +21,7 @@
 
 epsilon = 1e-05
 masked_score = -1e30
+MASKS = (0, 2, 1, 3)
 nt = (((1,), (1,)), ((), ()))
 
 
@@ -35,8 +36,12 @@
     return jnp.sum(from_everyone(shard, axis), axis=0)
 
 
+def exchanged(shard, axis, mask):
+    return lax.ppermute(shard, axis, [(i, i ^ mask) for i in range(lax.axis_size(axis))])
+
+
 def swapped(shard):
-    return lax.ppermute(shard, CORE, [(0, 1), (1, 0)])
+    return exchanged(shard, CORE, 1)
 
 
 def neighbours(inside, outside):
@@ -45,18 +50,18 @@
     return swapped(inside), lax.ppermute(outside, SP, pairs + [(b, a) for a, b in pairs])
 
 
-def whole_weights(own_ref, other_ref, w_ref, at):
+def whole_weights(own_ref, other_ref, w_ref, at, sources):
     core = lax.axis_index(CORE)
     xs, zs, rows = own_ref.shape[:3]
     lanes = slice(at, at + w_ref.shape[1])
-    for z in range(zs):
-        for x in range(xs):
-            base = (z * xs + x) * 2 * rows
+    for slot, source in enumerate(sources):
+        for z in range(zs):
+            base = (z * xs + source) * 2 * rows
             w_ref[pl.ds(pl.multiple_of(base + core * rows, rows), rows), :] = own_ref[
-                x, z, :, lanes
+                slot, z, :, lanes
             ]
             w_ref[pl.ds(pl.multiple_of(base + (1 - core) * rows, rows), rows), :] = other_ref[
-                x, z, :, lanes
+                slot, z, :, lanes
             ]
 
 
@@ -77,7 +82,7 @@
     tokens_ref, own_ref, other_ref, kv_ref, chan_ref, inside_ref, outside_ref, w_ref
 ):
     rows = tokens_ref.shape[1]
-    whole_weights(own_ref, other_ref, w_ref, 0)
+    whole_weights(own_ref, other_ref, w_ref, 0, range(own_ref.shape[0]))
     kv_cols = kv_ref.shape[1]
     kv_ref[...] = projected(tokens_ref, w_ref, 0, kv_cols)
     chan_ref[...] = projected(tokens_ref, w_ref, kv_cols, chan_ref.shape[1])
@@ -164,7 +169,9 @@
     band_ref,
 ):
     rows, query_cols = query_ref.shape
-    whole_weights(own_ref, other_ref, w_ref, own_ref.shape[3] - query_cols)
+    whole_weights(
+        own_ref, other_ref, w_ref, own_ref.shape[3] - query_cols, range(own_ref.shape[0])
+    )
     query_ref[...] = projected(tokens_ref, w_ref, 0, query_cols)
     split_band(kv_ref[...], band_ref)
     for b in range(1, rows // WINDOW - 1):
@@ -253,7 +260,8 @@
     zs = own_ref.shape[1] // lax.axis_size(TP)
     at = own_ref.shape[3] - hidden_ref.shape[1]
     mine = pl.ds(to * zs, zs)
-    whole_weights(own_ref.at[:, mine], other_ref.at[:, mine], w_ref, at)
+    sources = [lax.axis_index(X) ^ m for m in MASKS]
+    whole_weights(own_ref.at[:, mine], other_ref.at[:, mine], w_ref, at, sources)
     for part in range(count):
         attended_ref, pooled_ref = mixed_refs[2 * part : 2 * part + 2]
         rows, query_cols = attended_ref.shape
@@ -296,8 +304,13 @@
         (w_key, w_value, w_pool_in, w_query, w_out_attn.T, w_out_pool.T), axis=1
     )
     over_z = lax.all_gather(packed, Z, axis=0)
-    over_x = from_everyone(over_z, X)
-    own1, own2 = over_x[..., :in_cols], over_x[..., in_cols:]
+    for_all = jnp.broadcast_to(over_z[..., :in_cols], (lax.axis_size(X), *over_z.shape[:2], in_cols))
+    for_all, piece = lax.optimization_barrier((for_all, over_z[..., in_cols:]))
+    own1 = lax.all_to_all(for_all, X, 0, 0, tiled=True)
+    pieces = [piece]
+    for mask in MASKS[1:]:
+        pieces.append(exchanged(pieces[0], X, mask))
+    own2 = jnp.stack(pieces)
     other1 = swapped(own1)
     other2 = swapped(own2)
 
@@ -362,8 +375,7 @@
 
     def sent(mask, *mixed):
         block = multiplied(mask, *mixed)
-        count = lax.axis_size(TP)
-        return lax.ppermute(block, TP, [(i, i ^ mask) for i in range(count)])
+        return exchanged(block, TP, mask)
 
     far = jnp.concatenate([sent(2, inner), sent(2, outer)])
     partials = [sent(1, inner, outer), sent(3, inner, outer), far]

time: 150 us -> 150 us (level)
  the two profiles are of different devices: /device:TPU:32 before, /device:TPU:1 now
where the time goes in v9:
time: 150 us; the launch traced here: 149 us
  blocking collectives  55.7 us (37%)
  starting transfers between devices  46.2 us (31%)
  waiting for transfers between devices  25.9 us (17%)
  Pallas kernels  14.3 us (10%)
  local copies, waits for them, and re-layouts  3.42 us (2%)
  other arithmetic  3.01 us (2%)
    ppermute x10, starting transfers between devices, exchanged(): lax.ppermute(shard, axis, [(i, i ^ mask) for i in range(lax.axis_size(axi...  39.8 us
    all_gather x1, blocking collectives, layer(): over_z = lax.all_gather(packed, Z, axis=0)  32.1 us
    ppermute x10, waiting for transfers between devices, exchanged(): lax.ppermute(shard, axis, [(i, i ^ mask) for i in range(lax.axis_size(axi...  25.9 us
    all_to_all x1, blocking collectives, layer(): own1 = lax.all_to_all(for_all, X, 0, 0, tiled=True)  15.1 us
    all_to_all x1, blocking collectives, from_everyone(): lax.all_to_all(jnp.broadcast_to(shard[None], (count, *shard.shape)), axis...  8.5 us
    pallas_call x1, Pallas kernels, layer(): pl.pallas_call(functools.partial(inner_kernel, seq_len), out_shape=[rows_...  5.82 us
    all_to_all x1, starting transfers between devices, from_everyone(): lax.all_to_all(jnp.broadcast_to(shard[None], (count, *shard.shape)), axis...  4.46 us
    pallas_call x1, Pallas kernels, layer(): pl.pallas_call(project_kernel, out_shape=[rows_of(2 * key_cols), rows_of(...  3.37 us
  transfers between devices with their start and end apart: 12, of which 5 were waited for; matrix products, arithmetic and copies ran while one was open for 0% of the time, Pallas kernels for 9%

profile of v9, /device:TPU:1, one launch (start us, length us, event | category | flops | bytes accessed | tf_op | source)
XLA Modules:
  0.0 149.0 jit_solution(13812929336356447054)
XLA Ops:
  0.0 0.9 concatenate.9
  0.9 32.1 %all-gather = bf16[256,1152]{1,0:T(8,128)(2,1)S(1)} all-gather(bf16[16,1152]{1,0:T(8,128)(2,1)S(1)} %concatenate.9), channel_id=2, replica_groups=mesh['sp_0'=16,'sp_1'=4,'sp_2'=2,'tp'=4] {'sp_0'}, dimensions={0}, use_global_device_ids=true | all-gather | bytes 626688 | tf_op jit(solution)/shard_map/all_gather | solution.py:306
  33.2 15.1 %all_to_all.15.own_ref = bf16[4,16,16,640]{3,2,1,0:T(8,128)(2,1)S(1)} all-to-all(bf16[4,16,16,640]{3,2,1,0:T(8,128)(2,1)S(1)} %broadcast_in_dim.7), channel_id=1, replica_groups=mesh['sp_0'=16,'sp_1'=4,'sp_2'=2,'tp'=4] {'sp_1'}, dimensions={0} | all-to-all | bytes 2621440 | tf_op jit(solution)/shard_map/all_to_all | solution.py:309
  48.3 1.5 broadcast_in_dim.6
  49.7 4.5 %all-to-all-start = ((bf16[4,512,512]{2,1,0:T(8,128)(2,1)}), bf16[4,512,512]{2,1,0:T(8,128)(2,1)}, u32[]{:S(2)}, u32[]{:S(2)}) async-start(bf16[4,512,512]{2,1,0:T(8,128)(2,1)} %broadcast_in_dim.6), calls=%async_computation | async-start | bytes 4194304 | tf_op jit(solution)/shard_map/all_to_all | solution.py:30
  54.2 11.6 %collective-permute-start = (bf16[4,16,16,640]{3,2,1,0:T(8,128)(2,1)S(1)}, bf16[4,16,16,640]{3,2,1,0:T(8,128)(2,1)}, u32[]{:S(2)}, u32[]{:S(2)}) collective-permute-start(bf16[4,16,16,640]{3,2,1,0:T(8,128)(2,1)S(1)} %all_to_all.15.own_ref), channel_id=1, source_target_pairs={{0,4},{4,0},{1,5},{5,1},{2,6},{6,2},{3,7},{7,3},{8,12},{12,8},{9,1... | collective-permute-start | bytes 3932168 | tf_op jit(solution)/shard_map/ppermute | solution.py:40
  65.8 2.8 %collective-permute-start.5 = (bf16[16,16,512]{2,1,0:T(8,128)(2,1)S(1)}, bf16[16,16,512]{2,1,0:T(8,128)(2,1)S(1)}, u32[]{:S(2)}, u32[]{:S(2)}) collective-permute-start(bf16[16,16,512]{2,1,0:T(8,128)(2,1)S(1)} %slice.29), channel_id=1, source_target_pairs={{0,24},{8,16},{16,8},{24,0},{1,25},{9,17},{17,9},{25,1},{2,26},{10... | collective-permute-start | bytes 786440 | tf_op jit(solution)/shard_map/ppermute | solution.py:40
  68.6 1.9 %collective-permute-start.4 = (bf16[16,16,512]{2,1,0:T(8,128)(2,1)S(1)}, bf16[16,16,512]{2,1,0:T(8,128)(2,1)S(1)}, u32[]{:S(2)}, u32[]{:S(2)}) collective-permute-start(bf16[16,16,512]{2,1,0:T(8,128)(2,1)S(1)} %slice.29), channel_id=1, source_target_pairs={{0,8},{8,0},{16,24},{24,16},{1,9},{9,1},{17,25},{25,17},{2,10},{10... | collective-permute-start | bytes 786440 | tf_op jit(solution)/shard_map/ppermute | solution.py:40
  70.5 4.9 %collective-permute-start.3 = (bf16[16,16,512]{2,1,0:T(8,128)(2,1)S(1)}, bf16[16,16,512]{2,1,0:T(8,128)(2,1)S(1)}, u32[]{:S(2)}, u32[]{:S(2)}) collective-permute-start(bf16[16,16,512]{2,1,0:T(8,128)(2,1)S(1)} %slice.29), channel_id=1, source_target_pairs={{0,16},{8,24},{16,0},{24,8},{1,17},{9,25},{17,1},{25,9},{2,18},{10... | collective-permute-start | bytes 786440 | tf_op jit(solution)/shard_map/ppermute | solution.py:40
  75.4 1.5 collective-permute-done.5
  76.9 1.3 collective-permute-done.4
  78.2 7.0 %collective-permute-done.3 = bf16[16,16,512]{2,1,0:T(8,128)(2,1)S(1)} collective-permute-done((bf16[16,16,512]{2,1,0:T(8,128)(2,1)S(1)}, bf16[16,16,512]{2,1,0:T(8,128)(2,1)S(1)}, u32[]{:S(2)}, u32[]{:S(2)}) %collective-permute-start.3) | collective-permute-done | bytes 262176 | tf_op jit(solution)/shard_map/ppermute | solution.py:40
  85.4 3.2 %collective-permute-start.6 = (bf16[4,16,16,512]{3,2,1,0:T(8,128)(2,1)S(1)}, bf16[4,16,16,512]{3,2,1,0:T(8,128)(2,1)S(1)}, u32[]{:S(2)}, u32[]{:S(2)}) collective-permute-start(bf16[4,16,16,512]{3,2,1,0:T(8,128)(2,1)S(1)} %pad_maximum_fusion.refs_4_.refs_2_), channel_id=1, source_target_pairs={{0,4},{4,0},{1,5},{5,1},{2,6},{6,2},{3,7},{7,3},{8,12},{12,8},{9,1... | collective-permute-start | bytes 3145736 | tf_op jit(solution)/shard_map/ppermute | solution.py:40
  88.6 3.4 %project.1 = (bf16[512,128]{1,0:T(8,128)(2,1)S(1)}, bf16[512,256]{1,0:T(8,128)(2,1)S(1)}, bf16[144,128]{1,0:T(8,128)(2,1)S(1)}, bf16[144,128]{1,0:T(8,128)(2,1)S(1)}) custom-call(bf16[4,512,512]{2,1,0:T(8,128)(2,1)} %all-to-all-done.tokens_ref, bf16[4,16,16,640]{3,2,1,0:T(8,128)(2,1)S(1)} %all_to_all.15.own_ref, ...), custom_call_target="tpu_custom_call" | custom-call | flops 805306368 | bytes 4194304 | tf_op jit(solution)/shard_map/project/pallas_call | solution.py:324
  92.0 1.9 %collective-permute-start.1 = (bf16[144,128]{1,0:T(8,128)(2,1)S(1)}, bf16[144,128]{1,0:T(8,128)(2,1)S(1)}, u32[]{:S(2)}, u32[]{:S(2)}) collective-permute-start(bf16[144,128]{1,0:T(8,128)(2,1)S(1)} %get-tuple-element.22), channel_id=1, source_target_pairs={{0,4},{4,0},{1,5},{5,1},{2,6},{6,2},{3,7},{7,3},{8,12},{12,8},{9,1... | collective-permute-start | bytes 110600 | tf_op jit(solution)/shard_map/ppermute | solution.py:40
  93.9 1.9 %collective-permute-start.2 = (bf16[144,128]{1,0:T(8,128)(2,1)S(1)}, bf16[144,128]{1,0:T(8,128)(2,1)S(1)}, u32[]{:S(2)}, u32[]{:S(2)}) collective-permute-start(bf16[144,128]{1,0:T(8,128)(2,1)S(1)} %get-tuple-element.23), channel_id=1, source_target_pairs={{4,8},{12,16},{20,24},{28,32},{36,40},{44,48},{52,56},{60,64},{68,... | collective-permute-start | bytes 110600 | tf_op jit(solution)/shard_map/ppermute | solution.py:50
  95.8 5.8 %inner.1 = (bf16[512,256]{1,0:T(8,128)(2,1)S(1)}, bf16[256,256]{1,0:T(8,128)(2,1)S(1)}, bf16[256,256]{1,0:T(8,128)(2,1)S(1)}) custom-call(bf16[4,512,512]{2,1,0:T(8,128)(2,1)} %all-to-all-done.tokens_ref, bf16[4,16,16,640]{3,2,1,0:T(8,128)(2,1)S(1)} %all_to_all.15.own_ref, bf16[4,16,16,640]{3,2,1,0:T(8,128)(2,1)} %collective-permute-done.other_ref, ...), custom_call_target="tpu_custom_call" | custom-call | flops 536870912 | bytes 4194304 | tf_op jit(solution)/shard_map/inner/pallas_call | solution.py:337
  101.7 2.8 %outer.1 = (bf16[256,256]{1,0:T(8,128)(2,1)S(1)}, bf16[256,256]{1,0:T(8,128)(2,1)S(1)}) custom-call(bf16[512,256]{1,0:T(8,128)(2,1)S(1)} %get-tuple-element.21.query_ref, bf16[512,128]{1,0:T(8,128)(2,1)S(1)} %get-tuple-element.17.kv_ref, bf16[512,256]{1,0:T(8,128)(2,1)S(1)} %get-tuple-element.18.chan_ref, ...), custom_call_target="tpu_custom_call" | custom-call | flops 536870912 | bytes 2097152 | tf_op jit(solution)/shard_map/outer/pallas_call | solution.py:350
  104.5 0.5 shard_map.111
  105.0 4.9 %collective-permute-start.8 = (bf16[512,512]{1,0:T(8,128)(2,1)S(1)}, bf16[512,512]{1,0:T(8,128)(2,1)S(1)}, u32[]{:S(2)}, u32[]{:S(2)}) collective-permute-start(bf16[512,512]{1,0:T(8,128)(2,1)S(1)} %shard_map.111), channel_id=1, source_target_pairs={{0,3},{1,2},{2,1},{3,0},{4,7},{5,6},{6,5},{7,4},{8,11},{9,10},{10,... | collective-permute-start | bytes 1572872 | tf_op jit(solution)/shard_map/ppermute | solution.py:40
  109.9 0.5 shard_map.110
  110.4 1.9 %collective-permute-start.7 = (bf16[512,512]{1,0:T(8,128)(2,1)S(1)}, bf16[512,512]{1,0:T(8,128)(2,1)S(1)}, u32[]{:S(2)}, u32[]{:S(2)}) collective-permute-start(bf16[512,512]{1,0:T(8,128)(2,1)S(1)} %shard_map.110), channel_id=1, source_target_pairs={{0,1},{1,0},{2,3},{3,2},{4,5},{5,4},{6,7},{7,6},{8,9},{9,8},{10,11... | collective-permute-start | bytes 1572872 | tf_op jit(solution)/shard_map/ppermute | solution.py:40
  112.7 3.1 %collective-permute-start.9 = (bf16[256,512]{1,0:T(8,128)(2,1)S(1)}, bf16[256,512]{1,0:T(8,128)(2,1)S(1)}, u32[]{:S(2)}, u32[]{:S(2)}) collective-permute-start(bf16[256,512]{1,0:T(8,128)(2,1)S(1)} %shard_map.112), channel_id=1, source_target_pairs={{0,2},{1,3},{2,0},{3,1},{4,6},{5,7},{6,4},{7,5},{8,10},{9,11},{10,... | collective-permute-start | bytes 786440 | tf_op jit(solution)/shard_map/ppermute | solution.py:40
  116.2 3.7 %collective-permute-start.10 = (bf16[256,512]{1,0:T(8,128)(2,1)S(1)}, bf16[256,512]{1,0:T(8,128)(2,1)S(1)}, u32[]{:S(2)}, u32[]{:S(2)}) collective-permute-start(bf16[256,512]{1,0:T(8,128)(2,1)S(1)} %shard_map.113), channel_id=1, source_target_pairs={{0,2},{1,3},{2,0},{3,1},{4,6},{5,7},{6,4},{7,5},{8,10},{9,11},{10,... | collective-permute-start | bytes 786440 | tf_op jit(solution)/shard_map/ppermute | solution.py:40
  119.9 0.5 shard_map.109
  120.5 11.1 %collective-permute-done.9 = bf16[256,512]{1,0:T(8,128)(2,1)S(1)} collective-permute-done((bf16[256,512]{1,0:T(8,128)(2,1)S(1)}, bf16[256,512]{1,0:T(8,128)(2,1)S(1)}, u32[]{:S(2)}, u32[]{:S(2)}) %collective-permute-start.9) | collective-permute-done | bytes 262176 | tf_op jit(solution)/shard_map/ppermute | solution.py:40
  131.6 5.0 %collective-permute-done.10 = bf16[256,512]{1,0:T(8,128)(2,1)S(1)} collective-permute-done((bf16[256,512]{1,0:T(8,128)(2,1)S(1)}, bf16[256,512]{1,0:T(8,128)(2,1)S(1)}, u32[]{:S(2)}, u32[]{:S(2)}) %collective-permute-start.10) | collective-permute-done | bytes 262176 | tf_op jit(solution)/shard_map/ppermute | solution.py:40
  136.7 0.8 copy-done.3
  137.5 0.4 fusion
  138.0 8.5 %all_to_all.16 = f32[4,2,512]{2,1,0:T(2,128)S(1)} all-to-all(f32[4,2,512]{2,1,0:T(2,128)S(1)} %broadcast_in_dim.8), channel_id=1, replica_groups=mesh['sp_0'=16,'sp_1'=4,'sp_2'=2,'tp'=4] {'tp'}, dimensions={0} | all-to-all | bytes 32768 | tf_op jit(solution)/shard_map/all_to_all | solution.py:30
  146.5 1.6 %multiply_convert_fusion = bf16[512,512]{1,0:T(8,128)(2,1)S(1)} fusion(f32[512]{0:T(512)S(1)} %copy-done.7, f32[512]{0:T(512)S(1)} %add_rsqrt_fusion, f32[512]{0:T(512)S(1)} %bitcast.21, bf16[256,512]{1,0:T(8,128)(2,1)} %copy-done.5, bf16[256,512]{1,0:T(8,128)(2,1)} %copy-done.4, bf16[512,512]{1,0:T(8,128)(2,1)S(1)} %collective-permute-done.8, ...), kind=kLoop, calls=%fused_computation.1 | loop fusion | flops 3670016 | bytes 2627584 | tf_op jit(solution)/shard_map/convert_element_type | solution.py:390
  148.1 0.8 pad_maximum_fusion.1
  (35 shorter events, 1.2 us)
Async XLA Ops:
  33.2 15.1 %copy-start.6 = (bf16[512,512]{1,0:T(8,128)(2,1)S(1)}, bf16[512,512]{1,0:T(8,128)(2,1)}, u32[]{:S(2)}) copy-start(bf16[512,512]{1,0:T(8,128)(2,1)} %param.11) | copy-start | bytes 1572868
  49.7 38.8 %all-to-all-start = ((bf16[4,512,512]{2,1,0:T(8,128)(2,1)}), bf16[4,512,512]{2,1,0:T(8,128)(2,1)}, u32[]{:S(2)}, u32[]{:S(2)}) async-start(bf16[4,512,512]{2,1,0:T(8,128)(2,1)} %broadcast_in_dim.6), calls=%async_computation | async-start | bytes 4194304 | tf_op jit(solution)/shard_map/all_to_all | solution.py:30
  54.2 34.4 %collective-permute-start = (bf16[4,16,16,640]{3,2,1,0:T(8,128)(2,1)S(1)}, bf16[4,16,16,640]{3,2,1,0:T(8,128)(2,1)}, u32[]{:S(2)}, u32[]{:S(2)}) collective-permute-start(bf16[4,16,16,640]{3,2,1,0:T(8,128)(2,1)S(1)} %all_to_all.15.own_ref), channel_id=1, source_target_pairs={{0,4},{4,0},{1,5},{5,1},{2,6},{6,2},{3,7},{7,3},{8,12},{12,8},{9,1... | collective-permute-start | bytes 3932168 | tf_op jit(solution)/shard_map/ppermute | solution.py:40
  65.8 11.1 %collective-permute-start.5 = (bf16[16,16,512]{2,1,0:T(8,128)(2,1)S(1)}, bf16[16,16,512]{2,1,0:T(8,128)(2,1)S(1)}, u32[]{:S(2)}, u32[]{:S(2)}) collective-permute-start(bf16[16,16,512]{2,1,0:T(8,128)(2,1)S(1)} %slice.29), channel_id=1, source_target_pairs={{0,24},{8,16},{16,8},{24,0},{1,25},{9,17},{17,9},{25,1},{2,26},{10... | collective-permute-start | bytes 786440 | tf_op jit(solution)/shard_map/ppermute | solution.py:40
  68.6 9.6 %collective-permute-start.4 = (bf16[16,16,512]{2,1,0:T(8,128)(2,1)S(1)}, bf16[16,16,512]{2,1,0:T(8,128)(2,1)S(1)}, u32[]{:S(2)}, u32[]{:S(2)}) collective-permute-start(bf16[16,16,512]{2,1,0:T(8,128)(2,1)S(1)} %slice.29), channel_id=1, source_target_pairs={{0,8},{8,0},{16,24},{24,16},{1,9},{9,1},{17,25},{25,17},{2,10},{10... | collective-permute-start | bytes 786440 | tf_op jit(solution)/shard_map/ppermute | solution.py:40
  70.5 14.7 %collective-permute-start.3 = (bf16[16,16,512]{2,1,0:T(8,128)(2,1)S(1)}, bf16[16,16,512]{2,1,0:T(8,128)(2,1)S(1)}, u32[]{:S(2)}, u32[]{:S(2)}) collective-permute-start(bf16[16,16,512]{2,1,0:T(8,128)(2,1)S(1)} %slice.29), channel_id=1, source_target_pairs={{0,16},{8,24},{16,0},{24,8},{1,17},{9,25},{17,1},{25,9},{2,18},{10... | collective-permute-start | bytes 786440 | tf_op jit(solution)/shard_map/ppermute | solution.py:40
  85.3 10.5 %copy-start = (bf16[1,256,256]{2,1,0:T(8,128)(2,1)S(1)}, bf16[1,256,256]{2,1,0:T(8,128)(2,1)}, u32[]{:S(2)}) copy-start(bf16[1,256,256]{2,1,0:T(8,128)(2,1)} %w_pool_ref.3) | copy-start | bytes 393220
  85.3 10.5 %copy-start.1 = (f32[256]{0:T(256)S(1)}, f32[256]{0:T(256)}, u32[]{:S(2)}) copy-start(f32[256]{0:T(256)} %param.18) | copy-start | bytes 3076
  85.3 10.5 %copy-start.2 = (f32[4]{0:T(128)S(1)}, f32[4]{0:T(128)}, u32[]{:S(2)}) copy-start(f32[4]{0:T(128)} %sink_ref.3) | copy-start | bytes 52
  85.4 19.1 %collective-permute-start.6 = (bf16[4,16,16,512]{3,2,1,0:T(8,128)(2,1)S(1)}, bf16[4,16,16,512]{3,2,1,0:T(8,128)(2,1)S(1)}, u32[]{:S(2)}, u32[]{:S(2)}) collective-permute-start(bf16[4,16,16,512]{3,2,1,0:T(8,128)(2,1)S(1)} %pad_maximum_fusion.refs_4_.refs_2_), channel_id=1, source_target_pairs={{0,4},{4,0},{1,5},{5,1},{2,6},{6,2},{3,7},{7,3},{8,12},{12,8},{9,1... | collective-permute-start | bytes 3145736 | tf_op jit(solution)/shard_map/ppermute | solution.py:40
  92.0 9.7 %collective-permute-start.1 = (bf16[144,128]{1,0:T(8,128)(2,1)S(1)}, bf16[144,128]{1,0:T(8,128)(2,1)S(1)}, u32[]{:S(2)}, u32[]{:S(2)}) collective-permute-start(bf16[144,128]{1,0:T(8,128)(2,1)S(1)} %get-tuple-element.22), channel_id=1, source_target_pairs={{0,4},{4,0},{1,5},{5,1},{2,6},{6,2},{3,7},{7,3},{8,12},{12,8},{9,1... | collective-permute-start | bytes 110600 | tf_op jit(solution)/shard_map/ppermute | solution.py:40
  93.9 7.8 %collective-permute-start.2 = (bf16[144,128]{1,0:T(8,128)(2,1)S(1)}, bf16[144,128]{1,0:T(8,128)(2,1)S(1)}, u32[]{:S(2)}, u32[]{:S(2)}) collective-permute-start(bf16[144,128]{1,0:T(8,128)(2,1)S(1)} %get-tuple-element.23), channel_id=1, source_target_pairs={{4,8},{12,16},{20,24},{28,32},{36,40},{44,48},{52,56},{60,64},{68,... | collective-permute-start | bytes 110600 | tf_op jit(solution)/shard_map/ppermute | solution.py:50
  105.0 31.6 %collective-permute-start.8 = (bf16[512,512]{1,0:T(8,128)(2,1)S(1)}, bf16[512,512]{1,0:T(8,128)(2,1)S(1)}, u32[]{:S(2)}, u32[]{:S(2)}) collective-permute-start(bf16[512,512]{1,0:T(8,128)(2,1)S(1)} %shard_map.111), channel_id=1, source_target_pairs={{0,3},{1,2},{2,1},{3,0},{4,7},{5,6},{6,5},{7,4},{8,11},{9,10},{10,... | collective-permute-start | bytes 1572872 | tf_op jit(solution)/shard_map/ppermute | solution.py:40
  110.4 26.2 %collective-permute-start.7 = (bf16[512,512]{1,0:T(8,128)(2,1)S(1)}, bf16[512,512]{1,0:T(8,128)(2,1)S(1)}, u32[]{:S(2)}, u32[]{:S(2)}) collective-permute-start(bf16[512,512]{1,0:T(8,128)(2,1)S(1)} %shard_map.110), channel_id=1, source_target_pairs={{0,1},{1,0},{2,3},{3,2},{4,5},{5,4},{6,7},{7,6},{8,9},{9,8},{10,11... | collective-permute-start | bytes 1572872 | tf_op jit(solution)/shard_map/ppermute | solution.py:40
  112.7 18.9 %collective-permute-start.9 = (bf16[256,512]{1,0:T(8,128)(2,1)S(1)}, bf16[256,512]{1,0:T(8,128)(2,1)S(1)}, u32[]{:S(2)}, u32[]{:S(2)}) collective-permute-start(bf16[256,512]{1,0:T(8,128)(2,1)S(1)} %shard_map.112), channel_id=1, source_target_pairs={{0,2},{1,3},{2,0},{3,1},{4,6},{5,7},{6,4},{7,5},{8,10},{9,11},{10,... | collective-permute-start | bytes 786440 | tf_op jit(solution)/shard_map/ppermute | solution.py:40
  116.2 20.4 %collective-permute-start.10 = (bf16[256,512]{1,0:T(8,128)(2,1)S(1)}, bf16[256,512]{1,0:T(8,128)(2,1)S(1)}, u32[]{:S(2)}, u32[]{:S(2)}) collective-permute-start(bf16[256,512]{1,0:T(8,128)(2,1)S(1)} %shard_map.113), channel_id=1, source_target_pairs={{0,2},{1,3},{2,0},{3,1},{4,6},{5,7},{6,4},{7,5},{8,10},{9,11},{10,... | collective-permute-start | bytes 786440 | tf_op jit(solution)/shard_map/ppermute | solution.py:40
  120.5 26.0 %copy-start.7 = (f32[512]{0:T(512)S(1)}, f32[512]{0:T(512)}, u32[]{:S(2)}) copy-start(f32[512]{0:T(512)} %param.21) | copy-start | bytes 6148
  131.6 6.3 %copy-start.4 = (bf16[256,512]{1,0:T(8,128)(2,1)}, bf16[256,512]{1,0:T(8,128)(2,1)S(1)}, u32[]{:S(2)}) copy-start(bf16[256,512]{1,0:T(8,128)(2,1)S(1)} %collective-permute-done.9) | copy-start | bytes 786436
  136.6 1.3 copy-start.5
  136.6 0.8 copy-start.3

commit v10 on v8

--- a/solution.py
+++ b/solution.py
@@ -21,6 +21,7 @@
 
 epsilon = 1e-05
 masked_score = -1e30
+MASKS = (0, 2, 1, 3)
 nt = (((1,), (1,)), ((), ()))
 
 
@@ -35,8 +36,12 @@
     return jnp.sum(from_everyone(shard, axis), axis=0)
 
 
+def exchanged(shard, axis, mask):
+    return lax.ppermute(shard, axis, [(i, i ^ mask) for i in range(lax.axis_size(axis))])
+
+
 def swapped(shard):
-    return lax.ppermute(shard, CORE, [(0, 1), (1, 0)])
+    return exchanged(shard, CORE, 1)
 
 
 def neighbours(inside, outside):
@@ -60,27 +65,26 @@
             ]
 
 
-def projected(tokens_ref, w_ref, at, width):
-    depth = tokens_ref.shape[2]
+def projected(tokens_refs, w_ref, at, width):
+    depth = tokens_refs[0].shape[1]
     total = None
-    for p in range(tokens_ref.shape[0]):
+    for mask, tokens_ref in zip(MASKS, tokens_refs):
+        features = pl.ds(pl.multiple_of((lax.axis_index(TP) ^ mask) * depth, depth), depth)
         part = jnp.dot(
-            tokens_ref[p],
-            w_ref[p * depth : (p + 1) * depth, at : at + width],
-            preferred_element_type=F32,
+            tokens_ref[...], w_ref[features, at : at + width], preferred_element_type=F32
         )
         total = part if total is None else total + part
     return total.astype(BF16)
 
 
-def project_kernel(
-    tokens_ref, own_ref, other_ref, kv_ref, chan_ref, inside_ref, outside_ref, w_ref
-):
-    rows = tokens_ref.shape[1]
+def project_kernel(*refs):
+    tokens_refs = refs[: len(MASKS)]
+    own_ref, other_ref, kv_ref, chan_ref, inside_ref, outside_ref, w_ref = refs[len(MASKS) :]
+    rows = kv_ref.shape[0]
     whole_weights(own_ref, other_ref, w_ref, 0)
     kv_cols = kv_ref.shape[1]
-    kv_ref[...] = projected(tokens_ref, w_ref, 0, kv_cols)
-    chan_ref[...] = projected(tokens_ref, w_ref, kv_cols, chan_ref.shape[1])
+    kv_ref[...] = projected(tokens_refs, w_ref, 0, kv_cols)
+    chan_ref[...] = projected(tokens_refs, w_ref, kv_cols, chan_ref.shape[1])
 
     def rim(kv_at, chan_at):
         edge = chan_ref[chan_at : chan_at + RIM].astype(F32)
@@ -147,25 +151,13 @@
     return (pooled * scale_ref[...]).astype(BF16)
 
 
-def inner_kernel(
-    seq_len,
-    tokens_ref,
-    own_ref,
-    other_ref,
-    kv_ref,
-    chan_ref,
-    sink_ref,
-    w_pool_ref,
-    scale_ref,
-    query_ref,
-    attended_ref,
-    pooled_ref,
-    w_ref,
-    band_ref,
-):
+def inner_kernel(seq_len, *refs):
+    tokens_refs = refs[: len(MASKS)]
+    own_ref, other_ref, kv_ref, chan_ref, sink_ref, w_pool_ref, scale_ref = refs[len(MASKS) : -5]
+    query_ref, attended_ref, pooled_ref, w_ref, band_ref = refs[-5:]
     rows, query_cols = query_ref.shape
     whole_weights(own_ref, other_ref, w_ref, own_ref.shape[3] - query_cols)
-    query_ref[...] = projected(tokens_ref, w_ref, 0, query_cols)
+    query_ref[...] = projected(tokens_refs, w_ref, 0, query_cols)
     split_band(kv_ref[...], band_ref)
     for b in range(1, rows // WINDOW - 1):
         attend_block(
@@ -291,7 +283,9 @@
     share = out_gain.shape[0]
     model_width = share * lax.axis_size(TP)
 
-    gathered = from_everyone(tokens, TP)
+    gathered = [tokens]
+    for mask in MASKS[1:]:
+        gathered.append(exchanged(tokens, TP, mask))
     packed = jnp.concatenate(
         (w_key, w_value, w_pool_in, w_query, w_out_attn.T, w_out_pool.T), axis=1
     )
@@ -311,20 +305,20 @@
     kv, chan, inside, outside = pl.pallas_call(
         project_kernel,
         out_shape=[rows_of(2 * key_cols), rows_of(chan_cols), rim_shape, rim_shape],
-        in_specs=[VMEM] * 3,
+        in_specs=[VMEM] * 6,
         out_specs=[VMEM] * 4,
         scratch_shapes=[pltpu.VMEM((model_width, 2 * key_cols + chan_cols), BF16)],
         compiler_params=LIMIT,
         cost_estimate=cost(2 * rows * model_width * (in_cols - query_cols), 4 << 20),
         name="project",
-    )(gathered, own1, other1)
+    )(*gathered, own1, other1)
     inside, outside = neighbours(inside, outside)
     half = rows // 2
     scale = pool_scale.reshape(1, -1)
     query, *inner = pl.pallas_call(
         functools.partial(inner_kernel, seq_len),
         out_shape=[rows_of(query_cols), rows_of(query_cols, half), rows_of(chan_cols, half)],
-        in_specs=[VMEM] * 5 + [SMEM] + [VMEM] * 2,
+        in_specs=[VMEM] * 8 + [SMEM] + [VMEM] * 2,
         out_specs=[VMEM] * 3,
         scratch_shapes=[
             pltpu.VMEM((model_width, query_cols), BF16),
@@ -333,7 +327,7 @@
         compiler_params=LIMIT,
         cost_estimate=cost(2 * rows * model_width * query_cols, 4 << 20),
         name="inner",
-    )(gathered, own1, other1, kv, chan, sink, w_pool, scale)
+    )(*gathered, own1, other1, kv, chan, sink, w_pool, scale)
     outer = pl.pallas_call(
         functools.partial(outer_kernel, seq_len),
         out_shape=[rows_of(query_cols, half), rows_of(chan_cols, half)],
@@ -362,8 +356,7 @@
 
     def sent(mask, *mixed):
         block = multiplied(mask, *mixed)
-        count = lax.axis_size(TP)
-        return lax.ppermute(block, TP, [(i, i ^ mask) for i in range(count)])
+        return exchanged(block, TP, mask)
 
     far = jnp.concatenate([sent(2, inner), sent(2, outer)])
     partials = [sent(1, inner, outer), sent(3, inner, outer), far]

time: 150 us -> 157 us (1.047)
  the two profiles are of different devices: /device:TPU:32 before, /device:TPU:4 now
where the time goes in v10:
time: 157 us; the launch traced here: 156 us
  blocking collectives  71.7 us (46%)
  waiting for transfers between devices  35.5 us (23%)
  starting transfers between devices  34.9 us (22%)
  Pallas kernels  11 us (7%)
  other arithmetic  1.67 us (1%)
    all_gather x1, blocking collectives, layer(): over_z = lax.all_gather(packed, Z, axis=0)  38.9 us
    ppermute x10, waiting for transfers between devices, exchanged(): lax.ppermute(shard, axis, [(i, i ^ mask) for i in range(lax.axis_size(axi...  35.5 us
    all_to_all x2, blocking collectives, from_everyone(): lax.all_to_all(jnp.broadcast_to(shard[None], (count, *shard.shape)), axis...  32.8 us
    ppermute x10, starting transfers between devices, exchanged(): lax.ppermute(shard, axis, [(i, i ^ mask) for i in range(lax.axis_size(axi...  31.1 us
    pallas_call x1, Pallas kernels, layer(): pl.pallas_call(functools.partial(inner_kernel, seq_len), out_shape=[rows_...  4.41 us
    ppermute x1, starting transfers between devices, neighbours(): lax.ppermute(outside, SP, pairs + [(b, a) for a, b in pairs])  3.83 us
  transfers between devices with their start and end apart: 11, of which 6 were waited for; matrix products, arithmetic and copies ran while one was open for 0% of the time, Pallas kernels for 7%

profile of v10, /device:TPU:4, one launch (start us, length us, event | category | flops | bytes accessed | tf_op | source)
XLA Modules:
  0.0 156.4 jit_solution(17559806014708148927)
XLA Ops:
  0.0 0.9 concatenate.9
  0.9 38.9 %all-gather = bf16[256,1152]{1,0:T(8,128)(2,1)S(1)} all-gather(bf16[16,1152]{1,0:T(8,128)(2,1)S(1)} %concatenate.9), channel_id=2, replica_groups=mesh['sp_0'=16,'sp_1'=4,'sp_2'=2,'tp'=4] {'sp_0'}, dimensions={0}, use_global_device_ids=true | all-gather | bytes 626688 | tf_op jit(solution)/shard_map/all_gather | solution.py:292
  39.9 23.5 %all_to_all.10 = bf16[4,16,16,1152]{3,2,1,0:T(8,128)(2,1)S(1)} all-to-all(bf16[4,16,16,1152]{3,2,1,0:T(8,128)(2,1)S(1)} %broadcast_in_dim.4), channel_id=1, replica_groups=mesh['sp_0'=16,'sp_1'=4,'sp_2'=2,'tp'=4] {'sp_1'}, dimensions={0} | all-to-all | bytes 4718592 | tf_op jit(solution)/shard_map/all_to_all | solution.py:30
  63.5 2.1 %collective-permute-start.3 = (bf16[4,16,16,640]{3,2,1,0:T(8,128)(2,1)S(1)}, bf16[4,16,16,640]{3,2,1,0:T(8,128)(2,1)S(1)}, u32[]{:S(2)}, u32[]{:S(2)}) collective-permute-start(bf16[4,16,16,640]{3,2,1,0:T(8,128)(2,1)S(1)} %slice.28.refs_4_), channel_id=1, source_target_pairs={{0,4},{4,0},{1,5},{5,1},{2,6},{6,2},{3,7},{7,3},{8,12},{12,8},{9,1... | collective-permute-start | bytes 3932168 | tf_op jit(solution)/shard_map/ppermute | solution.py:40
  65.7 2.5 %collective-permute-start.6 = (bf16[4,16,16,512]{3,2,1,0:T(8,128)(2,1)S(1)}, bf16[4,16,16,512]{3,2,1,0:T(8,128)(2,1)S(1)}, u32[]{:S(2)}, u32[]{:S(2)}) collective-permute-start(bf16[4,16,16,512]{3,2,1,0:T(8,128)(2,1)S(1)} %slice.29.refs_4_.refs_2_), channel_id=1, source_target_pairs={{0,4},{4,0},{1,5},{5,1},{2,6},{6,2},{3,7},{7,3},{8,12},{12,8},{9,1... | collective-permute-start | bytes 3145736 | tf_op jit(solution)/shard_map/ppermute | solution.py:40
  68.3 4.9 %collective-permute-start.2 = (bf16[512,512]{1,0:T(8,128)(2,1)S(1)}, bf16[512,512]{1,0:T(8,128)(2,1)S(1)}, u32[]{:S(2)}, u32[]{:S(2)}) collective-permute-start(bf16[512,512]{1,0:T(8,128)(2,1)S(1)} %copy-done), channel_id=1, source_target_pairs={{0,3},{1,2},{2,1},{3,0},{4,7},{5,6},{6,5},{7,4},{8,11},{9,10},{10,... | collective-permute-start | bytes 1572872 | tf_op jit(solution)/shard_map/ppermute | solution.py:40
  73.2 2.0 %collective-permute-start.1 = (bf16[512,512]{1,0:T(8,128)(2,1)S(1)}, bf16[512,512]{1,0:T(8,128)(2,1)S(1)}, u32[]{:S(2)}, u32[]{:S(2)}) collective-permute-start(bf16[512,512]{1,0:T(8,128)(2,1)S(1)} %copy-done), channel_id=1, source_target_pairs={{0,1},{1,0},{2,3},{3,2},{4,5},{5,4},{6,7},{7,6},{8,9},{9,8},{10,11... | collective-permute-start | bytes 1572872 | tf_op jit(solution)/shard_map/ppermute | solution.py:40
  75.3 3.5 %collective-permute-start = (bf16[512,512]{1,0:T(8,128)(2,1)S(1)}, bf16[512,512]{1,0:T(8,128)(2,1)S(1)}, u32[]{:S(2)}, u32[]{:S(2)}) collective-permute-start(bf16[512,512]{1,0:T(8,128)(2,1)S(1)} %copy-done), channel_id=1, source_target_pairs={{0,2},{1,3},{2,0},{3,1},{4,6},{5,7},{6,4},{7,5},{8,10},{9,11},{10,... | collective-permute-start | bytes 1572872 | tf_op jit(solution)/shard_map/ppermute | solution.py:40
  78.7 6.6 %collective-permute-done.2.refs_3_ = bf16[512,512]{1,0:T(8,128)(2,1)S(1)} collective-permute-done((bf16[512,512]{1,0:T(8,128)(2,1)S(1)}, bf16[512,512]{1,0:T(8,128)(2,1)S(1)}, u32[]{:S(2)}, u32[]{:S(2)}) %collective-permute-start.2) | collective-permute-done | bytes 524320 | tf_op jit(solution)/shard_map/ppermute | solution.py:40
  85.3 4.6 %collective-permute-done.1.refs_2_ = bf16[512,512]{1,0:T(8,128)(2,1)S(1)} collective-permute-done((bf16[512,512]{1,0:T(8,128)(2,1)S(1)}, bf16[512,512]{1,0:T(8,128)(2,1)S(1)}, u32[]{:S(2)}, u32[]{:S(2)}) %collective-permute-start.1) | collective-permute-done | bytes 524320 | tf_op jit(solution)/shard_map/ppermute | solution.py:40
  89.9 9.7 %collective-permute-done.refs_1_ = bf16[512,512]{1,0:T(8,128)(2,1)S(1)} collective-permute-done((bf16[512,512]{1,0:T(8,128)(2,1)S(1)}, bf16[512,512]{1,0:T(8,128)(2,1)S(1)}, u32[]{:S(2)}, u32[]{:S(2)}) %collective-permute-start) | collective-permute-done | bytes 524320 | tf_op jit(solution)/shard_map/ppermute | solution.py:40
  99.6 1.4 project.1
  101.1 1.9 %collective-permute-start.4 = (bf16[144,128]{1,0:T(8,128)(2,1)S(1)}, bf16[144,128]{1,0:T(8,128)(2,1)S(1)}, u32[]{:S(2)}, u32[]{:S(2)}) collective-permute-start(bf16[144,128]{1,0:T(8,128)(2,1)S(1)} %get-tuple-element.19), channel_id=1, source_target_pairs={{0,4},{4,0},{1,5},{5,1},{2,6},{6,2},{3,7},{7,3},{8,12},{12,8},{9,1... | collective-permute-start | bytes 110600 | tf_op jit(solution)/shard_map/ppermute | solution.py:40
  103.0 3.8 %collective-permute-start.5 = (bf16[144,128]{1,0:T(8,128)(2,1)S(1)}, bf16[144,128]{1,0:T(8,128)(2,1)S(1)}, u32[]{:S(2)}, u32[]{:S(2)}) collective-permute-start(bf16[144,128]{1,0:T(8,128)(2,1)S(1)} %get-tuple-element.20), channel_id=1, source_target_pairs={{4,8},{12,16},{20,24},{28,32},{36,40},{44,48},{52,56},{60,64},{68,... | collective-permute-start | bytes 110600 | tf_op jit(solution)/shard_map/ppermute | solution.py:50
  106.8 4.4 %inner.1 = (bf16[512,256]{1,0:T(8,128)(2,1)S(1)}, bf16[256,256]{1,0:T(8,128)(2,1)S(1)}, bf16[256,256]{1,0:T(8,128)(2,1)S(1)}) custom-call(bf16[512,512]{1,0:T(8,128)(2,1)S(1)} %copy-done, bf16[512,512]{1,0:T(8,128)(2,1)S(1)} %collective-permute-done.refs_1_, bf16[512,512]{1,0:T(8,128)(2,1)S(1)} %collective-permute-done.1.refs_2_, ...), custom_call_target="tpu_custom_call" | custom-call | flops 536870912 | bytes 4194304 | tf_op jit(solution)/shard_map/inner/pallas_call | solution.py:318
  111.3 2.8 %outer.1 = (bf16[256,256]{1,0:T(8,128)(2,1)S(1)}, bf16[256,256]{1,0:T(8,128)(2,1)S(1)}) custom-call(bf16[512,256]{1,0:T(8,128)(2,1)S(1)} %get-tuple-element.18.query_ref, bf16[512,128]{1,0:T(8,128)(2,1)S(1)} %get-tuple-element.14.refs_6_.kv_ref, bf16[512,256]{1,0:T(8,128)(2,1)S(1)} %get-tuple-element.15.refs_7_.chan_ref, ...), custom_call_target="tpu_custom_call" | custom-call | flops 536870912 | bytes 2097152 | tf_op jit(solution)/shard_map/outer/pallas_call | solution.py:331
  114.1 0.5 shard_map.110
  114.6 2.2 %collective-permute-start.7 = (bf16[512,512]{1,0:T(8,128)(2,1)S(1)}, bf16[512,512]{1,0:T(8,128)(2,1)S(1)}, u32[]{:S(2)}, u32[]{:S(2)}) collective-permute-start(bf16[512,512]{1,0:T(8,128)(2,1)S(1)} %shard_map.110), channel_id=1, source_target_pairs={{0,1},{1,0},{2,3},{3,2},{4,5},{5,4},{6,7},{7,6},{8,9},{9,8},{10,11... | collective-permute-start | bytes 1572872 | tf_op jit(solution)/shard_map/ppermute | solution.py:40
  116.8 0.5 shard_map.111
  117.4 4.6 %collective-permute-start.8 = (bf16[512,512]{1,0:T(8,128)(2,1)S(1)}, bf16[512,512]{1,0:T(8,128)(2,1)S(1)}, u32[]{:S(2)}, u32[]{:S(2)}) collective-permute-start(bf16[512,512]{1,0:T(8,128)(2,1)S(1)} %shard_map.111), channel_id=1, source_target_pairs={{0,3},{1,2},{2,1},{3,0},{4,7},{5,6},{6,5},{7,4},{8,11},{9,10},{10,... | collective-permute-start | bytes 1572872 | tf_op jit(solution)/shard_map/ppermute | solution.py:40
  121.9 0.4 shard_map.112
  122.3 3.4 %collective-permute-start.9 = (bf16[256,512]{1,0:T(8,128)(2,1)S(1)}, bf16[256,512]{1,0:T(8,128)(2,1)S(1)}, u32[]{:S(2)}, u32[]{:S(2)}) collective-permute-start(bf16[256,512]{1,0:T(8,128)(2,1)S(1)} %shard_map.112), channel_id=1, source_target_pairs={{0,2},{1,3},{2,0},{3,1},{4,6},{5,7},{6,4},{7,5},{8,10},{9,11},{10,... | collective-permute-start | bytes 786440 | tf_op jit(solution)/shard_map/ppermute | solution.py:40
  125.7 0.4 shard_map.113
  126.1 4.0 %collective-permute-start.10 = (bf16[256,512]{1,0:T(8,128)(2,1)S(1)}, bf16[256,512]{1,0:T(8,128)(2,1)S(1)}, u32[]{:S(2)}, u32[]{:S(2)}) collective-permute-start(bf16[256,512]{1,0:T(8,128)(2,1)S(1)} %shard_map.113), channel_id=1, source_target_pairs={{0,2},{1,3},{2,0},{3,1},{4,6},{5,7},{6,4},{7,5},{8,10},{9,11},{10,... | collective-permute-start | bytes 786440 | tf_op jit(solution)/shard_map/ppermute | solution.py:40
  130.1 0.5 shard_map.109
  130.6 8.8 %collective-permute-done.9 = bf16[256,512]{1,0:T(8,128)(2,1)S(1)} collective-permute-done((bf16[256,512]{1,0:T(8,128)(2,1)S(1)}, bf16[256,512]{1,0:T(8,128)(2,1)S(1)}, u32[]{:S(2)}, u32[]{:S(2)}) %collective-permute-start.9) | collective-permute-done | bytes 262176 | tf_op jit(solution)/shard_map/ppermute | solution.py:40
  139.4 4.7 %collective-permute-done.10 = bf16[256,512]{1,0:T(8,128)(2,1)S(1)} collective-permute-done((bf16[256,512]{1,0:T(8,128)(2,1)S(1)}, bf16[256,512]{1,0:T(8,128)(2,1)S(1)}, u32[]{:S(2)}, u32[]{:S(2)}) %collective-permute-start.10) | collective-permute-done | bytes 262176 | tf_op jit(solution)/shard_map/ppermute | solution.py:40
  144.1 1.2 collective-permute-done.8
  145.3 0.4 fusion
  145.7 9.4 %all_to_all.11 = f32[4,2,512]{2,1,0:T(2,128)S(1)} all-to-all(f32[4,2,512]{2,1,0:T(2,128)S(1)} %broadcast_in_dim.5), channel_id=1, replica_groups=mesh['sp_0'=16,'sp_1'=4,'sp_2'=2,'tp'=4] {'tp'}, dimensions={0} | all-to-all | bytes 32768 | tf_op jit(solution)/shard_map/all_to_all | solution.py:30
  155.2 0.4 multiply_convert_fusion
  155.6 0.8 pad_maximum_fusion
  (25 shorter events, 0.5 us)
Async XLA Ops:
  63.4 4.9 %copy-start = (bf16[512,512]{1,0:T(8,128)(2,1)S(1)}, bf16[512,512]{1,0:T(8,128)(2,1)}, u32[]{:S(2)}) copy-start(bf16[512,512]{1,0:T(8,128)(2,1)} %refs_0_.3) | copy-start | bytes 1572868
  63.5 36.1 %collective-permute-start.3 = (bf16[4,16,16,640]{3,2,1,0:T(8,128)(2,1)S(1)}, bf16[4,16,16,640]{3,2,1,0:T(8,128)(2,1)S(1)}, u32[]{:S(2)}, u32[]{:S(2)}) collective-permute-start(bf16[4,16,16,640]{3,2,1,0:T(8,128)(2,1)S(1)} %slice.28.refs_4_), channel_id=1, source_target_pairs={{0,4},{4,0},{1,5},{5,1},{2,6},{6,2},{3,7},{7,3},{8,12},{12,8},{9,1... | collective-permute-start | bytes 3932168 | tf_op jit(solution)/shard_map/ppermute | solution.py:40
  65.7 41.1 %copy-start.1 = (bf16[1,256,256]{2,1,0:T(8,128)(2,1)S(1)}, bf16[1,256,256]{2,1,0:T(8,128)(2,1)}, u32[]{:S(2)}) copy-start(bf16[1,256,256]{2,1,0:T(8,128)(2,1)} %w_pool_ref.1) | copy-start | bytes 393220
  65.7 41.1 %copy-start.2 = (f32[256]{0:T(256)S(1)}, f32[256]{0:T(256)}, u32[]{:S(2)}) copy-start(f32[256]{0:T(256)} %param.18) | copy-start | bytes 3076
  65.7 41.1 %copy-start.3 = (f32[4]{0:T(128)S(1)}, f32[4]{0:T(128)}, u32[]{:S(2)}) copy-start(f32[4]{0:T(128)} %sink_ref.1) | copy-start | bytes 52
  65.7 48.4 %collective-permute-start.6 = (bf16[4,16,16,512]{3,2,1,0:T(8,128)(2,1)S(1)}, bf16[4,16,16,512]{3,2,1,0:T(8,128)(2,1)S(1)}, u32[]{:S(2)}, u32[]{:S(2)}) collective-permute-start(bf16[4,16,16,512]{3,2,1,0:T(8,128)(2,1)S(1)} %slice.29.refs_4_.refs_2_), channel_id=1, source_target_pairs={{0,4},{4,0},{1,5},{5,1},{2,6},{6,2},{3,7},{7,3},{8,12},{12,8},{9,1... | collective-permute-start | bytes 3145736 | tf_op jit(solution)/shard_map/ppermute | solution.py:40
  68.3 17.0 %collective-permute-start.2 = (bf16[512,512]{1,0:T(8,128)(2,1)S(1)}, bf16[512,512]{1,0:T(8,128)(2,1)S(1)}, u32[]{:S(2)}, u32[]{:S(2)}) collective-permute-start(bf16[512,512]{1,0:T(8,128)(2,1)S(1)} %copy-done), channel_id=1, source_target_pairs={{0,3},{1,2},{2,1},{3,0},{4,7},{5,6},{6,5},{7,4},{8,11},{9,10},{10,... | collective-permute-start | bytes 1572872 | tf_op jit(solution)/shard_map/ppermute | solution.py:40
  73.2 16.7 %collective-permute-start.1 = (bf16[512,512]{1,0:T(8,128)(2,1)S(1)}, bf16[512,512]{1,0:T(8,128)(2,1)S(1)}, u32[]{:S(2)}, u32[]{:S(2)}) collective-permute-start(bf16[512,512]{1,0:T(8,128)(2,1)S(1)} %copy-done), channel_id=1, source_target_pairs={{0,1},{1,0},{2,3},{3,2},{4,5},{5,4},{6,7},{7,6},{8,9},{9,8},{10,11... | collective-permute-start | bytes 1572872 | tf_op jit(solution)/shard_map/ppermute | solution.py:40
  75.3 24.4 %collective-permute-start = (bf16[512,512]{1,0:T(8,128)(2,1)S(1)}, bf16[512,512]{1,0:T(8,128)(2,1)S(1)}, u32[]{:S(2)}, u32[]{:S(2)}) collective-permute-start(bf16[512,512]{1,0:T(8,128)(2,1)S(1)} %copy-done), channel_id=1, source_target_pairs={{0,2},{1,3},{2,0},{3,1},{4,6},{5,7},{6,4},{7,5},{8,10},{9,11},{10,... | collective-permute-start | bytes 1572872 | tf_op jit(solution)/shard_map/ppermute | solution.py:40
  101.1 10.2 %collective-permute-start.4 = (bf16[144,128]{1,0:T(8,128)(2,1)S(1)}, bf16[144,128]{1,0:T(8,128)(2,1)S(1)}, u32[]{:S(2)}, u32[]{:S(2)}) collective-permute-start(bf16[144,128]{1,0:T(8,128)(2,1)S(1)} %get-tuple-element.19), channel_id=1, source_target_pairs={{0,4},{4,0},{1,5},{5,1},{2,6},{6,2},{3,7},{7,3},{8,12},{12,8},{9,1... | collective-permute-start | bytes 110600 | tf_op jit(solution)/shard_map/ppermute | solution.py:40
  103.0 8.3 %collective-permute-start.5 = (bf16[144,128]{1,0:T(8,128)(2,1)S(1)}, bf16[144,128]{1,0:T(8,128)(2,1)S(1)}, u32[]{:S(2)}, u32[]{:S(2)}) collective-permute-start(bf16[144,128]{1,0:T(8,128)(2,1)S(1)} %get-tuple-element.20), channel_id=1, source_target_pairs={{4,8},{12,16},{20,24},{28,32},{36,40},{44,48},{52,56},{60,64},{68,... | collective-permute-start | bytes 110600 | tf_op jit(solution)/shard_map/ppermute | solution.py:50
  114.6 29.5 %collective-permute-start.7 = (bf16[512,512]{1,0:T(8,128)(2,1)S(1)}, bf16[512,512]{1,0:T(8,128)(2,1)S(1)}, u32[]{:S(2)}, u32[]{:S(2)}) collective-permute-start(bf16[512,512]{1,0:T(8,128)(2,1)S(1)} %shard_map.110), channel_id=1, source_target_pairs={{0,1},{1,0},{2,3},{3,2},{4,5},{5,4},{6,7},{7,6},{8,9},{9,8},{10,11... | collective-permute-start | bytes 1572872 | tf_op jit(solution)/shard_map/ppermute | solution.py:40
  117.4 27.9 %collective-permute-start.8 = (bf16[512,512]{1,0:T(8,128)(2,1)S(1)}, bf16[512,512]{1,0:T(8,128)(2,1)S(1)}, u32[]{:S(2)}, u32[]{:S(2)}) collective-permute-start(bf16[512,512]{1,0:T(8,128)(2,1)S(1)} %shard_map.111), channel_id=1, source_target_pairs={{0,3},{1,2},{2,1},{3,0},{4,7},{5,6},{6,5},{7,4},{8,11},{9,10},{10,... | collective-permute-start | bytes 1572872 | tf_op jit(solution)/shard_map/ppermute | solution.py:40
  122.3 17.1 %collective-permute-start.9 = (bf16[256,512]{1,0:T(8,128)(2,1)S(1)}, bf16[256,512]{1,0:T(8,128)(2,1)S(1)}, u32[]{:S(2)}, u32[]{:S(2)}) collective-permute-start(bf16[256,512]{1,0:T(8,128)(2,1)S(1)} %shard_map.112), channel_id=1, source_target_pairs={{0,2},{1,3},{2,0},{3,1},{4,6},{5,7},{6,4},{7,5},{8,10},{9,11},{10,... | collective-permute-start | bytes 786440 | tf_op jit(solution)/shard_map/ppermute | solution.py:40
  126.1 29.0 %copy-start.4 = (f32[512]{0:T(512)S(1)}, f32[512]{0:T(512)}, u32[]{:S(2)}) copy-start(f32[512]{0:T(512)} %param.21) | copy-start | bytes 6148
  126.1 18.0 %collective-permute-start.10 = (bf16[256,512]{1,0:T(8,128)(2,1)S(1)}, bf16[256,512]{1,0:T(8,128)(2,1)S(1)}, u32[]{:S(2)}, u32[]{:S(2)}) collective-permute-start(bf16[256,512]{1,0:T(8,128)(2,1)S(1)} %shard_map.113), channel_id=1, source_target_pairs={{0,2},{1,3},{2,0},{3,1},{4,6},{5,7},{6,4},{7,5},{8,10},{9,11},{10,... | collective-permute-start | bytes 786440 | tf_op jit(solution)/shard_map/ppermute | solution.py:40

commit v11 on v8

--- a/solution.py
+++ b/solution.py
@@ -73,6 +73,31 @@
     return total.astype(BF16)
 
 
+def copies_kernel(shard_ref, copies_ref, held_ref, read_sems, write_sems):
+    count, chunks = copies_ref.shape[0], read_sems.shape[0]
+    rows = shard_ref.shape[0] // chunks
+    reads = [
+        pltpu.make_async_copy(
+            shard_ref.at[pl.ds(i * rows, rows)], held_ref.at[pl.ds(i * rows, rows)], read_sems.at[i]
+        )
+        for i in range(chunks)
+    ]
+    for read in reads:
+        read.start()
+    writes = []
+    for i in range(chunks):
+        reads[i].wait()
+        here = pl.ds(i * rows, rows)
+        for to in range(count):
+            write = pltpu.make_async_copy(
+                held_ref.at[here], copies_ref.at[to, here], write_sems.at[i, to]
+            )
+            write.start()
+            writes.append(write)
+    for write in writes:
+        write.wait()
+
+
 def project_kernel(
     tokens_ref, own_ref, other_ref, kv_ref, chan_ref, inside_ref, outside_ref, w_ref
 ):
@@ -103,13 +128,10 @@
     band_ref[3] = jnp.where(low, 0.0, kv).astype(BF16)
 
 
-def attend_block(queries, first_key, edge, seq_len, band_ref, at, sink_ref, attended_ref, to):
+def attend_block(queries, band_ref, at, sink_ref, attended_ref, to):
     row = lax.broadcasted_iota(jnp.int32, (WINDOW, 3 * WINDOW), 0)
     col = lax.broadcasted_iota(jnp.int32, (WINDOW, 3 * WINDOW), 1)
     keep = (col >= row) & (col <= row + 2 * WINDOW)
-    if edge:
-        key_pos = col + first_key
-        keep = keep & (key_pos >= 0) & (key_pos < seq_len)
     band = pl.ds(at, 3 * WINDOW)
     for pair in range(queries.shape[1] // PAIR):
         lanes = slice(pair * PAIR, (pair + 1) * PAIR)
@@ -126,6 +148,42 @@
             probs = (raised * (1.0 / total)).astype(BF16)
             attended += jnp.dot(probs, band_ref[2 + side, band], preferred_element_type=F32)
         attended_ref[to : to + WINDOW, lanes] = attended.astype(BF16)
+
+
+def split_band_across(kv, keys_ref, values_ref):
+    kv = kv.astype(F32)
+    low = lax.broadcasted_iota(jnp.int32, kv.shape, 1) < HEAD_DIM
+    keys_ref[0] = jnp.where(low, kv, 0.0).astype(BF16)
+    keys_ref[1] = jnp.where(low, 0.0, pltpu.roll(kv, HEAD_DIM, 1)).astype(BF16)
+    values_ref[...] = kv.T[HEAD_DIM:].astype(BF16)
+
+
+def attend_edge(queries, has_before, has_after, keys_ref, values_ref, at, sink_ref, out_ref, to):
+    key = lax.broadcasted_iota(jnp.int32, (WINDOW, WINDOW), 0)
+    query = lax.broadcasted_iota(jnp.int32, (WINDOW, WINDOW), 1)
+    band = pl.ds(at, 3 * WINDOW)
+    keep_before, keep_after = (key >= query) & has_before, (key <= query) & has_after
+    for pair in range(queries.shape[1] // PAIR):
+        lanes = slice(pair * PAIR, (pair + 1) * PAIR)
+        attended = []
+        for side in range(2):
+            scores = lax.dot_general(
+                keys_ref[side, band], queries[:, lanes], nt, preferred_element_type=F32
+            ) * HEAD_DIM ** (-0.5)
+            thirds = (
+                jnp.where(keep_before, scores[:WINDOW], masked_score),
+                scores[WINDOW : 2 * WINDOW],
+                jnp.where(keep_after, scores[2 * WINDOW :], masked_score),
+            )
+            sink = sink_ref[2 * pair + side]
+            most = jnp.maximum(jnp.maximum(thirds[0], thirds[2]), thirds[1])
+            top = jnp.maximum(jnp.max(most, axis=0, keepdims=True), sink)
+            raised = [jnp.exp(third - top) for third in thirds]
+            total = jnp.sum(raised[0] + raised[1] + raised[2], axis=0, keepdims=True)
+            scale = 1.0 / (total + jnp.exp(sink - top))
+            probs = jnp.concatenate([(third * scale).astype(BF16) for third in raised])
+            attended.append(jnp.dot(values_ref[:, band], probs, preferred_element_type=F32))
+        out_ref[to : to + WINDOW, lanes] = jnp.concatenate(attended).T.astype(BF16)
 
 
 def pooled_rows(chan, centre, first_pos, seq_len, w_pool_ref, scale_ref):
@@ -170,9 +228,6 @@
     for b in range(1, rows // WINDOW - 1):
         attend_block(
             query_ref[b * WINDOW : (b + 1) * WINDOW],
-            0,
-            False,
-            seq_len,
             band_ref,
             (b - 1) * WINDOW,
             sink_ref,
@@ -199,7 +254,8 @@
     scale_ref,
     attended_ref,
     pooled_ref,
-    band_ref,
+    keys_ref,
+    values_ref,
 ):
     rows = chan_ref.shape[0]
     offset = lax.axis_index(SP) * rows
@@ -207,7 +263,7 @@
     inside, outside = inside_ref[...].astype(F32), outside_ref[...].astype(F32)
     before, after = jnp.where(ahead, outside, inside), jnp.where(ahead, inside, outside)
 
-    split_band(
+    split_band_across(
         jnp.concatenate(
             [
                 before[:WINDOW],
@@ -216,15 +272,16 @@
                 after[:WINDOW],
             ]
         ),
-        band_ref,
+        keys_ref,
+        values_ref,
     )
     for edge, start in enumerate((0, rows - WINDOW)):
-        attend_block(
+        attend_edge(
             query_ref[start : start + WINDOW],
-            offset + start - WINDOW,
-            True,
-            seq_len,
-            band_ref,
+            offset + start > 0,
+            offset + start + WINDOW < seq_len,
+            keys_ref,
+            values_ref,
             edge * 3 * WINDOW,
             sink_ref,
             attended_ref,
@@ -267,6 +324,7 @@
 
 VMEM = pl.BlockSpec(memory_space=pltpu.VMEM)
 SMEM = pl.BlockSpec(memory_space=pltpu.SMEM)
+ANY = pl.BlockSpec(memory_space=pl.ANY)
 LIMIT = pltpu.CompilerParams(vmem_limit_bytes=20 * 1024 * 1024)
 
 
@@ -291,7 +349,23 @@
     share = out_gain.shape[0]
     model_width = share * lax.axis_size(TP)
 
-    gathered = from_everyone(tokens, TP)
+    count, chunks = lax.axis_size(TP), 4
+    copies = pl.pallas_call(
+        copies_kernel,
+        out_shape=jax.ShapeDtypeStruct((count, *tokens.shape), BF16),
+        in_specs=[ANY],
+        out_specs=ANY,
+        scratch_shapes=[
+            pltpu.VMEM(tokens.shape, BF16),
+            pltpu.SemaphoreType.DMA((chunks,)),
+            pltpu.SemaphoreType.DMA((chunks, count)),
+        ],
+        cost_estimate=pl.CostEstimate(
+            flops=0, bytes_accessed=5 * tokens.size * 2, transcendentals=0
+        ),
+        name="copies",
+    )(tokens)
+    gathered = lax.all_to_all(copies, TP, 0, 0, tiled=True)
     packed = jnp.concatenate(
         (w_key, w_value, w_pool_in, w_query, w_out_attn.T, w_out_pool.T), axis=1
     )
@@ -339,7 +413,10 @@
         out_shape=[rows_of(query_cols, half), rows_of(chan_cols, half)],
         in_specs=[VMEM] * 5 + [SMEM] + [VMEM] * 2,
         out_specs=[VMEM] * 2,
-        scratch_shapes=[pltpu.VMEM((4, 6 * WINDOW, PAIR), BF16)],
+        scratch_shapes=[
+            pltpu.VMEM((2, 6 * WINDOW, PAIR), BF16),
+            pltpu.VMEM((HEAD_DIM, 6 * WINDOW), BF16),
+        ],
         compiler_params=LIMIT,
         cost_estimate=cost(2 * rows * model_width * query_cols, 2 << 20),
         name="outer",

time: 150 us -> 151 us (level)
  blocking collectives: 70.9 us -> 44.1 us
  waiting for transfers between devices: 28 us -> 48.1 us
  starting transfers between devices: 26.6 us -> 30.9 us
  Pallas kernels: 14.4 us -> 16.5 us
    all_to_all x2 -> x1, blocking collectives: 34.5 us -> 7.71 us  [from_everyone(): lax.all_to_all(jnp.broadcast_to(shard[None], (count, *shard.shape)), axis...]
    all_to_all x0 -> x1, waiting for transfers between devices: none -> 11.3 us  [layer(): gathered = lax.all_to_all(copies, TP, 0, 0, tiled=True)]
    all_to_all x1, waiting for transfers between devices: 11.3 us -> 20.1 us  [from_everyone(): lax.all_to_all(jnp.broadcast_to(shard[None], (count, *shard.shape)), axis...]
    all_to_all x0 -> x1, starting transfers between devices: none -> 4.46 us  [layer(): gathered = lax.all_to_all(copies, TP, 0, 0, tiled=True)]
    pallas_call x0 -> x1, Pallas kernels: none -> 2.38 us  [layer(): pl.pallas_call(copies_kernel, out_shape=jax.ShapeDtypeStruct((count, *tok...]
  transfers between devices with their start and end apart: 9 -> 10, of which waited for: 3 -> 4; matrix products, arithmetic and copies ran while one was open for 2% -> 2% of each run, Pallas kernels for 9% -> 11%
where the time goes in v11:
time: 151 us; the launch traced here: 150 us
  waiting for transfers between devices  48.1 us (32%)
  blocking collectives  44.1 us (29%)
  starting transfers between devices  30.9 us (20%)
  Pallas kernels  16.5 us (11%)
  local copies, waits for them, and re-layouts  7.52 us (5%)
  other arithmetic  2.8 us (2%)
    all_gather x1, blocking collectives, layer(): over_z = lax.all_gather(packed, Z, axis=0)  36.4 us
    all_to_all x1, waiting for transfers between devices, from_everyone(): lax.all_to_all(jnp.broadcast_to(shard[None], (count, *shard.shape)), axis...  20.1 us
    ppermute x4, waiting for transfers between devices, sent(): return lax.ppermute(block, TP, [(i, i ^ mask) for i in range(count)])  16.7 us
    ppermute x4, starting transfers between devices, sent(): return lax.ppermute(block, TP, [(i, i ^ mask) for i in range(count)])  12.3 us
    all_to_all x1, waiting for transfers between devices, layer(): gathered = lax.all_to_all(copies, TP, 0, 0, tiled=True)  11.3 us
    all_to_all x1, blocking collectives, from_everyone(): lax.all_to_all(jnp.broadcast_to(shard[None], (count, *shard.shape)), axis...  7.71 us
    ppermute x3, starting transfers between devices, swapped(): return lax.ppermute(shard, CORE, [(0, 1), (1, 0)])  6.38 us
    pallas_call x1, Pallas kernels, layer(): pl.pallas_call(functools.partial(inner_kernel, seq_len), out_shape=[rows_...  5.82 us
  transfers between devices with their start and end apart: 10, of which 4 were waited for; matrix products, arithmetic and copies ran while one was open for 2% of the time, Pallas kernels for 11%

profile of v11, /device:TPU:32, one launch (start us, length us, event | category | flops | bytes accessed | tf_op | source)
XLA Modules:
  0.0 150.2 jit_solution(60211173431440503)
XLA Ops:
  0.0 0.9 concatenate.9
  0.9 36.4 %all-gather = bf16[256,1152]{1,0:T(8,128)(2,1)S(1)} all-gather(bf16[16,1152]{1,0:T(8,128)(2,1)S(1)} %concatenate.9), channel_id=2, replica_groups=mesh['sp_0'=16,'sp_1'=4,'sp_2'=2,'tp'=4] {'sp_0'}, dimensions={0}, use_global_device_ids=true | all-gather | bytes 626688 | tf_op jit(solution)/shard_map/all_gather | solution.py:372
  37.3 1.6 %broadcast_in_dim.4 = bf16[4,16,16,1152]{3,2,1,0:T(8,128)(2,1)} broadcast(bf16[16,16,1152]{2,1,0:T(8,128)(2,1)S(1)} %bitcast.10), dimensions={1,2,3} | broadcast | bytes 2949120 | tf_op jit(solution)/shard_map/broadcast_in_dim | solution.py:30
  38.9 4.3 %all-to-all-start.1 = ((bf16[4,16,16,1152]{3,2,1,0:T(8,128)(2,1)}), bf16[4,16,16,1152]{3,2,1,0:T(8,128)(2,1)S(1)}, u32[]{:S(2)}, u32[]{:S(2)}) async-start(bf16[4,16,16,1152]{3,2,1,0:T(8,128)(2,1)} %broadcast_in_dim.4), calls=%async_computation.1 | async-start | bytes 4718592 | tf_op jit(solution)/shard_map/all_to_all | solution.py:29
  43.2 2.4 %copies.1 = bf16[4,512,512]{2,1,0:T(8,128)(2,1)} custom-call(bf16[512,512]{1,0:T(8,128)(2,1)} %shard_ref.1), custom_call_target="tpu_custom_call" | custom-call | bytes 2621440 | tf_op jit(solution)/shard_map/copies/pallas_call | solution.py:353
  45.6 20.1 %all-to-all-done.1 = bf16[4,16,16,1152]{3,2,1,0:T(8,128)(2,1)S(1)} async-done(((bf16[4,16,16,1152]{3,2,1,0:T(8,128)(2,1)}), bf16[4,16,16,1152]{3,2,1,0:T(8,128)(2,1)S(1)}, u32[]{:S(2)}, u32[]{:S(2)}) %all-to-all-start.1) | async-done | bytes 2359328 | tf_op jit(solution)/shard_map/all_to_all | solution.py:29
  65.6 1.4 copy-done.3
  67.1 4.5 %all-to-all-start = ((bf16[4,512,512]{2,1,0:T(8,128)(2,1)}), bf16[4,512,512]{2,1,0:T(8,128)(2,1)}, u32[]{:S(2)}, u32[]{:S(2)}) async-start(bf16[4,512,512]{2,1,0:T(8,128)(2,1)} %copies.1), calls=%async_computation | async-start | bytes 4194304 | tf_op jit(solution)/shard_map/all_to_all | solution.py:368
  71.5 1.4 slice.28.own_ref
  73.0 1.9 %collective-permute-start = (bf16[4,16,16,640]{3,2,1,0:T(8,128)(2,1)S(1)}, bf16[4,16,16,640]{3,2,1,0:T(8,128)(2,1)}, u32[]{:S(2)}, u32[]{:S(2)}) collective-permute-start(bf16[4,16,16,640]{3,2,1,0:T(8,128)(2,1)S(1)} %slice.28.own_ref), channel_id=1, source_target_pairs={{0,4},{4,0},{1,5},{5,1},{2,6},{6,2},{3,7},{7,3},{8,12},{12,8},{9,1... | collective-permute-start | bytes 3932168 | tf_op jit(solution)/shard_map/ppermute | solution.py:39
  74.9 1.3 slice.29.refs_4_.refs_2_
  76.2 2.5 %collective-permute-start.3 = (bf16[4,16,16,512]{3,2,1,0:T(8,128)(2,1)S(1)}, bf16[4,16,16,512]{3,2,1,0:T(8,128)(2,1)S(1)}, u32[]{:S(2)}, u32[]{:S(2)}) collective-permute-start(bf16[4,16,16,512]{3,2,1,0:T(8,128)(2,1)S(1)} %slice.29.refs_4_.refs_2_), channel_id=1, source_target_pairs={{0,4},{4,0},{1,5},{5,1},{2,6},{6,2},{3,7},{7,3},{8,12},{12,8},{9,1... | collective-permute-start | bytes 3145736 | tf_op jit(solution)/shard_map/ppermute | solution.py:39
  78.8 11.3 %all-to-all-done.tokens_ref = bf16[4,512,512]{2,1,0:T(8,128)(2,1)} async-done(((bf16[4,512,512]{2,1,0:T(8,128)(2,1)}), bf16[4,512,512]{2,1,0:T(8,128)(2,1)}, u32[]{:S(2)}, u32[]{:S(2)}) %all-to-all-start) | async-done | bytes 2097184 | tf_op jit(solution)/shard_map/all_to_all | solution.py:368
  90.1 3.4 %project.1 = (bf16[512,128]{1,0:T(8,128)(2,1)S(1)}, bf16[512,256]{1,0:T(8,128)(2,1)S(1)}, bf16[144,128]{1,0:T(8,128)(2,1)S(1)}, bf16[144,128]{1,0:T(8,128)(2,1)S(1)}) custom-call(bf16[4,512,512]{2,1,0:T(8,128)(2,1)} %all-to-all-done.tokens_ref, bf16[4,16,16,640]{3,2,1,0:T(8,128)(2,1)S(1)} %slice.28.own_ref, ...), custom_call_target="tpu_custom_call" | custom-call | flops 805306368 | bytes 4194304 | tf_op jit(solution)/shard_map/project/pallas_call | solution.py:385
  93.5 1.9 %collective-permute-start.1 = (bf16[144,128]{1,0:T(8,128)(2,1)S(1)}, bf16[144,128]{1,0:T(8,128)(2,1)S(1)}, u32[]{:S(2)}, u32[]{:S(2)}) collective-permute-start(bf16[144,128]{1,0:T(8,128)(2,1)S(1)} %get-tuple-element.19), channel_id=1, source_target_pairs={{0,4},{4,0},{1,5},{5,1},{2,6},{6,2},{3,7},{7,3},{8,12},{12,8},{9,1... | collective-permute-start | bytes 110600 | tf_op jit(solution)/shard_map/ppermute | solution.py:39
  95.4 3.4 %collective-permute-start.2 = (bf16[144,128]{1,0:T(8,128)(2,1)S(1)}, bf16[144,128]{1,0:T(8,128)(2,1)S(1)}, u32[]{:S(2)}, u32[]{:S(2)}) collective-permute-start(bf16[144,128]{1,0:T(8,128)(2,1)S(1)} %get-tuple-element.20), channel_id=1, source_target_pairs={{4,8},{12,16},{20,24},{28,32},{36,40},{44,48},{52,56},{60,64},{68,... | collective-permute-start | bytes 110600 | tf_op jit(solution)/shard_map/ppermute | solution.py:45
  98.9 5.8 %inner.1 = (bf16[512,256]{1,0:T(8,128)(2,1)S(1)}, bf16[256,256]{1,0:T(8,128)(2,1)S(1)}, bf16[256,256]{1,0:T(8,128)(2,1)S(1)}) custom-call(bf16[4,512,512]{2,1,0:T(8,128)(2,1)} %all-to-all-done.tokens_ref, bf16[4,16,16,640]{3,2,1,0:T(8,128)(2,1)S(1)} %slice.28.own_ref, bf16[4,16,16,640]{3,2,1,0:T(8,128)(2,1)} %collective-permute-done.other_ref, ...), custom_call_target="tpu_custom_call" | custom-call | flops 536870912 | bytes 4194304 | tf_op jit(solution)/shard_map/inner/pallas_call | solution.py:398
  104.7 2.6 %outer.1 = (bf16[256,256]{1,0:T(8,128)(2,1)S(1)}, bf16[256,256]{1,0:T(8,128)(2,1)S(1)}) custom-call(bf16[512,256]{1,0:T(8,128)(2,1)S(1)} %get-tuple-element.18.query_ref, bf16[512,128]{1,0:T(8,128)(2,1)S(1)} %get-tuple-element.14.kv_ref, bf16[512,256]{1,0:T(8,128)(2,1)S(1)} %get-tuple-element.15.chan_ref, ...), custom_call_target="tpu_custom_call" | custom-call | flops 536870912 | bytes 2097152 | tf_op jit(solution)/shard_map/outer/pallas_call | solution.py:411
  107.3 0.5 shard_map.111
  107.8 3.1 %collective-permute-start.5 = (bf16[512,512]{1,0:T(8,128)(2,1)S(1)}, bf16[512,512]{1,0:T(8,128)(2,1)S(1)}, u32[]{:S(2)}, u32[]{:S(2)}) collective-permute-start(bf16[512,512]{1,0:T(8,128)(2,1)S(1)} %shard_map.111), channel_id=1, source_target_pairs={{0,3},{1,2},{2,1},{3,0},{4,7},{5,6},{6,5},{7,4},{8,11},{9,10},{10,... | collective-permute-start | bytes 1572872 | tf_op jit(solution)/shard_map/ppermute | solution.py:443
  110.9 0.5 shard_map.110
  111.4 1.9 %collective-permute-start.4 = (bf16[512,512]{1,0:T(8,128)(2,1)S(1)}, bf16[512,512]{1,0:T(8,128)(2,1)S(1)}, u32[]{:S(2)}, u32[]{:S(2)}) collective-permute-start(bf16[512,512]{1,0:T(8,128)(2,1)S(1)} %shard_map.110), channel_id=1, source_target_pairs={{0,1},{1,0},{2,3},{3,2},{4,5},{5,4},{6,7},{7,6},{8,9},{9,8},{10,11... | collective-permute-start | bytes 1572872 | tf_op jit(solution)/shard_map/ppermute | solution.py:443
  113.8 5.4 %collective-permute-start.6 = (bf16[256,512]{1,0:T(8,128)(2,1)S(1)}, bf16[256,512]{1,0:T(8,128)(2,1)S(1)}, u32[]{:S(2)}, u32[]{:S(2)}) collective-permute-start(bf16[256,512]{1,0:T(8,128)(2,1)S(1)} %shard_map.112), channel_id=1, source_target_pairs={{0,2},{1,3},{2,0},{3,1},{4,6},{5,7},{6,4},{7,5},{8,10},{9,11},{10,... | collective-permute-start | bytes 786440 | tf_op jit(solution)/shard_map/ppermute | solution.py:443
  119.6 1.9 %collective-permute-start.7 = (bf16[256,512]{1,0:T(8,128)(2,1)S(1)}, bf16[256,512]{1,0:T(8,128)(2,1)S(1)}, u32[]{:S(2)}, u32[]{:S(2)}) collective-permute-start(bf16[256,512]{1,0:T(8,128)(2,1)S(1)} %shard_map.113), channel_id=1, source_target_pairs={{0,2},{1,3},{2,0},{3,1},{4,6},{5,7},{6,4},{7,5},{8,10},{9,11},{10,... | collective-permute-start | bytes 786440 | tf_op jit(solution)/shard_map/ppermute | solution.py:443
  121.5 0.5 shard_map.109
  122.1 13.2 %collective-permute-done.6 = bf16[256,512]{1,0:T(8,128)(2,1)S(1)} collective-permute-done((bf16[256,512]{1,0:T(8,128)(2,1)S(1)}, bf16[256,512]{1,0:T(8,128)(2,1)S(1)}, u32[]{:S(2)}, u32[]{:S(2)}) %collective-permute-start.6) | collective-permute-done | bytes 262176 | tf_op jit(solution)/shard_map/ppermute | solution.py:443
  135.3 3.5 %collective-permute-done.7 = bf16[256,512]{1,0:T(8,128)(2,1)S(1)} collective-permute-done((bf16[256,512]{1,0:T(8,128)(2,1)S(1)}, bf16[256,512]{1,0:T(8,128)(2,1)S(1)}, u32[]{:S(2)}, u32[]{:S(2)}) %collective-permute-start.7) | collective-permute-done | bytes 262176 | tf_op jit(solution)/shard_map/ppermute | solution.py:443
  138.8 0.8 copy-done.4
  139.6 0.4 fusion
  140.1 7.7 %all_to_all.15 = f32[4,2,512]{2,1,0:T(2,128)S(1)} all-to-all(f32[4,2,512]{2,1,0:T(2,128)S(1)} %broadcast_in_dim.5), channel_id=1, replica_groups=mesh['sp_0'=16,'sp_1'=4,'sp_2'=2,'tp'=4] {'tp'}, dimensions={0} | all-to-all | bytes 32768 | tf_op jit(solution)/shard_map/all_to_all | solution.py:29
  147.9 1.5 multiply_convert_fusion
  149.4 0.8 pad_maximum_fusion
  (27 shorter events, 0.9 us)
Async XLA Ops:
  38.9 26.7 %all-to-all-start.1 = ((bf16[4,16,16,1152]{3,2,1,0:T(8,128)(2,1)}), bf16[4,16,16,1152]{3,2,1,0:T(8,128)(2,1)S(1)}, u32[]{:S(2)}, u32[]{:S(2)}) async-start(bf16[4,16,16,1152]{3,2,1,0:T(8,128)(2,1)} %broadcast_in_dim.4), calls=%async_computation.1 | async-start | bytes 4718592 | tf_op jit(solution)/shard_map/all_to_all | solution.py:29
  65.6 1.4 copy-start.3
  67.1 23.0 %all-to-all-start = ((bf16[4,512,512]{2,1,0:T(8,128)(2,1)}), bf16[4,512,512]{2,1,0:T(8,128)(2,1)}, u32[]{:S(2)}, u32[]{:S(2)}) async-start(bf16[4,512,512]{2,1,0:T(8,128)(2,1)} %copies.1), calls=%async_computation | async-start | bytes 4194304 | tf_op jit(solution)/shard_map/all_to_all | solution.py:368
  73.0 17.1 %collective-permute-start = (bf16[4,16,16,640]{3,2,1,0:T(8,128)(2,1)S(1)}, bf16[4,16,16,640]{3,2,1,0:T(8,128)(2,1)}, u32[]{:S(2)}, u32[]{:S(2)}) collective-permute-start(bf16[4,16,16,640]{3,2,1,0:T(8,128)(2,1)S(1)} %slice.28.own_ref), channel_id=1, source_target_pairs={{0,4},{4,0},{1,5},{5,1},{2,6},{6,2},{3,7},{7,3},{8,12},{12,8},{9,1... | collective-permute-start | bytes 3932168 | tf_op jit(solution)/shard_map/ppermute | solution.py:39
  76.2 22.6 %copy-start = (bf16[1,256,256]{2,1,0:T(8,128)(2,1)S(1)}, bf16[1,256,256]{2,1,0:T(8,128)(2,1)}, u32[]{:S(2)}) copy-start(bf16[1,256,256]{2,1,0:T(8,128)(2,1)} %w_pool_ref.3) | copy-start | bytes 393220
  76.2 22.6 %copy-start.1 = (f32[256]{0:T(256)S(1)}, f32[256]{0:T(256)}, u32[]{:S(2)}) copy-start(f32[256]{0:T(256)} %param.18) | copy-start | bytes 3076
  76.2 22.6 %copy-start.2 = (f32[4]{0:T(128)S(1)}, f32[4]{0:T(128)}, u32[]{:S(2)}) copy-start(f32[4]{0:T(128)} %sink_ref.3) | copy-start | bytes 52
  76.2 31.1 %collective-permute-start.3 = (bf16[4,16,16,512]{3,2,1,0:T(8,128)(2,1)S(1)}, bf16[4,16,16,512]{3,2,1,0:T(8,128)(2,1)S(1)}, u32[]{:S(2)}, u32[]{:S(2)}) collective-permute-start(bf16[4,16,16,512]{3,2,1,0:T(8,128)(2,1)S(1)} %slice.29.refs_4_.refs_2_), channel_id=1, source_target_pairs={{0,4},{4,0},{1,5},{5,1},{2,6},{6,2},{3,7},{7,3},{8,12},{12,8},{9,1... | collective-permute-start | bytes 3145736 | tf_op jit(solution)/shard_map/ppermute | solution.py:39
  93.5 11.2 %collective-permute-start.1 = (bf16[144,128]{1,0:T(8,128)(2,1)S(1)}, bf16[144,128]{1,0:T(8,128)(2,1)S(1)}, u32[]{:S(2)}, u32[]{:S(2)}) collective-permute-start(bf16[144,128]{1,0:T(8,128)(2,1)S(1)} %get-tuple-element.19), channel_id=1, source_target_pairs={{0,4},{4,0},{1,5},{5,1},{2,6},{6,2},{3,7},{7,3},{8,12},{12,8},{9,1... | collective-permute-start | bytes 110600 | tf_op jit(solution)/shard_map/ppermute | solution.py:39
  95.4 9.3 %collective-permute-start.2 = (bf16[144,128]{1,0:T(8,128)(2,1)S(1)}, bf16[144,128]{1,0:T(8,128)(2,1)S(1)}, u32[]{:S(2)}, u32[]{:S(2)}) collective-permute-start(bf16[144,128]{1,0:T(8,128)(2,1)S(1)} %get-tuple-element.20), channel_id=1, source_target_pairs={{4,8},{12,16},{20,24},{28,32},{36,40},{44,48},{52,56},{60,64},{68,... | collective-permute-start | bytes 110600 | tf_op jit(solution)/shard_map/ppermute | solution.py:45
  107.8 31.0 %collective-permute-start.5 = (bf16[512,512]{1,0:T(8,128)(2,1)S(1)}, bf16[512,512]{1,0:T(8,128)(2,1)S(1)}, u32[]{:S(2)}, u32[]{:S(2)}) collective-permute-start(bf16[512,512]{1,0:T(8,128)(2,1)S(1)} %shard_map.111), channel_id=1, source_target_pairs={{0,3},{1,2},{2,1},{3,0},{4,7},{5,6},{6,5},{7,4},{8,11},{9,10},{10,... | collective-permute-start | bytes 1572872 | tf_op jit(solution)/shard_map/ppermute | solution.py:443
  111.4 27.4 %collective-permute-start.4 = (bf16[512,512]{1,0:T(8,128)(2,1)S(1)}, bf16[512,512]{1,0:T(8,128)(2,1)S(1)}, u32[]{:S(2)}, u32[]{:S(2)}) collective-permute-start(bf16[512,512]{1,0:T(8,128)(2,1)S(1)} %shard_map.110), channel_id=1, source_target_pairs={{0,1},{1,0},{2,3},{3,2},{4,5},{5,4},{6,7},{7,6},{8,9},{9,8},{10,11... | collective-permute-start | bytes 1572872 | tf_op jit(solution)/shard_map/ppermute | solution.py:443
  113.8 21.5 %collective-permute-start.6 = (bf16[256,512]{1,0:T(8,128)(2,1)S(1)}, bf16[256,512]{1,0:T(8,128)(2,1)S(1)}, u32[]{:S(2)}, u32[]{:S(2)}) collective-permute-start(bf16[256,512]{1,0:T(8,128)(2,1)S(1)} %shard_map.112), channel_id=1, source_target_pairs={{0,2},{1,3},{2,0},{3,1},{4,6},{5,7},{6,4},{7,5},{8,10},{9,11},{10,... | collective-permute-start | bytes 786440 | tf_op jit(solution)/shard_map/ppermute | solution.py:443
  119.6 28.3 %copy-start.6 = (f32[512]{0:T(512)S(1)}, f32[512]{0:T(512)}, u32[]{:S(2)}) copy-start(f32[512]{0:T(512)} %param.21) | copy-start | bytes 6148
  119.6 19.2 %collective-permute-start.7 = (bf16[256,512]{1,0:T(8,128)(2,1)S(1)}, bf16[256,512]{1,0:T(8,128)(2,1)S(1)}, u32[]{:S(2)}, u32[]{:S(2)}) collective-permute-start(bf16[256,512]{1,0:T(8,128)(2,1)S(1)} %shard_map.113), channel_id=1, source_target_pairs={{0,2},{1,3},{2,0},{3,1},{4,6},{5,7},{6,4},{7,5},{8,10},{9,11},{10,... | collective-permute-start | bytes 786440 | tf_op jit(solution)/shard_map/ppermute | solution.py:443
  138.8 1.3 copy-start.5
  138.8 0.8 copy-start.4

commit v12 on v11

--- a/solution.py
+++ b/solution.py
@@ -221,19 +221,18 @@
     w_ref,
     band_ref,
 ):
-    rows, query_cols = query_ref.shape
+    rows, query_cols = kv_ref.shape[0], query_ref.shape[1]
     whole_weights(own_ref, other_ref, w_ref, own_ref.shape[3] - query_cols)
-    query_ref[...] = projected(tokens_ref, w_ref, 0, query_cols)
     split_band(kv_ref[...], band_ref)
-    for b in range(1, rows // WINDOW - 1):
-        attend_block(
-            query_ref[b * WINDOW : (b + 1) * WINDOW],
-            band_ref,
-            (b - 1) * WINDOW,
-            sink_ref,
-            attended_ref,
-            (b - 1) * WINDOW,
-        )
+    for b in (1, rows // WINDOW - 2, 0, rows // WINDOW - 1):
+        here = slice(b * WINDOW, (b + 1) * WINDOW)
+        queries = projected(tokens_ref.at[:, here], w_ref, 0, query_cols)
+        if 0 < b < rows // WINDOW - 1:
+            attend_block(
+                queries, band_ref, (b - 1) * WINDOW, sink_ref, attended_ref, (b - 1) * WINDOW
+            )
+        else:
+            query_ref[min(b, 1) * WINDOW : (min(b, 1) + 1) * WINDOW] = queries
     near = 2 * RIM
     chan = chan_ref[WINDOW - near : rows - WINDOW + near].astype(F32)
     offset = lax.axis_index(SP) * rows + WINDOW
@@ -277,7 +276,7 @@
     )
     for edge, start in enumerate((0, rows - WINDOW)):
         attend_edge(
-            query_ref[start : start + WINDOW],
+            query_ref[edge * WINDOW : (edge + 1) * WINDOW],
             offset + start > 0,
             offset + start + WINDOW < seq_len,
             keys_ref,
@@ -397,7 +396,7 @@
     scale = pool_scale.reshape(1, -1)
     query, *inner = pl.pallas_call(
         functools.partial(inner_kernel, seq_len),
-        out_shape=[rows_of(query_cols), rows_of(query_cols, half), rows_of(chan_cols, half)],
+        out_shape=[rows_of(query_cols, half), rows_of(query_cols, half), rows_of(chan_cols, half)],
         in_specs=[VMEM] * 5 + [SMEM] + [VMEM] * 2,
         out_specs=[VMEM] * 3,
         scratch_shapes=[

time: 151 us -> 151 us (level)
  transfers between devices with their start and end apart: 10 -> 10, of which waited for: 4 -> 4; matrix products, arithmetic and copies ran while one was open for 2% -> 2% of each run, Pallas kernels for 11% -> 10%
where the time goes in v12:
time: 151 us; the launch traced here: 150 us
  waiting for transfers between devices  48.1 us (32%)
  blocking collectives  44.1 us (29%)
  starting transfers between devices  30.9 us (20%)
  Pallas kernels  16.1 us (11%)
  local copies, waits for them, and re-layouts  7.52 us (5%)
  other arithmetic  2.8 us (2%)
    all_gather x1, blocking collectives, layer(): over_z = lax.all_gather(packed, Z, axis=0)  36.4 us
    all_to_all x1, waiting for transfers between devices, from_everyone(): lax.all_to_all(jnp.broadcast_to(shard[None], (count, *shard.shape)), axis...  20.1 us
    ppermute x4, waiting for transfers between devices, sent(): return lax.ppermute(block, TP, [(i, i ^ mask) for i in range(count)])  16.7 us
    ppermute x4, starting transfers between devices, sent(): return lax.ppermute(block, TP, [(i, i ^ mask) for i in range(count)])  12.3 us
    all_to_all x1, waiting for transfers between devices, layer(): gathered = lax.all_to_all(copies, TP, 0, 0, tiled=True)  11.3 us
    all_to_all x1, blocking collectives, from_everyone(): lax.all_to_all(jnp.broadcast_to(shard[None], (count, *shard.shape)), axis...  7.71 us
    ppermute x3, starting transfers between devices, swapped(): return lax.ppermute(shard, CORE, [(0, 1), (1, 0)])  6.38 us
    pallas_call x1, Pallas kernels, layer(): pl.pallas_call(functools.partial(inner_kernel, seq_len), out_shape=[rows_...  5.42 us
  transfers between devices with their start and end apart: 10, of which 4 were waited for; matrix products, arithmetic and copies ran while one was open for 2% of the time, Pallas kernels for 10%

profile of v12, /device:TPU:32, one launch (start us, length us, event | category | flops | bytes accessed | tf_op | source)
XLA Modules:
  0.0 149.8 jit_solution(9120556895021921924)
XLA Ops:
  0.0 0.9 concatenate.9
  0.9 36.4 %all-gather = bf16[256,1152]{1,0:T(8,128)(2,1)S(1)} all-gather(bf16[16,1152]{1,0:T(8,128)(2,1)S(1)} %concatenate.9), channel_id=2, replica_groups=mesh['sp_0'=16,'sp_1'=4,'sp_2'=2,'tp'=4] {'sp_0'}, dimensions={0}, use_global_device_ids=true | all-gather | bytes 626688 | tf_op jit(solution)/shard_map/all_gather | solution.py:371
  37.3 1.6 %broadcast_in_dim.4 = bf16[4,16,16,1152]{3,2,1,0:T(8,128)(2,1)} broadcast(bf16[16,16,1152]{2,1,0:T(8,128)(2,1)S(1)} %bitcast.10), dimensions={1,2,3} | broadcast | bytes 2949120 | tf_op jit(solution)/shard_map/broadcast_in_dim | solution.py:30
  38.9 4.3 %all-to-all-start.1 = ((bf16[4,16,16,1152]{3,2,1,0:T(8,128)(2,1)}), bf16[4,16,16,1152]{3,2,1,0:T(8,128)(2,1)S(1)}, u32[]{:S(2)}, u32[]{:S(2)}) async-start(bf16[4,16,16,1152]{3,2,1,0:T(8,128)(2,1)} %broadcast_in_dim.4), calls=%async_computation.1 | async-start | bytes 4718592 | tf_op jit(solution)/shard_map/all_to_all | solution.py:29
  43.2 2.4 %copies.1 = bf16[4,512,512]{2,1,0:T(8,128)(2,1)} custom-call(bf16[512,512]{1,0:T(8,128)(2,1)} %shard_ref.1), custom_call_target="tpu_custom_call" | custom-call | bytes 2621440 | tf_op jit(solution)/shard_map/copies/pallas_call | solution.py:352
  45.6 20.1 %all-to-all-done.1 = bf16[4,16,16,1152]{3,2,1,0:T(8,128)(2,1)S(1)} async-done(((bf16[4,16,16,1152]{3,2,1,0:T(8,128)(2,1)}), bf16[4,16,16,1152]{3,2,1,0:T(8,128)(2,1)S(1)}, u32[]{:S(2)}, u32[]{:S(2)}) %all-to-all-start.1) | async-done | bytes 2359328 | tf_op jit(solution)/shard_map/all_to_all | solution.py:29
  65.6 1.4 copy-done.3
  67.1 4.5 %all-to-all-start = ((bf16[4,512,512]{2,1,0:T(8,128)(2,1)}), bf16[4,512,512]{2,1,0:T(8,128)(2,1)}, u32[]{:S(2)}, u32[]{:S(2)}) async-start(bf16[4,512,512]{2,1,0:T(8,128)(2,1)} %copies.1), calls=%async_computation | async-start | bytes 4194304 | tf_op jit(solution)/shard_map/all_to_all | solution.py:367
  71.5 1.4 slice.28.own_ref
  73.0 1.9 %collective-permute-start = (bf16[4,16,16,640]{3,2,1,0:T(8,128)(2,1)S(1)}, bf16[4,16,16,640]{3,2,1,0:T(8,128)(2,1)}, u32[]{:S(2)}, u32[]{:S(2)}) collective-permute-start(bf16[4,16,16,640]{3,2,1,0:T(8,128)(2,1)S(1)} %slice.28.own_ref), channel_id=1, source_target_pairs={{0,4},{4,0},{1,5},{5,1},{2,6},{6,2},{3,7},{7,3},{8,12},{12,8},{9,1... | collective-permute-start | bytes 3932168 | tf_op jit(solution)/shard_map/ppermute | solution.py:39
  74.9 1.3 slice.29.refs_4_.refs_2_
  76.2 2.5 %collective-permute-start.3 = (bf16[4,16,16,512]{3,2,1,0:T(8,128)(2,1)S(1)}, bf16[4,16,16,512]{3,2,1,0:T(8,128)(2,1)S(1)}, u32[]{:S(2)}, u32[]{:S(2)}) collective-permute-start(bf16[4,16,16,512]{3,2,1,0:T(8,128)(2,1)S(1)} %slice.29.refs_4_.refs_2_), channel_id=1, source_target_pairs={{0,4},{4,0},{1,5},{5,1},{2,6},{6,2},{3,7},{7,3},{8,12},{12,8},{9,1... | collective-permute-start | bytes 3145736 | tf_op jit(solution)/shard_map/ppermute | solution.py:39
  78.8 11.3 %all-to-all-done.tokens_ref = bf16[4,512,512]{2,1,0:T(8,128)(2,1)} async-done(((bf16[4,512,512]{2,1,0:T(8,128)(2,1)}), bf16[4,512,512]{2,1,0:T(8,128)(2,1)}, u32[]{:S(2)}, u32[]{:S(2)}) %all-to-all-start) | async-done | bytes 2097184 | tf_op jit(solution)/shard_map/all_to_all | solution.py:367
  90.1 3.4 %project.1 = (bf16[512,128]{1,0:T(8,128)(2,1)S(1)}, bf16[512,256]{1,0:T(8,128)(2,1)S(1)}, bf16[144,128]{1,0:T(8,128)(2,1)S(1)}, bf16[144,128]{1,0:T(8,128)(2,1)S(1)}) custom-call(bf16[4,512,512]{2,1,0:T(8,128)(2,1)} %all-to-all-done.tokens_ref, bf16[4,16,16,640]{3,2,1,0:T(8,128)(2,1)S(1)} %slice.28.own_ref, ...), custom_call_target="tpu_custom_call" | custom-call | flops 805306368 | bytes 4194304 | tf_op jit(solution)/shard_map/project/pallas_call | solution.py:384
  93.5 1.9 %collective-permute-start.1 = (bf16[144,128]{1,0:T(8,128)(2,1)S(1)}, bf16[144,128]{1,0:T(8,128)(2,1)S(1)}, u32[]{:S(2)}, u32[]{:S(2)}) collective-permute-start(bf16[144,128]{1,0:T(8,128)(2,1)S(1)} %get-tuple-element.19), channel_id=1, source_target_pairs={{0,4},{4,0},{1,5},{5,1},{2,6},{6,2},{3,7},{7,3},{8,12},{12,8},{9,1... | collective-permute-start | bytes 110600 | tf_op jit(solution)/shard_map/ppermute | solution.py:39
  95.4 3.4 %collective-permute-start.2 = (bf16[144,128]{1,0:T(8,128)(2,1)S(1)}, bf16[144,128]{1,0:T(8,128)(2,1)S(1)}, u32[]{:S(2)}, u32[]{:S(2)}) collective-permute-start(bf16[144,128]{1,0:T(8,128)(2,1)S(1)} %get-tuple-element.20), channel_id=1, source_target_pairs={{4,8},{12,16},{20,24},{28,32},{36,40},{44,48},{52,56},{60,64},{68,... | collective-permute-start | bytes 110600 | tf_op jit(solution)/shard_map/ppermute | solution.py:45
  98.9 5.4 %inner.1 = (bf16[256,256]{1,0:T(8,128)(2,1)S(1)}, bf16[256,256]{1,0:T(8,128)(2,1)S(1)}, bf16[256,256]{1,0:T(8,128)(2,1)S(1)}) custom-call(bf16[4,512,512]{2,1,0:T(8,128)(2,1)} %all-to-all-done.tokens_ref, bf16[4,16,16,640]{3,2,1,0:T(8,128)(2,1)S(1)} %slice.28.own_ref, bf16[4,16,16,640]{3,2,1,0:T(8,128)(2,1)} %collective-permute-done.other_ref, ...), custom_call_target="tpu_custom_call" | custom-call | flops 536870912 | bytes 4194304 | tf_op jit(solution)/shard_map/inner/pallas_call | solution.py:397
  104.3 2.6 %outer.1 = (bf16[256,256]{1,0:T(8,128)(2,1)S(1)}, bf16[256,256]{1,0:T(8,128)(2,1)S(1)}) custom-call(bf16[256,256]{1,0:T(8,128)(2,1)S(1)} %get-tuple-element.18.query_ref, bf16[512,128]{1,0:T(8,128)(2,1)S(1)} %get-tuple-element.14.kv_ref, bf16[512,256]{1,0:T(8,128)(2,1)S(1)} %get-tuple-element.15.chan_ref, ...), custom_call_target="tpu_custom_call" | custom-call | flops 536870912 | bytes 2097152 | tf_op jit(solution)/shard_map/outer/pallas_call | solution.py:410
  106.9 0.5 shard_map.111
  107.4 3.1 %collective-permute-start.5 = (bf16[512,512]{1,0:T(8,128)(2,1)S(1)}, bf16[512,512]{1,0:T(8,128)(2,1)S(1)}, u32[]{:S(2)}, u32[]{:S(2)}) collective-permute-start(bf16[512,512]{1,0:T(8,128)(2,1)S(1)} %shard_map.111), channel_id=1, source_target_pairs={{0,3},{1,2},{2,1},{3,0},{4,7},{5,6},{6,5},{7,4},{8,11},{9,10},{10,... | collective-permute-start | bytes 1572872 | tf_op jit(solution)/shard_map/ppermute | solution.py:442
  110.5 0.5 shard_map.110
  111.0 1.9 %collective-permute-start.4 = (bf16[512,512]{1,0:T(8,128)(2,1)S(1)}, bf16[512,512]{1,0:T(8,128)(2,1)S(1)}, u32[]{:S(2)}, u32[]{:S(2)}) collective-permute-start(bf16[512,512]{1,0:T(8,128)(2,1)S(1)} %shard_map.110), channel_id=1, source_target_pairs={{0,1},{1,0},{2,3},{3,2},{4,5},{5,4},{6,7},{7,6},{8,9},{9,8},{10,11... | collective-permute-start | bytes 1572872 | tf_op jit(solution)/shard_map/ppermute | solution.py:442
  113.4 5.4 %collective-permute-start.6 = (bf16[256,512]{1,0:T(8,128)(2,1)S(1)}, bf16[256,512]{1,0:T(8,128)(2,1)S(1)}, u32[]{:S(2)}, u32[]{:S(2)}) collective-permute-start(bf16[256,512]{1,0:T(8,128)(2,1)S(1)} %shard_map.112), channel_id=1, source_target_pairs={{0,2},{1,3},{2,0},{3,1},{4,6},{5,7},{6,4},{7,5},{8,10},{9,11},{10,... | collective-permute-start | bytes 786440 | tf_op jit(solution)/shard_map/ppermute | solution.py:442
  119.2 1.9 %collective-permute-start.7 = (bf16[256,512]{1,0:T(8,128)(2,1)S(1)}, bf16[256,512]{1,0:T(8,128)(2,1)S(1)}, u32[]{:S(2)}, u32[]{:S(2)}) collective-permute-start(bf16[256,512]{1,0:T(8,128)(2,1)S(1)} %shard_map.113), channel_id=1, source_target_pairs={{0,2},{1,3},{2,0},{3,1},{4,6},{5,7},{6,4},{7,5},{8,10},{9,11},{10,... | collective-permute-start | bytes 786440 | tf_op jit(solution)/shard_map/ppermute | solution.py:442
  121.1 0.5 shard_map.109
  121.7 13.2 %collective-permute-done.6 = bf16[256,512]{1,0:T(8,128)(2,1)S(1)} collective-permute-done((bf16[256,512]{1,0:T(8,128)(2,1)S(1)}, bf16[256,512]{1,0:T(8,128)(2,1)S(1)}, u32[]{:S(2)}, u32[]{:S(2)}) %collective-permute-start.6) | collective-permute-done | bytes 262176 | tf_op jit(solution)/shard_map/ppermute | solution.py:442
  134.9 3.5 %collective-permute-done.7 = bf16[256,512]{1,0:T(8,128)(2,1)S(1)} collective-permute-done((bf16[256,512]{1,0:T(8,128)(2,1)S(1)}, bf16[256,512]{1,0:T(8,128)(2,1)S(1)}, u32[]{:S(2)}, u32[]{:S(2)}) %collective-permute-start.7) | collective-permute-done | bytes 262176 | tf_op jit(solution)/shard_map/ppermute | solution.py:442
  138.4 0.8 copy-done.4
  139.2 0.4 fusion
  139.7 7.7 %all_to_all.15 = f32[4,2,512]{2,1,0:T(2,128)S(1)} all-to-all(f32[4,2,512]{2,1,0:T(2,128)S(1)} %broadcast_in_dim.5), channel_id=1, replica_groups=mesh['sp_0'=16,'sp_1'=4,'sp_2'=2,'tp'=4] {'tp'}, dimensions={0} | all-to-all | bytes 32768 | tf_op jit(solution)/shard_map/all_to_all | solution.py:29
  147.5 1.5 multiply_convert_fusion
  149.0 0.8 pad_maximum_fusion
  (27 shorter events, 0.9 us)
Async XLA Ops:
  38.9 26.7 %all-to-all-start.1 = ((bf16[4,16,16,1152]{3,2,1,0:T(8,128)(2,1)}), bf16[4,16,16,1152]{3,2,1,0:T(8,128)(2,1)S(1)}, u32[]{:S(2)}, u32[]{:S(2)}) async-start(bf16[4,16,16,1152]{3,2,1,0:T(8,128)(2,1)} %broadcast_in_dim.4), calls=%async_computation.1 | async-start | bytes 4718592 | tf_op jit(solution)/shard_map/all_to_all | solution.py:29
  65.6 1.4 copy-start.3
  67.1 23.0 %all-to-all-start = ((bf16[4,512,512]{2,1,0:T(8,128)(2,1)}), bf16[4,512,512]{2,1,0:T(8,128)(2,1)}, u32[]{:S(2)}, u32[]{:S(2)}) async-start(bf16[4,512,512]{2,1,0:T(8,128)(2,1)} %copies.1), calls=%async_computation | async-start | bytes 4194304 | tf_op jit(solution)/shard_map/all_to_all | solution.py:367
  73.0 17.1 %collective-permute-start = (bf16[4,16,16,640]{3,2,1,0:T(8,128)(2,1)S(1)}, bf16[4,16,16,640]{3,2,1,0:T(8,128)(2,1)}, u32[]{:S(2)}, u32[]{:S(2)}) collective-permute-start(bf16[4,16,16,640]{3,2,1,0:T(8,128)(2,1)S(1)} %slice.28.own_ref), channel_id=1, source_target_pairs={{0,4},{4,0},{1,5},{5,1},{2,6},{6,2},{3,7},{7,3},{8,12},{12,8},{9,1... | collective-permute-start | bytes 3932168 | tf_op jit(solution)/shard_map/ppermute | solution.py:39
  76.2 22.6 %copy-start = (bf16[1,256,256]{2,1,0:T(8,128)(2,1)S(1)}, bf16[1,256,256]{2,1,0:T(8,128)(2,1)}, u32[]{:S(2)}) copy-start(bf16[1,256,256]{2,1,0:T(8,128)(2,1)} %w_pool_ref.3) | copy-start | bytes 393220
  76.2 22.6 %copy-start.1 = (f32[256]{0:T(256)S(1)}, f32[256]{0:T(256)}, u32[]{:S(2)}) copy-start(f32[256]{0:T(256)} %param.18) | copy-start | bytes 3076
  76.2 22.6 %copy-start.2 = (f32[4]{0:T(128)S(1)}, f32[4]{0:T(128)}, u32[]{:S(2)}) copy-start(f32[4]{0:T(128)} %sink_ref.3) | copy-start | bytes 52
  76.2 30.7 %collective-permute-start.3 = (bf16[4,16,16,512]{3,2,1,0:T(8,128)(2,1)S(1)}, bf16[4,16,16,512]{3,2,1,0:T(8,128)(2,1)S(1)}, u32[]{:S(2)}, u32[]{:S(2)}) collective-permute-start(bf16[4,16,16,512]{3,2,1,0:T(8,128)(2,1)S(1)} %slice.29.refs_4_.refs_2_), channel_id=1, source_target_pairs={{0,4},{4,0},{1,5},{5,1},{2,6},{6,2},{3,7},{7,3},{8,12},{12,8},{9,1... | collective-permute-start | bytes 3145736 | tf_op jit(solution)/shard_map/ppermute | solution.py:39
  93.5 10.8 %collective-permute-start.1 = (bf16[144,128]{1,0:T(8,128)(2,1)S(1)}, bf16[144,128]{1,0:T(8,128)(2,1)S(1)}, u32[]{:S(2)}, u32[]{:S(2)}) collective-permute-start(bf16[144,128]{1,0:T(8,128)(2,1)S(1)} %get-tuple-element.19), channel_id=1, source_target_pairs={{0,4},{4,0},{1,5},{5,1},{2,6},{6,2},{3,7},{7,3},{8,12},{12,8},{9,1... | collective-permute-start | bytes 110600 | tf_op jit(solution)/shard_map/ppermute | solution.py:39
  95.4 8.9 %collective-permute-start.2 = (bf16[144,128]{1,0:T(8,128)(2,1)S(1)}, bf16[144,128]{1,0:T(8,128)(2,1)S(1)}, u32[]{:S(2)}, u32[]{:S(2)}) collective-permute-start(bf16[144,128]{1,0:T(8,128)(2,1)S(1)} %get-tuple-element.20), channel_id=1, source_target_pairs={{4,8},{12,16},{20,24},{28,32},{36,40},{44,48},{52,56},{60,64},{68,... | collective-permute-start | bytes 110600 | tf_op jit(solution)/shard_map/ppermute | solution.py:45
  107.4 31.0 %collective-permute-start.5 = (bf16[512,512]{1,0:T(8,128)(2,1)S(1)}, bf16[512,512]{1,0:T(8,128)(2,1)S(1)}, u32[]{:S(2)}, u32[]{:S(2)}) collective-permute-start(bf16[512,512]{1,0:T(8,128)(2,1)S(1)} %shard_map.111), channel_id=1, source_target_pairs={{0,3},{1,2},{2,1},{3,0},{4,7},{5,6},{6,5},{7,4},{8,11},{9,10},{10,... | collective-permute-start | bytes 1572872 | tf_op jit(solution)/shard_map/ppermute | solution.py:442
  111.0 27.4 %collective-permute-start.4 = (bf16[512,512]{1,0:T(8,128)(2,1)S(1)}, bf16[512,512]{1,0:T(8,128)(2,1)S(1)}, u32[]{:S(2)}, u32[]{:S(2)}) collective-permute-start(bf16[512,512]{1,0:T(8,128)(2,1)S(1)} %shard_map.110), channel_id=1, source_target_pairs={{0,1},{1,0},{2,3},{3,2},{4,5},{5,4},{6,7},{7,6},{8,9},{9,8},{10,11... | collective-permute-start | bytes 1572872 | tf_op jit(solution)/shard_map/ppermute | solution.py:442
  113.4 21.5 %collective-permute-start.6 = (bf16[256,512]{1,0:T(8,128)(2,1)S(1)}, bf16[256,512]{1,0:T(8,128)(2,1)S(1)}, u32[]{:S(2)}, u32[]{:S(2)}) collective-permute-start(bf16[256,512]{1,0:T(8,128)(2,1)S(1)} %shard_map.112), channel_id=1, source_target_pairs={{0,2},{1,3},{2,0},{3,1},{4,6},{5,7},{6,4},{7,5},{8,10},{9,11},{10,... | collective-permute-start | bytes 786440 | tf_op jit(solution)/shard_map/ppermute | solution.py:442
  119.2 28.3 %copy-start.6 = (f32[512]{0:T(512)S(1)}, f32[512]{0:T(512)}, u32[]{:S(2)}) copy-start(f32[512]{0:T(512)} %param.21) | copy-start | bytes 6148
  119.2 19.2 %collective-permute-start.7 = (bf16[256,512]{1,0:T(8,128)(2,1)S(1)}, bf16[256,512]{1,0:T(8,128)(2,1)S(1)}, u32[]{:S(2)}, u32[]{:S(2)}) collective-permute-start(bf16[256,512]{1,0:T(8,128)(2,1)S(1)} %shard_map.113), channel_id=1, source_target_pairs={{0,2},{1,3},{2,0},{3,1},{4,6},{5,7},{6,4},{7,5},{8,10},{9,11},{10,... | collective-permute-start | bytes 786440 | tf_op jit(solution)/shard_map/ppermute | solution.py:442
  138.4 1.3 copy-start.5
  138.4 0.8 copy-start.4

commit v13 on v12

--- a/solution.py
+++ b/solution.py
@@ -42,7 +42,8 @@
 def neighbours(inside, outside):
     count = lax.axis_size(SP)
     pairs = [(i, i + 1) for i in range(1, count - 1, 2)]
-    return swapped(inside), lax.ppermute(outside, SP, pairs + [(b, a) for a, b in pairs])
+    from_outside = lax.ppermute(outside, SP, pairs + [(b, a) for a, b in pairs])
+    return swapped(inside), from_outside
 
 
 def whole_weights(own_ref, other_ref, w_ref, at):
@@ -221,18 +222,17 @@
     w_ref,
     band_ref,
 ):
-    rows, query_cols = kv_ref.shape[0], query_ref.shape[1]
+    rows, query_cols = query_ref.shape
     whole_weights(own_ref, other_ref, w_ref, own_ref.shape[3] - query_cols)
     split_band(kv_ref[...], band_ref)
     for b in (1, rows // WINDOW - 2, 0, rows // WINDOW - 1):
         here = slice(b * WINDOW, (b + 1) * WINDOW)
         queries = projected(tokens_ref.at[:, here], w_ref, 0, query_cols)
+        query_ref[here] = queries
         if 0 < b < rows // WINDOW - 1:
             attend_block(
                 queries, band_ref, (b - 1) * WINDOW, sink_ref, attended_ref, (b - 1) * WINDOW
             )
-        else:
-            query_ref[min(b, 1) * WINDOW : (min(b, 1) + 1) * WINDOW] = queries
     near = 2 * RIM
     chan = chan_ref[WINDOW - near : rows - WINDOW + near].astype(F32)
     offset = lax.axis_index(SP) * rows + WINDOW
@@ -276,7 +276,7 @@
     )
     for edge, start in enumerate((0, rows - WINDOW)):
         attend_edge(
-            query_ref[edge * WINDOW : (edge + 1) * WINDOW],
+            query_ref[start : start + WINDOW],
             offset + start > 0,
             offset + start + WINDOW < seq_len,
             keys_ref,
@@ -396,7 +396,7 @@
     scale = pool_scale.reshape(1, -1)
     query, *inner = pl.pallas_call(
         functools.partial(inner_kernel, seq_len),
-        out_shape=[rows_of(query_cols, half), rows_of(query_cols, half), rows_of(chan_cols, half)],
+        out_shape=[rows_of(query_cols), rows_of(query_cols, half), rows_of(chan_cols, half)],
         in_specs=[VMEM] * 5 + [SMEM] + [VMEM] * 2,
         out_specs=[VMEM] * 3,
         scratch_shapes=[

time: 151 us -> 151 us (level)
  no operation moved by 1% of the time
where the time goes in v13:
time: 151 us; the launch traced here: 150 us
  waiting for transfers between devices  48.1 us (32%)
  blocking collectives  44.1 us (29%)
  starting transfers between devices  30.9 us (20%)
  Pallas kernels  16.1 us (11%)
  local copies, waits for them, and re-layouts  7.52 us (5%)
  other arithmetic  2.8 us (2%)
    all_gather x1, blocking collectives, layer(): over_z = lax.all_gather(packed, Z, axis=0)  36.4 us
    all_to_all x1, waiting for transfers between devices, from_everyone(): lax.all_to_all(jnp.broadcast_to(shard[None], (count, *shard.shape)), axis...  20.1 us
    ppermute x4, waiting for transfers between devices, sent(): return lax.ppermute(block, TP, [(i, i ^ mask) for i in range(count)])  16.7 us
    ppermute x4, starting transfers between devices, sent(): return lax.ppermute(block, TP, [(i, i ^ mask) for i in range(count)])  12.3 us
    all_to_all x1, waiting for transfers between devices, layer(): gathered = lax.all_to_all(copies, TP, 0, 0, tiled=True)  11.3 us
    all_to_all x1, blocking collectives, from_everyone(): lax.all_to_all(jnp.broadcast_to(shard[None], (count, *shard.shape)), axis...  7.71 us
    ppermute x3, starting transfers between devices, swapped(): return lax.ppermute(shard, CORE, [(0, 1), (1, 0)])  6.38 us
    pallas_call x1, Pallas kernels, layer(): pl.pallas_call(functools.partial(inner_kernel, seq_len), out_shape=[rows_...  5.42 us
  transfers between devices with their start and end apart: 10, of which 4 were waited for; matrix products, arithmetic and copies ran while one was open for 2% of the time, Pallas kernels for 10%

profile of v13, /device:TPU:32, one launch (start us, length us, event | category | flops | bytes accessed | tf_op | source)
XLA Modules:
  0.0 149.8 jit_solution(4687565011289558013)
XLA Ops:
  0.0 0.9 concatenate.9
  0.9 36.4 %all-gather = bf16[256,1152]{1,0:T(8,128)(2,1)S(1)} all-gather(bf16[16,1152]{1,0:T(8,128)(2,1)S(1)} %concatenate.9), channel_id=2, replica_groups=mesh['sp_0'=16,'sp_1'=4,'sp_2'=2,'tp'=4] {'sp_0'}, dimensions={0}, use_global_device_ids=true | all-gather | bytes 626688 | tf_op jit(solution)/shard_map/all_gather | solution.py:371
  37.3 1.6 %broadcast_in_dim.4 = bf16[4,16,16,1152]{3,2,1,0:T(8,128)(2,1)} broadcast(bf16[16,16,1152]{2,1,0:T(8,128)(2,1)S(1)} %bitcast.10), dimensions={1,2,3} | broadcast | bytes 2949120 | tf_op jit(solution)/shard_map/broadcast_in_dim | solution.py:30
  38.9 4.3 %all-to-all-start.1 = ((bf16[4,16,16,1152]{3,2,1,0:T(8,128)(2,1)}), bf16[4,16,16,1152]{3,2,1,0:T(8,128)(2,1)S(1)}, u32[]{:S(2)}, u32[]{:S(2)}) async-start(bf16[4,16,16,1152]{3,2,1,0:T(8,128)(2,1)} %broadcast_in_dim.4), calls=%async_computation.1 | async-start | bytes 4718592 | tf_op jit(solution)/shard_map/all_to_all | solution.py:29
  43.2 2.4 %copies.1 = bf16[4,512,512]{2,1,0:T(8,128)(2,1)} custom-call(bf16[512,512]{1,0:T(8,128)(2,1)} %shard_ref.1), custom_call_target="tpu_custom_call" | custom-call | bytes 2621440 | tf_op jit(solution)/shard_map/copies/pallas_call | solution.py:352
  45.6 20.1 %all-to-all-done.1 = bf16[4,16,16,1152]{3,2,1,0:T(8,128)(2,1)S(1)} async-done(((bf16[4,16,16,1152]{3,2,1,0:T(8,128)(2,1)}), bf16[4,16,16,1152]{3,2,1,0:T(8,128)(2,1)S(1)}, u32[]{:S(2)}, u32[]{:S(2)}) %all-to-all-start.1) | async-done | bytes 2359328 | tf_op jit(solution)/shard_map/all_to_all | solution.py:29
  65.6 1.4 copy-done.3
  67.1 4.5 %all-to-all-start = ((bf16[4,512,512]{2,1,0:T(8,128)(2,1)}), bf16[4,512,512]{2,1,0:T(8,128)(2,1)}, u32[]{:S(2)}, u32[]{:S(2)}) async-start(bf16[4,512,512]{2,1,0:T(8,128)(2,1)} %copies.1), calls=%async_computation | async-start | bytes 4194304 | tf_op jit(solution)/shard_map/all_to_all | solution.py:367
  71.5 1.4 slice.28.own_ref
  73.0 1.9 %collective-permute-start = (bf16[4,16,16,640]{3,2,1,0:T(8,128)(2,1)S(1)}, bf16[4,16,16,640]{3,2,1,0:T(8,128)(2,1)}, u32[]{:S(2)}, u32[]{:S(2)}) collective-permute-start(bf16[4,16,16,640]{3,2,1,0:T(8,128)(2,1)S(1)} %slice.28.own_ref), channel_id=1, source_target_pairs={{0,4},{4,0},{1,5},{5,1},{2,6},{6,2},{3,7},{7,3},{8,12},{12,8},{9,1... | collective-permute-start | bytes 3932168 | tf_op jit(solution)/shard_map/ppermute | solution.py:39
  74.9 1.3 slice.29.refs_4_.refs_2_
  76.2 2.5 %collective-permute-start.3 = (bf16[4,16,16,512]{3,2,1,0:T(8,128)(2,1)S(1)}, bf16[4,16,16,512]{3,2,1,0:T(8,128)(2,1)S(1)}, u32[]{:S(2)}, u32[]{:S(2)}) collective-permute-start(bf16[4,16,16,512]{3,2,1,0:T(8,128)(2,1)S(1)} %slice.29.refs_4_.refs_2_), channel_id=1, source_target_pairs={{0,4},{4,0},{1,5},{5,1},{2,6},{6,2},{3,7},{7,3},{8,12},{12,8},{9,1... | collective-permute-start | bytes 3145736 | tf_op jit(solution)/shard_map/ppermute | solution.py:39
  78.8 11.3 %all-to-all-done.tokens_ref = bf16[4,512,512]{2,1,0:T(8,128)(2,1)} async-done(((bf16[4,512,512]{2,1,0:T(8,128)(2,1)}), bf16[4,512,512]{2,1,0:T(8,128)(2,1)}, u32[]{:S(2)}, u32[]{:S(2)}) %all-to-all-start) | async-done | bytes 2097184 | tf_op jit(solution)/shard_map/all_to_all | solution.py:367
  90.1 3.4 %project.1 = (bf16[512,128]{1,0:T(8,128)(2,1)S(1)}, bf16[512,256]{1,0:T(8,128)(2,1)S(1)}, bf16[144,128]{1,0:T(8,128)(2,1)S(1)}, bf16[144,128]{1,0:T(8,128)(2,1)S(1)}) custom-call(bf16[4,512,512]{2,1,0:T(8,128)(2,1)} %all-to-all-done.tokens_ref, bf16[4,16,16,640]{3,2,1,0:T(8,128)(2,1)S(1)} %slice.28.own_ref, ...), custom_call_target="tpu_custom_call" | custom-call | flops 805306368 | bytes 4194304 | tf_op jit(solution)/shard_map/project/pallas_call | solution.py:384
  93.5 1.9 %collective-permute-start.1 = (bf16[144,128]{1,0:T(8,128)(2,1)S(1)}, bf16[144,128]{1,0:T(8,128)(2,1)S(1)}, u32[]{:S(2)}, u32[]{:S(2)}) collective-permute-start(bf16[144,128]{1,0:T(8,128)(2,1)S(1)} %get-tuple-element.19), channel_id=1, source_target_pairs={{0,4},{4,0},{1,5},{5,1},{2,6},{6,2},{3,7},{7,3},{8,12},{12,8},{9,1... | collective-permute-start | bytes 110600 | tf_op jit(solution)/shard_map/ppermute | solution.py:39
  95.4 3.4 %collective-permute-start.2 = (bf16[144,128]{1,0:T(8,128)(2,1)S(1)}, bf16[144,128]{1,0:T(8,128)(2,1)S(1)}, u32[]{:S(2)}, u32[]{:S(2)}) collective-permute-start(bf16[144,128]{1,0:T(8,128)(2,1)S(1)} %get-tuple-element.20), channel_id=1, source_target_pairs={{4,8},{12,16},{20,24},{28,32},{36,40},{44,48},{52,56},{60,64},{68,... | collective-permute-start | bytes 110600 | tf_op jit(solution)/shard_map/ppermute | solution.py:45
  98.9 5.4 %inner.1 = (bf16[512,256]{1,0:T(8,128)(2,1)S(1)}, bf16[256,256]{1,0:T(8,128)(2,1)S(1)}, bf16[256,256]{1,0:T(8,128)(2,1)S(1)}) custom-call(bf16[4,512,512]{2,1,0:T(8,128)(2,1)} %all-to-all-done.tokens_ref, bf16[4,16,16,640]{3,2,1,0:T(8,128)(2,1)S(1)} %slice.28.own_ref, bf16[4,16,16,640]{3,2,1,0:T(8,128)(2,1)} %collective-permute-done.other_ref, ...), custom_call_target="tpu_custom_call" | custom-call | flops 536870912 | bytes 4194304 | tf_op jit(solution)/shard_map/inner/pallas_call | solution.py:397
  104.3 2.6 %outer.1 = (bf16[256,256]{1,0:T(8,128)(2,1)S(1)}, bf16[256,256]{1,0:T(8,128)(2,1)S(1)}) custom-call(bf16[512,256]{1,0:T(8,128)(2,1)S(1)} %get-tuple-element.18.query_ref, bf16[512,128]{1,0:T(8,128)(2,1)S(1)} %get-tuple-element.14.kv_ref, bf16[512,256]{1,0:T(8,128)(2,1)S(1)} %get-tuple-element.15.chan_ref, ...), custom_call_target="tpu_custom_call" | custom-call | flops 536870912 | bytes 2097152 | tf_op jit(solution)/shard_map/outer/pallas_call | solution.py:410
  106.9 0.5 shard_map.111
  107.4 3.1 %collective-permute-start.5 = (bf16[512,512]{1,0:T(8,128)(2,1)S(1)}, bf16[512,512]{1,0:T(8,128)(2,1)S(1)}, u32[]{:S(2)}, u32[]{:S(2)}) collective-permute-start(bf16[512,512]{1,0:T(8,128)(2,1)S(1)} %shard_map.111), channel_id=1, source_target_pairs={{0,3},{1,2},{2,1},{3,0},{4,7},{5,6},{6,5},{7,4},{8,11},{9,10},{10,... | collective-permute-start | bytes 1572872 | tf_op jit(solution)/shard_map/ppermute | solution.py:442
  110.5 0.5 shard_map.110
  111.0 1.9 %collective-permute-start.4 = (bf16[512,512]{1,0:T(8,128)(2,1)S(1)}, bf16[512,512]{1,0:T(8,128)(2,1)S(1)}, u32[]{:S(2)}, u32[]{:S(2)}) collective-permute-start(bf16[512,512]{1,0:T(8,128)(2,1)S(1)} %shard_map.110), channel_id=1, source_target_pairs={{0,1},{1,0},{2,3},{3,2},{4,5},{5,4},{6,7},{7,6},{8,9},{9,8},{10,11... | collective-permute-start | bytes 1572872 | tf_op jit(solution)/shard_map/ppermute | solution.py:442
  113.4 5.4 %collective-permute-start.6 = (bf16[256,512]{1,0:T(8,128)(2,1)S(1)}, bf16[256,512]{1,0:T(8,128)(2,1)S(1)}, u32[]{:S(2)}, u32[]{:S(2)}) collective-permute-start(bf16[256,512]{1,0:T(8,128)(2,1)S(1)} %shard_map.112), channel_id=1, source_target_pairs={{0,2},{1,3},{2,0},{3,1},{4,6},{5,7},{6,4},{7,5},{8,10},{9,11},{10,... | collective-permute-start | bytes 786440 | tf_op jit(solution)/shard_map/ppermute | solution.py:442
  119.2 1.9 %collective-permute-start.7 = (bf16[256,512]{1,0:T(8,128)(2,1)S(1)}, bf16[256,512]{1,0:T(8,128)(2,1)S(1)}, u32[]{:S(2)}, u32[]{:S(2)}) collective-permute-start(bf16[256,512]{1,0:T(8,128)(2,1)S(1)} %shard_map.113), channel_id=1, source_target_pairs={{0,2},{1,3},{2,0},{3,1},{4,6},{5,7},{6,4},{7,5},{8,10},{9,11},{10,... | collective-permute-start | bytes 786440 | tf_op jit(solution)/shard_map/ppermute | solution.py:442
  121.1 0.5 shard_map.109
  121.7 13.2 %collective-permute-done.6 = bf16[256,512]{1,0:T(8,128)(2,1)S(1)} collective-permute-done((bf16[256,512]{1,0:T(8,128)(2,1)S(1)}, bf16[256,512]{1,0:T(8,128)(2,1)S(1)}, u32[]{:S(2)}, u32[]{:S(2)}) %collective-permute-start.6) | collective-permute-done | bytes 262176 | tf_op jit(solution)/shard_map/ppermute | solution.py:442
  134.9 3.5 %collective-permute-done.7 = bf16[256,512]{1,0:T(8,128)(2,1)S(1)} collective-permute-done((bf16[256,512]{1,0:T(8,128)(2,1)S(1)}, bf16[256,512]{1,0:T(8,128)(2,1)S(1)}, u32[]{:S(2)}, u32[]{:S(2)}) %collective-permute-start.7) | collective-permute-done | bytes 262176 | tf_op jit(solution)/shard_map/ppermute | solution.py:442
  138.4 0.8 copy-done.4
  139.2 0.4 fusion
  139.7 7.7 %all_to_all.15 = f32[4,2,512]{2,1,0:T(2,128)S(1)} all-to-all(f32[4,2,512]{2,1,0:T(2,128)S(1)} %broadcast_in_dim.5), channel_id=1, replica_groups=mesh['sp_0'=16,'sp_1'=4,'sp_2'=2,'tp'=4] {'tp'}, dimensions={0} | all-to-all | bytes 32768 | tf_op jit(solution)/shard_map/all_to_all | solution.py:29
  147.5 1.5 multiply_convert_fusion
  149.0 0.8 pad_maximum_fusion
  (27 shorter events, 0.9 us)
Async XLA Ops:
  38.9 26.7 %all-to-all-start.1 = ((bf16[4,16,16,1152]{3,2,1,0:T(8,128)(2,1)}), bf16[4,16,16,1152]{3,2,1,0:T(8,128)(2,1)S(1)}, u32[]{:S(2)}, u32[]{:S(2)}) async-start(bf16[4,16,16,1152]{3,2,1,0:T(8,128)(2,1)} %broadcast_in_dim.4), calls=%async_computation.1 | async-start | bytes 4718592 | tf_op jit(solution)/shard_map/all_to_all | solution.py:29
  65.6 1.4 copy-start.3
  67.1 23.0 %all-to-all-start = ((bf16[4,512,512]{2,1,0:T(8,128)(2,1)}), bf16[4,512,512]{2,1,0:T(8,128)(2,1)}, u32[]{:S(2)}, u32[]{:S(2)}) async-start(bf16[4,512,512]{2,1,0:T(8,128)(2,1)} %copies.1), calls=%async_computation | async-start | bytes 4194304 | tf_op jit(solution)/shard_map/all_to_all | solution.py:367
  73.0 17.1 %collective-permute-start = (bf16[4,16,16,640]{3,2,1,0:T(8,128)(2,1)S(1)}, bf16[4,16,16,640]{3,2,1,0:T(8,128)(2,1)}, u32[]{:S(2)}, u32[]{:S(2)}) collective-permute-start(bf16[4,16,16,640]{3,2,1,0:T(8,128)(2,1)S(1)} %slice.28.own_ref), channel_id=1, source_target_pairs={{0,4},{4,0},{1,5},{5,1},{2,6},{6,2},{3,7},{7,3},{8,12},{12,8},{9,1... | collective-permute-start | bytes 3932168 | tf_op jit(solution)/shard_map/ppermute | solution.py:39
  76.2 22.6 %copy-start = (bf16[1,256,256]{2,1,0:T(8,128)(2,1)S(1)}, bf16[1,256,256]{2,1,0:T(8,128)(2,1)}, u32[]{:S(2)}) copy-start(bf16[1,256,256]{2,1,0:T(8,128)(2,1)} %w_pool_ref.3) | copy-start | bytes 393220
  76.2 22.6 %copy-start.1 = (f32[256]{0:T(256)S(1)}, f32[256]{0:T(256)}, u32[]{:S(2)}) copy-start(f32[256]{0:T(256)} %param.18) | copy-start | bytes 3076
  76.2 22.6 %copy-start.2 = (f32[4]{0:T(128)S(1)}, f32[4]{0:T(128)}, u32[]{:S(2)}) copy-start(f32[4]{0:T(128)} %sink_ref.3) | copy-start | bytes 52
  76.2 30.7 %collective-permute-start.3 = (bf16[4,16,16,512]{3,2,1,0:T(8,128)(2,1)S(1)}, bf16[4,16,16,512]{3,2,1,0:T(8,128)(2,1)S(1)}, u32[]{:S(2)}, u32[]{:S(2)}) collective-permute-start(bf16[4,16,16,512]{3,2,1,0:T(8,128)(2,1)S(1)} %slice.29.refs_4_.refs_2_), channel_id=1, source_target_pairs={{0,4},{4,0},{1,5},{5,1},{2,6},{6,2},{3,7},{7,3},{8,12},{12,8},{9,1... | collective-permute-start | bytes 3145736 | tf_op jit(solution)/shard_map/ppermute | solution.py:39
  93.5 10.8 %collective-permute-start.1 = (bf16[144,128]{1,0:T(8,128)(2,1)S(1)}, bf16[144,128]{1,0:T(8,128)(2,1)S(1)}, u32[]{:S(2)}, u32[]{:S(2)}) collective-permute-start(bf16[144,128]{1,0:T(8,128)(2,1)S(1)} %get-tuple-element.19), channel_id=1, source_target_pairs={{0,4},{4,0},{1,5},{5,1},{2,6},{6,2},{3,7},{7,3},{8,12},{12,8},{9,1... | collective-permute-start | bytes 110600 | tf_op jit(solution)/shard_map/ppermute | solution.py:39
  95.4 8.9 %collective-permute-start.2 = (bf16[144,128]{1,0:T(8,128)(2,1)S(1)}, bf16[144,128]{1,0:T(8,128)(2,1)S(1)}, u32[]{:S(2)}, u32[]{:S(2)}) collective-permute-start(bf16[144,128]{1,0:T(8,128)(2,1)S(1)} %get-tuple-element.20), channel_id=1, source_target_pairs={{4,8},{12,16},{20,24},{28,32},{36,40},{44,48},{52,56},{60,64},{68,... | collective-permute-start | bytes 110600 | tf_op jit(solution)/shard_map/ppermute | solution.py:45
  107.4 31.0 %collective-permute-start.5 = (bf16[512,512]{1,0:T(8,128)(2,1)S(1)}, bf16[512,512]{1,0:T(8,128)(2,1)S(1)}, u32[]{:S(2)}, u32[]{:S(2)}) collective-permute-start(bf16[512,512]{1,0:T(8,128)(2,1)S(1)} %shard_map.111), channel_id=1, source_target_pairs={{0,3},{1,2},{2,1},{3,0},{4,7},{5,6},{6,5},{7,4},{8,11},{9,10},{10,... | collective-permute-start | bytes 1572872 | tf_op jit(solution)/shard_map/ppermute | solution.py:442
  111.0 27.4 %collective-permute-start.4 = (bf16[512,512]{1,0:T(8,128)(2,1)S(1)}, bf16[512,512]{1,0:T(8,128)(2,1)S(1)}, u32[]{:S(2)}, u32[]{:S(2)}) collective-permute-start(bf16[512,512]{1,0:T(8,128)(2,1)S(1)} %shard_map.110), channel_id=1, source_target_pairs={{0,1},{1,0},{2,3},{3,2},{4,5},{5,4},{6,7},{7,6},{8,9},{9,8},{10,11... | collective-permute-start | bytes 1572872 | tf_op jit(solution)/shard_map/ppermute | solution.py:442
  113.4 21.5 %collective-permute-start.6 = (bf16[256,512]{1,0:T(8,128)(2,1)S(1)}, bf16[256,512]{1,0:T(8,128)(2,1)S(1)}, u32[]{:S(2)}, u32[]{:S(2)}) collective-permute-start(bf16[256,512]{1,0:T(8,128)(2,1)S(1)} %shard_map.112), channel_id=1, source_target_pairs={{0,2},{1,3},{2,0},{3,1},{4,6},{5,7},{6,4},{7,5},{8,10},{9,11},{10,... | collective-permute-start | bytes 786440 | tf_op jit(solution)/shard_map/ppermute | solution.py:442
  119.2 28.3 %copy-start.6 = (f32[512]{0:T(512)S(1)}, f32[512]{0:T(512)}, u32[]{:S(2)}) copy-start(f32[512]{0:T(512)} %param.21) | copy-start | bytes 6148
  119.2 19.2 %collective-permute-start.7 = (bf16[256,512]{1,0:T(8,128)(2,1)S(1)}, bf16[256,512]{1,0:T(8,128)(2,1)S(1)}, u32[]{:S(2)}, u32[]{:S(2)}) collective-permute-start(bf16[256,512]{1,0:T(8,128)(2,1)S(1)} %shard_map.113), channel_id=1, source_target_pairs={{0,2},{1,3},{2,0},{3,1},{4,6},{5,7},{6,4},{7,5},{8,10},{9,11},{10,... | collective-permute-start | bytes 786440 | tf_op jit(solution)/shard_map/ppermute | solution.py:442
  138.4 1.3 copy-start.5
  138.4 0.8 copy-start.4

commit v14 on v13

--- a/solution.py
+++ b/solution.py
@@ -42,8 +42,7 @@
 def neighbours(inside, outside):
     count = lax.axis_size(SP)
     pairs = [(i, i + 1) for i in range(1, count - 1, 2)]
-    from_outside = lax.ppermute(outside, SP, pairs + [(b, a) for a, b in pairs])
-    return swapped(inside), from_outside
+    return swapped(inside), lax.ppermute(outside, SP, pairs + [(b, a) for a, b in pairs])
 
 
 def whole_weights(own_ref, other_ref, w_ref, at):
@@ -321,6 +320,13 @@
     ).astype(BF16)
 
 
+def with_far_block(kernel, ins, outs, *refs):
+    own_ref, other_ref = refs[ins : ins + 2]
+    made, sent_ref = refs[ins + 2 : ins + 2 + outs], refs[ins + 2 + outs]
+    kernel(*refs[:ins], *made, *refs[ins + 3 + outs : -2])
+    out_kernel(2, 1, *made[-2:], own_ref, other_ref, sent_ref, *refs[-2:])
+
+
 VMEM = pl.BlockSpec(memory_space=pltpu.VMEM)
 SMEM = pl.BlockSpec(memory_space=pltpu.SMEM)
 ANY = pl.BlockSpec(memory_space=pl.ANY)
@@ -394,32 +400,47 @@
     inside, outside = neighbours(inside, outside)
     half = rows // 2
     scale = pool_scale.reshape(1, -1)
-    query, *inner = pl.pallas_call(
-        functools.partial(inner_kernel, seq_len),
-        out_shape=[rows_of(query_cols), rows_of(query_cols, half), rows_of(chan_cols, half)],
-        in_specs=[VMEM] * 5 + [SMEM] + [VMEM] * 2,
-        out_specs=[VMEM] * 3,
+    far_scratch = [
+        pltpu.VMEM((half, hidden_cols), BF16),
+        pltpu.VMEM((share, hidden_cols), BF16),
+    ]
+    query, *inner, far_inner = pl.pallas_call(
+        functools.partial(with_far_block, functools.partial(inner_kernel, seq_len), 8, 3),
+        out_shape=[
+            rows_of(query_cols),
+            rows_of(query_cols, half),
+            rows_of(chan_cols, half),
+            rows_of(share, half),
+        ],
+        in_specs=[VMEM] * 5 + [SMEM] + [VMEM] * 4,
+        out_specs=[VMEM] * 4,
         scratch_shapes=[
             pltpu.VMEM((model_width, query_cols), BF16),
             pltpu.VMEM((4, rows, PAIR), BF16),
+            *far_scratch,
         ],
         compiler_params=LIMIT,
         cost_estimate=cost(2 * rows * model_width * query_cols, 4 << 20),
         name="inner",
-    )(gathered, own1, other1, kv, chan, sink, w_pool, scale)
-    outer = pl.pallas_call(
-        functools.partial(outer_kernel, seq_len),
-        out_shape=[rows_of(query_cols, half), rows_of(chan_cols, half)],
-        in_specs=[VMEM] * 5 + [SMEM] + [VMEM] * 2,
-        out_specs=[VMEM] * 2,
+    )(gathered, own1, other1, kv, chan, sink, w_pool, scale, own2, other2)
+    *outer, far_outer = pl.pallas_call(
+        functools.partial(with_far_block, functools.partial(outer_kernel, seq_len), 8, 2),
+        out_shape=[
+            rows_of(query_cols, half),
+            rows_of(chan_cols, half),
+            rows_of(share, half),
+        ],
+        in_specs=[VMEM] * 5 + [SMEM] + [VMEM] * 4,
+        out_specs=[VMEM] * 3,
         scratch_shapes=[
             pltpu.VMEM((2, 6 * WINDOW, PAIR), BF16),
             pltpu.VMEM((HEAD_DIM, 6 * WINDOW), BF16),
+            *far_scratch,
         ],
         compiler_params=LIMIT,
         cost_estimate=cost(2 * rows * model_width * query_cols, 2 << 20),
         name="outer",
-    )(query, kv, chan, inside, outside, sink, w_pool, scale)
+    )(query, kv, chan, inside, outside, sink, w_pool, scale, own2, other2)
 
     def multiplied(mask, *mixed):
         count = len(mixed)
@@ -436,13 +457,11 @@
             cost_estimate=cost(2 * count * half * share * hidden_cols, 1 << 20),
         )(*(a for pair in mixed for a in pair), own2, other2)
 
-    def sent(mask, *mixed):
-        block = multiplied(mask, *mixed)
-        count = lax.axis_size(TP)
-        return lax.ppermute(block, TP, [(i, i ^ mask) for i in range(count)])
-
-    far = jnp.concatenate([sent(2, inner), sent(2, outer)])
-    partials = [sent(1, inner, outer), sent(3, inner, outer), far]
+    def sent(mask, block):
+        return lax.ppermute(block, TP, [(i, i ^ mask) for i in range(lax.axis_size(TP))])
+
+    far = jnp.concatenate([sent(2, far_inner), sent(2, far_outer)])
+    partials = [sent(1, multiplied(1, inner, outer)), sent(3, multiplied(3, inner, outer)), far]
     mix = multiplied(0, inner, outer).astype(F32)
     for partial in partials:
         mix = mix + partial.astype(F32)

time: 151 us -> 151 us (level)
  transfers between devices with their start and end apart: 10 -> 10, of which waited for: 4 -> 4; matrix products, arithmetic and copies ran while one was open for 2% -> 2% of each run, Pallas kernels for 10% -> 8%
where the time goes in v14:
time: 151 us; the launch traced here: 150 us
  waiting for transfers between devices  48.9 us (32%)
  blocking collectives  44.1 us (29%)
  starting transfers between devices  30.9 us (20%)
  Pallas kernels  15.8 us (10%)
  local copies, waits for them, and re-layouts  7.52 us (5%)
  other arithmetic  2.8 us (2%)
    all_gather x1, blocking collectives, layer(): over_z = lax.all_gather(packed, Z, axis=0)  36.4 us
    all_to_all x1, waiting for transfers between devices, from_everyone(): lax.all_to_all(jnp.broadcast_to(shard[None], (count, *shard.shape)), axis...  20.1 us
    ppermute x4, waiting for transfers between devices, sent(): lax.ppermute(block, TP, [(i, i ^ mask) for i in range(lax.axis_size(TP))])  17.6 us
    ppermute x4, starting transfers between devices, sent(): lax.ppermute(block, TP, [(i, i ^ mask) for i in range(lax.axis_size(TP))])  12.3 us
    all_to_all x1, waiting for transfers between devices, layer(): gathered = lax.all_to_all(copies, TP, 0, 0, tiled=True)  11.3 us
    all_to_all x1, blocking collectives, from_everyone(): lax.all_to_all(jnp.broadcast_to(shard[None], (count, *shard.shape)), axis...  7.71 us
    ppermute x3, starting transfers between devices, swapped(): return lax.ppermute(shard, CORE, [(0, 1), (1, 0)])  6.38 us
    pallas_call x1, Pallas kernels, layer(): pl.pallas_call(functools.partial(with_far_block, functools.partial(inner_...  5.62 us
  transfers between devices with their start and end apart: 10, of which 4 were waited for; matrix products, arithmetic and copies ran while one was open for 2% of the time, Pallas kernels for 8%

profile of v14, /device:TPU:32, one launch (start us, length us, event | category | flops | bytes accessed | tf_op | source)
XLA Modules:
  0.0 150.3 jit_solution(14664361803083478872)
XLA Ops:
  0.0 0.9 concatenate.9
  0.9 36.4 %all-gather = bf16[256,1152]{1,0:T(8,128)(2,1)S(1)} all-gather(bf16[16,1152]{1,0:T(8,128)(2,1)S(1)} %concatenate.9), channel_id=2, replica_groups=mesh['sp_0'=16,'sp_1'=4,'sp_2'=2,'tp'=4] {'sp_0'}, dimensions={0}, use_global_device_ids=true | all-gather | bytes 626688 | tf_op jit(solution)/shard_map/all_gather | solution.py:377
  37.3 1.6 %broadcast_in_dim.4 = bf16[4,16,16,1152]{3,2,1,0:T(8,128)(2,1)} broadcast(bf16[16,16,1152]{2,1,0:T(8,128)(2,1)S(1)} %bitcast.10), dimensions={1,2,3} | broadcast | bytes 2949120 | tf_op jit(solution)/shard_map/broadcast_in_dim | solution.py:30
  38.9 4.3 %all-to-all-start.1 = ((bf16[4,16,16,1152]{3,2,1,0:T(8,128)(2,1)}), bf16[4,16,16,1152]{3,2,1,0:T(8,128)(2,1)S(1)}, u32[]{:S(2)}, u32[]{:S(2)}) async-start(bf16[4,16,16,1152]{3,2,1,0:T(8,128)(2,1)} %broadcast_in_dim.4), calls=%async_computation.1 | async-start | bytes 4718592 | tf_op jit(solution)/shard_map/all_to_all | solution.py:29
  43.2 2.4 %copies.1 = bf16[4,512,512]{2,1,0:T(8,128)(2,1)} custom-call(bf16[512,512]{1,0:T(8,128)(2,1)} %shard_ref.1), custom_call_target="tpu_custom_call" | custom-call | bytes 2621440 | tf_op jit(solution)/shard_map/copies/pallas_call | solution.py:358
  45.6 20.1 %all-to-all-done.1 = bf16[4,16,16,1152]{3,2,1,0:T(8,128)(2,1)S(1)} async-done(((bf16[4,16,16,1152]{3,2,1,0:T(8,128)(2,1)}), bf16[4,16,16,1152]{3,2,1,0:T(8,128)(2,1)S(1)}, u32[]{:S(2)}, u32[]{:S(2)}) %all-to-all-start.1) | async-done | bytes 2359328 | tf_op jit(solution)/shard_map/all_to_all | solution.py:29
  65.6 1.4 copy-done.3
  67.1 4.5 %all-to-all-start = ((bf16[4,512,512]{2,1,0:T(8,128)(2,1)}), bf16[4,512,512]{2,1,0:T(8,128)(2,1)}, u32[]{:S(2)}, u32[]{:S(2)}) async-start(bf16[4,512,512]{2,1,0:T(8,128)(2,1)} %copies.1), calls=%async_computation | async-start | bytes 4194304 | tf_op jit(solution)/shard_map/all_to_all | solution.py:373
  71.5 1.4 slice.28.own_ref.refs_1_
  73.0 1.9 %collective-permute-start = (bf16[4,16,16,640]{3,2,1,0:T(8,128)(2,1)S(1)}, bf16[4,16,16,640]{3,2,1,0:T(8,128)(2,1)}, u32[]{:S(2)}, u32[]{:S(2)}) collective-permute-start(bf16[4,16,16,640]{3,2,1,0:T(8,128)(2,1)S(1)} %slice.28.own_ref.refs_1_), channel_id=1, source_target_pairs={{0,4},{4,0},{1,5},{5,1},{2,6},{6,2},{3,7},{7,3},{8,12},{12,8},{9,1... | collective-permute-start | bytes 3932168 | tf_op jit(solution)/shard_map/ppermute | solution.py:39
  74.9 1.3 slice.29.refs_8_.refs_4_
  76.2 2.5 %collective-permute-start.1 = (bf16[4,16,16,512]{3,2,1,0:T(8,128)(2,1)S(1)}, bf16[4,16,16,512]{3,2,1,0:T(8,128)(2,1)S(1)}, u32[]{:S(2)}, u32[]{:S(2)}) collective-permute-start(bf16[4,16,16,512]{3,2,1,0:T(8,128)(2,1)S(1)} %slice.29.refs_8_.refs_4_), channel_id=1, source_target_pairs={{0,4},{4,0},{1,5},{5,1},{2,6},{6,2},{3,7},{7,3},{8,12},{12,8},{9,1... | collective-permute-start | bytes 3145736 | tf_op jit(solution)/shard_map/ppermute | solution.py:39
  78.8 11.3 %all-to-all-done.tokens_ref.refs_0_ = bf16[4,512,512]{2,1,0:T(8,128)(2,1)} async-done(((bf16[4,512,512]{2,1,0:T(8,128)(2,1)}), bf16[4,512,512]{2,1,0:T(8,128)(2,1)}, u32[]{:S(2)}, u32[]{:S(2)}) %all-to-all-start) | async-done | bytes 2097184 | tf_op jit(solution)/shard_map/all_to_all | solution.py:373
  90.1 3.4 %project.1 = (bf16[512,128]{1,0:T(8,128)(2,1)S(1)}, bf16[512,256]{1,0:T(8,128)(2,1)S(1)}, bf16[144,128]{1,0:T(8,128)(2,1)S(1)}, bf16[144,128]{1,0:T(8,128)(2,1)S(1)}) custom-call(bf16[4,512,512]{2,1,0:T(8,128)(2,1)} %all-to-all-done.tokens_ref.refs_0_, bf16[4,16,16,640]{3,2,1,0:T(8,128)(2,1)S(1)} %slice.28.own_ref.refs_1_, ...), custom_call_target="tpu_custom_call" | custom-call | flops 805306368 | bytes 4194304 | tf_op jit(solution)/shard_map/project/pallas_call | solution.py:390
  93.5 1.9 %collective-permute-start.2 = (bf16[144,128]{1,0:T(8,128)(2,1)S(1)}, bf16[144,128]{1,0:T(8,128)(2,1)S(1)}, u32[]{:S(2)}, u32[]{:S(2)}) collective-permute-start(bf16[144,128]{1,0:T(8,128)(2,1)S(1)} %get-tuple-element.21), channel_id=1, source_target_pairs={{0,4},{4,0},{1,5},{5,1},{2,6},{6,2},{3,7},{7,3},{8,12},{12,8},{9,1... | collective-permute-start | bytes 110600 | tf_op jit(solution)/shard_map/ppermute | solution.py:39
  95.4 3.4 %collective-permute-start.3 = (bf16[144,128]{1,0:T(8,128)(2,1)S(1)}, bf16[144,128]{1,0:T(8,128)(2,1)S(1)}, u32[]{:S(2)}, u32[]{:S(2)}) collective-permute-start(bf16[144,128]{1,0:T(8,128)(2,1)S(1)} %get-tuple-element.22), channel_id=1, source_target_pairs={{4,8},{12,16},{20,24},{28,32},{36,40},{44,48},{52,56},{60,64},{68,... | collective-permute-start | bytes 110600 | tf_op jit(solution)/shard_map/ppermute | solution.py:45
  98.9 5.6 %inner.1 = (bf16[512,256]{1,0:T(8,128)(2,1)S(1)}, bf16[256,256]{1,0:T(8,128)(2,1)S(1)}, bf16[256,256]{1,0:T(8,128)(2,1)S(1)}, bf16[256,512]{1,0:T(8,128)(2,1)S(1)}) custom-call(bf16[4,512,512]{2,1,0:T(8,128)(2,1)} %all-to-all-done.tokens_ref.refs_0_, bf16[4,16,16,640]{3,2,1,0:T(8,128)(2,1)S(1)} %slice.28.own_ref.refs_1_, ...), custom_call_target="tpu_custom_call" | custom-call | flops 536870912 | bytes 4194304 | tf_op jit(solution)/shard_map/inner/pallas_call | solution.py:407
  104.5 2.8 %outer.1 = (bf16[256,256]{1,0:T(8,128)(2,1)S(1)}, bf16[256,256]{1,0:T(8,128)(2,1)S(1)}, bf16[256,512]{1,0:T(8,128)(2,1)S(1)}) custom-call(bf16[512,256]{1,0:T(8,128)(2,1)S(1)} %get-tuple-element.20.refs_0_, bf16[512,128]{1,0:T(8,128)(2,1)S(1)} %get-tuple-element.16.refs_3_.refs_1_, bf16[512,256]{1,0:T(8,128)(2,1)S(1)} %get-tuple-element.17.refs_4_.refs_2_, ...), custom_call_target="tpu_custom_call" | custom-call | flops 536870912 | bytes 2097152 | tf_op jit(solution)/shard_map/outer/pallas_call | solution.py:426
  107.4 0.5 shard_map.111
  107.9 3.1 %collective-permute-start.5 = (bf16[512,512]{1,0:T(8,128)(2,1)S(1)}, bf16[512,512]{1,0:T(8,128)(2,1)S(1)}, u32[]{:S(2)}, u32[]{:S(2)}) collective-permute-start(bf16[512,512]{1,0:T(8,128)(2,1)S(1)} %shard_map.111), channel_id=1, source_target_pairs={{0,3},{1,2},{2,1},{3,0},{4,7},{5,6},{6,5},{7,4},{8,11},{9,10},{10,... | collective-permute-start | bytes 1572872 | tf_op jit(solution)/shard_map/ppermute | solution.py:461
  111.0 0.5 shard_map.110
  111.5 1.9 %collective-permute-start.4 = (bf16[512,512]{1,0:T(8,128)(2,1)S(1)}, bf16[512,512]{1,0:T(8,128)(2,1)S(1)}, u32[]{:S(2)}, u32[]{:S(2)}) collective-permute-start(bf16[512,512]{1,0:T(8,128)(2,1)S(1)} %shard_map.110), channel_id=1, source_target_pairs={{0,1},{1,0},{2,3},{3,2},{4,5},{5,4},{6,7},{7,6},{8,9},{9,8},{10,11... | collective-permute-start | bytes 1572872 | tf_op jit(solution)/shard_map/ppermute | solution.py:461
  113.4 5.4 %collective-permute-start.6 = (bf16[256,512]{1,0:T(8,128)(2,1)S(1)}, bf16[256,512]{1,0:T(8,128)(2,1)S(1)}, u32[]{:S(2)}, u32[]{:S(2)}) collective-permute-start(bf16[256,512]{1,0:T(8,128)(2,1)S(1)} %get-tuple-element.25), channel_id=1, source_target_pairs={{0,2},{1,3},{2,0},{3,1},{4,6},{5,7},{6,4},{7,5},{8,10},{9,11},{10,... | collective-permute-start | bytes 786440 | tf_op jit(solution)/shard_map/ppermute | solution.py:461
  118.9 1.9 %collective-permute-start.7 = (bf16[256,512]{1,0:T(8,128)(2,1)S(1)}, bf16[256,512]{1,0:T(8,128)(2,1)S(1)}, u32[]{:S(2)}, u32[]{:S(2)}) collective-permute-start(bf16[256,512]{1,0:T(8,128)(2,1)S(1)} %get-tuple-element.26), channel_id=1, source_target_pairs={{0,2},{1,3},{2,0},{3,1},{4,6},{5,7},{6,4},{7,5},{8,10},{9,11},{10,... | collective-permute-start | bytes 786440 | tf_op jit(solution)/shard_map/ppermute | solution.py:461
  120.8 0.5 shard_map.109
  121.3 14.0 %collective-permute-done.6 = bf16[256,512]{1,0:T(8,128)(2,1)S(1)} collective-permute-done((bf16[256,512]{1,0:T(8,128)(2,1)S(1)}, bf16[256,512]{1,0:T(8,128)(2,1)S(1)}, u32[]{:S(2)}, u32[]{:S(2)}) %collective-permute-start.6) | collective-permute-done | bytes 262176 | tf_op jit(solution)/shard_map/ppermute | solution.py:461
  135.3 3.6 %collective-permute-done.7 = bf16[256,512]{1,0:T(8,128)(2,1)S(1)} collective-permute-done((bf16[256,512]{1,0:T(8,128)(2,1)S(1)}, bf16[256,512]{1,0:T(8,128)(2,1)S(1)}, u32[]{:S(2)}, u32[]{:S(2)}) %collective-permute-start.7) | collective-permute-done | bytes 262176 | tf_op jit(solution)/shard_map/ppermute | solution.py:461
  138.9 0.8 copy-done.4
  139.7 0.4 fusion
  140.2 7.7 %all_to_all.15 = f32[4,2,512]{2,1,0:T(2,128)S(1)} all-to-all(f32[4,2,512]{2,1,0:T(2,128)S(1)} %broadcast_in_dim.5), channel_id=1, replica_groups=mesh['sp_0'=16,'sp_1'=4,'sp_2'=2,'tp'=4] {'tp'}, dimensions={0} | all-to-all | bytes 32768 | tf_op jit(solution)/shard_map/all_to_all | solution.py:29
  147.9 1.5 multiply_convert_fusion
  149.5 0.8 pad_maximum_fusion
  (25 shorter events, 0.1 us)
Async XLA Ops:
  38.9 26.7 %all-to-all-start.1 = ((bf16[4,16,16,1152]{3,2,1,0:T(8,128)(2,1)}), bf16[4,16,16,1152]{3,2,1,0:T(8,128)(2,1)S(1)}, u32[]{:S(2)}, u32[]{:S(2)}) async-start(bf16[4,16,16,1152]{3,2,1,0:T(8,128)(2,1)} %broadcast_in_dim.4), calls=%async_computation.1 | async-start | bytes 4718592 | tf_op jit(solution)/shard_map/all_to_all | solution.py:29
  65.6 1.4 copy-start.3
  67.1 23.0 %all-to-all-start = ((bf16[4,512,512]{2,1,0:T(8,128)(2,1)}), bf16[4,512,512]{2,1,0:T(8,128)(2,1)}, u32[]{:S(2)}, u32[]{:S(2)}) async-start(bf16[4,512,512]{2,1,0:T(8,128)(2,1)} %copies.1), calls=%async_computation | async-start | bytes 4194304 | tf_op jit(solution)/shard_map/all_to_all | solution.py:373
  73.0 17.1 %collective-permute-start = (bf16[4,16,16,640]{3,2,1,0:T(8,128)(2,1)S(1)}, bf16[4,16,16,640]{3,2,1,0:T(8,128)(2,1)}, u32[]{:S(2)}, u32[]{:S(2)}) collective-permute-start(bf16[4,16,16,640]{3,2,1,0:T(8,128)(2,1)S(1)} %slice.28.own_ref.refs_1_), channel_id=1, source_target_pairs={{0,4},{4,0},{1,5},{5,1},{2,6},{6,2},{3,7},{7,3},{8,12},{12,8},{9,1... | collective-permute-start | bytes 3932168 | tf_op jit(solution)/shard_map/ppermute | solution.py:39
  76.2 22.6 %copy-start = (bf16[1,256,256]{2,1,0:T(8,128)(2,1)S(1)}, bf16[1,256,256]{2,1,0:T(8,128)(2,1)}, u32[]{:S(2)}) copy-start(bf16[1,256,256]{2,1,0:T(8,128)(2,1)} %refs_6_.3) | copy-start | bytes 393220
  76.2 22.6 %copy-start.1 = (f32[256]{0:T(256)S(1)}, f32[256]{0:T(256)}, u32[]{:S(2)}) copy-start(f32[256]{0:T(256)} %param.18) | copy-start | bytes 3076
  76.2 22.6 %copy-start.2 = (f32[4]{0:T(128)S(1)}, f32[4]{0:T(128)}, u32[]{:S(2)}) copy-start(f32[4]{0:T(128)} %refs_5_.3) | copy-start | bytes 52
  76.2 22.6 %collective-permute-start.1 = (bf16[4,16,16,512]{3,2,1,0:T(8,128)(2,1)S(1)}, bf16[4,16,16,512]{3,2,1,0:T(8,128)(2,1)S(1)}, u32[]{:S(2)}, u32[]{:S(2)}) collective-permute-start(bf16[4,16,16,512]{3,2,1,0:T(8,128)(2,1)S(1)} %slice.29.refs_8_.refs_4_), channel_id=1, source_target_pairs={{0,4},{4,0},{1,5},{5,1},{2,6},{6,2},{3,7},{7,3},{8,12},{12,8},{9,1... | collective-permute-start | bytes 3145736 | tf_op jit(solution)/shard_map/ppermute | solution.py:39
  93.5 11.0 %collective-permute-start.2 = (bf16[144,128]{1,0:T(8,128)(2,1)S(1)}, bf16[144,128]{1,0:T(8,128)(2,1)S(1)}, u32[]{:S(2)}, u32[]{:S(2)}) collective-permute-start(bf16[144,128]{1,0:T(8,128)(2,1)S(1)} %get-tuple-element.21), channel_id=1, source_target_pairs={{0,4},{4,0},{1,5},{5,1},{2,6},{6,2},{3,7},{7,3},{8,12},{12,8},{9,1... | collective-permute-start | bytes 110600 | tf_op jit(solution)/shard_map/ppermute | solution.py:39
  95.4 9.1 %collective-permute-start.3 = (bf16[144,128]{1,0:T(8,128)(2,1)S(1)}, bf16[144,128]{1,0:T(8,128)(2,1)S(1)}, u32[]{:S(2)}, u32[]{:S(2)}) collective-permute-start(bf16[144,128]{1,0:T(8,128)(2,1)S(1)} %get-tuple-element.22), channel_id=1, source_target_pairs={{4,8},{12,16},{20,24},{28,32},{36,40},{44,48},{52,56},{60,64},{68,... | collective-permute-start | bytes 110600 | tf_op jit(solution)/shard_map/ppermute | solution.py:45
  107.9 31.0 %collective-permute-start.5 = (bf16[512,512]{1,0:T(8,128)(2,1)S(1)}, bf16[512,512]{1,0:T(8,128)(2,1)S(1)}, u32[]{:S(2)}, u32[]{:S(2)}) collective-permute-start(bf16[512,512]{1,0:T(8,128)(2,1)S(1)} %shard_map.111), channel_id=1, source_target_pairs={{0,3},{1,2},{2,1},{3,0},{4,7},{5,6},{6,5},{7,4},{8,11},{9,10},{10,... | collective-permute-start | bytes 1572872 | tf_op jit(solution)/shard_map/ppermute | solution.py:461
  111.5 27.4 %collective-permute-start.4 = (bf16[512,512]{1,0:T(8,128)(2,1)S(1)}, bf16[512,512]{1,0:T(8,128)(2,1)S(1)}, u32[]{:S(2)}, u32[]{:S(2)}) collective-permute-start(bf16[512,512]{1,0:T(8,128)(2,1)S(1)} %shard_map.110), channel_id=1, source_target_pairs={{0,1},{1,0},{2,3},{3,2},{4,5},{5,4},{6,7},{7,6},{8,9},{9,8},{10,11... | collective-permute-start | bytes 1572872 | tf_op jit(solution)/shard_map/ppermute | solution.py:461
  113.4 21.9 %collective-permute-start.6 = (bf16[256,512]{1,0:T(8,128)(2,1)S(1)}, bf16[256,512]{1,0:T(8,128)(2,1)S(1)}, u32[]{:S(2)}, u32[]{:S(2)}) collective-permute-start(bf16[256,512]{1,0:T(8,128)(2,1)S(1)} %get-tuple-element.25), channel_id=1, source_target_pairs={{0,2},{1,3},{2,0},{3,1},{4,6},{5,7},{6,4},{7,5},{8,10},{9,11},{10,... | collective-permute-start | bytes 786440 | tf_op jit(solution)/shard_map/ppermute | solution.py:461
  118.8 29.1 %copy-start.6 = (f32[512]{0:T(512)S(1)}, f32[512]{0:T(512)}, u32[]{:S(2)}) copy-start(f32[512]{0:T(512)} %param.21) | copy-start | bytes 6148
  118.9 20.0 %collective-permute-start.7 = (bf16[256,512]{1,0:T(8,128)(2,1)S(1)}, bf16[256,512]{1,0:T(8,128)(2,1)S(1)}, u32[]{:S(2)}, u32[]{:S(2)}) collective-permute-start(bf16[256,512]{1,0:T(8,128)(2,1)S(1)} %get-tuple-element.26), channel_id=1, source_target_pairs={{0,2},{1,3},{2,0},{3,1},{4,6},{5,7},{6,4},{7,5},{8,10},{9,11},{10,... | collective-permute-start | bytes 786440 | tf_op jit(solution)/shard_map/ppermute | solution.py:461
  138.9 1.3 copy-start.5
  138.9 0.8 copy-start.4
